TPU v7x, 512 devices: a whole 4x8x8 slice. The times are simulated.
512 devices in a mesh: sp: 64 (over z, y), fs: 4 (over x), tp: 2 (over core).
Axes of the slice: x: 4, y: 8, z: 8, core: 2. Of those that a mesh axis runs over, the one named last changes fastest.
Arguments:
- tokens: bfloat16 [16384, 2048], P('sp'), may hold values from -6 to 6
- norm_gain: float32 [2048], replicated, may hold values from 0.1 to 1.9
- conv_value: bfloat16 [2048, 1024], P('sp', ('fs', 'tp')), may hold values from -0.125 to 0.125
- conv_gate: bfloat16 [2048, 1024], P('sp', ('fs', 'tp')), may hold values from -0.125 to 0.125
- mixer_gate: bfloat16 [2048, 1024], P('sp', ('fs', 'tp')), may hold values from -0.125 to 0.125
- state_input: bfloat16 [2048, 1024], P('sp', ('fs', 'tp')), may hold values from -0.125 to 0.125
- write_projection: bfloat16 [2048, 1024], P('sp', ('fs', 'tp')), may hold values from -0.125 to 0.125
- state_read: bfloat16 [2048, 1024], P('sp', ('fs', 'tp')), may hold values from -0.125 to 0.125
- step_proj: bfloat16 [2048, 16], replicated, may hold values from -0.125 to 0.125
- step_bias: float32 [16], P(('fs', 'tp')), may hold values from -6 to -0.5
- decay_log: float32 [16], P(('fs', 'tp')), may hold values from -9 to -1.5
- decay_extra: float32 [16, 16384], P(('fs', 'tp'), 'sp'), may hold values from -0.8 to 0
- input_taps: float32 [4, 1024], P(None, ('fs', 'tp')), may hold values from -3 to 3
- write_taps: float32 [4, 1024], P(None, ('fs', 'tp')), may hold values from -3 to 3
- fetch_kernel_coefficients: float32 [4, 1024], P(None, ('fs', 'tp')), may hold values from -3 to 3
- long_taps: float32 [31, 1024], P(None, ('fs', 'tp')), may hold values from -5 to 5
- conv_gain: float32 [1024], P(('fs', 'tp')), may hold values from 0.1 to 1.9
- state_gain: float32 [1024], P(('fs', 'tp')), may hold values from 0.1 to 1.9
- conv_output: bfloat16 [2048, 1024], P('sp', ('fs', 'tp')), may hold values from -0.125 to 0.125
- state_output: bfloat16 [2048, 1024], P('sp', ('fs', 'tp')), may hold values from -0.125 to 0.125
- initial_state: float32 [16, 64, 128], P(('fs', 'tp')), may hold values from -12 to 12
Outputs:
- mixed: bfloat16 [16384, 2048], P(('sp', 'fs', 'tp'))
All inputs are finite; a program needn't handle non-finite values.
Results may differ from a plain program's by a relative error of at most 0.017.
Values may be sent and summed in bfloat16 or wider, within the bound.
No kernel may reach another device: no remote copies, remote signals or barrier semaphores. Data moves between devices by JAX's collectives and lax.ppermute only.
A program may use at most 64 MiB of HBM per device.

v0:
```python
import jax
import jax.numpy as jnp
from jax import lax
from jax.experimental import pallas as pl
from jax.experimental.pallas import tpu as pltpu
from jax.sharding import Mesh
from jax.sharding import PartitionSpec as P


C_CH = 1024
STATE = 128
D_INNER = 1024
WIDE = 31
SHORT = 4
HALO = 32
EPS = 1e-06
LOGS = 16
SP = ("sp_0", "sp_1")
FT = ("fs", "tp")
f32 = jnp.float32
bf16 = jnp.bfloat16
VMEM = pl.BlockSpec(memory_space=pltpu.VMEM)
SMEM = pl.BlockSpec(memory_space=pltpu.SMEM)
HIGHEST = lax.Precision.HIGHEST
SMALL = pltpu.CompilerParams(vmem_limit_bytes=12 * 2**20)


def dot(a, b, ca, cb, precision=None):
    return lax.dot_general(a, b, (((ca,), (cb,)), ((), ())), precision=precision, preferred_element_type=f32)


def sds(shape, dtype):
    return jax.ShapeDtypeStruct(shape, dtype)


def held(*arrays):
    return tuple(pltpu.with_memory_space_constraint(a, pltpu.VMEM) for a in arrays)


def fetched(*arrays):
    return tuple(pltpu.with_memory_space_constraint(a, pltpu.HBM) for a in arrays)


def lay_out(shards, copies):
    rows, ch = shards[0].shape
    n = len(shards)

    def body(*refs):
        for i in range(n):
            w = refs[i][...]
            for k in range(copies):
                refs[n][k, :, i * ch : (i + 1) * ch] = w

    return pl.pallas_call(
        body, out_shape=sds((copies, rows, n * ch), bf16), in_specs=[VMEM] * n, out_specs=VMEM, compiler_params=SMALL
    )(*fetched(*shards))


def copies_of(block, copies):
    def body(ref, out):
        for k in range(copies):
            out[k] = ref[...]

    return pl.pallas_call(
        body, out_shape=sds((copies, *block.shape), bf16), in_specs=[VMEM], out_specs=VMEM, compiler_params=SMALL
    )(*held(block))


def log_rows(logs):
    hi = logs.astype(bf16).astype(f32)
    mid = (logs - hi).astype(bf16).astype(f32)
    lo = logs - hi - mid
    row = lax.broadcasted_iota(jnp.int32, (LOGS, STATE), 0)
    return jnp.where(row == 0, hi, jnp.where(row == 1, mid, jnp.where(row == 2, lo, 0.0))).astype(bf16)


def local_states(normed, first, taps, step, left, total, copies):
    ext, d = normed.shape
    rows, ch = step.shape
    ny, nz, piece, _ = first.shape

    def body(nref, wref, tref, sref, lref, logs, send, xs, w16, buf, wall):
        for y in range(ny):
            for z in range(nz):
                wall[(z * ny + y) * piece : (z * ny + y + 1) * piece, :] = wref[y, z]
        buf[...] = dot(nref[...], wall[...], 1, 0).astype(bf16).astype(f32)
        at = HALO - SHORT + 1
        mix = sum(buf[at + i : at + i + rows, :] * tref[i : i + 1, :] for i in range(SHORT))
        act = jax.nn.silu(mix)
        x = act[:, :ch] * sref[...]
        w = act[:, ch:].astype(bf16)
        xs[...] = x.astype(bf16)
        w16[...] = w
        ends = dot((x * lref[...]).astype(bf16), w, 0, 0).astype(bf16)
        tail = log_rows(logs[...])
        for k in range(copies):
            send[k, :ch, :] = ends
            send[k, ch:, :] = tail

    return pl.pallas_call(
        body,
        out_shape=(sds((copies, ch + LOGS, STATE), bf16), pltpu.VMEM((rows, ch), bf16), pltpu.VMEM((rows, STATE), bf16)),
        in_specs=[VMEM] * 6,
        out_specs=(VMEM,) * 3,
        scratch_shapes=[pltpu.VMEM((ext, 2 * ch), f32), pltpu.VMEM((d, 2 * ch), bf16)],
        compiler_params=SMALL, name="local_states",
    )(*held(normed, first, taps, step, left, total))


def spread_heads(c, heads, p):
    return jnp.concatenate([jnp.broadcast_to(c[:, h : h + 1], (p, STATE)) for h in range(heads)], 0)


def line_states(got, index, heads, p, copies):
    n, size, _ = got.shape
    ch = heads * p

    def body(at, ref, enter, before, send):
        zero = jnp.zeros((1, STATE), f32)
        acc_in, acc_all = zero, zero
        ent = jnp.zeros((ch, STATE), f32)
        tot = jnp.zeros((ch, STATE), f32)
        for k in reversed(range(n)):
            logs = jnp.sum(ref[k, ch:, :].astype(f32), axis=0, keepdims=True)
            inside = (k < at[0]).astype(f32)
            piece = ref[k, :ch, :].astype(f32)
            ent = ent + piece * spread_heads(inside * jnp.exp(acc_in), heads, p)
            tot = tot + piece * spread_heads(jnp.exp(acc_all), heads, p)
            acc_in = acc_in + inside * logs
            acc_all = acc_all + logs
        enter[...] = ent
        before[...] = jnp.broadcast_to(acc_in, (8, STATE))
        line, tail = tot.astype(bf16), log_rows(acc_all)
        for k in range(copies):
            send[k, :ch, :] = line
            send[k, ch:, :] = tail

    return pl.pallas_call(
        body,
        out_shape=(pltpu.VMEM((ch, STATE), f32), pltpu.VMEM((8, STATE), f32), sds((copies, size, STATE), bf16)),
        in_specs=[SMEM, VMEM],
        out_specs=(VMEM,) * 3,
        compiler_params=SMALL, name="line_states",
    )(index, *held(got))


def rows_local(normed, rest, ftaps, ltaps, xs, w16, cum, cum_t):
    ext, d = normed.shape
    rows, ch = xs.shape
    heads = cum_t.shape[0]
    p = ch // heads
    steps = 4
    kb = d // steps
    part = 64

    def body(nref, wref, ftaps, ltaps, xs, w16, cum, cum_t, read16, zgate, mixed, inner, back, acc, glu):
        k = pl.program_id(0)
        at_k = pl.ds(pl.multiple_of(k * kb, kb), kb)
        term = dot(nref[:, at_k], wref[:, : 4 * ch], 1, 0)
        back[at_k, :] = wref[:, 4 * ch :]

        @pl.when(k == 0)
        def _():
            acc[...] = term

        @pl.when(k > 0)
        def _():
            acc[...] += term

        @pl.when(k == steps - 1)
        def _():
            glu[...] = acc[:, 2 * ch : 3 * ch].astype(bf16).astype(f32) * jax.nn.sigmoid(
                acc[:, 3 * ch :].astype(bf16).astype(f32)
            )
            acc[:, : 2 * ch] = acc[:, : 2 * ch].astype(bf16).astype(f32)
            s_at, l_at = HALO - SHORT + 1, HALO - WIDE + 1
            read = sum(acc[s_at + i : s_at + i + rows, :ch] * ftaps[i : i + 1, :] for i in range(SHORT))
            read = jax.nn.silu(read).astype(bf16)
            read16[...] = read
            zgate[...] = jax.nn.silu(acc[HALO:, ch : 2 * ch])
            scores = dot(read, w16[...], 1, 1)
            lower = lax.broadcasted_iota(jnp.int32, (rows, rows), 0) >= lax.broadcasted_iota(jnp.int32, (rows, rows), 1)
            lane = lax.broadcasted_iota(jnp.int32, (rows, ch), 1)
            y = jnp.zeros((rows, ch), f32)
            for h in range(heads):
                gap = jnp.where(lower, cum[:, h * p : h * p + 1] - cum_t[h : h + 1, :], 0.0)
                m = jnp.where(lower, jnp.exp(gap) * scores, 0.0).astype(bf16)
                x = jnp.where(lane // p == h, xs[...].astype(f32), 0.0).astype(bf16)
                y = y + dot(m, x, 1, 0)
            inner[...] = y
            for r in range(0, rows, part):
                mixed[r : r + part, :] = sum(
                    glu[l_at + r + i : l_at + r + i + part, :] * ltaps[i : i + 1, :] for i in range(WIDE)
                )

    small = (ftaps, ltaps, xs, w16, cum, cum_t)
    return pl.pallas_call(
        body,
        grid=(steps,),
        out_shape=(
            pltpu.VMEM((rows, STATE), bf16), pltpu.VMEM((rows, ch), f32), pltpu.VMEM((rows, ch), f32),
            pltpu.VMEM((rows, ch), f32), pltpu.VMEM((d, 2 * ch), bf16),
        ),
        in_specs=[VMEM, pl.BlockSpec((kb, 6 * ch), lambda k: (k, 0)), *[VMEM] * len(small)],
        out_specs=(VMEM,) * 5,
        scratch_shapes=[pltpu.VMEM((ext, 4 * ch), f32), pltpu.VMEM((ext, ch), f32)],
        compiler_params=SMALL, name="rows_local",
    )(*held(normed), *fetched(rest), *held(*small))


def rows_done(got, enter, before, init, index, read16, zgate, mixed, inner, cum, gain, copies):
    rows, ch = mixed.shape
    n, _, _ = got.shape
    heads = init.shape[0]
    p = ch // heads

    def body(at, got, enter, before, init, read16, zgate, mixed, inner, cum, gain, sums, pre):
        acc_in = jnp.zeros((1, STATE), f32)
        start = enter[...]
        b = before[0:1, :]
        for j in reversed(range(n)):
            logs = jnp.sum(got[j, ch:, :].astype(f32), axis=0, keepdims=True)
            inside = (j < at[0]).astype(f32)
            start = start + got[j, :ch, :].astype(f32) * spread_heads(inside * jnp.exp(acc_in + b), heads, p)
            acc_in = acc_in + inside * logs
        start = start + init[...].reshape(ch, STATE) * spread_heads(jnp.exp(acc_in + b), heads, p)
        y = inner[...] + dot(read16[...], start.astype(bf16), 1, 1) * jnp.exp(cum[...])
        gated = y * zgate[...]
        mix = mixed[...]
        squares = jnp.concatenate([mix, mix * mix, gated * gated], 1)
        pick = lax.broadcasted_iota(jnp.int32, (8, 3 * ch), 1) // ch == lax.broadcasted_iota(jnp.int32, (8, 3 * ch), 0)
        found = dot(jnp.where(pick, 1.0, 0.0), squares, 1, 1, HIGHEST)
        for j in range(copies):
            sums[j] = found[:3]
        pre[:, :ch] = mix.astype(bf16)
        pre[:, ch:] = (gated * gain[...]).astype(bf16)

    return pl.pallas_call(
        body,
        out_shape=(sds((copies, 3, rows), f32), pltpu.VMEM((rows, 2 * ch), bf16)),
        in_specs=[SMEM, *[VMEM] * 10],
        out_specs=(VMEM, VMEM),
        compiler_params=SMALL, name="rows_done",
    )(index, *held(got, enter, before, init, read16, zgate, mixed, inner, cum, gain))


def output_rows(sums, both, gains, own, other, index, nf, nt):
    copies, _, rows = sums.shape
    ch = gains.shape[1]
    d = own.shape[0]
    piece = rows // (nf * nt)

    def body(at, sref, bref, gref, wa, wb, out, cols, act):
        tp = at[0]
        s = sref[0]
        for j in range(1, copies):
            s = s + sref[j]
        cols[...] = jnp.transpose(jnp.concatenate([s, jnp.zeros((5, rows), f32)], 0))
        for i in range(nf):
            at_row = pl.multiple_of(i * (nt * piece) + tp * piece, piece)
            here = slice(i * piece, (i + 1) * piece)
            t = cols[pl.ds(at_row, piece), :]
            mean = t[:, 0:1] / C_CH
            rstd = lax.rsqrt(t[:, 1:2] / C_CH - mean * mean + EPS)
            scale = lax.rsqrt(t[:, 2:3] / D_INNER + EPS)
            for j in range(nt):
                src = tp if j == 0 else 1 - tp
                a = bref[pl.ds(pl.multiple_of(src * rows + at_row, piece), piece), :].astype(f32)
                conv = jax.nn.silu((a[:, :ch] - mean) * rstd * gref[pl.ds(src, 1), :])
                act[here, 2 * j * ch : (2 * j + 1) * ch] = conv.astype(bf16)
                act[here, (2 * j + 1) * ch : (2 * j + 2) * ch] = (a[:, ch:] * scale).astype(bf16)
        term = dot(act[:, : 2 * ch], wa[...], 1, 1) + dot(act[:, 2 * ch :], wb[...], 1, 1)
        out[...] = term.astype(bf16).reshape(nf, piece, d)

    return pl.pallas_call(
        body,
        out_shape=sds((nf, piece, d), bf16),
        in_specs=[SMEM, *[VMEM] * 5],
        out_specs=VMEM,
        scratch_shapes=[pltpu.VMEM((rows, 8), f32), pltpu.VMEM((nf * piece, 4 * ch), bf16)],
        compiler_params=SMALL, name="output_rows",
    )(index, *held(sums, both, gains, own, other))


def per_device(
    tokens, norm_gain, conv_value, conv_gate, mixer_gate, state_input, write_projection, state_read,
    step_proj, step_bias, decay_log, decay_extra, input_taps, write_taps, fetch_taps, long_taps,
    conv_gain, state_gain, conv_output, state_output, initial_state,
):
    rows = tokens.shape[0]
    ch = conv_value.shape[1]
    heads = step_bias.shape[0]
    p = ch // heads
    nf, nt = lax.axis_size("fs"), lax.axis_size("tp")
    iz, iy, tp = (lax.axis_index(a).astype(jnp.int32).reshape(1) for a in ("sp_0", "sp_1", "tp"))
    ny = lax.axis_size("sp_1")
    first = lay_out((state_input, write_projection), lax.axis_size("sp_0"))
    first = lax.all_to_all(first, "sp_0", 0, 0, tiled=True)
    rest = lay_out((state_read, mixer_gate, conv_value, conv_gate, conv_output, state_output), ny)
    rest = lax.all_to_all(rest, "sp_1", 0, 0, tiled=True).reshape(-1, 6 * ch)
    rest = lax.all_gather(rest, "sp_0", axis=0, tiled=True)
    first = copies_of(first, ny)
    first = lax.all_to_all(first, "sp_1", 0, 0, tiled=True)
    n = lax.axis_size(SP)
    halo = lax.ppermute(tokens[rows - HALO :], SP, [(i, i + 1) for i in range(n - 1)])
    v = jnp.concatenate([halo, tokens], 0).astype(f32)
    normed = (v * lax.rsqrt(jnp.mean(v * v, axis=1, keepdims=True) + EPS) * norm_gain).astype(bf16)
    step_all = jnp.dot(normed[HALO:], step_proj, preferred_element_type=f32)
    me = lax.axis_index("fs") * nt + lax.axis_index("tp")
    step = jax.nn.softplus(lax.dynamic_slice_in_dim(step_all, me * heads, heads, 1) + step_bias)
    log_step = (-jnp.exp(decay_log) * step + decay_extra.T).T
    cum_t = jnp.cumsum(log_step, axis=1)
    total = cum_t[:, -1]
    cum = jnp.repeat(cum_t.T, p, axis=1)
    step = jnp.repeat(step, p, axis=1)
    left = jnp.repeat(jnp.exp(total[:, None] - cum_t).T, p, axis=1)
    total = jnp.pad(total[None], ((0, 0), (0, STATE - heads)))
    gains = lax.all_gather(conv_gain, "tp")
    taps = jnp.concatenate([input_taps, write_taps], 1)
    send, xs, w16 = local_states(normed, first, taps, step, left, total, ny)
    got = lax.all_to_all(send, "sp_1", 0, 0, tiled=True)
    enter, before, send = line_states(got, iy, heads, p, lax.axis_size("sp_0"))
    got = lax.all_to_all(send, "sp_0", 0, 0, tiled=True)
    read16, zgate, mixed, inner, back = rows_local(normed, rest, fetch_taps, long_taps, xs, w16, cum, cum_t)
    back_other = lax.ppermute(back, "tp", [(i, nt - 1 - i) for i in range(nt)])
    sums, pre = rows_done(
        got, enter, before, initial_state, iz, read16, zgate, mixed, inner, cum, state_gain[None], nf * nt
    )
    sums = lax.all_to_all(sums, FT, 0, 0, tiled=True)
    both = lax.all_gather(pre, "tp", axis=0, tiled=True)
    out = output_rows(sums, both, gains, back, back_other, tp, nf, nt)
    pieces = lax.all_to_all(out, "fs", 0, 0, tiled=True)
    return jnp.sum(pieces.astype(f32), 0).astype(bf16)


def solution(mesh):
    torus = Mesh(
        mesh.devices.reshape(8, 8, mesh.shape["fs"], mesh.shape["tp"]), ("sp_0", "sp_1", "fs", "tp")
    )
    w = P(SP, FT)
    in_specs = (
        P(SP, None), P(), w, w, w, w, w, w, P(), P(FT), P(FT), P(FT, SP), P(None, FT), P(None, FT), P(None, FT),
        P(None, FT), P(FT), P(FT), w, w, P(FT, None, None),
    )

    return jax.shard_map(per_device, mesh=torus, in_specs=in_specs, out_specs=P((*SP, *FT), None), check_vma=False)
```

profile of v0, /device:TPU:1, one launch (start us, length us, event | category | flops | bytes accessed | tf_op | source)
XLA Modules:
  0.0 149.9 jit_solution(12350014131818070161)
XLA Ops:
  6.5 0.9 shard_map.201
  7.5 19.1 %all_to_all.35 = bf16[8,32,768]{2,1,0:T(8,128)(2,1)} all-to-all(bf16[8,32,768]{2,1,0:T(8,128)(2,1)S(1)} %shard_map.201), channel_id=1, replica_groups=mesh['sp_0'=8,'sp_1'=8,'fs'=4,'tp'=2] {'sp_1'}, dimensions={0} | all-to-all | bytes 786432 | tf_op jit(solution)/shard_map/all_to_all | solution.py:300
  26.6 0.0 all-gather.4.cloned.1.call-update
  26.6 0.9 slice.15
  27.6 1.6 %collective-permute-start = (bf16[32,2048]{1,0:T(8,128)(2,1)S(1)}, bf16[32,2048]{1,0:T(8,128)(2,1)S(1)}, u32[]{:S(2)}, u32[]{:S(2)}) collective-permute-start(bf16[32,2048]{1,0:T(8,128)(2,1)S(1)} %slice.15), channel_id=1, source_target_pairs={{0,8},{8,16},{16,24},{24,32},{32,40},{40,48},{48,56},{56,64},{64,7... | collective-permute-start | bytes 393224 | tf_op jit(solution)/shard_map/ppermute | solution.py:305
  29.2 1.4 shard_map.199
  30.6 12.8 %all-to-all-start = ((bf16[8,32,256]{2,1,0:T(8,128)(2,1)}), bf16[8,32,256]{2,1,0:T(8,128)(2,1)S(1)}, u32[]{:S(2)}, u32[]{:S(2)}) async-start(bf16[8,32,256]{2,1,0:T(8,128)(2,1)} %shard_map.199), calls=%async_computation | async-start | bytes 262144 | tf_op jit(solution)/shard_map/all_to_all | solution.py:298
  43.4 0.7 exponential_negate_fusion
  44.0 0.7 pad_maximum_fusion.1.tref
  44.7 0.3 fusion
  45.0 7.5 %all-to-all-done.ref = bf16[8,32,256]{2,1,0:T(8,128)(2,1)S(1)} async-done(((bf16[8,32,256]{2,1,0:T(8,128)(2,1)}), bf16[8,32,256]{2,1,0:T(8,128)(2,1)S(1)}, u32[]{:S(2)}, u32[]{:S(2)}) %all-to-all-start) | async-done | bytes 131104 | tf_op jit(solution)/shard_map/all_to_all | solution.py:298
  52.6 1.1 shard_map.200
  53.7 4.4 %all-to-all-start.1 = ((bf16[8,8,32,256]{3,2,1,0:T(8,128)(2,1)}), bf16[8,8,32,256]{3,2,1,0:T(8,128)(2,1)S(1)}, u32[]{:S(2)}, u32[]{:S(2)}) async-start(bf16[8,8,32,256]{3,2,1,0:T(8,128)(2,1)} %shard_map.200), calls=%async_computation.1 | async-start | bytes 2097152 | tf_op jit(solution)/shard_map/all_to_all | solution.py:303
  58.1 0.0 copy-start.8
  58.1 1.6 %fusion.2.nref = bf16[288,2048]{1,0:T(8,128)(2,1)S(1)} fusion(f32[2048]{0:T(1024)S(1)} %copy-done.6, f32[288]{0:T(512)S(1)} %add_rsqrt_fusion, bf16[256,2048]{1,0:T(8,128)(2,1)} %param.21, bf16[32,2048]{1,0:T(8,128)(2,1)S(1)} %collective-permute-done), kind=kLoop, calls=%fused_computation.4 | loop fusion | flops 4128768 | bytes 2368640 | tf_op jit(solution)/shard_map/convert_element_type | solution.py:307
  59.7 0.4 fusion.3
  60.1 0.0 copy-done.8
  60.1 0.0 copy-start.2
  60.1 0.0 copy-start.3
  60.2 0.1 fusion.5
  60.3 0.6 reduce-window.6
  60.9 0.2 slice_reduce_fusion
  61.1 0.2 reduce-window.9
  61.2 0.1 add_bitcast_fusion
  61.3 0.2 slice_reduce_fusion.1
  61.5 0.1 exponential_bitcast_fusion
  61.6 0.1 copy.32.lref
  61.7 0.1 copy.31.sref
  61.8 21.9 %all-to-all-done.1.wref = bf16[8,8,32,256]{3,2,1,0:T(8,128)(2,1)S(1)} async-done(((bf16[8,8,32,256]{3,2,1,0:T(8,128)(2,1)}), bf16[8,8,32,256]{3,2,1,0:T(8,128)(2,1)S(1)}, u32[]{:S(2)}, u32[]{:S(2)}) %all-to-all-start.1) | async-done | bytes 1048608 | tf_op jit(solution)/shard_map/all_to_all | solution.py:303
  83.8 1.7 %local_states.1 = (bf16[8,144,128]{2,1,0:T(8,128)(2,1)}, bf16[256,128]{1,0:T(8,128)(2,1)S(1)}, bf16[256,128]{1,0:T(8,128)(2,1)S(1)}) custom-call(bf16[288,2048]{1,0:T(8,128)(2,1)S(1)} %fusion.2.nref, bf16[8,8,32,256]{3,2,1,0:T(8,128)(2,1)S(1)} %all-to-all-done.1.wref, f32[4,256]{1,0:T(4,128)S(1)} %pad_maximum_fusion.1.tref, f32[256,128]{1,0:T(8,128)S(1)} %copy.31.sref, ...), custom_call_target="tpu_custom_call" | custom-call | tf_op jit(solution)/shard_map/local_states/pallas_call | solution.py:100
  85.4 3.4 %all-to-all-start.2 = ((bf16[8,144,128]{2,1,0:T(8,128)(2,1)}), bf16[8,144,128]{2,1,0:T(8,128)(2,1)S(1)}, u32[]{:S(2)}, u32[]{:S(2)}) async-start(bf16[8,144,128]{2,1,0:T(8,128)(2,1)} %get-tuple-element.18), calls=%async_computation.2 | async-start | bytes 589824 | tf_op jit(solution)/shard_map/all_to_all | solution.py:321
  88.9 0.1 copy.33.cum
  89.0 0.0 all-gather.4.cloned.1.call-done.wref
  89.0 0.0 copy-start.9
  89.0 0.0 copy-start.1
  89.0 4.2 %rows_local.1 = (bf16[256,128]{1,0:T(8,128)(2,1)S(1)}, f32[256,128]{1,0:T(8,128)S(1)}, f32[256,128]{1,0:T(8,128)S(1)}, f32[256,128]{1,0:T(8,128)S(1)}, bf16[2048,256]{1,0:T(8,128)(2,1)S(1)}) custom-call(bf16[288,2048]{1,0:T(8,128)(2,1)S(1)} %fusion.2.nref, bf16[2048,768]{1,0:T(8,128)(2,1)} %all-gather.4.cloned.1.call-done.wref, f32[4,128]{1,0:T(4,128)S(1)} %copy-done.3, ...), custom_call_target="tpu_custom_call" | custom-call | tf_op jit(solution)/shard_map/rows_local/pallas_call | solution.py:197
  93.3 6.0 %collective-permute-start.1 = (bf16[2048,256]{1,0:T(8,128)(2,1)S(1)}, bf16[2048,256]{1,0:T(8,128)(2,1)}, u32[]{:S(2)}, u32[]{:S(2)}) collective-permute-start(bf16[2048,256]{1,0:T(8,128)(2,1)S(1)} %get-tuple-element.30.wa), channel_id=1, source_target_pairs={{0,1},{1,0},{2,3},{3,2},{4,5},{5,4},{6,7},{7,6},{8,9},{9,8},{10,11... | collective-permute-start | bytes 3145736 | tf_op jit(solution)/shard_map/ppermute | solution.py:325
  99.3 0.9 line_states.1
  100.2 3.4 %all-to-all-start.3 = ((bf16[8,144,128]{2,1,0:T(8,128)(2,1)}), bf16[8,144,128]{2,1,0:T(8,128)(2,1)S(1)}, u32[]{:S(2)}, u32[]{:S(2)}) async-start(bf16[8,144,128]{2,1,0:T(8,128)(2,1)} %get-tuple-element.19), calls=%async_computation.3 | async-start | bytes 589824 | tf_op jit(solution)/shard_map/all_to_all | solution.py:323
  103.7 5.8 %all-gather.1 = f32[2,1,128]{2,1,0:T(1,128)S(1)} all-gather(f32[1,1,128]{2,1,0:T(1,128)S(1)} %bitcast.44), channel_id=2, replica_groups=mesh['sp_0'=8,'sp_1'=8,'fs'=4,'tp'=2] {'tp'}, dimensions={0}, use_global_device_ids=true | all-gather | bytes 1536 | tf_op jit(solution)/shard_map/all_gather | solution.py:318
  109.5 3.8 %all-to-all-done.3.got = bf16[8,144,128]{2,1,0:T(8,128)(2,1)S(1)} async-done(((bf16[8,144,128]{2,1,0:T(8,128)(2,1)}), bf16[8,144,128]{2,1,0:T(8,128)(2,1)S(1)}, u32[]{:S(2)}, u32[]{:S(2)}) %all-to-all-start.3) | async-done | bytes 294944 | tf_op jit(solution)/shard_map/all_to_all | solution.py:323
  113.2 1.3 rows_done.1
  114.5 9.8 %all-to-all-start.5 = ((f32[8,3,256]{2,1,0:T(4,128)}), f32[8,3,256]{2,1,0:T(4,128)S(1)}, u32[]{:S(2)}, u32[]{:S(2)}) async-start(f32[8,3,256]{2,1,0:T(4,128)} %get-tuple-element.28), calls=%async_computation.5 | async-start | bytes 65536 | tf_op jit(solution)/shard_map/all_to_all | solution.py:329
  124.4 2.0 %all_gather.13.bref = bf16[512,256]{1,0:T(8,128)(2,1)S(1)} all-gather(bf16[256,256]{1,0:T(8,128)(2,1)S(1)} %get-tuple-element.29), channel_id=1, replica_groups=mesh['sp_0'=8,'sp_1'=8,'fs'=4,'tp'=2] {'tp'}, dimensions={0}, use_global_device_ids=true | all-gather | bytes 393216 | tf_op jit(solution)/shard_map/all_gather | solution.py:330
  126.3 2.7 %all-to-all-done.5.sref = f32[8,3,256]{2,1,0:T(4,128)S(1)} async-done(((f32[8,3,256]{2,1,0:T(4,128)}), f32[8,3,256]{2,1,0:T(4,128)S(1)}, u32[]{:S(2)}, u32[]{:S(2)}) %all-to-all-start.5) | async-done | bytes 24608 | tf_op jit(solution)/shard_map/all_to_all | solution.py:329
  129.1 2.3 %output_rows.1 = bf16[4,32,2048]{2,1,0:T(8,128)(2,1)S(1)} custom-call(s32[1]{0:T(128)} %bitcast.at, f32[8,3,256]{2,1,0:T(4,128)S(1)} %all-to-all-done.5.sref, bf16[512,256]{1,0:T(8,128)(2,1)S(1)} %all_gather.13.bref, f32[2,128]{1,0:T(2,128)S(1)} %bitcast.36, bf16[2048,256]{1,0:T(8,128)(2,1)S(1)} %get-tuple-element.30.wa, ...), custom_call_target="tpu_custom_call" | custom-call | tf_op jit(solution)/shard_map/output_rows/pallas_call | solution.py:275
  131.4 10.9 %all_to_all.36 = bf16[4,32,2048]{2,1,0:T(8,128)(2,1)S(1)} all-to-all(bf16[4,32,2048]{2,1,0:T(8,128)(2,1)S(1)} %output_rows.1), channel_id=1, replica_groups=mesh['sp_0'=8,'sp_1'=8,'fs'=4,'tp'=2] {'fs'}, dimensions={0} | all-to-all | bytes 1048576 | tf_op jit(solution)/shard_map/all_to_all | solution.py:332
  142.3 0.7 reduce_sum.22
  (25 shorter events, 0.1 us)
Async XLA Ops:
  6.5 53.2 %copy-start = (bf16[2048,16]{0,1:T(8,128)(2,1)S(1)}, bf16[2048,16]{0,1:T(8,128)(2,1)}, u32[]{:S(2)}) copy-start(bf16[2048,16]{0,1:T(8,128)(2,1)} %param.29) | copy-start | bytes 196612
  6.5 38.2 %copy-start.5 = (bf16[256,2048]{1,0:T(8,128)(2,1)S(1)}, bf16[256,2048]{1,0:T(8,128)(2,1)}, u32[]{:S(2)}) copy-start(bf16[256,2048]{1,0:T(8,128)(2,1)} %param.21) | copy-start | bytes 3145732
  6.5 82.4 %all-gather.4.cloned.1.call-start = ((), (), s32[]{:S(2)}) async-start(), calls=%async_computation.7 | async-start | bytes 3538944 | tf_op jit(solution)/shard_map/all_gather | solution.py:301
  27.6 17.2 %collective-permute-start = (bf16[32,2048]{1,0:T(8,128)(2,1)S(1)}, bf16[32,2048]{1,0:T(8,128)(2,1)S(1)}, u32[]{:S(2)}, u32[]{:S(2)}) collective-permute-start(bf16[32,2048]{1,0:T(8,128)(2,1)S(1)} %slice.15), channel_id=1, source_target_pairs={{0,8},{8,16},{16,24},{24,32},{32,40},{40,48},{48,56},{56,64},{64,7... | collective-permute-start | bytes 393224 | tf_op jit(solution)/shard_map/ppermute | solution.py:305
  30.6 27.6 %copy-start.6 = (f32[2048]{0:T(1024)S(1)}, f32[2048]{0:T(1024)}, u32[]{:S(2)}) copy-start(f32[2048]{0:T(1024)} %param.22) | copy-start | bytes 24580
  30.6 22.0 %all-to-all-start = ((bf16[8,32,256]{2,1,0:T(8,128)(2,1)}), bf16[8,32,256]{2,1,0:T(8,128)(2,1)S(1)}, u32[]{:S(2)}, u32[]{:S(2)}) async-start(bf16[8,32,256]{2,1,0:T(8,128)(2,1)} %shard_map.199), calls=%async_computation | async-start | bytes 262144 | tf_op jit(solution)/shard_map/all_to_all | solution.py:298
  53.7 30.1 %all-to-all-start.1 = ((bf16[8,8,32,256]{3,2,1,0:T(8,128)(2,1)}), bf16[8,8,32,256]{3,2,1,0:T(8,128)(2,1)S(1)}, u32[]{:S(2)}, u32[]{:S(2)}) async-start(bf16[8,8,32,256]{3,2,1,0:T(8,128)(2,1)} %shard_map.200), calls=%async_computation.1 | async-start | bytes 2097152 | tf_op jit(solution)/shard_map/all_to_all | solution.py:303
  58.1 2.0 %copy-start.7 = (f32[2,256]{1,0:T(2,128)S(1)}, f32[2,256]{1,0:T(2,128)}, u32[]{:S(2)}) copy-start(f32[2,256]{1,0:T(2,128)} %param.32) | copy-start | bytes 6148
  58.1 2.0 %copy-start.8 = (f32[2]{0:T(128)S(1)}, f32[2]{0:T(128)}, u32[]{:S(2)}) copy-start(f32[2]{0:T(128)} %param.30) | copy-start | bytes 28
  60.1 28.9 %copy-start.2 = (f32[31,128]{1,0:T(8,128)S(1)}, f32[31,128]{1,0:T(8,128)}, u32[]{:S(2)}) copy-start(f32[31,128]{1,0:T(8,128)} %ltaps.1) | copy-start | bytes 47620
  60.1 28.8 %copy-start.3 = (f32[4,128]{1,0:T(4,128)S(1)}, f32[4,128]{1,0:T(4,128)}, u32[]{:S(2)}) copy-start(f32[4,128]{1,0:T(4,128)} %ftaps.1) | copy-start | bytes 6148
  85.4 13.9 %all-to-all-start.2 = ((bf16[8,144,128]{2,1,0:T(8,128)(2,1)}), bf16[8,144,128]{2,1,0:T(8,128)(2,1)S(1)}, u32[]{:S(2)}, u32[]{:S(2)}) async-start(bf16[8,144,128]{2,1,0:T(8,128)(2,1)} %get-tuple-element.18), calls=%async_computation.2 | async-start | bytes 589824 | tf_op jit(solution)/shard_map/all_to_all | solution.py:321
  89.0 14.6 %copy-start.9 = (f32[128]{0:T(128)S(1)}, f32[128]{0:T(128)}, u32[]{:S(2)}) copy-start(f32[128]{0:T(128)} %param.37) | copy-start | bytes 1540
  89.0 24.2 %copy-start.1 = (f32[2,64,128]{2,1,0:T(8,128)S(1)}, f32[2,64,128]{2,1,0:T(8,128)}, u32[]{:S(2)}) copy-start(f32[2,64,128]{2,1,0:T(8,128)} %init.1) | copy-start | bytes 196612
  89.0 24.2 %copy-start.4 = (f32[128]{0:T(128)S(1)}, f32[128]{0:T(128)}, u32[]{:S(2)}) copy-start(f32[128]{0:T(128)} %param.38) | copy-start | bytes 1540
  93.3 35.8 %collective-permute-start.1 = (bf16[2048,256]{1,0:T(8,128)(2,1)S(1)}, bf16[2048,256]{1,0:T(8,128)(2,1)}, u32[]{:S(2)}, u32[]{:S(2)}) collective-permute-start(bf16[2048,256]{1,0:T(8,128)(2,1)S(1)} %get-tuple-element.30.wa), channel_id=1, source_target_pairs={{0,1},{1,0},{2,3},{3,2},{4,5},{5,4},{6,7},{7,6},{8,9},{9,8},{10,11... | collective-permute-start | bytes 3145736 | tf_op jit(solution)/shard_map/ppermute | solution.py:325
  100.2 13.0 %all-to-all-start.3 = ((bf16[8,144,128]{2,1,0:T(8,128)(2,1)}), bf16[8,144,128]{2,1,0:T(8,128)(2,1)S(1)}, u32[]{:S(2)}, u32[]{:S(2)}) async-start(bf16[8,144,128]{2,1,0:T(8,128)(2,1)} %get-tuple-element.19), calls=%async_computation.3 | async-start | bytes 589824 | tf_op jit(solution)/shard_map/all_to_all | solution.py:323
  114.5 14.5 %all-to-all-start.5 = ((f32[8,3,256]{2,1,0:T(4,128)}), f32[8,3,256]{2,1,0:T(4,128)S(1)}, u32[]{:S(2)}, u32[]{:S(2)}) async-start(f32[8,3,256]{2,1,0:T(4,128)} %get-tuple-element.28), calls=%async_computation.5 | async-start | bytes 65536 | tf_op jit(solution)/shard_map/all_to_all | solution.py:329
Sparse Core Ops, SparseCore 0:
  26.8 53.0 all-gather.3
where the time goes:
time: 151 us; the launch traced here: 150 us
  starting transfers between devices  41.5 us (27%)
  blocking collectives  37.9 us (25%)
  waiting for transfers between devices  36 us (24%)
  Pallas kernels  13.7 us (9%)
  between operations  13.7 us (9%)
  other arithmetic  5.05 us (3%)
  local copies, waits for them, and re-layouts  1.65 us (1%)
    all_to_all x1, waiting for transfers between devices, per_device(): first = lax.all_to_all(first, 'sp_1', 0, 0, tiled=True)  21.9 us
    all_to_all x1, blocking collectives, per_device(): rest = lax.all_to_all(rest, 'sp_1', 0, 0, tiled=True).reshape(-1, 6 * ch)  19.1 us
    all_to_all x1, starting transfers between devices, per_device(): first = lax.all_to_all(first, 'sp_0', 0, 0, tiled=True)  12.8 us
    all_to_all x1, blocking collectives, per_device(): pieces = lax.all_to_all(out, 'fs', 0, 0, tiled=True)  10.9 us
    all_to_all x1, starting transfers between devices, per_device(): sums = lax.all_to_all(sums, FT, 0, 0, tiled=True)  9.82 us
    all_to_all x1, waiting for transfers between devices, per_device(): first = lax.all_to_all(first, 'sp_0', 0, 0, tiled=True)  7.54 us
    ppermute x1, starting transfers between devices, per_device(): back_other = lax.ppermute(back, 'tp', [(i, nt - 1 - i) for i in range(nt)])  6 us
    all_gather x1, blocking collectives, per_device(): gains = lax.all_gather(conv_gain, 'tp')  5.84 us
  transfers between devices with their start and end apart: 8, of which 4 were waited for; matrix products, arithmetic and copies ran while one was open for 4% of the time, Pallas kernels for 7%

commit v1 on v0

--- a/solution.py
+++ b/solution.py
@@ -294,11 +294,10 @@
     nf, nt = lax.axis_size("fs"), lax.axis_size("tp")
     iz, iy, tp = (lax.axis_index(a).astype(jnp.int32).reshape(1) for a in ("sp_0", "sp_1", "tp"))
     ny = lax.axis_size("sp_1")
+    rest = lay_out((state_read, mixer_gate, conv_value, conv_gate, conv_output, state_output), 1)
+    rest = lax.all_gather(rest[0], SP, axis=0, tiled=True)
     first = lay_out((state_input, write_projection), lax.axis_size("sp_0"))
     first = lax.all_to_all(first, "sp_0", 0, 0, tiled=True)
-    rest = lay_out((state_read, mixer_gate, conv_value, conv_gate, conv_output, state_output), ny)
-    rest = lax.all_to_all(rest, "sp_1", 0, 0, tiled=True).reshape(-1, 6 * ch)
-    rest = lax.all_gather(rest, "sp_0", axis=0, tiled=True)
     first = copies_of(first, ny)
     first = lax.all_to_all(first, "sp_1", 0, 0, tiled=True)
     n = lax.axis_size(SP)

time: 151 us -> 166 us (1.099)
  waiting for transfers between devices: 36 us -> 74.5 us
  blocking collectives: 37.9 us -> 14.7 us
  starting transfers between devices: 41.5 us -> 38.5 us
    all_gather x1, waiting for transfers between devices: 0.02 us -> 30.5 us  [per_device(): rest = lax.all_gather(rest[0], SP, axis=0, tiled=True)]
    all_to_all x1 -> x0, blocking collectives: 19.1 us -> none  [per_device(): rest = lax.all_to_all(rest, 'sp_1', 0, 0, tiled=True).reshape(-1, 6 * ch)]
    all_to_all x1, waiting for transfers between devices: 3.75 us -> 11.3 us  [per_device(): got = lax.all_to_all(send, 'sp_0', 0, 0, tiled=True)]
    all_to_all x1, starting transfers between devices: 9.82 us -> 4.8 us  [per_device(): sums = lax.all_to_all(sums, FT, 0, 0, tiled=True)]
    all_gather x1, blocking collectives: 5.84 us -> 1.81 us  [per_device(): gains = lax.all_gather(conv_gain, 'tp')]
    all_to_all x1, waiting for transfers between devices: 21.9 us -> 24.9 us  [per_device(): first = lax.all_to_all(first, 'sp_1', 0, 0, tiled=True)]
    all_to_all x1, starting transfers between devices: 12.8 us -> 10.2 us  [per_device(): first = lax.all_to_all(first, 'sp_0', 0, 0, tiled=True)]
    all_to_all x1, waiting for transfers between devices: 7.54 us -> 5.03 us  [per_device(): first = lax.all_to_all(first, 'sp_0', 0, 0, tiled=True)]
  transfers between devices with their start and end apart: 8 -> 8, of which waited for: 4 -> 5; matrix products, arithmetic and copies ran while one was open for 4% -> 5% of each run, Pallas kernels for 7% -> 6%
where the time goes in v1:
time: 166 us; the launch traced here: 164 us
  waiting for transfers between devices  74.5 us (45%)
  starting transfers between devices  38.5 us (23%)
  blocking collectives  14.7 us (9%)
  Pallas kernels  14.3 us (9%)
  between operations  13.6 us (8%)
  other arithmetic  6.26 us (4%)
    all_gather x1, waiting for transfers between devices, per_device(): rest = lax.all_gather(rest[0], SP, axis=0, tiled=True)  30.5 us
    all_to_all x1, waiting for transfers between devices, per_device(): first = lax.all_to_all(first, 'sp_1', 0, 0, tiled=True)  24.9 us
    all_to_all x1, waiting for transfers between devices, per_device(): got = lax.all_to_all(send, 'sp_0', 0, 0, tiled=True)  11.3 us
    all_to_all x1, blocking collectives, per_device(): pieces = lax.all_to_all(out, 'fs', 0, 0, tiled=True)  10.9 us
    all_to_all x1, starting transfers between devices, per_device(): first = lax.all_to_all(first, 'sp_0', 0, 0, tiled=True)  10.2 us
    ppermute x1, starting transfers between devices, per_device(): back_other = lax.ppermute(back, 'tp', [(i, nt - 1 - i) for i in range(nt)])  5.96 us
    all_to_all x1, starting transfers between devices, per_device(): first = lax.all_to_all(first, 'sp_1', 0, 0, tiled=True)  5.92 us
    all_to_all x1, waiting for transfers between devices, per_device(): first = lax.all_to_all(first, 'sp_0', 0, 0, tiled=True)  5.03 us
  transfers between devices with their start and end apart: 8, of which 5 were waited for; matrix products, arithmetic and copies ran while one was open for 5% of the time, Pallas kernels for 6%

profile of v1, /device:TPU:1, one launch (start us, length us, event | category | flops | bytes accessed | tf_op | source)
XLA Modules:
  0.0 163.9 jit_solution(14437709738038909141)
XLA Ops:
  6.5 1.4 shard_map.201
  8.0 0.0 all-gather.5.cloned.1.call-update
  8.0 0.9 slice.15
  8.9 4.0 %collective-permute-start = (bf16[32,2048]{1,0:T(8,128)(2,1)S(1)}, bf16[32,2048]{1,0:T(8,128)(2,1)S(1)}, u32[]{:S(2)}, u32[]{:S(2)}) collective-permute-start(bf16[32,2048]{1,0:T(8,128)(2,1)S(1)} %slice.15), channel_id=1, source_target_pairs={{0,8},{8,16},{16,24},{24,32},{32,40},{40,48},{48,56},{56,64},{64,7... | collective-permute-start | bytes 393224 | tf_op jit(solution)/shard_map/ppermute | solution.py:304
  13.0 1.4 shard_map.199
  14.3 10.2 %all-to-all-start = ((bf16[8,32,256]{2,1,0:T(8,128)(2,1)}), bf16[8,32,256]{2,1,0:T(8,128)(2,1)S(1)}, u32[]{:S(2)}, u32[]{:S(2)}) async-start(bf16[8,32,256]{2,1,0:T(8,128)(2,1)} %shard_map.199), calls=%async_computation | async-start | bytes 262144 | tf_op jit(solution)/shard_map/all_to_all | solution.py:300
  24.5 0.7 exponential_negate_fusion
  25.2 0.7 pad_maximum_fusion.1.tref
  25.9 0.0 collective-permute-done
  25.9 1.5 fusion
  27.4 5.0 %all-to-all-done.ref = bf16[8,32,256]{2,1,0:T(8,128)(2,1)S(1)} async-done(((bf16[8,32,256]{2,1,0:T(8,128)(2,1)}), bf16[8,32,256]{2,1,0:T(8,128)(2,1)S(1)}, u32[]{:S(2)}, u32[]{:S(2)}) %all-to-all-start) | async-done | bytes 131104 | tf_op jit(solution)/shard_map/all_to_all | solution.py:300
  32.5 1.1 shard_map.200
  33.5 5.9 %all-to-all-start.1 = ((bf16[8,8,32,256]{3,2,1,0:T(8,128)(2,1)}), bf16[8,8,32,256]{3,2,1,0:T(8,128)(2,1)S(1)}, u32[]{:S(2)}, u32[]{:S(2)}) async-start(bf16[8,8,32,256]{3,2,1,0:T(8,128)(2,1)} %shard_map.200), calls=%async_computation.1 | async-start | bytes 2097152 | tf_op jit(solution)/shard_map/all_to_all | solution.py:302
  39.5 0.0 copy-start.7
  39.5 1.6 fusion.2.nref
  41.1 0.4 fusion.3
  41.4 0.0 copy-done.7
  41.5 0.0 copy-start.2
  41.5 0.0 copy-start.3
  41.5 0.1 fusion.5
  41.6 0.6 reduce-window.6
  42.2 0.2 slice_reduce_fusion
  42.4 0.2 reduce-window.9
  42.6 0.1 add_bitcast_fusion
  42.6 0.2 slice_reduce_fusion.1
  42.8 0.1 exponential_bitcast_fusion
  42.9 0.1 copy.32.lref
  43.1 0.1 copy.31.sref
  43.2 24.9 %all-to-all-done.1.wref = bf16[8,8,32,256]{3,2,1,0:T(8,128)(2,1)S(1)} async-done(((bf16[8,8,32,256]{3,2,1,0:T(8,128)(2,1)}), bf16[8,8,32,256]{3,2,1,0:T(8,128)(2,1)S(1)}, u32[]{:S(2)}, u32[]{:S(2)}) %all-to-all-start.1) | async-done | bytes 1048608 | tf_op jit(solution)/shard_map/all_to_all | solution.py:302
  68.1 1.7 %local_states.1 = (bf16[8,144,128]{2,1,0:T(8,128)(2,1)}, bf16[256,128]{1,0:T(8,128)(2,1)S(1)}, bf16[256,128]{1,0:T(8,128)(2,1)S(1)}) custom-call(bf16[288,2048]{1,0:T(8,128)(2,1)S(1)} %fusion.2.nref, bf16[8,8,32,256]{3,2,1,0:T(8,128)(2,1)S(1)} %all-to-all-done.1.wref, f32[4,256]{1,0:T(4,128)S(1)} %pad_maximum_fusion.1.tref, f32[256,128]{1,0:T(8,128)S(1)} %copy.31.sref, ...), custom_call_target="tpu_custom_call" | custom-call | tf_op jit(solution)/shard_map/local_states/pallas_call | solution.py:100
  69.7 3.4 %all-to-all-start.2 = ((bf16[8,144,128]{2,1,0:T(8,128)(2,1)}), bf16[8,144,128]{2,1,0:T(8,128)(2,1)S(1)}, u32[]{:S(2)}, u32[]{:S(2)}) async-start(bf16[8,144,128]{2,1,0:T(8,128)(2,1)} %get-tuple-element.18), calls=%async_computation.2 | async-start | bytes 589824 | tf_op jit(solution)/shard_map/all_to_all | solution.py:320
  73.2 0.1 copy.33.cum
  73.3 30.5 %all-gather.5.cloned.1.call-done = bf16[1,2048,768]{2,1,0:T(8,128)(2,1)} async-done(((bf16[1,32,768]{2,1,0:T(8,128)(2,1)}), bf16[1,2048,768]{2,1,0:T(8,128)(2,1)}) %all-gather.5.cloned.1.call-update) | async-done | bytes 3145744 | tf_op jit(solution)/shard_map/all_gather | solution.py:298
  103.8 0.0 copy-start.4
  103.8 4.3 %rows_local.1 = (bf16[256,128]{1,0:T(8,128)(2,1)S(1)}, f32[256,128]{1,0:T(8,128)S(1)}, f32[256,128]{1,0:T(8,128)S(1)}, f32[256,128]{1,0:T(8,128)S(1)}, bf16[2048,256]{1,0:T(8,128)(2,1)S(1)}) custom-call(bf16[288,2048]{1,0:T(8,128)(2,1)S(1)} %fusion.2.nref, bf16[2048,768]{1,0:T(8,128)(2,1)} %bitcast.38, f32[4,128]{1,0:T(4,128)S(1)} %copy-done.3, ...), custom_call_target="tpu_custom_call" | custom-call | tf_op jit(solution)/shard_map/rows_local/pallas_call | solution.py:197
  108.1 6.0 %collective-permute-start.1 = (bf16[2048,256]{1,0:T(8,128)(2,1)S(1)}, bf16[2048,256]{1,0:T(8,128)(2,1)}, u32[]{:S(2)}, u32[]{:S(2)}) collective-permute-start(bf16[2048,256]{1,0:T(8,128)(2,1)S(1)} %get-tuple-element.30.wa), channel_id=1, source_target_pairs={{0,1},{1,0},{2,3},{3,2},{4,5},{5,4},{6,7},{7,6},{8,9},{9,8},{10,11... | collective-permute-start | bytes 3145736 | tf_op jit(solution)/shard_map/ppermute | solution.py:324
  114.1 0.0 all-to-all-done.2.ref
  114.1 0.9 line_states.1
  115.0 4.2 %all-to-all-start.3 = ((bf16[8,144,128]{2,1,0:T(8,128)(2,1)}), bf16[8,144,128]{2,1,0:T(8,128)(2,1)S(1)}, u32[]{:S(2)}, u32[]{:S(2)}) async-start(bf16[8,144,128]{2,1,0:T(8,128)(2,1)} %get-tuple-element.19), calls=%async_computation.3 | async-start | bytes 589824 | tf_op jit(solution)/shard_map/all_to_all | solution.py:322
  119.2 1.8 %all-gather.2 = f32[2,1,128]{2,1,0:T(1,128)S(1)} all-gather(f32[1,1,128]{2,1,0:T(1,128)S(1)} %bitcast.44), channel_id=3, replica_groups=mesh['sp_0'=8,'sp_1'=8,'fs'=4,'tp'=2] {'tp'}, dimensions={0}, use_global_device_ids=true | all-gather | bytes 1536 | tf_op jit(solution)/shard_map/all_gather | solution.py:317
  121.1 11.3 %all-to-all-done.3.got = bf16[8,144,128]{2,1,0:T(8,128)(2,1)S(1)} async-done(((bf16[8,144,128]{2,1,0:T(8,128)(2,1)}), bf16[8,144,128]{2,1,0:T(8,128)(2,1)S(1)}, u32[]{:S(2)}, u32[]{:S(2)}) %all-to-all-start.3) | async-done | bytes 294944 | tf_op jit(solution)/shard_map/all_to_all | solution.py:322
  132.3 1.3 rows_done.1
  133.6 4.8 %all-to-all-start.4 = ((f32[8,3,256]{2,1,0:T(4,128)}), f32[8,3,256]{2,1,0:T(4,128)S(1)}, u32[]{:S(2)}, u32[]{:S(2)}) async-start(f32[8,3,256]{2,1,0:T(4,128)} %get-tuple-element.28), calls=%async_computation.4 | async-start | bytes 65536 | tf_op jit(solution)/shard_map/all_to_all | solution.py:328
  138.4 2.0 %all_gather.13.bref = bf16[512,256]{1,0:T(8,128)(2,1)S(1)} all-gather(bf16[256,256]{1,0:T(8,128)(2,1)S(1)} %get-tuple-element.29), channel_id=1, replica_groups=mesh['sp_0'=8,'sp_1'=8,'fs'=4,'tp'=2] {'tp'}, dimensions={0}, use_global_device_ids=true | all-gather | bytes 393216 | tf_op jit(solution)/shard_map/all_gather | solution.py:329
  140.4 2.7 %all-to-all-done.4.sref = f32[8,3,256]{2,1,0:T(4,128)S(1)} async-done(((f32[8,3,256]{2,1,0:T(4,128)}), f32[8,3,256]{2,1,0:T(4,128)S(1)}, u32[]{:S(2)}, u32[]{:S(2)}) %all-to-all-start.4) | async-done | bytes 24608 | tf_op jit(solution)/shard_map/all_to_all | solution.py:328
  143.1 2.3 %output_rows.1 = bf16[4,32,2048]{2,1,0:T(8,128)(2,1)S(1)} custom-call(s32[1]{0:T(128)} %bitcast.at, f32[8,3,256]{2,1,0:T(4,128)S(1)} %all-to-all-done.4.sref, bf16[512,256]{1,0:T(8,128)(2,1)S(1)} %all_gather.13.bref, f32[2,128]{1,0:T(2,128)S(1)} %bitcast.36, bf16[2048,256]{1,0:T(8,128)(2,1)S(1)} %get-tuple-element.30.wa, ...), custom_call_target="tpu_custom_call" | custom-call | tf_op jit(solution)/shard_map/output_rows/pallas_call | solution.py:275
  145.4 10.9 %all_to_all.30 = bf16[4,32,2048]{2,1,0:T(8,128)(2,1)S(1)} all-to-all(bf16[4,32,2048]{2,1,0:T(8,128)(2,1)S(1)} %output_rows.1), channel_id=1, replica_groups=mesh['sp_0'=8,'sp_1'=8,'fs'=4,'tp'=2] {'fs'}, dimensions={0} | all-to-all | bytes 1048576 | tf_op jit(solution)/shard_map/all_to_all | solution.py:331
  156.4 0.7 reduce_sum.22
  (22 shorter events, 0.1 us)
Async XLA Ops:
  6.5 34.5 %copy-start = (bf16[2048,16]{0,1:T(8,128)(2,1)S(1)}, bf16[2048,16]{0,1:T(8,128)(2,1)}, u32[]{:S(2)}) copy-start(bf16[2048,16]{0,1:T(8,128)(2,1)} %param.29) | copy-start | bytes 196612
  6.5 97.3 %all-gather.5.cloned.1.call-start = ((), (), s32[]{:S(2)}) async-start(), calls=%async_computation.6 | async-start | bytes 3194880 | tf_op jit(solution)/shard_map/all_gather | solution.py:298
  8.9 17.0 %collective-permute-start = (bf16[32,2048]{1,0:T(8,128)(2,1)S(1)}, bf16[32,2048]{1,0:T(8,128)(2,1)S(1)}, u32[]{:S(2)}, u32[]{:S(2)}) collective-permute-start(bf16[32,2048]{1,0:T(8,128)(2,1)S(1)} %slice.15), channel_id=1, source_target_pairs={{0,8},{8,16},{16,24},{24,32},{32,40},{40,48},{48,56},{56,64},{64,7... | collective-permute-start | bytes 393224 | tf_op jit(solution)/shard_map/ppermute | solution.py:304
  14.3 25.1 %copy-start.5 = (f32[2048]{0:T(1024)S(1)}, f32[2048]{0:T(1024)}, u32[]{:S(2)}) copy-start(f32[2048]{0:T(1024)} %param.22) | copy-start | bytes 24580
  14.3 18.1 %all-to-all-start = ((bf16[8,32,256]{2,1,0:T(8,128)(2,1)}), bf16[8,32,256]{2,1,0:T(8,128)(2,1)S(1)}, u32[]{:S(2)}, u32[]{:S(2)}) async-start(bf16[8,32,256]{2,1,0:T(8,128)(2,1)} %shard_map.199), calls=%async_computation | async-start | bytes 262144 | tf_op jit(solution)/shard_map/all_to_all | solution.py:300
  33.5 34.6 %all-to-all-start.1 = ((bf16[8,8,32,256]{3,2,1,0:T(8,128)(2,1)}), bf16[8,8,32,256]{3,2,1,0:T(8,128)(2,1)S(1)}, u32[]{:S(2)}, u32[]{:S(2)}) async-start(bf16[8,8,32,256]{3,2,1,0:T(8,128)(2,1)} %shard_map.200), calls=%async_computation.1 | async-start | bytes 2097152 | tf_op jit(solution)/shard_map/all_to_all | solution.py:302
  39.4 2.0 %copy-start.6 = (f32[2,256]{1,0:T(2,128)S(1)}, f32[2,256]{1,0:T(2,128)}, u32[]{:S(2)}) copy-start(f32[2,256]{1,0:T(2,128)} %param.32) | copy-start | bytes 6148
  39.5 2.0 %copy-start.7 = (f32[2]{0:T(128)S(1)}, f32[2]{0:T(128)}, u32[]{:S(2)}) copy-start(f32[2]{0:T(128)} %param.30) | copy-start | bytes 28
  41.5 62.4 %copy-start.2 = (f32[31,128]{1,0:T(8,128)S(1)}, f32[31,128]{1,0:T(8,128)}, u32[]{:S(2)}) copy-start(f32[31,128]{1,0:T(8,128)} %ltaps.1) | copy-start | bytes 47620
  41.5 62.4 %copy-start.3 = (f32[4,128]{1,0:T(4,128)S(1)}, f32[4,128]{1,0:T(4,128)}, u32[]{:S(2)}) copy-start(f32[4,128]{1,0:T(4,128)} %ftaps.1) | copy-start | bytes 6148
  69.7 44.3 %all-to-all-start.2 = ((bf16[8,144,128]{2,1,0:T(8,128)(2,1)}), bf16[8,144,128]{2,1,0:T(8,128)(2,1)S(1)}, u32[]{:S(2)}, u32[]{:S(2)}) async-start(bf16[8,144,128]{2,1,0:T(8,128)(2,1)} %get-tuple-element.18), calls=%async_computation.2 | async-start | bytes 589824 | tf_op jit(solution)/shard_map/all_to_all | solution.py:320
  103.8 15.4 %copy-start.8 = (f32[128]{0:T(128)S(1)}, f32[128]{0:T(128)}, u32[]{:S(2)}) copy-start(f32[128]{0:T(128)} %param.37) | copy-start | bytes 1540
  103.8 28.5 %copy-start.1 = (f32[2,64,128]{2,1,0:T(8,128)S(1)}, f32[2,64,128]{2,1,0:T(8,128)}, u32[]{:S(2)}) copy-start(f32[2,64,128]{2,1,0:T(8,128)} %init.1) | copy-start | bytes 196612
  103.8 28.5 %copy-start.4 = (f32[128]{0:T(128)S(1)}, f32[128]{0:T(128)}, u32[]{:S(2)}) copy-start(f32[128]{0:T(128)} %param.38) | copy-start | bytes 1540
  108.1 35.0 %collective-permute-start.1 = (bf16[2048,256]{1,0:T(8,128)(2,1)S(1)}, bf16[2048,256]{1,0:T(8,128)(2,1)}, u32[]{:S(2)}, u32[]{:S(2)}) collective-permute-start(bf16[2048,256]{1,0:T(8,128)(2,1)S(1)} %get-tuple-element.30.wa), channel_id=1, source_target_pairs={{0,1},{1,0},{2,3},{3,2},{4,5},{5,4},{6,7},{7,6},{8,9},{9,8},{10,11... | collective-permute-start | bytes 3145736 | tf_op jit(solution)/shard_map/ppermute | solution.py:324
  115.0 17.3 %all-to-all-start.3 = ((bf16[8,144,128]{2,1,0:T(8,128)(2,1)}), bf16[8,144,128]{2,1,0:T(8,128)(2,1)S(1)}, u32[]{:S(2)}, u32[]{:S(2)}) async-start(bf16[8,144,128]{2,1,0:T(8,128)(2,1)} %get-tuple-element.19), calls=%async_computation.3 | async-start | bytes 589824 | tf_op jit(solution)/shard_map/all_to_all | solution.py:322
  133.6 9.5 %all-to-all-start.4 = ((f32[8,3,256]{2,1,0:T(4,128)}), f32[8,3,256]{2,1,0:T(4,128)S(1)}, u32[]{:S(2)}, u32[]{:S(2)}) async-start(f32[8,3,256]{2,1,0:T(4,128)} %get-tuple-element.28), calls=%async_computation.4 | async-start | bytes 65536 | tf_op jit(solution)/shard_map/all_to_all | solution.py:328
Sparse Core Ops, SparseCore 0:
  10.3 93.4 all-gather.4

commit v2 on v0

--- a/solution.py
+++ b/solution.py
@@ -56,16 +56,6 @@
     )(*fetched(*shards))
 
 
-def copies_of(block, copies):
-    def body(ref, out):
-        for k in range(copies):
-            out[k] = ref[...]
-
-    return pl.pallas_call(
-        body, out_shape=sds((copies, *block.shape), bf16), in_specs=[VMEM], out_specs=VMEM, compiler_params=SMALL
-    )(*held(block))
-
-
 def log_rows(logs):
     hi = logs.astype(bf16).astype(f32)
     mid = (logs - hi).astype(bf16).astype(f32)
@@ -75,15 +65,11 @@
 
 
 def local_states(normed, first, taps, step, left, total, copies):
-    ext, d = normed.shape
+    ext, _ = normed.shape
     rows, ch = step.shape
-    ny, nz, piece, _ = first.shape
-
-    def body(nref, wref, tref, sref, lref, logs, send, xs, w16, buf, wall):
-        for y in range(ny):
-            for z in range(nz):
-                wall[(z * ny + y) * piece : (z * ny + y + 1) * piece, :] = wref[y, z]
-        buf[...] = dot(nref[...], wall[...], 1, 0).astype(bf16).astype(f32)
+
+    def body(nref, wref, tref, sref, lref, logs, send, xs, w16, buf):
+        buf[...] = dot(nref[...], wref[...], 1, 0).astype(bf16).astype(f32)
         at = HALO - SHORT + 1
         mix = sum(buf[at + i : at + i + rows, :] * tref[i : i + 1, :] for i in range(SHORT))
         act = jax.nn.silu(mix)
@@ -102,7 +88,7 @@
         out_shape=(sds((copies, ch + LOGS, STATE), bf16), pltpu.VMEM((rows, ch), bf16), pltpu.VMEM((rows, STATE), bf16)),
         in_specs=[VMEM] * 6,
         out_specs=(VMEM,) * 3,
-        scratch_shapes=[pltpu.VMEM((ext, 2 * ch), f32), pltpu.VMEM((d, 2 * ch), bf16)],
+        scratch_shapes=[pltpu.VMEM((ext, 2 * ch), f32)],
         compiler_params=SMALL, name="local_states",
     )(*held(normed, first, taps, step, left, total))
 
@@ -294,13 +280,11 @@
     nf, nt = lax.axis_size("fs"), lax.axis_size("tp")
     iz, iy, tp = (lax.axis_index(a).astype(jnp.int32).reshape(1) for a in ("sp_0", "sp_1", "tp"))
     ny = lax.axis_size("sp_1")
-    first = lay_out((state_input, write_projection), lax.axis_size("sp_0"))
-    first = lax.all_to_all(first, "sp_0", 0, 0, tiled=True)
     rest = lay_out((state_read, mixer_gate, conv_value, conv_gate, conv_output, state_output), ny)
     rest = lax.all_to_all(rest, "sp_1", 0, 0, tiled=True).reshape(-1, 6 * ch)
     rest = lax.all_gather(rest, "sp_0", axis=0, tiled=True)
-    first = copies_of(first, ny)
-    first = lax.all_to_all(first, "sp_1", 0, 0, tiled=True)
+    first = lay_out((state_input, write_projection), lax.axis_size(SP))
+    first = lax.all_to_all(first, SP, 0, 0, tiled=True).reshape(-1, 2 * ch)
     n = lax.axis_size(SP)
     halo = lax.ppermute(tokens[rows - HALO :], SP, [(i, i + 1) for i in range(n - 1)])
     v = jnp.concatenate([halo, tokens], 0).astype(f32)

time: 151 us -> 158 us (1.046)
  waiting for transfers between devices: 36 us -> 51.8 us
  blocking collectives: 37.9 us -> 34 us
  other arithmetic: 5.05 us -> 2.46 us
  starting transfers between devices: 41.5 us -> 39.5 us
    all_gather x1, waiting for transfers between devices: 0.02 us -> 14.9 us  [per_device(): rest = lax.all_gather(rest, 'sp_0', axis=0, tiled=True)]
    all_to_all x1, waiting for transfers between devices: 3.75 us -> 11.3 us  [per_device(): got = lax.all_to_all(send, 'sp_0', 0, 0, tiled=True)]
    all_to_all x1, starting transfers between devices: 3.42 us -> 9.98 us  [per_device(): got = lax.all_to_all(send, 'sp_1', 0, 0, tiled=True)]
    all_to_all x2 -> x1, waiting for transfers between devices: 29.5 us -> 22.9 us  [per_device(): first = lax.all_to_all(first, SP, 0, 0, tiled=True).reshape(-1, 2 * ch)]
    all_to_all x1, starting transfers between devices: 9.82 us -> 4.71 us  [per_device(): sums = lax.all_to_all(sums, FT, 0, 0, tiled=True)]
    all_gather x1, blocking collectives: 5.84 us -> 1.81 us  [per_device(): gains = lax.all_gather(conv_gain, 'tp')]
    ppermute x1, starting transfers between devices: 6 us -> 2.75 us  [per_device(): back_other = lax.ppermute(back, 'tp', [(i, nt - 1 - i) for i in range(nt)])]
    all_to_all x2 -> x1, starting transfers between devices: 17.2 us -> 16.6 us  [per_device(): first = lax.all_to_all(first, SP, 0, 0, tiled=True).reshape(-1, 2 * ch)]
  transfers between devices with their start and end apart: 8 -> 7, of which waited for: 4 -> 4; matrix products, arithmetic and copies ran while one was open for 4% -> 2% of each run, Pallas kernels for 7% -> 6%
where the time goes in v2:
time: 158 us; the launch traced here: 157 us
  waiting for transfers between devices  51.8 us (33%)
  starting transfers between devices  39.5 us (25%)
  blocking collectives  34 us (22%)
  between operations  13.7 us (9%)
  Pallas kernels  13.2 us (8%)
  other arithmetic  2.46 us (2%)
  local copies, waits for them, and re-layouts  1.67 us (1%)
    all_to_all x1, waiting for transfers between devices, per_device(): first = lax.all_to_all(first, SP, 0, 0, tiled=True).reshape(-1, 2 * ch)  22.9 us
    all_to_all x1, blocking collectives, per_device(): rest = lax.all_to_all(rest, 'sp_1', 0, 0, tiled=True).reshape(-1, 6 * ch)  19.3 us
    all_to_all x1, starting transfers between devices, per_device(): first = lax.all_to_all(first, SP, 0, 0, tiled=True).reshape(-1, 2 * ch)  16.6 us
    all_gather x1, waiting for transfers between devices, per_device(): rest = lax.all_gather(rest, 'sp_0', axis=0, tiled=True)  14.9 us
    all_to_all x1, waiting for transfers between devices, per_device(): got = lax.all_to_all(send, 'sp_0', 0, 0, tiled=True)  11.3 us
    all_to_all x1, blocking collectives, per_device(): pieces = lax.all_to_all(out, 'fs', 0, 0, tiled=True)  10.9 us
    all_to_all x1, starting transfers between devices, per_device(): got = lax.all_to_all(send, 'sp_1', 0, 0, tiled=True)  9.98 us
    all_to_all x1, starting transfers between devices, per_device(): sums = lax.all_to_all(sums, FT, 0, 0, tiled=True)  4.71 us
  transfers between devices with their start and end apart: 7, of which 4 were waited for; matrix products, arithmetic and copies ran while one was open for 2% of the time, Pallas kernels for 6%

profile of v2, /device:TPU:1, one launch (start us, length us, event | category | flops | bytes accessed | tf_op | source)
XLA Modules:
  0.0 156.8 jit_solution(2043859977383437559)
XLA Ops:
  6.5 0.9 shard_map.200
  7.4 0.0 copy-start.11
  7.4 0.0 copy-start.8
  7.4 0.0 copy-start.9
  7.4 0.0 copy-start.5
  7.5 19.3 %all_to_all.30 = bf16[8,32,768]{2,1,0:T(8,128)(2,1)} all-to-all(bf16[8,32,768]{2,1,0:T(8,128)(2,1)S(1)} %shard_map.200), channel_id=1, replica_groups=mesh['sp_0'=8,'sp_1'=8,'fs'=4,'tp'=2] {'sp_1'}, dimensions={0} | all-to-all | bytes 786432 | tf_op jit(solution)/shard_map/all_to_all | solution.py:284
  26.7 0.0 all-gather.4.cloned.1.call-update
  26.8 0.0 copy-start.6
  26.8 0.9 slice.15
  27.7 1.6 %collective-permute-start = (bf16[32,2048]{1,0:T(8,128)(2,1)S(1)}, bf16[32,2048]{1,0:T(8,128)(2,1)S(1)}, u32[]{:S(2)}, u32[]{:S(2)}) collective-permute-start(bf16[32,2048]{1,0:T(8,128)(2,1)S(1)} %slice.15), channel_id=1, source_target_pairs={{0,8},{8,16},{16,24},{24,32},{32,40},{40,48},{48,56},{56,64},{64,7... | collective-permute-start | bytes 393224 | tf_op jit(solution)/shard_map/ppermute | solution.py:289
  29.3 2.0 %shard_map.199 = bf16[64,32,256]{2,1,0:T(8,128)(2,1)} custom-call(bf16[32,128]{1,0:T(8,128)(2,1)} %refs_0_.2, bf16[32,128]{1,0:T(8,128)(2,1)} %refs_1_.2), custom_call_target="tpu_custom_call" | custom-call | tf_op jit(solution)/shard_map/pallas_call | solution.py:54
  31.3 16.6 %all-to-all-start = ((bf16[64,32,256]{2,1,0:T(8,128)(2,1)}), bf16[64,32,256]{2,1,0:T(8,128)(2,1)S(1)}, u32[]{:S(2)}, u32[]{:S(2)}) async-start(bf16[64,32,256]{2,1,0:T(8,128)(2,1)} %shard_map.199), calls=%async_computation | async-start | bytes 2097152 | tf_op jit(solution)/shard_map/all_to_all | solution.py:287
  48.0 0.0 copy-start.7
  48.0 0.0 copy-start.10
  48.0 0.3 fusion
  48.3 0.3 fusion.2.nref
  48.7 0.4 fusion.3
  49.1 0.0 copy-done.10
  49.1 0.0 copy-start.2
  49.1 0.0 copy-start.3
  49.1 0.1 fusion.5
  49.2 0.6 reduce-window.6
  49.9 0.2 slice_reduce_fusion
  50.0 0.2 reduce-window.9
  50.2 0.1 add_bitcast_fusion
  50.3 0.2 slice_reduce_fusion.1
  50.5 0.1 exponential_bitcast_fusion
  50.6 0.1 copy.32.lref
  50.7 0.1 copy.31.sref
  50.8 22.9 %all-to-all-done = bf16[64,32,256]{2,1,0:T(8,128)(2,1)S(1)} async-done(((bf16[64,32,256]{2,1,0:T(8,128)(2,1)}), bf16[64,32,256]{2,1,0:T(8,128)(2,1)S(1)}, u32[]{:S(2)}, u32[]{:S(2)}) %all-to-all-start) | async-done | bytes 1048608 | tf_op jit(solution)/shard_map/all_to_all | solution.py:287
  73.7 1.7 %local_states.1 = (bf16[8,144,128]{2,1,0:T(8,128)(2,1)}, bf16[256,128]{1,0:T(8,128)(2,1)S(1)}, bf16[256,128]{1,0:T(8,128)(2,1)S(1)}) custom-call(bf16[288,2048]{1,0:T(8,128)(2,1)S(1)} %fusion.2.nref, bf16[2048,256]{1,0:T(8,128)(2,1)S(1)} %bitcast.34, f32[4,256]{1,0:T(4,128)S(1)} %pad_maximum_fusion.1.tref, f32[256,128]{1,0:T(8,128)S(1)} %copy.31.sref, ...), custom_call_target="tpu_custom_call" | custom-call | tf_op jit(solution)/shard_map/local_states/pallas_call | solution.py:86
  75.4 10.0 %all-to-all-start.1 = ((bf16[8,144,128]{2,1,0:T(8,128)(2,1)}), bf16[8,144,128]{2,1,0:T(8,128)(2,1)S(1)}, u32[]{:S(2)}, u32[]{:S(2)}) async-start(bf16[8,144,128]{2,1,0:T(8,128)(2,1)} %get-tuple-element.18), calls=%async_computation.1 | async-start | bytes 589824 | tf_op jit(solution)/shard_map/all_to_all | solution.py:305
  85.4 0.1 copy.33.cum
  85.5 14.9 %all-gather.4.cloned.1.call-done.wref = bf16[2048,768]{1,0:T(8,128)(2,1)} async-done(((bf16[256,768]{1,0:T(8,128)(2,1)}), bf16[2048,768]{1,0:T(8,128)(2,1)}) %all-gather.4.cloned.1.call-update) | async-done | bytes 3145744 | tf_op jit(solution)/shard_map/all_gather | solution.py:285
  100.3 0.0 copy-start.4
  100.4 4.2 %rows_local.1 = (bf16[256,128]{1,0:T(8,128)(2,1)S(1)}, f32[256,128]{1,0:T(8,128)S(1)}, f32[256,128]{1,0:T(8,128)S(1)}, f32[256,128]{1,0:T(8,128)S(1)}, bf16[2048,256]{1,0:T(8,128)(2,1)S(1)}) custom-call(bf16[288,2048]{1,0:T(8,128)(2,1)S(1)} %fusion.2.nref, bf16[2048,768]{1,0:T(8,128)(2,1)} %all-gather.4.cloned.1.call-done.wref, f32[4,128]{1,0:T(4,128)S(1)} %copy-done.3, ...), custom_call_target="tpu_custom_call" | custom-call | tf_op jit(solution)/shard_map/rows_local/pallas_call | solution.py:183
  104.6 2.8 %collective-permute-start.1 = (bf16[2048,256]{1,0:T(8,128)(2,1)S(1)}, bf16[2048,256]{1,0:T(8,128)(2,1)}, u32[]{:S(2)}, u32[]{:S(2)}) collective-permute-start(bf16[2048,256]{1,0:T(8,128)(2,1)S(1)} %get-tuple-element.30.wa), channel_id=1, source_target_pairs={{0,1},{1,0},{2,3},{3,2},{4,5},{5,4},{6,7},{7,6},{8,9},{9,8},{10,11... | collective-permute-start | bytes 3145736 | tf_op jit(solution)/shard_map/ppermute | solution.py:309
  107.4 0.9 line_states.1
  108.3 3.9 %all-to-all-start.2 = ((bf16[8,144,128]{2,1,0:T(8,128)(2,1)}), bf16[8,144,128]{2,1,0:T(8,128)(2,1)S(1)}, u32[]{:S(2)}, u32[]{:S(2)}) async-start(bf16[8,144,128]{2,1,0:T(8,128)(2,1)} %get-tuple-element.19), calls=%async_computation.2 | async-start | bytes 589824 | tf_op jit(solution)/shard_map/all_to_all | solution.py:307
  112.2 1.8 %all-gather.1 = f32[2,1,128]{2,1,0:T(1,128)S(1)} all-gather(f32[1,1,128]{2,1,0:T(1,128)S(1)} %bitcast.46), channel_id=2, replica_groups=mesh['sp_0'=8,'sp_1'=8,'fs'=4,'tp'=2] {'tp'}, dimensions={0}, use_global_device_ids=true | all-gather | bytes 1536 | tf_op jit(solution)/shard_map/all_gather | solution.py:302
  114.0 11.3 %all-to-all-done.2.got = bf16[8,144,128]{2,1,0:T(8,128)(2,1)S(1)} async-done(((bf16[8,144,128]{2,1,0:T(8,128)(2,1)}), bf16[8,144,128]{2,1,0:T(8,128)(2,1)S(1)}, u32[]{:S(2)}, u32[]{:S(2)}) %all-to-all-start.2) | async-done | bytes 294944 | tf_op jit(solution)/shard_map/all_to_all | solution.py:307
  125.2 1.3 rows_done.1
  126.5 4.7 %all-to-all-start.4 = ((f32[8,3,256]{2,1,0:T(4,128)}), f32[8,3,256]{2,1,0:T(4,128)S(1)}, u32[]{:S(2)}, u32[]{:S(2)}) async-start(f32[8,3,256]{2,1,0:T(4,128)} %get-tuple-element.28), calls=%async_computation.4 | async-start | bytes 65536 | tf_op jit(solution)/shard_map/all_to_all | solution.py:313
  131.2 2.0 %all_gather.13.bref = bf16[512,256]{1,0:T(8,128)(2,1)S(1)} all-gather(bf16[256,256]{1,0:T(8,128)(2,1)S(1)} %get-tuple-element.29), channel_id=1, replica_groups=mesh['sp_0'=8,'sp_1'=8,'fs'=4,'tp'=2] {'tp'}, dimensions={0}, use_global_device_ids=true | all-gather | bytes 393216 | tf_op jit(solution)/shard_map/all_gather | solution.py:314
  133.2 2.7 %all-to-all-done.4.sref = f32[8,3,256]{2,1,0:T(4,128)S(1)} async-done(((f32[8,3,256]{2,1,0:T(4,128)}), f32[8,3,256]{2,1,0:T(4,128)S(1)}, u32[]{:S(2)}, u32[]{:S(2)}) %all-to-all-start.4) | async-done | bytes 24608 | tf_op jit(solution)/shard_map/all_to_all | solution.py:313
  135.9 2.3 %output_rows.1 = bf16[4,32,2048]{2,1,0:T(8,128)(2,1)S(1)} custom-call(s32[1]{0:T(128)} %bitcast.at, f32[8,3,256]{2,1,0:T(4,128)S(1)} %all-to-all-done.4.sref, bf16[512,256]{1,0:T(8,128)(2,1)S(1)} %all_gather.13.bref, f32[2,128]{1,0:T(2,128)S(1)} %bitcast.38, bf16[2048,256]{1,0:T(8,128)(2,1)S(1)} %get-tuple-element.30.wa, ...), custom_call_target="tpu_custom_call" | custom-call | tf_op jit(solution)/shard_map/output_rows/pallas_call | solution.py:261
  138.2 10.9 %all_to_all.31 = bf16[4,32,2048]{2,1,0:T(8,128)(2,1)S(1)} all-to-all(bf16[4,32,2048]{2,1,0:T(8,128)(2,1)S(1)} %output_rows.1), channel_id=1, replica_groups=mesh['sp_0'=8,'sp_1'=8,'fs'=4,'tp'=2] {'fs'}, dimensions={0} | all-to-all | bytes 1048576 | tf_op jit(solution)/shard_map/all_to_all | solution.py:316
  149.2 0.7 reduce_sum.22
  (28 shorter events, 0.1 us)
Async XLA Ops:
  6.5 42.2 %copy-start = (bf16[2048,16]{0,1:T(8,128)(2,1)S(1)}, bf16[2048,16]{0,1:T(8,128)(2,1)}, u32[]{:S(2)}) copy-start(bf16[2048,16]{0,1:T(8,128)(2,1)} %param.29) | copy-start | bytes 196612
  6.5 93.8 %all-gather.4.cloned.1.call-start = ((), (), s32[]{:S(2)}) async-start(), calls=%async_computation.6 | async-start | bytes 3538944 | tf_op jit(solution)/shard_map/all_gather | solution.py:285
  7.4 40.5 %copy-start.11 = (f32[2]{0:T(128)S(1)}, f32[2]{0:T(128)}, u32[]{:S(2)}) copy-start(f32[2]{0:T(128)} %param.31) | copy-start | bytes 28
  7.4 40.5 %copy-start.8 = (f32[4,128]{1,0:T(4,128)S(1)}, f32[4,128]{1,0:T(4,128)}, u32[]{:S(2)}) copy-start(f32[4,128]{1,0:T(4,128)} %param.34) | copy-start | bytes 6148
  7.4 40.5 %copy-start.9 = (f32[4,128]{1,0:T(4,128)S(1)}, f32[4,128]{1,0:T(4,128)}, u32[]{:S(2)}) copy-start(f32[4,128]{1,0:T(4,128)} %param.33) | copy-start | bytes 6148
  7.4 40.6 %copy-start.5 = (bf16[256,2048]{1,0:T(8,128)(2,1)S(1)}, bf16[256,2048]{1,0:T(8,128)(2,1)}, u32[]{:S(2)}) copy-start(bf16[256,2048]{1,0:T(8,128)(2,1)} %param.21) | copy-start | bytes 3145732
  26.8 21.6 %copy-start.6 = (f32[2048]{0:T(1024)S(1)}, f32[2048]{0:T(1024)}, u32[]{:S(2)}) copy-start(f32[2048]{0:T(1024)} %param.22) | copy-start | bytes 24580
  27.7 20.3 %collective-permute-start = (bf16[32,2048]{1,0:T(8,128)(2,1)S(1)}, bf16[32,2048]{1,0:T(8,128)(2,1)S(1)}, u32[]{:S(2)}, u32[]{:S(2)}) collective-permute-start(bf16[32,2048]{1,0:T(8,128)(2,1)S(1)} %slice.15), channel_id=1, source_target_pairs={{0,8},{8,16},{16,24},{24,32},{32,40},{40,48},{48,56},{56,64},{64,7... | collective-permute-start | bytes 393224 | tf_op jit(solution)/shard_map/ppermute | solution.py:289
  31.3 42.4 %all-to-all-start = ((bf16[64,32,256]{2,1,0:T(8,128)(2,1)}), bf16[64,32,256]{2,1,0:T(8,128)(2,1)S(1)}, u32[]{:S(2)}, u32[]{:S(2)}) async-start(bf16[64,32,256]{2,1,0:T(8,128)(2,1)} %shard_map.199), calls=%async_computation | async-start | bytes 2097152 | tf_op jit(solution)/shard_map/all_to_all | solution.py:287
  48.0 1.1 copy-start.7
  48.0 1.1 copy-start.10
  49.1 51.2 %copy-start.2 = (f32[31,128]{1,0:T(8,128)S(1)}, f32[31,128]{1,0:T(8,128)}, u32[]{:S(2)}) copy-start(f32[31,128]{1,0:T(8,128)} %ltaps.1) | copy-start | bytes 47620
  49.1 51.2 %copy-start.3 = (f32[4,128]{1,0:T(4,128)S(1)}, f32[4,128]{1,0:T(4,128)}, u32[]{:S(2)}) copy-start(f32[4,128]{1,0:T(4,128)} %ftaps.1) | copy-start | bytes 6148
  75.4 32.0 %all-to-all-start.1 = ((bf16[8,144,128]{2,1,0:T(8,128)(2,1)}), bf16[8,144,128]{2,1,0:T(8,128)(2,1)S(1)}, u32[]{:S(2)}, u32[]{:S(2)}) async-start(bf16[8,144,128]{2,1,0:T(8,128)(2,1)} %get-tuple-element.18), calls=%async_computation.1 | async-start | bytes 589824 | tf_op jit(solution)/shard_map/all_to_all | solution.py:305
  100.3 11.8 %copy-start.12 = (f32[128]{0:T(128)S(1)}, f32[128]{0:T(128)}, u32[]{:S(2)}) copy-start(f32[128]{0:T(128)} %param.37) | copy-start | bytes 1540
  100.3 24.9 %copy-start.1 = (f32[2,64,128]{2,1,0:T(8,128)S(1)}, f32[2,64,128]{2,1,0:T(8,128)}, u32[]{:S(2)}) copy-start(f32[2,64,128]{2,1,0:T(8,128)} %init.1) | copy-start | bytes 196612
  100.3 24.9 %copy-start.4 = (f32[128]{0:T(128)S(1)}, f32[128]{0:T(128)}, u32[]{:S(2)}) copy-start(f32[128]{0:T(128)} %param.38) | copy-start | bytes 1540
  104.6 31.3 %collective-permute-start.1 = (bf16[2048,256]{1,0:T(8,128)(2,1)S(1)}, bf16[2048,256]{1,0:T(8,128)(2,1)}, u32[]{:S(2)}, u32[]{:S(2)}) collective-permute-start(bf16[2048,256]{1,0:T(8,128)(2,1)S(1)} %get-tuple-element.30.wa), channel_id=1, source_target_pairs={{0,1},{1,0},{2,3},{3,2},{4,5},{5,4},{6,7},{7,6},{8,9},{9,8},{10,11... | collective-permute-start | bytes 3145736 | tf_op jit(solution)/shard_map/ppermute | solution.py:309
  108.3 16.9 %all-to-all-start.2 = ((bf16[8,144,128]{2,1,0:T(8,128)(2,1)}), bf16[8,144,128]{2,1,0:T(8,128)(2,1)S(1)}, u32[]{:S(2)}, u32[]{:S(2)}) async-start(bf16[8,144,128]{2,1,0:T(8,128)(2,1)} %get-tuple-element.19), calls=%async_computation.2 | async-start | bytes 589824 | tf_op jit(solution)/shard_map/all_to_all | solution.py:307
  126.5 9.4 %all-to-all-start.4 = ((f32[8,3,256]{2,1,0:T(4,128)}), f32[8,3,256]{2,1,0:T(4,128)S(1)}, u32[]{:S(2)}, u32[]{:S(2)}) async-start(f32[8,3,256]{2,1,0:T(4,128)} %get-tuple-element.28), calls=%async_computation.4 | async-start | bytes 65536 | tf_op jit(solution)/shard_map/all_to_all | solution.py:313
Sparse Core Ops, SparseCore 0:
  26.9 73.3 all-gather.3

commit v3 on v2

--- a/solution.py
+++ b/solution.py
@@ -14,7 +14,7 @@
 SHORT = 4
 HALO = 32
 EPS = 1e-06
-LOGS = 16
+LOGS = 8
 SP = ("sp_0", "sp_1")
 FT = ("fs", "tp")
 f32 = jnp.float32
@@ -135,61 +135,70 @@
     rows, ch = xs.shape
     heads = cum_t.shape[0]
     p = ch // heads
-    steps = 4
-    kb = d // steps
+    ny, nz, piece, _ = rest.shape
     part = 64
 
-    def body(nref, wref, ftaps, ltaps, xs, w16, cum, cum_t, read16, zgate, mixed, inner, back, acc, glu):
-        k = pl.program_id(0)
-        at_k = pl.ds(pl.multiple_of(k * kb, kb), kb)
-        term = dot(nref[:, at_k], wref[:, : 4 * ch], 1, 0)
-        back[at_k, :] = wref[:, 4 * ch :]
-
-        @pl.when(k == 0)
-        def _():
-            acc[...] = term
-
-        @pl.when(k > 0)
-        def _():
-            acc[...] += term
-
-        @pl.when(k == steps - 1)
-        def _():
-            glu[...] = acc[:, 2 * ch : 3 * ch].astype(bf16).astype(f32) * jax.nn.sigmoid(
-                acc[:, 3 * ch :].astype(bf16).astype(f32)
+    def body(nref, wref, ftaps, ltaps, xs, w16, cum, cum_t, read16, zgate, mixed, inner, back, acc, glu, wall, sems):
+        def copies(z, y):
+            at = (z * ny + y) * piece
+            return (
+                pltpu.make_async_copy(wref.at[y, z, :, : 4 * ch], wall.at[at : at + piece, :], sems.at[z, y, 0]),
+                pltpu.make_async_copy(wref.at[y, z, :, 4 * ch :], back.at[at : at + piece, :], sems.at[z, y, 1]),
             )
-            acc[:, : 2 * ch] = acc[:, : 2 * ch].astype(bf16).astype(f32)
-            s_at, l_at = HALO - SHORT + 1, HALO - WIDE + 1
-            read = sum(acc[s_at + i : s_at + i + rows, :ch] * ftaps[i : i + 1, :] for i in range(SHORT))
-            read = jax.nn.silu(read).astype(bf16)
-            read16[...] = read
-            zgate[...] = jax.nn.silu(acc[HALO:, ch : 2 * ch])
-            scores = dot(read, w16[...], 1, 1)
-            lower = lax.broadcasted_iota(jnp.int32, (rows, rows), 0) >= lax.broadcasted_iota(jnp.int32, (rows, rows), 1)
-            lane = lax.broadcasted_iota(jnp.int32, (rows, ch), 1)
-            y = jnp.zeros((rows, ch), f32)
-            for h in range(heads):
-                gap = jnp.where(lower, cum[:, h * p : h * p + 1] - cum_t[h : h + 1, :], 0.0)
-                m = jnp.where(lower, jnp.exp(gap) * scores, 0.0).astype(bf16)
-                x = jnp.where(lane // p == h, xs[...].astype(f32), 0.0).astype(bf16)
-                y = y + dot(m, x, 1, 0)
-            inner[...] = y
-            for r in range(0, rows, part):
-                mixed[r : r + part, :] = sum(
-                    glu[l_at + r + i : l_at + r + i + part, :] * ltaps[i : i + 1, :] for i in range(WIDE)
-                )
+
+        for z in range(nz):
+            for y in range(ny):
+                copies(z, y)[0].start()
+        for z in range(nz):
+            for y in range(ny):
+                copies(z, y)[1].start()
+        for z in range(0, nz, 2):
+            for y in range(ny):
+                copies(z, y)[0].wait()
+                copies(z + 1, y)[0].wait()
+            here = slice(z * ny * piece, (z + 2) * ny * piece)
+            term = dot(nref[:, here], wall[here, :], 1, 0)
+            acc[...] = term if z == 0 else acc[...] + term
+        glu[...] = acc[:, 2 * ch : 3 * ch].astype(bf16).astype(f32) * jax.nn.sigmoid(
+            acc[:, 3 * ch :].astype(bf16).astype(f32)
+        )
+        acc[:, : 2 * ch] = acc[:, : 2 * ch].astype(bf16).astype(f32)
+        s_at, l_at = HALO - SHORT + 1, HALO - WIDE + 1
+        read = sum(acc[s_at + i : s_at + i + rows, :ch] * ftaps[i : i + 1, :] for i in range(SHORT))
+        read = jax.nn.silu(read).astype(bf16)
+        read16[...] = read
+        zgate[...] = jax.nn.silu(acc[HALO:, ch : 2 * ch])
+        scores = dot(read, w16[...], 1, 1)
+        lower = lax.broadcasted_iota(jnp.int32, (rows, rows), 0) >= lax.broadcasted_iota(jnp.int32, (rows, rows), 1)
+        lane = lax.broadcasted_iota(jnp.int32, (rows, ch), 1)
+        out = jnp.zeros((rows, ch), f32)
+        for h in range(heads):
+            gap = jnp.where(lower, cum[:, h * p : h * p + 1] - cum_t[h : h + 1, :], 0.0)
+            m = jnp.where(lower, jnp.exp(gap) * scores, 0.0).astype(bf16)
+            x = jnp.where(lane // p == h, xs[...].astype(f32), 0.0).astype(bf16)
+            out = out + dot(m, x, 1, 0)
+        inner[...] = out
+        for r in range(0, rows, part):
+            mixed[r : r + part, :] = sum(
+                glu[l_at + r + i : l_at + r + i + part, :] * ltaps[i : i + 1, :] for i in range(WIDE)
+            )
+        for z in range(nz):
+            for y in range(ny):
+                copies(z, y)[1].wait()
 
     small = (ftaps, ltaps, xs, w16, cum, cum_t)
     return pl.pallas_call(
         body,
-        grid=(steps,),
         out_shape=(
             pltpu.VMEM((rows, STATE), bf16), pltpu.VMEM((rows, ch), f32), pltpu.VMEM((rows, ch), f32),
             pltpu.VMEM((rows, ch), f32), pltpu.VMEM((d, 2 * ch), bf16),
         ),
-        in_specs=[VMEM, pl.BlockSpec((kb, 6 * ch), lambda k: (k, 0)), *[VMEM] * len(small)],
+        in_specs=[VMEM, pl.BlockSpec(memory_space=pltpu.HBM), *[VMEM] * len(small)],
         out_specs=(VMEM,) * 5,
-        scratch_shapes=[pltpu.VMEM((ext, 4 * ch), f32), pltpu.VMEM((ext, ch), f32)],
+        scratch_shapes=[
+            pltpu.VMEM((ext, 4 * ch), f32), pltpu.VMEM((ext, ch), f32), pltpu.VMEM((d, 4 * ch), bf16),
+            pltpu.SemaphoreType.DMA((nz, ny, 2)),
+        ],
         compiler_params=SMALL, name="rows_local",
     )(*held(normed), *fetched(rest), *held(*small))
 
@@ -280,9 +289,9 @@
     nf, nt = lax.axis_size("fs"), lax.axis_size("tp")
     iz, iy, tp = (lax.axis_index(a).astype(jnp.int32).reshape(1) for a in ("sp_0", "sp_1", "tp"))
     ny = lax.axis_size("sp_1")
-    rest = lay_out((state_read, mixer_gate, conv_value, conv_gate, conv_output, state_output), ny)
-    rest = lax.all_to_all(rest, "sp_1", 0, 0, tiled=True).reshape(-1, 6 * ch)
-    rest = lax.all_gather(rest, "sp_0", axis=0, tiled=True)
+    rest = lay_out((state_read, mixer_gate, conv_value, conv_gate, conv_output, state_output), lax.axis_size("sp_0"))
+    rest = lax.all_to_all(rest, "sp_0", 0, 0, tiled=True)
+    rest = lax.all_gather(rest, "sp_1", axis=0)
     first = lay_out((state_input, write_projection), lax.axis_size(SP))
     first = lax.all_to_all(first, SP, 0, 0, tiled=True).reshape(-1, 2 * ch)
     n = lax.axis_size(SP)

time: 158 us -> 181 us (1.15)
  waiting for transfers between devices: 51.8 us -> 72.6 us
  starting transfers between devices: 39.5 us -> 32 us
  local copies, waits for them, and re-layouts: 1.67 us -> 8.47 us
  blocking collectives: 34 us -> 39.6 us
  Pallas kernels: 13.2 us -> 11 us
    all_to_all x1, waiting for transfers between devices: 22.9 us -> 35.7 us  [per_device(): first = lax.all_to_all(first, SP, 0, 0, tiled=True).reshape(-1, 2 * ch)]
    all_to_all x1, waiting for transfers between devices: 0.01 us -> 12.7 us  [per_device(): got = lax.all_to_all(send, 'sp_1', 0, 0, tiled=True)]
    all_to_all x1, starting transfers between devices: 16.6 us -> 7.96 us  [per_device(): first = lax.all_to_all(first, SP, 0, 0, tiled=True).reshape(-1, 2 * ch)]
    unnamed x27 -> x45, local copies, waits for them, and re-layouts: 0.09 us -> 6.89 us
    all_to_all x1, starting transfers between devices: 9.98 us -> 4.08 us  [per_device(): got = lax.all_to_all(send, 'sp_1', 0, 0, tiled=True)]
    all_to_all x1, blocking collectives: 19.3 us -> 24.5 us  [per_device(): rest = lax.all_to_all(rest, 'sp_0', 0, 0, tiled=True)]
    all_to_all x1, starting transfers between devices: 3.86 us -> 7.1 us  [per_device(): got = lax.all_to_all(send, 'sp_0', 0, 0, tiled=True)]
    all_gather x1, waiting for transfers between devices: 14.9 us -> 12.3 us  [per_device(): rest = lax.all_gather(rest, 'sp_1', axis=0)]
  transfers between devices with their start and end apart: 7 -> 7, of which waited for: 4 -> 5; matrix products, arithmetic and copies ran while one was open for 2% -> 2% of each run, Pallas kernels for 6% -> 3%
where the time goes in v3:
time: 181 us; the launch traced here: 180 us
  waiting for transfers between devices  72.6 us (40%)
  blocking collectives  39.6 us (22%)
  starting transfers between devices  32 us (18%)
  between operations  13.7 us (8%)
  Pallas kernels  11 us (6%)
  local copies, waits for them, and re-layouts  8.47 us (5%)
  other arithmetic  2.46 us (1%)
    all_to_all x1, waiting for transfers between devices, per_device(): first = lax.all_to_all(first, SP, 0, 0, tiled=True).reshape(-1, 2 * ch)  35.7 us
    all_to_all x1, blocking collectives, per_device(): rest = lax.all_to_all(rest, 'sp_0', 0, 0, tiled=True)  24.5 us
    all_to_all x1, waiting for transfers between devices, per_device(): got = lax.all_to_all(send, 'sp_1', 0, 0, tiled=True)  12.7 us
    all_gather x1, waiting for transfers between devices, per_device(): rest = lax.all_gather(rest, 'sp_1', axis=0)  12.3 us
    all_to_all x1, blocking collectives, per_device(): pieces = lax.all_to_all(out, 'fs', 0, 0, tiled=True)  10.9 us
    all_to_all x1, waiting for transfers between devices, per_device(): got = lax.all_to_all(send, 'sp_0', 0, 0, tiled=True)  9.09 us
    all_to_all x1, starting transfers between devices, per_device(): first = lax.all_to_all(first, SP, 0, 0, tiled=True).reshape(-1, 2 * ch)  7.96 us
    all_to_all x1, starting transfers between devices, per_device(): got = lax.all_to_all(send, 'sp_0', 0, 0, tiled=True)  7.1 us
  transfers between devices with their start and end apart: 7, of which 5 were waited for; matrix products, arithmetic and copies ran while one was open for 2% of the time, Pallas kernels for 3%

profile of v3, /device:TPU:1, one launch (start us, length us, event | category | flops | bytes accessed | tf_op | source)
XLA Modules:
  0.0 180.2 jit_solution(4516491269173222913)
XLA Ops:
  6.5 0.9 shard_map.200
  7.5 24.5 %all_to_all.30 = bf16[8,32,768]{2,1,0:T(8,128)(2,1)} all-to-all(bf16[8,32,768]{2,1,0:T(8,128)(2,1)S(1)} %shard_map.200), channel_id=1, replica_groups=mesh['sp_0'=8,'sp_1'=8,'fs'=4,'tp'=2] {'sp_0'}, dimensions={0} | all-to-all | bytes 786432 | tf_op jit(solution)/shard_map/all_to_all | solution.py:293
  31.9 0.0 all-gather.5.cloned.1.call-update
  32.0 0.9 slice.15
  32.9 3.2 %collective-permute-start = (bf16[32,2048]{1,0:T(8,128)(2,1)S(1)}, bf16[32,2048]{1,0:T(8,128)(2,1)S(1)}, u32[]{:S(2)}, u32[]{:S(2)}) collective-permute-start(bf16[32,2048]{1,0:T(8,128)(2,1)S(1)} %slice.15), channel_id=1, source_target_pairs={{0,8},{8,16},{16,24},{24,32},{32,40},{40,48},{48,56},{56,64},{64,7... | collective-permute-start | bytes 393224 | tf_op jit(solution)/shard_map/ppermute | solution.py:298
  36.1 1.9 %shard_map.199 = bf16[64,32,256]{2,1,0:T(8,128)(2,1)} custom-call(bf16[32,128]{1,0:T(8,128)(2,1)} %refs_0_.2, bf16[32,128]{1,0:T(8,128)(2,1)} %refs_1_.2), custom_call_target="tpu_custom_call" | custom-call | tf_op jit(solution)/shard_map/pallas_call | solution.py:54
  38.0 8.0 %all-to-all-start = ((bf16[64,32,256]{2,1,0:T(8,128)(2,1)}), bf16[64,32,256]{2,1,0:T(8,128)(2,1)S(1)}, u32[]{:S(2)}, u32[]{:S(2)}) async-start(bf16[64,32,256]{2,1,0:T(8,128)(2,1)} %shard_map.199), calls=%async_computation | async-start | bytes 2097152 | tf_op jit(solution)/shard_map/all_to_all | solution.py:296
  46.1 0.3 fusion
  46.5 0.3 fusion.2.nref
  46.8 0.4 fusion.3
  47.2 0.0 copy-done.19
  47.2 0.1 fusion.5
  47.3 0.6 reduce-window.6
  48.0 0.2 slice_reduce_fusion
  48.1 0.2 reduce-window.9
  48.3 0.1 add_bitcast_fusion
  48.4 0.2 slice_reduce_fusion.1
  48.6 0.1 exponential_bitcast_fusion
  48.7 0.1 copy.32.lref
  48.8 0.1 copy.31.sref
  48.9 0.1 copy.33.cum
  49.0 35.7 %all-to-all-done = bf16[64,32,256]{2,1,0:T(8,128)(2,1)S(1)} async-done(((bf16[64,32,256]{2,1,0:T(8,128)(2,1)}), bf16[64,32,256]{2,1,0:T(8,128)(2,1)S(1)}, u32[]{:S(2)}, u32[]{:S(2)}) %all-to-all-start) | async-done | bytes 1048608 | tf_op jit(solution)/shard_map/all_to_all | solution.py:296
  84.7 0.9 local_states.1
  85.7 0.7 copy-done.1
  86.4 12.3 %all-gather.5.cloned.1.call-done = bf16[64,32,768]{2,1,0:T(8,128)(2,1)} async-done(((bf16[8,32,768]{2,1,0:T(8,128)(2,1)}), bf16[64,32,768]{2,1,0:T(8,128)(2,1)}) %all-gather.5.cloned.1.call-update) | async-done | bytes 3145744 | tf_op jit(solution)/shard_map/all_gather | solution.py:294
  98.7 4.0 %rows_local.1 = (bf16[256,128]{1,0:T(8,128)(2,1)S(1)}, f32[256,128]{1,0:T(8,128)S(1)}, f32[256,128]{1,0:T(8,128)S(1)}, f32[256,128]{1,0:T(8,128)S(1)}, bf16[2048,256]{1,0:T(8,128)(2,1)S(1)}) custom-call(bf16[288,2048]{1,0:T(8,128)(2,1)S(1)} %fusion.2.nref, bf16[8,8,32,768]{3,2,1,0:T(8,128)(2,1)} %bitcast.40, f32[4,128]{1,0:T(4,128)S(1)} %copy-done.12, ...), custom_call_target="tpu_custom_call" | custom-call | tf_op jit(solution)/shard_map/rows_local/pallas_call | solution.py:190
  102.7 0.6 copy-done.2
  103.4 0.6 copy-done.4
  104.0 0.6 copy-done.6
  104.7 0.6 copy-done.9
  105.3 3.5 %collective-permute-start.1 = (bf16[2048,256]{1,0:T(8,128)(2,1)S(1)}, bf16[2048,256]{1,0:T(8,128)(2,1)S(1)}, u32[]{:S(2)}, u32[]{:S(2)}) collective-permute-start(bf16[2048,256]{1,0:T(8,128)(2,1)S(1)} %get-tuple-element.30.wa), channel_id=1, source_target_pairs={{0,1},{1,0},{2,3},{3,2},{4,5},{5,4},{6,7},{7,6},{8,9},{9,8},{10,11... | collective-permute-start | bytes 3145736 | tf_op jit(solution)/shard_map/ppermute | solution.py:318
  108.8 4.1 %all-to-all-start.1 = ((bf16[8,136,128]{2,1,0:T(8,128)(2,1)}), bf16[8,136,128]{2,1,0:T(8,128)(2,1)S(1)}, u32[]{:S(2)}, u32[]{:S(2)}) async-start(bf16[8,136,128]{2,1,0:T(8,128)(2,1)} %copy-done.1), calls=%async_computation.1 | async-start | bytes 557056 | tf_op jit(solution)/shard_map/all_to_all | solution.py:314
  112.9 12.7 %all-to-all-done.1.ref = bf16[8,136,128]{2,1,0:T(8,128)(2,1)S(1)} async-done(((bf16[8,136,128]{2,1,0:T(8,128)(2,1)}), bf16[8,136,128]{2,1,0:T(8,128)(2,1)S(1)}, u32[]{:S(2)}, u32[]{:S(2)}) %all-to-all-start.1) | async-done | bytes 278560 | tf_op jit(solution)/shard_map/all_to_all | solution.py:314
  125.6 0.9 line_states.1
  126.5 7.1 %all-to-all-start.2 = ((bf16[8,136,128]{2,1,0:T(8,128)(2,1)}), bf16[8,136,128]{2,1,0:T(8,128)(2,1)S(1)}, u32[]{:S(2)}, u32[]{:S(2)}) async-start(bf16[8,136,128]{2,1,0:T(8,128)(2,1)} %get-tuple-element.19), calls=%async_computation.2 | async-start | bytes 557056 | tf_op jit(solution)/shard_map/all_to_all | solution.py:316
  133.6 2.2 %all-gather.2 = f32[2,1,128]{2,1,0:T(1,128)S(1)} all-gather(f32[1,1,128]{2,1,0:T(1,128)S(1)} %bitcast.46), channel_id=3, replica_groups=mesh['sp_0'=8,'sp_1'=8,'fs'=4,'tp'=2] {'tp'}, dimensions={0}, use_global_device_ids=true | all-gather | bytes 1536 | tf_op jit(solution)/shard_map/all_gather | solution.py:311
  135.8 9.1 %all-to-all-done.2.got = bf16[8,136,128]{2,1,0:T(8,128)(2,1)S(1)} async-done(((bf16[8,136,128]{2,1,0:T(8,128)(2,1)}), bf16[8,136,128]{2,1,0:T(8,128)(2,1)S(1)}, u32[]{:S(2)}, u32[]{:S(2)}) %all-to-all-start.2) | async-done | bytes 278560 | tf_op jit(solution)/shard_map/all_to_all | solution.py:316
  144.9 0.9 copy-done.3
  145.8 0.9 copy-done.5
  146.7 0.9 copy-done.7
  147.6 0.8 copy-done.10
  148.5 1.3 rows_done.1
  149.7 6.1 %all-to-all-start.4 = ((f32[8,3,256]{2,1,0:T(4,128)}), f32[8,3,256]{2,1,0:T(4,128)S(1)}, u32[]{:S(2)}, u32[]{:S(2)}) async-start(f32[8,3,256]{2,1,0:T(4,128)} %get-tuple-element.28), calls=%async_computation.4 | async-start | bytes 65536 | tf_op jit(solution)/shard_map/all_to_all | solution.py:322
  155.9 2.0 %all_gather.17.bref = bf16[512,256]{1,0:T(8,128)(2,1)S(1)} all-gather(bf16[256,256]{1,0:T(8,128)(2,1)S(1)} %get-tuple-element.29), channel_id=1, replica_groups=mesh['sp_0'=8,'sp_1'=8,'fs'=4,'tp'=2] {'tp'}, dimensions={0}, use_global_device_ids=true | all-gather | bytes 393216 | tf_op jit(solution)/shard_map/all_gather | solution.py:323
  157.8 2.7 %all-to-all-done.4.sref = f32[8,3,256]{2,1,0:T(4,128)S(1)} async-done(((f32[8,3,256]{2,1,0:T(4,128)}), f32[8,3,256]{2,1,0:T(4,128)S(1)}, u32[]{:S(2)}, u32[]{:S(2)}) %all-to-all-start.4) | async-done | bytes 24608 | tf_op jit(solution)/shard_map/all_to_all | solution.py:322
  160.6 1.1 output_rows.1
  161.7 10.9 %all_to_all.31 = bf16[4,32,2048]{2,1,0:T(8,128)(2,1)S(1)} all-to-all(bf16[4,32,2048]{2,1,0:T(8,128)(2,1)S(1)} %output_rows.1), channel_id=1, replica_groups=mesh['sp_0'=8,'sp_1'=8,'fs'=4,'tp'=2] {'fs'}, dimensions={0} | all-to-all | bytes 1048576 | tf_op jit(solution)/shard_map/all_to_all | solution.py:325
  172.6 0.7 reduce_sum.22
  (46 shorter events, 0.2 us)
Async XLA Ops:
  6.5 40.3 %copy-start = (bf16[2048,16]{0,1:T(8,128)(2,1)S(1)}, bf16[2048,16]{0,1:T(8,128)(2,1)}, u32[]{:S(2)}) copy-start(bf16[2048,16]{0,1:T(8,128)(2,1)} %param.29) | copy-start | bytes 196612
  6.5 92.1 %all-gather.5.cloned.1.call-start = ((), (), s32[]{:S(2)}) async-start(), calls=%async_computation.6 | async-start | bytes 3538944 | tf_op jit(solution)/shard_map/all_gather | solution.py:294
  7.4 38.6 %copy-start.20 = (f32[2]{0:T(128)S(1)}, f32[2]{0:T(128)}, u32[]{:S(2)}) copy-start(f32[2]{0:T(128)} %param.31) | copy-start | bytes 28
  7.4 38.6 %copy-start.17 = (f32[4,128]{1,0:T(4,128)S(1)}, f32[4,128]{1,0:T(4,128)}, u32[]{:S(2)}) copy-start(f32[4,128]{1,0:T(4,128)} %param.34) | copy-start | bytes 6148
  7.4 38.6 %copy-start.18 = (f32[4,128]{1,0:T(4,128)S(1)}, f32[4,128]{1,0:T(4,128)}, u32[]{:S(2)}) copy-start(f32[4,128]{1,0:T(4,128)} %param.33) | copy-start | bytes 6148
  7.4 38.7 %copy-start.14 = (bf16[256,2048]{1,0:T(8,128)(2,1)S(1)}, bf16[256,2048]{1,0:T(8,128)(2,1)}, u32[]{:S(2)}) copy-start(bf16[256,2048]{1,0:T(8,128)(2,1)} %param.21) | copy-start | bytes 3145732
  31.9 14.5 %copy-start.15 = (f32[2048]{0:T(1024)S(1)}, f32[2048]{0:T(1024)}, u32[]{:S(2)}) copy-start(f32[2048]{0:T(1024)} %param.22) | copy-start | bytes 24580
  32.9 13.2 %collective-permute-start = (bf16[32,2048]{1,0:T(8,128)(2,1)S(1)}, bf16[32,2048]{1,0:T(8,128)(2,1)S(1)}, u32[]{:S(2)}, u32[]{:S(2)}) collective-permute-start(bf16[32,2048]{1,0:T(8,128)(2,1)S(1)} %slice.15), channel_id=1, source_target_pairs={{0,8},{8,16},{16,24},{24,32},{32,40},{40,48},{48,56},{56,64},{64,7... | collective-permute-start | bytes 393224 | tf_op jit(solution)/shard_map/ppermute | solution.py:298
  38.0 46.7 %all-to-all-start = ((bf16[64,32,256]{2,1,0:T(8,128)(2,1)}), bf16[64,32,256]{2,1,0:T(8,128)(2,1)S(1)}, u32[]{:S(2)}, u32[]{:S(2)}) async-start(bf16[64,32,256]{2,1,0:T(8,128)(2,1)} %shard_map.199), calls=%async_computation | async-start | bytes 2097152 | tf_op jit(solution)/shard_map/all_to_all | solution.py:296
  46.1 1.1 copy-start.16
  46.1 1.1 copy-start.19
  46.8 51.9 %copy-start.11 = (f32[31,128]{1,0:T(8,128)S(1)}, f32[31,128]{1,0:T(8,128)}, u32[]{:S(2)}) copy-start(f32[31,128]{1,0:T(8,128)} %ltaps.1) | copy-start | bytes 47620
  46.8 51.9 %copy-start.12 = (f32[4,128]{1,0:T(4,128)S(1)}, f32[4,128]{1,0:T(4,128)}, u32[]{:S(2)}) copy-start(f32[4,128]{1,0:T(4,128)} %ftaps.1) | copy-start | bytes 6148
  85.7 0.7 copy-start.1
  98.7 34.9 %copy-start.21 = (f32[128]{0:T(128)S(1)}, f32[128]{0:T(128)}, u32[]{:S(2)}) copy-start(f32[128]{0:T(128)} %param.37) | copy-start | bytes 1540
  98.7 46.2 %copy-start.8 = (f32[2,64,128]{2,1,0:T(8,128)S(1)}, f32[2,64,128]{2,1,0:T(8,128)}, u32[]{:S(2)}) copy-start(f32[2,64,128]{2,1,0:T(8,128)} %init.1) | copy-start | bytes 196612
  98.7 46.2 %copy-start.13 = (f32[128]{0:T(128)S(1)}, f32[128]{0:T(128)}, u32[]{:S(2)}) copy-start(f32[128]{0:T(128)} %param.38) | copy-start | bytes 1540
  102.7 0.7 copy-start.2
  103.4 0.6 copy-start.4
  104.0 0.6 copy-start.6
  104.7 0.6 copy-start.9
  105.3 55.3 %collective-permute-start.1 = (bf16[2048,256]{1,0:T(8,128)(2,1)S(1)}, bf16[2048,256]{1,0:T(8,128)(2,1)S(1)}, u32[]{:S(2)}, u32[]{:S(2)}) collective-permute-start(bf16[2048,256]{1,0:T(8,128)(2,1)S(1)} %get-tuple-element.30.wa), channel_id=1, source_target_pairs={{0,1},{1,0},{2,3},{3,2},{4,5},{5,4},{6,7},{7,6},{8,9},{9,8},{10,11... | collective-permute-start | bytes 3145736 | tf_op jit(solution)/shard_map/ppermute | solution.py:318
  108.8 16.8 %all-to-all-start.1 = ((bf16[8,136,128]{2,1,0:T(8,128)(2,1)}), bf16[8,136,128]{2,1,0:T(8,128)(2,1)S(1)}, u32[]{:S(2)}, u32[]{:S(2)}) async-start(bf16[8,136,128]{2,1,0:T(8,128)(2,1)} %copy-done.1), calls=%async_computation.1 | async-start | bytes 557056 | tf_op jit(solution)/shard_map/all_to_all | solution.py:314
  126.5 18.4 %all-to-all-start.2 = ((bf16[8,136,128]{2,1,0:T(8,128)(2,1)}), bf16[8,136,128]{2,1,0:T(8,128)(2,1)S(1)}, u32[]{:S(2)}, u32[]{:S(2)}) async-start(bf16[8,136,128]{2,1,0:T(8,128)(2,1)} %get-tuple-element.19), calls=%async_computation.2 | async-start | bytes 557056 | tf_op jit(solution)/shard_map/all_to_all | solution.py:316
  144.9 0.9 copy-start.3
  145.8 0.9 copy-start.5
  146.7 0.9 copy-start.7
  147.6 0.8 copy-start.10
  149.7 10.8 %all-to-all-start.4 = ((f32[8,3,256]{2,1,0:T(4,128)}), f32[8,3,256]{2,1,0:T(4,128)S(1)}, u32[]{:S(2)}, u32[]{:S(2)}) async-start(f32[8,3,256]{2,1,0:T(4,128)} %get-tuple-element.28), calls=%async_computation.4 | async-start | bytes 65536 | tf_op jit(solution)/shard_map/all_to_all | solution.py:322
Sparse Core Ops, SparseCore 0:
  32.1 66.5 all-gather.4

commit v4 on v3

--- a/solution.py
+++ b/solution.py
@@ -135,30 +135,27 @@
     rows, ch = xs.shape
     heads = cum_t.shape[0]
     p = ch // heads
-    ny, nz, piece, _ = rest.shape
-    part = 64
+    part, n = 64, 8
+    kc = d // n
 
     def body(nref, wref, ftaps, ltaps, xs, w16, cum, cum_t, read16, zgate, mixed, inner, back, acc, glu, wall, sems):
-        def copies(z, y):
-            at = (z * ny + y) * piece
-            return (
-                pltpu.make_async_copy(wref.at[y, z, :, : 4 * ch], wall.at[at : at + piece, :], sems.at[z, y, 0]),
-                pltpu.make_async_copy(wref.at[y, z, :, 4 * ch :], back.at[at : at + piece, :], sems.at[z, y, 1]),
-            )
-
-        for z in range(nz):
-            for y in range(ny):
-                copies(z, y)[0].start()
-        for z in range(nz):
-            for y in range(ny):
-                copies(z, y)[1].start()
-        for z in range(0, nz, 2):
-            for y in range(ny):
-                copies(z, y)[0].wait()
-                copies(z + 1, y)[0].wait()
-            here = slice(z * ny * piece, (z + 2) * ny * piece)
-            term = dot(nref[:, here], wall[here, :], 1, 0)
-            acc[...] = term if z == 0 else acc[...] + term
+        def fetch(i):
+            at = slice(i * kc, (i + 1) * kc)
+            return pltpu.make_async_copy(wref.at[at, : 4 * ch], wall.at[at, :], sems.at[0, i])
+
+        def fetch_back(i):
+            at = slice(i * kc, (i + 1) * kc)
+            return pltpu.make_async_copy(wref.at[at, 4 * ch :], back.at[at, :], sems.at[1, i])
+
+        for i in range(n):
+            fetch(i).start()
+        for i in range(n):
+            fetch_back(i).start()
+        for i in range(n):
+            fetch(i).wait()
+            at = slice(i * kc, (i + 1) * kc)
+            term = dot(nref[:, at], wall[at, :], 1, 0)
+            acc[...] = term if i == 0 else acc[...] + term
         glu[...] = acc[:, 2 * ch : 3 * ch].astype(bf16).astype(f32) * jax.nn.sigmoid(
             acc[:, 3 * ch :].astype(bf16).astype(f32)
         )
@@ -171,20 +168,19 @@
         scores = dot(read, w16[...], 1, 1)
         lower = lax.broadcasted_iota(jnp.int32, (rows, rows), 0) >= lax.broadcasted_iota(jnp.int32, (rows, rows), 1)
         lane = lax.broadcasted_iota(jnp.int32, (rows, ch), 1)
-        out = jnp.zeros((rows, ch), f32)
+        y = jnp.zeros((rows, ch), f32)
         for h in range(heads):
             gap = jnp.where(lower, cum[:, h * p : h * p + 1] - cum_t[h : h + 1, :], 0.0)
             m = jnp.where(lower, jnp.exp(gap) * scores, 0.0).astype(bf16)
             x = jnp.where(lane // p == h, xs[...].astype(f32), 0.0).astype(bf16)
-            out = out + dot(m, x, 1, 0)
-        inner[...] = out
+            y = y + dot(m, x, 1, 0)
+        inner[...] = y
         for r in range(0, rows, part):
             mixed[r : r + part, :] = sum(
                 glu[l_at + r + i : l_at + r + i + part, :] * ltaps[i : i + 1, :] for i in range(WIDE)
             )
-        for z in range(nz):
-            for y in range(ny):
-                copies(z, y)[1].wait()
+        for i in range(n):
+            fetch_back(i).wait()
 
     small = (ftaps, ltaps, xs, w16, cum, cum_t)
     return pl.pallas_call(
@@ -197,7 +193,7 @@
         out_specs=(VMEM,) * 5,
         scratch_shapes=[
             pltpu.VMEM((ext, 4 * ch), f32), pltpu.VMEM((ext, ch), f32), pltpu.VMEM((d, 4 * ch), bf16),
-            pltpu.SemaphoreType.DMA((nz, ny, 2)),
+            pltpu.SemaphoreType.DMA((2, n)),
         ],
         compiler_params=SMALL, name="rows_local",
     )(*held(normed), *fetched(rest), *held(*small))
@@ -289,9 +285,9 @@
     nf, nt = lax.axis_size("fs"), lax.axis_size("tp")
     iz, iy, tp = (lax.axis_index(a).astype(jnp.int32).reshape(1) for a in ("sp_0", "sp_1", "tp"))
     ny = lax.axis_size("sp_1")
-    rest = lay_out((state_read, mixer_gate, conv_value, conv_gate, conv_output, state_output), lax.axis_size("sp_0"))
-    rest = lax.all_to_all(rest, "sp_0", 0, 0, tiled=True)
-    rest = lax.all_gather(rest, "sp_1", axis=0)
+    rest = lay_out((state_read, mixer_gate, conv_value, conv_gate, conv_output, state_output), ny)
+    rest = lax.all_to_all(rest, "sp_1", 0, 0, tiled=True).reshape(-1, 6 * ch)
+    rest = lax.all_gather(rest, "sp_0", axis=0, tiled=True)
     first = lay_out((state_input, write_projection), lax.axis_size(SP))
     first = lax.all_to_all(first, SP, 0, 0, tiled=True).reshape(-1, 2 * ch)
     n = lax.axis_size(SP)

time: 181 us -> 180 us (level)
  starting transfers between devices: 32 us -> 37.4 us
  blocking collectives: 39.6 us -> 34.4 us
    all_to_all x1, waiting for transfers between devices: 35.7 us -> 22.8 us  [per_device(): first = lax.all_to_all(first, SP, 0, 0, tiled=True).reshape(-1, 2 * ch)]
    all_gather x1, waiting for transfers between devices: 12.3 us -> 25 us  [per_device(): rest = lax.all_gather(rest, 'sp_0', axis=0, tiled=True)]
    all_to_all x1, starting transfers between devices: 7.96 us -> 16.6 us  [per_device(): first = lax.all_to_all(first, SP, 0, 0, tiled=True).reshape(-1, 2 * ch)]
    all_to_all x1, blocking collectives: 24.5 us -> 19.3 us  [per_device(): rest = lax.all_to_all(rest, 'sp_1', 0, 0, tiled=True).reshape(-1, 6 * ch)]
    all_to_all x1, starting transfers between devices: 7.1 us -> 3.86 us  [per_device(): got = lax.all_to_all(send, 'sp_0', 0, 0, tiled=True)]
    all_to_all x1, starting transfers between devices: 4.08 us -> 6.46 us  [per_device(): got = lax.all_to_all(send, 'sp_1', 0, 0, tiled=True)]
where the time goes in v4:
time: 180 us; the launch traced here: 179 us
  waiting for transfers between devices  72.4 us (40%)
  starting transfers between devices  37.4 us (21%)
  blocking collectives  34.4 us (19%)
  between operations  13.7 us (8%)
  Pallas kernels  9.87 us (5%)
  local copies, waits for them, and re-layouts  8.47 us (5%)
  other arithmetic  2.46 us (1%)
    all_gather x1, waiting for transfers between devices, per_device(): rest = lax.all_gather(rest, 'sp_0', axis=0, tiled=True)  25 us
    all_to_all x1, waiting for transfers between devices, per_device(): first = lax.all_to_all(first, SP, 0, 0, tiled=True).reshape(-1, 2 * ch)  22.8 us
    all_to_all x1, blocking collectives, per_device(): rest = lax.all_to_all(rest, 'sp_1', 0, 0, tiled=True).reshape(-1, 6 * ch)  19.3 us
    all_to_all x1, starting transfers between devices, per_device(): first = lax.all_to_all(first, SP, 0, 0, tiled=True).reshape(-1, 2 * ch)  16.6 us
    all_to_all x1, waiting for transfers between devices, per_device(): got = lax.all_to_all(send, 'sp_1', 0, 0, tiled=True)  12.7 us
    all_to_all x1, blocking collectives, per_device(): pieces = lax.all_to_all(out, 'fs', 0, 0, tiled=True)  11 us
    all_to_all x1, waiting for transfers between devices, per_device(): got = lax.all_to_all(send, 'sp_0', 0, 0, tiled=True)  9.09 us
    unnamed x45, local copies, waits for them, and re-layouts  6.89 us
  transfers between devices with their start and end apart: 7, of which 5 were waited for; matrix products, arithmetic and copies ran while one was open for 2% of the time, Pallas kernels for 3%

profile of v4, /device:TPU:1, one launch (start us, length us, event | category | flops | bytes accessed | tf_op | source)
XLA Modules:
  0.0 179.1 jit_solution(1910361047043483169)
XLA Ops:
  6.5 0.9 shard_map.200
  7.5 19.3 %all_to_all.30 = bf16[8,32,768]{2,1,0:T(8,128)(2,1)} all-to-all(bf16[8,32,768]{2,1,0:T(8,128)(2,1)S(1)} %shard_map.200), channel_id=1, replica_groups=mesh['sp_0'=8,'sp_1'=8,'fs'=4,'tp'=2] {'sp_1'}, dimensions={0} | all-to-all | bytes 786432 | tf_op jit(solution)/shard_map/all_to_all | solution.py:289
  26.7 0.0 all-gather.4.cloned.1.call-update
  26.8 0.9 slice.15
  27.7 1.6 collective-permute-start
  29.3 1.9 %shard_map.199 = bf16[64,32,256]{2,1,0:T(8,128)(2,1)} custom-call(bf16[32,128]{1,0:T(8,128)(2,1)} %refs_0_.2, bf16[32,128]{1,0:T(8,128)(2,1)} %refs_1_.2), custom_call_target="tpu_custom_call" | custom-call | tf_op jit(solution)/shard_map/pallas_call | solution.py:54
  31.3 16.6 %all-to-all-start = ((bf16[64,32,256]{2,1,0:T(8,128)(2,1)}), bf16[64,32,256]{2,1,0:T(8,128)(2,1)S(1)}, u32[]{:S(2)}, u32[]{:S(2)}) async-start(bf16[64,32,256]{2,1,0:T(8,128)(2,1)} %shard_map.199), calls=%async_computation | async-start | bytes 2097152 | tf_op jit(solution)/shard_map/all_to_all | solution.py:292
  48.0 0.3 fusion
  48.3 0.3 fusion.2.nref
  48.7 0.4 fusion.3
  49.1 0.0 copy-done.19
  49.1 0.1 fusion.5
  49.2 0.6 reduce-window.6
  49.8 0.2 slice_reduce_fusion
  50.0 0.2 reduce-window.9
  50.2 0.1 add_bitcast_fusion
  50.2 0.2 slice_reduce_fusion.1
  50.4 0.1 exponential_bitcast_fusion
  50.5 0.1 copy.32.lref
  50.7 0.1 copy.31.sref
  50.8 0.1 copy.33.cum
  50.9 22.8 %all-to-all-done = bf16[64,32,256]{2,1,0:T(8,128)(2,1)S(1)} async-done(((bf16[64,32,256]{2,1,0:T(8,128)(2,1)}), bf16[64,32,256]{2,1,0:T(8,128)(2,1)S(1)}, u32[]{:S(2)}, u32[]{:S(2)}) %all-to-all-start) | async-done | bytes 1048608 | tf_op jit(solution)/shard_map/all_to_all | solution.py:292
  73.7 0.9 local_states.1
  74.6 0.7 copy-done.1
  75.3 25.0 %all-gather.4.cloned.1.call-done.wref = bf16[2048,768]{1,0:T(8,128)(2,1)} async-done(((bf16[256,768]{1,0:T(8,128)(2,1)}), bf16[2048,768]{1,0:T(8,128)(2,1)}) %all-gather.4.cloned.1.call-update) | async-done | bytes 3145744 | tf_op jit(solution)/shard_map/all_gather | solution.py:290
  100.4 2.9 %rows_local.1 = (bf16[256,128]{1,0:T(8,128)(2,1)S(1)}, f32[256,128]{1,0:T(8,128)S(1)}, f32[256,128]{1,0:T(8,128)S(1)}, f32[256,128]{1,0:T(8,128)S(1)}, bf16[2048,256]{1,0:T(8,128)(2,1)S(1)}) custom-call(bf16[288,2048]{1,0:T(8,128)(2,1)S(1)} %fusion.2.nref, bf16[2048,768]{1,0:T(8,128)(2,1)} %all-gather.4.cloned.1.call-done.wref, f32[4,128]{1,0:T(4,128)S(1)} %copy-done.12, ...), custom_call_target="tpu_custom_call" | custom-call | tf_op jit(solution)/shard_map/rows_local/pallas_call | solution.py:186
  103.3 0.6 copy-done.2
  103.9 0.6 copy-done.4
  104.6 0.6 copy-done.6
  105.2 0.6 copy-done.9
  105.8 2.7 %collective-permute-start.1 = (bf16[2048,256]{1,0:T(8,128)(2,1)S(1)}, bf16[2048,256]{1,0:T(8,128)(2,1)S(1)}, u32[]{:S(2)}, u32[]{:S(2)}) collective-permute-start(bf16[2048,256]{1,0:T(8,128)(2,1)S(1)} %get-tuple-element.30.wa), channel_id=1, source_target_pairs={{0,1},{1,0},{2,3},{3,2},{4,5},{5,4},{6,7},{7,6},{8,9},{9,8},{10,11... | collective-permute-start | bytes 3145736 | tf_op jit(solution)/shard_map/ppermute | solution.py:314
  108.6 6.5 %all-to-all-start.1 = ((bf16[8,136,128]{2,1,0:T(8,128)(2,1)}), bf16[8,136,128]{2,1,0:T(8,128)(2,1)S(1)}, u32[]{:S(2)}, u32[]{:S(2)}) async-start(bf16[8,136,128]{2,1,0:T(8,128)(2,1)} %copy-done.1), calls=%async_computation.1 | async-start | bytes 557056 | tf_op jit(solution)/shard_map/all_to_all | solution.py:310
  115.0 12.7 %all-to-all-done.1.ref = bf16[8,136,128]{2,1,0:T(8,128)(2,1)S(1)} async-done(((bf16[8,136,128]{2,1,0:T(8,128)(2,1)}), bf16[8,136,128]{2,1,0:T(8,128)(2,1)S(1)}, u32[]{:S(2)}, u32[]{:S(2)}) %all-to-all-start.1) | async-done | bytes 278560 | tf_op jit(solution)/shard_map/all_to_all | solution.py:310
  127.8 0.9 line_states.1
  128.6 3.9 %all-to-all-start.2 = ((bf16[8,136,128]{2,1,0:T(8,128)(2,1)}), bf16[8,136,128]{2,1,0:T(8,128)(2,1)S(1)}, u32[]{:S(2)}, u32[]{:S(2)}) async-start(bf16[8,136,128]{2,1,0:T(8,128)(2,1)} %get-tuple-element.19), calls=%async_computation.2 | async-start | bytes 557056 | tf_op jit(solution)/shard_map/all_to_all | solution.py:312
  132.5 2.2 %all-gather.1 = f32[2,1,128]{2,1,0:T(1,128)S(1)} all-gather(f32[1,1,128]{2,1,0:T(1,128)S(1)} %bitcast.46), channel_id=2, replica_groups=mesh['sp_0'=8,'sp_1'=8,'fs'=4,'tp'=2] {'tp'}, dimensions={0}, use_global_device_ids=true | all-gather | bytes 1536 | tf_op jit(solution)/shard_map/all_gather | solution.py:307
  134.7 9.1 %all-to-all-done.2.got = bf16[8,136,128]{2,1,0:T(8,128)(2,1)S(1)} async-done(((bf16[8,136,128]{2,1,0:T(8,128)(2,1)}), bf16[8,136,128]{2,1,0:T(8,128)(2,1)S(1)}, u32[]{:S(2)}, u32[]{:S(2)}) %all-to-all-start.2) | async-done | bytes 278560 | tf_op jit(solution)/shard_map/all_to_all | solution.py:312
  143.8 0.9 copy-done.3
  144.7 0.9 copy-done.5
  145.6 0.9 copy-done.7
  146.5 0.8 copy-done.10
  147.4 1.3 rows_done.1
  148.6 6.1 %all-to-all-start.4 = ((f32[8,3,256]{2,1,0:T(4,128)}), f32[8,3,256]{2,1,0:T(4,128)S(1)}, u32[]{:S(2)}, u32[]{:S(2)}) async-start(f32[8,3,256]{2,1,0:T(4,128)} %get-tuple-element.28), calls=%async_computation.4 | async-start | bytes 65536 | tf_op jit(solution)/shard_map/all_to_all | solution.py:318
  154.8 2.0 %all_gather.13.bref = bf16[512,256]{1,0:T(8,128)(2,1)S(1)} all-gather(bf16[256,256]{1,0:T(8,128)(2,1)S(1)} %get-tuple-element.29), channel_id=1, replica_groups=mesh['sp_0'=8,'sp_1'=8,'fs'=4,'tp'=2] {'tp'}, dimensions={0}, use_global_device_ids=true | all-gather | bytes 393216 | tf_op jit(solution)/shard_map/all_gather | solution.py:319
  156.8 2.7 %all-to-all-done.4.sref = f32[8,3,256]{2,1,0:T(4,128)S(1)} async-done(((f32[8,3,256]{2,1,0:T(4,128)}), f32[8,3,256]{2,1,0:T(4,128)S(1)}, u32[]{:S(2)}, u32[]{:S(2)}) %all-to-all-start.4) | async-done | bytes 24608 | tf_op jit(solution)/shard_map/all_to_all | solution.py:318
  159.5 1.1 output_rows.1
  160.6 11.0 %all_to_all.31 = bf16[4,32,2048]{2,1,0:T(8,128)(2,1)S(1)} all-to-all(bf16[4,32,2048]{2,1,0:T(8,128)(2,1)S(1)} %output_rows.1), channel_id=1, replica_groups=mesh['sp_0'=8,'sp_1'=8,'fs'=4,'tp'=2] {'fs'}, dimensions={0} | all-to-all | bytes 1048576 | tf_op jit(solution)/shard_map/all_to_all | solution.py:321
  171.5 0.7 reduce_sum.22
  (46 shorter events, 0.2 us)
Async XLA Ops:
  6.5 42.1 %copy-start = (bf16[2048,16]{0,1:T(8,128)(2,1)S(1)}, bf16[2048,16]{0,1:T(8,128)(2,1)}, u32[]{:S(2)}) copy-start(bf16[2048,16]{0,1:T(8,128)(2,1)} %param.29) | copy-start | bytes 196612
  6.5 93.8 %all-gather.4.cloned.1.call-start = ((), (), s32[]{:S(2)}) async-start(), calls=%async_computation.6 | async-start | bytes 3538944 | tf_op jit(solution)/shard_map/all_gather | solution.py:290
  7.4 40.5 %copy-start.20 = (f32[2]{0:T(128)S(1)}, f32[2]{0:T(128)}, u32[]{:S(2)}) copy-start(f32[2]{0:T(128)} %param.31) | copy-start | bytes 28
  7.4 40.5 %copy-start.17 = (f32[4,128]{1,0:T(4,128)S(1)}, f32[4,128]{1,0:T(4,128)}, u32[]{:S(2)}) copy-start(f32[4,128]{1,0:T(4,128)} %param.34) | copy-start | bytes 6148
  7.4 40.5 %copy-start.18 = (f32[4,128]{1,0:T(4,128)S(1)}, f32[4,128]{1,0:T(4,128)}, u32[]{:S(2)}) copy-start(f32[4,128]{1,0:T(4,128)} %param.33) | copy-start | bytes 6148
  7.4 40.5 %copy-start.14 = (bf16[256,2048]{1,0:T(8,128)(2,1)S(1)}, bf16[256,2048]{1,0:T(8,128)(2,1)}, u32[]{:S(2)}) copy-start(bf16[256,2048]{1,0:T(8,128)(2,1)} %param.21) | copy-start | bytes 3145732
  26.8 21.5 %copy-start.15 = (f32[2048]{0:T(1024)S(1)}, f32[2048]{0:T(1024)}, u32[]{:S(2)}) copy-start(f32[2048]{0:T(1024)} %param.22) | copy-start | bytes 24580
  27.7 20.3 %collective-permute-start = (bf16[32,2048]{1,0:T(8,128)(2,1)S(1)}, bf16[32,2048]{1,0:T(8,128)(2,1)S(1)}, u32[]{:S(2)}, u32[]{:S(2)}) collective-permute-start(bf16[32,2048]{1,0:T(8,128)(2,1)S(1)} %slice.15), channel_id=1, source_target_pairs={{0,8},{8,16},{16,24},{24,32},{32,40},{40,48},{48,56},{56,64},{64,7... | collective-permute-start | bytes 393224 | tf_op jit(solution)/shard_map/ppermute | solution.py:294
  31.3 42.4 %all-to-all-start = ((bf16[64,32,256]{2,1,0:T(8,128)(2,1)}), bf16[64,32,256]{2,1,0:T(8,128)(2,1)S(1)}, u32[]{:S(2)}, u32[]{:S(2)}) async-start(bf16[64,32,256]{2,1,0:T(8,128)(2,1)} %shard_map.199), calls=%async_computation | async-start | bytes 2097152 | tf_op jit(solution)/shard_map/all_to_all | solution.py:292
  47.9 1.1 copy-start.16
  47.9 1.1 copy-start.19
  48.7 51.7 %copy-start.11 = (f32[31,128]{1,0:T(8,128)S(1)}, f32[31,128]{1,0:T(8,128)}, u32[]{:S(2)}) copy-start(f32[31,128]{1,0:T(8,128)} %ltaps.1) | copy-start | bytes 47620
  48.7 51.7 %copy-start.12 = (f32[4,128]{1,0:T(4,128)S(1)}, f32[4,128]{1,0:T(4,128)}, u32[]{:S(2)}) copy-start(f32[4,128]{1,0:T(4,128)} %ftaps.1) | copy-start | bytes 6148
  74.6 0.7 copy-start.1
  100.3 32.2 %copy-start.21 = (f32[128]{0:T(128)S(1)}, f32[128]{0:T(128)}, u32[]{:S(2)}) copy-start(f32[128]{0:T(128)} %param.37) | copy-start | bytes 1540
  100.3 43.5 %copy-start.8 = (f32[2,64,128]{2,1,0:T(8,128)S(1)}, f32[2,64,128]{2,1,0:T(8,128)}, u32[]{:S(2)}) copy-start(f32[2,64,128]{2,1,0:T(8,128)} %init.1) | copy-start | bytes 196612
  100.3 43.5 %copy-start.13 = (f32[128]{0:T(128)S(1)}, f32[128]{0:T(128)}, u32[]{:S(2)}) copy-start(f32[128]{0:T(128)} %param.38) | copy-start | bytes 1540
  103.3 0.7 copy-start.2
  103.9 0.6 copy-start.4
  104.6 0.6 copy-start.6
  105.2 0.6 copy-start.9
  105.8 53.7 %collective-permute-start.1 = (bf16[2048,256]{1,0:T(8,128)(2,1)S(1)}, bf16[2048,256]{1,0:T(8,128)(2,1)S(1)}, u32[]{:S(2)}, u32[]{:S(2)}) collective-permute-start(bf16[2048,256]{1,0:T(8,128)(2,1)S(1)} %get-tuple-element.30.wa), channel_id=1, source_target_pairs={{0,1},{1,0},{2,3},{3,2},{4,5},{5,4},{6,7},{7,6},{8,9},{9,8},{10,11... | collective-permute-start | bytes 3145736 | tf_op jit(solution)/shard_map/ppermute | solution.py:314
  108.6 19.2 %all-to-all-start.1 = ((bf16[8,136,128]{2,1,0:T(8,128)(2,1)}), bf16[8,136,128]{2,1,0:T(8,128)(2,1)S(1)}, u32[]{:S(2)}, u32[]{:S(2)}) async-start(bf16[8,136,128]{2,1,0:T(8,128)(2,1)} %copy-done.1), calls=%async_computation.1 | async-start | bytes 557056 | tf_op jit(solution)/shard_map/all_to_all | solution.py:310
  128.6 15.2 %all-to-all-start.2 = ((bf16[8,136,128]{2,1,0:T(8,128)(2,1)}), bf16[8,136,128]{2,1,0:T(8,128)(2,1)S(1)}, u32[]{:S(2)}, u32[]{:S(2)}) async-start(bf16[8,136,128]{2,1,0:T(8,128)(2,1)} %get-tuple-element.19), calls=%async_computation.2 | async-start | bytes 557056 | tf_op jit(solution)/shard_map/all_to_all | solution.py:312
  143.8 0.9 copy-start.3
  144.7 0.9 copy-start.5
  145.6 0.9 copy-start.7
  146.5 0.8 copy-start.10
  148.6 10.9 %all-to-all-start.4 = ((f32[8,3,256]{2,1,0:T(4,128)}), f32[8,3,256]{2,1,0:T(4,128)S(1)}, u32[]{:S(2)}, u32[]{:S(2)}) async-start(f32[8,3,256]{2,1,0:T(4,128)} %get-tuple-element.28), calls=%async_computation.4 | async-start | bytes 65536 | tf_op jit(solution)/shard_map/all_to_all | solution.py:318
Sparse Core Ops, SparseCore 0:
  26.9 73.3 all-gather.3

commit v5 on v4

--- a/solution.py
+++ b/solution.py
@@ -54,6 +54,16 @@
     return pl.pallas_call(
         body, out_shape=sds((copies, rows, n * ch), bf16), in_specs=[VMEM] * n, out_specs=VMEM, compiler_params=SMALL
     )(*fetched(*shards))
+
+
+def copies_of(block, copies):
+    def body(ref, out):
+        for k in range(copies):
+            out[k] = ref[...]
+
+    return pl.pallas_call(
+        body, out_shape=sds((copies, *block.shape), bf16), in_specs=[VMEM], out_specs=VMEM, compiler_params=SMALL
+    )(*held(block))
 
 
 def log_rows(logs):
@@ -285,11 +295,12 @@
     nf, nt = lax.axis_size("fs"), lax.axis_size("tp")
     iz, iy, tp = (lax.axis_index(a).astype(jnp.int32).reshape(1) for a in ("sp_0", "sp_1", "tp"))
     ny = lax.axis_size("sp_1")
-    rest = lay_out((state_read, mixer_gate, conv_value, conv_gate, conv_output, state_output), ny)
-    rest = lax.all_to_all(rest, "sp_1", 0, 0, tiled=True).reshape(-1, 6 * ch)
-    rest = lax.all_gather(rest, "sp_0", axis=0, tiled=True)
-    first = lay_out((state_input, write_projection), lax.axis_size(SP))
-    first = lax.all_to_all(first, SP, 0, 0, tiled=True).reshape(-1, 2 * ch)
+    rest = lay_out((state_read, mixer_gate, conv_value, conv_gate, conv_output, state_output), 1)
+    rest = lax.all_gather(rest[0], SP, axis=0, tiled=True)
+    first = lay_out((state_input, write_projection), ny)
+    first = lax.all_to_all(first, "sp_1", 0, 0, tiled=True)
+    first = copies_of(first, lax.axis_size("sp_0"))
+    first = lax.all_to_all(first, "sp_0", 0, 0, tiled=True).reshape(-1, 2 * ch)
     n = lax.axis_size(SP)
     halo = lax.ppermute(tokens[rows - HALO :], SP, [(i, i + 1) for i in range(n - 1)])
     v = jnp.concatenate([halo, tokens], 0).astype(f32)

time: 180 us -> 184 us (1.022)
  blocking collectives: 34.4 us -> 15.1 us
  waiting for transfers between devices: 72.4 us -> 87.1 us
  starting transfers between devices: 37.4 us -> 41.5 us
  other arithmetic: 2.46 us -> 6.26 us
    all_to_all x1 -> x0, blocking collectives: 19.3 us -> none  [per_device(): rest = lax.all_to_all(rest, 'sp_1', 0, 0, tiled=True).reshape(-1, 6 * ch)]
    all_gather x1, waiting for transfers between devices: 25 us -> 32.5 us  [per_device(): rest = lax.all_gather(rest[0], SP, axis=0, tiled=True)]
    all_to_all x1 -> x2, waiting for transfers between devices: 22.8 us -> 30 us  [the longest x1 25 us: per_device(): first = lax.all_to_all(first, 'sp_0', 0, 0, tiled=True).reshape(-1, 2 * ch)]
    ppermute x1, starting transfers between devices: 2.73 us -> 6.24 us  [per_device(): back_other = lax.ppermute(back, 'tp', [(i, nt - 1 - i) for i in range(nt)])]
    ppermute x1, starting transfers between devices: 1.61 us -> 4.03 us  [per_device(): lax.ppermute(tokens[rows - HALO:], SP, [(i, i + 1) for i in range(n - 1)])]
    all_to_all x1 -> x2, starting transfers between devices: 16.6 us -> 16.1 us  [the longest x1 10 us: per_device(): first = lax.all_to_all(first, 'sp_0', 0, 0, tiled=True).reshape(-1, 2 * ch)]
    unnamed x45 -> x37, local copies, waits for them, and re-layouts: 6.89 us -> 6.87 us
  transfers between devices with their start and end apart: 7 -> 8, of which waited for: 5 -> 6; matrix products, arithmetic and copies ran while one was open for 2% -> 4% of each run, Pallas kernels for 3% -> 3%
where the time goes in v5:
time: 184 us; the launch traced here: 183 us
  waiting for transfers between devices  87.1 us (47%)
  starting transfers between devices  41.5 us (23%)
  blocking collectives  15.1 us (8%)
  between operations  13.6 us (7%)
  Pallas kernels  10.9 us (6%)
  local copies, waits for them, and re-layouts  8.45 us (5%)
  other arithmetic  6.26 us (3%)
    all_gather x1, waiting for transfers between devices, per_device(): rest = lax.all_gather(rest[0], SP, axis=0, tiled=True)  32.5 us
    all_to_all x1, waiting for transfers between devices, per_device(): first = lax.all_to_all(first, 'sp_0', 0, 0, tiled=True).reshape(-1, 2 * ch)  25 us
    all_to_all x1, waiting for transfers between devices, per_device(): got = lax.all_to_all(send, 'sp_1', 0, 0, tiled=True)  12.7 us
    all_to_all x1, blocking collectives, per_device(): pieces = lax.all_to_all(out, 'fs', 0, 0, tiled=True)  10.9 us
    all_to_all x1, starting transfers between devices, per_device(): first = lax.all_to_all(first, 'sp_0', 0, 0, tiled=True).reshape(-1, 2 * ch)  10 us
    all_to_all x1, waiting for transfers between devices, per_device(): got = lax.all_to_all(send, 'sp_0', 0, 0, tiled=True)  9.09 us
    unnamed x37, local copies, waits for them, and re-layouts  6.87 us
    ppermute x1, starting transfers between devices, per_device(): back_other = lax.ppermute(back, 'tp', [(i, nt - 1 - i) for i in range(nt)])  6.24 us
  transfers between devices with their start and end apart: 8, of which 6 were waited for; matrix products, arithmetic and copies ran while one was open for 4% of the time, Pallas kernels for 3%

profile of v5, /device:TPU:1, one launch (start us, length us, event | category | flops | bytes accessed | tf_op | source)
XLA Modules:
  0.0 183.3 jit_solution(10461289288792020408)
XLA Ops:
  6.5 1.4 shard_map.201
  8.0 0.9 slice.15
  8.9 4.0 %collective-permute-start = (bf16[32,2048]{1,0:T(8,128)(2,1)S(1)}, bf16[32,2048]{1,0:T(8,128)(2,1)S(1)}, u32[]{:S(2)}, u32[]{:S(2)}) collective-permute-start(bf16[32,2048]{1,0:T(8,128)(2,1)S(1)} %slice.15), channel_id=1, source_target_pairs={{0,8},{8,16},{16,24},{24,32},{32,40},{40,48},{48,56},{56,64},{64,7... | collective-permute-start | bytes 393224 | tf_op jit(solution)/shard_map/ppermute | solution.py:305
  13.0 1.4 shard_map.199
  14.3 6.1 %all-to-all-start = ((bf16[8,32,256]{2,1,0:T(8,128)(2,1)}), bf16[8,32,256]{2,1,0:T(8,128)(2,1)S(1)}, u32[]{:S(2)}, u32[]{:S(2)}) async-start(bf16[8,32,256]{2,1,0:T(8,128)(2,1)} %shard_map.199), calls=%async_computation | async-start | bytes 262144 | tf_op jit(solution)/shard_map/all_to_all | solution.py:301
  20.4 0.7 exponential_negate_fusion
  21.1 0.7 pad_maximum_fusion.1.tref
  21.8 1.5 fusion
  23.3 5.0 %all-to-all-done.ref = bf16[8,32,256]{2,1,0:T(8,128)(2,1)S(1)} async-done(((bf16[8,32,256]{2,1,0:T(8,128)(2,1)}), bf16[8,32,256]{2,1,0:T(8,128)(2,1)S(1)}, u32[]{:S(2)}, u32[]{:S(2)}) %all-to-all-start) | async-done | bytes 131104 | tf_op jit(solution)/shard_map/all_to_all | solution.py:301
  28.4 1.1 shard_map.200
  29.4 10.0 %all-to-all-start.1 = ((bf16[8,8,32,256]{3,2,1,0:T(8,128)(2,1)}), bf16[8,8,32,256]{3,2,1,0:T(8,128)(2,1)S(1)}, u32[]{:S(2)}, u32[]{:S(2)}) async-start(bf16[8,8,32,256]{3,2,1,0:T(8,128)(2,1)} %shard_map.200), calls=%async_computation.1 | async-start | bytes 2097152 | tf_op jit(solution)/shard_map/all_to_all | solution.py:303
  39.5 1.6 fusion.2.nref
  41.1 0.4 fusion.3
  41.5 0.1 fusion.5
  41.6 0.6 reduce-window.6
  42.2 0.2 slice_reduce_fusion
  42.4 0.2 reduce-window.9
  42.6 0.2 slice_reduce_fusion.1
  42.9 0.1 copy.32.lref
  43.0 0.1 copy.31.sref
  43.2 0.1 copy.33.cum
  43.3 25.0 %all-to-all-done.1 = bf16[8,8,32,256]{3,2,1,0:T(8,128)(2,1)S(1)} async-done(((bf16[8,8,32,256]{3,2,1,0:T(8,128)(2,1)}), bf16[8,8,32,256]{3,2,1,0:T(8,128)(2,1)S(1)}, u32[]{:S(2)}, u32[]{:S(2)}) %all-to-all-start.1) | async-done | bytes 1048608 | tf_op jit(solution)/shard_map/all_to_all | solution.py:303
  68.2 0.9 local_states.1
  69.2 0.7 copy-done.1
  69.9 32.5 %all-gather.5.cloned.1.call-done = bf16[1,2048,768]{2,1,0:T(8,128)(2,1)} async-done(((bf16[1,32,768]{2,1,0:T(8,128)(2,1)}), bf16[1,2048,768]{2,1,0:T(8,128)(2,1)}) %all-gather.5.cloned.1.call-update) | async-done | bytes 3145744 | tf_op jit(solution)/shard_map/all_gather | solution.py:299
  102.4 2.9 %rows_local.1 = (bf16[256,128]{1,0:T(8,128)(2,1)S(1)}, f32[256,128]{1,0:T(8,128)S(1)}, f32[256,128]{1,0:T(8,128)S(1)}, f32[256,128]{1,0:T(8,128)S(1)}, bf16[2048,256]{1,0:T(8,128)(2,1)S(1)}) custom-call(bf16[288,2048]{1,0:T(8,128)(2,1)S(1)} %fusion.2.nref, bf16[2048,768]{1,0:T(8,128)(2,1)} %bitcast.40, f32[4,128]{1,0:T(4,128)S(1)} %copy-done.12, ...), custom_call_target="tpu_custom_call" | custom-call | tf_op jit(solution)/shard_map/rows_local/pallas_call | solution.py:196
  105.3 0.6 copy-done.2
  106.0 0.6 copy-done.4
  106.6 0.6 copy-done.6
  107.2 0.6 copy-done.9
  107.9 6.2 %collective-permute-start.1 = (bf16[2048,256]{1,0:T(8,128)(2,1)S(1)}, bf16[2048,256]{1,0:T(8,128)(2,1)S(1)}, u32[]{:S(2)}, u32[]{:S(2)}) collective-permute-start(bf16[2048,256]{1,0:T(8,128)(2,1)S(1)} %get-tuple-element.30.wa), channel_id=1, source_target_pairs={{0,1},{1,0},{2,3},{3,2},{4,5},{5,4},{6,7},{7,6},{8,9},{9,8},{10,11... | collective-permute-start | bytes 3145736 | tf_op jit(solution)/shard_map/ppermute | solution.py:325
  114.1 5.2 %all-to-all-start.2 = ((bf16[8,136,128]{2,1,0:T(8,128)(2,1)}), bf16[8,136,128]{2,1,0:T(8,128)(2,1)S(1)}, u32[]{:S(2)}, u32[]{:S(2)}) async-start(bf16[8,136,128]{2,1,0:T(8,128)(2,1)} %copy-done.1), calls=%async_computation.2 | async-start | bytes 557056 | tf_op jit(solution)/shard_map/all_to_all | solution.py:321
  119.3 12.7 %all-to-all-done.2.ref = bf16[8,136,128]{2,1,0:T(8,128)(2,1)S(1)} async-done(((bf16[8,136,128]{2,1,0:T(8,128)(2,1)}), bf16[8,136,128]{2,1,0:T(8,128)(2,1)S(1)}, u32[]{:S(2)}, u32[]{:S(2)}) %all-to-all-start.2) | async-done | bytes 278560 | tf_op jit(solution)/shard_map/all_to_all | solution.py:321
  132.0 0.9 line_states.1
  132.9 3.8 %all-to-all-start.3 = ((bf16[8,136,128]{2,1,0:T(8,128)(2,1)}), bf16[8,136,128]{2,1,0:T(8,128)(2,1)S(1)}, u32[]{:S(2)}, u32[]{:S(2)}) async-start(bf16[8,136,128]{2,1,0:T(8,128)(2,1)} %get-tuple-element.19), calls=%async_computation.3 | async-start | bytes 557056 | tf_op jit(solution)/shard_map/all_to_all | solution.py:323
  136.8 2.2 %all-gather.2 = f32[2,1,128]{2,1,0:T(1,128)S(1)} all-gather(f32[1,1,128]{2,1,0:T(1,128)S(1)} %bitcast.46), channel_id=3, replica_groups=mesh['sp_0'=8,'sp_1'=8,'fs'=4,'tp'=2] {'tp'}, dimensions={0}, use_global_device_ids=true | all-gather | bytes 1536 | tf_op jit(solution)/shard_map/all_gather | solution.py:318
  139.0 9.1 %all-to-all-done.3.got = bf16[8,136,128]{2,1,0:T(8,128)(2,1)S(1)} async-done(((bf16[8,136,128]{2,1,0:T(8,128)(2,1)}), bf16[8,136,128]{2,1,0:T(8,128)(2,1)S(1)}, u32[]{:S(2)}, u32[]{:S(2)}) %all-to-all-start.3) | async-done | bytes 278560 | tf_op jit(solution)/shard_map/all_to_all | solution.py:323
  148.1 0.9 copy-done.3
  149.0 0.9 copy-done.5
  149.9 0.9 copy-done.7
  150.8 0.8 copy-done.10
  151.6 1.3 rows_done.1
  152.9 6.1 %all-to-all-start.4 = ((f32[8,3,256]{2,1,0:T(4,128)}), f32[8,3,256]{2,1,0:T(4,128)S(1)}, u32[]{:S(2)}, u32[]{:S(2)}) async-start(f32[8,3,256]{2,1,0:T(4,128)} %get-tuple-element.28), calls=%async_computation.4 | async-start | bytes 65536 | tf_op jit(solution)/shard_map/all_to_all | solution.py:329
  159.0 2.0 %all_gather.13.bref = bf16[512,256]{1,0:T(8,128)(2,1)S(1)} all-gather(bf16[256,256]{1,0:T(8,128)(2,1)S(1)} %get-tuple-element.29), channel_id=1, replica_groups=mesh['sp_0'=8,'sp_1'=8,'fs'=4,'tp'=2] {'tp'}, dimensions={0}, use_global_device_ids=true | all-gather | bytes 393216 | tf_op jit(solution)/shard_map/all_gather | solution.py:330
  161.0 2.7 %all-to-all-done.4.sref = f32[8,3,256]{2,1,0:T(4,128)S(1)} async-done(((f32[8,3,256]{2,1,0:T(4,128)}), f32[8,3,256]{2,1,0:T(4,128)S(1)}, u32[]{:S(2)}, u32[]{:S(2)}) %all-to-all-start.4) | async-done | bytes 24608 | tf_op jit(solution)/shard_map/all_to_all | solution.py:329
  163.7 1.1 output_rows.1
  164.8 10.9 %all_to_all.30 = bf16[4,32,2048]{2,1,0:T(8,128)(2,1)S(1)} all-to-all(bf16[4,32,2048]{2,1,0:T(8,128)(2,1)S(1)} %output_rows.1), channel_id=1, replica_groups=mesh['sp_0'=8,'sp_1'=8,'fs'=4,'tp'=2] {'fs'}, dimensions={0} | all-to-all | bytes 1048576 | tf_op jit(solution)/shard_map/all_to_all | solution.py:332
  175.8 0.7 reduce_sum.22
  (40 shorter events, 0.3 us)
Async XLA Ops:
  6.5 34.5 %copy-start = (bf16[2048,16]{0,1:T(8,128)(2,1)S(1)}, bf16[2048,16]{0,1:T(8,128)(2,1)}, u32[]{:S(2)}) copy-start(bf16[2048,16]{0,1:T(8,128)(2,1)} %param.29) | copy-start | bytes 196612
  6.5 95.8 %all-gather.5.cloned.1.call-start = ((), (), s32[]{:S(2)}) async-start(), calls=%async_computation.6 | async-start | bytes 3194880 | tf_op jit(solution)/shard_map/all_gather | solution.py:299
  8.9 12.8 %collective-permute-start = (bf16[32,2048]{1,0:T(8,128)(2,1)S(1)}, bf16[32,2048]{1,0:T(8,128)(2,1)S(1)}, u32[]{:S(2)}, u32[]{:S(2)}) collective-permute-start(bf16[32,2048]{1,0:T(8,128)(2,1)S(1)} %slice.15), channel_id=1, source_target_pairs={{0,8},{8,16},{16,24},{24,32},{32,40},{40,48},{48,56},{56,64},{64,7... | collective-permute-start | bytes 393224 | tf_op jit(solution)/shard_map/ppermute | solution.py:305
  14.3 25.1 %copy-start.14 = (f32[2048]{0:T(1024)S(1)}, f32[2048]{0:T(1024)}, u32[]{:S(2)}) copy-start(f32[2048]{0:T(1024)} %param.22) | copy-start | bytes 24580
  14.3 14.0 %all-to-all-start = ((bf16[8,32,256]{2,1,0:T(8,128)(2,1)}), bf16[8,32,256]{2,1,0:T(8,128)(2,1)S(1)}, u32[]{:S(2)}, u32[]{:S(2)}) async-start(bf16[8,32,256]{2,1,0:T(8,128)(2,1)} %shard_map.199), calls=%async_computation | async-start | bytes 262144 | tf_op jit(solution)/shard_map/all_to_all | solution.py:301
  29.4 38.8 %all-to-all-start.1 = ((bf16[8,8,32,256]{3,2,1,0:T(8,128)(2,1)}), bf16[8,8,32,256]{3,2,1,0:T(8,128)(2,1)S(1)}, u32[]{:S(2)}, u32[]{:S(2)}) async-start(bf16[8,8,32,256]{3,2,1,0:T(8,128)(2,1)} %shard_map.200), calls=%async_computation.1 | async-start | bytes 2097152 | tf_op jit(solution)/shard_map/all_to_all | solution.py:303
  39.4 2.0 %copy-start.15 = (f32[2,256]{1,0:T(2,128)S(1)}, f32[2,256]{1,0:T(2,128)}, u32[]{:S(2)}) copy-start(f32[2,256]{1,0:T(2,128)} %param.32) | copy-start | bytes 6148
  39.4 2.0 %copy-start.16 = (f32[2]{0:T(128)S(1)}, f32[2]{0:T(128)}, u32[]{:S(2)}) copy-start(f32[2]{0:T(128)} %param.30) | copy-start | bytes 28
  41.1 61.3 %copy-start.11 = (f32[31,128]{1,0:T(8,128)S(1)}, f32[31,128]{1,0:T(8,128)}, u32[]{:S(2)}) copy-start(f32[31,128]{1,0:T(8,128)} %ltaps.1) | copy-start | bytes 47620
  41.1 61.3 %copy-start.12 = (f32[4,128]{1,0:T(4,128)S(1)}, f32[4,128]{1,0:T(4,128)}, u32[]{:S(2)}) copy-start(f32[4,128]{1,0:T(4,128)} %ftaps.1) | copy-start | bytes 6148
  69.1 0.7 copy-start.1
  102.4 34.4 %copy-start.17 = (f32[128]{0:T(128)S(1)}, f32[128]{0:T(128)}, u32[]{:S(2)}) copy-start(f32[128]{0:T(128)} %param.37) | copy-start | bytes 1540
  102.4 45.7 %copy-start.8 = (f32[2,64,128]{2,1,0:T(8,128)S(1)}, f32[2,64,128]{2,1,0:T(8,128)}, u32[]{:S(2)}) copy-start(f32[2,64,128]{2,1,0:T(8,128)} %init.1) | copy-start | bytes 196612
  102.4 45.7 %copy-start.13 = (f32[128]{0:T(128)S(1)}, f32[128]{0:T(128)}, u32[]{:S(2)}) copy-start(f32[128]{0:T(128)} %param.38) | copy-start | bytes 1540
  105.3 0.7 copy-start.2
  106.0 0.6 copy-start.4
  106.6 0.6 copy-start.6
  107.2 0.6 copy-start.9
  107.9 55.9 %collective-permute-start.1 = (bf16[2048,256]{1,0:T(8,128)(2,1)S(1)}, bf16[2048,256]{1,0:T(8,128)(2,1)S(1)}, u32[]{:S(2)}, u32[]{:S(2)}) collective-permute-start(bf16[2048,256]{1,0:T(8,128)(2,1)S(1)} %get-tuple-element.30.wa), channel_id=1, source_target_pairs={{0,1},{1,0},{2,3},{3,2},{4,5},{5,4},{6,7},{7,6},{8,9},{9,8},{10,11... | collective-permute-start | bytes 3145736 | tf_op jit(solution)/shard_map/ppermute | solution.py:325
  114.1 17.9 %all-to-all-start.2 = ((bf16[8,136,128]{2,1,0:T(8,128)(2,1)}), bf16[8,136,128]{2,1,0:T(8,128)(2,1)S(1)}, u32[]{:S(2)}, u32[]{:S(2)}) async-start(bf16[8,136,128]{2,1,0:T(8,128)(2,1)} %copy-done.1), calls=%async_computation.2 | async-start | bytes 557056 | tf_op jit(solution)/shard_map/all_to_all | solution.py:321
  132.9 15.1 %all-to-all-start.3 = ((bf16[8,136,128]{2,1,0:T(8,128)(2,1)}), bf16[8,136,128]{2,1,0:T(8,128)(2,1)S(1)}, u32[]{:S(2)}, u32[]{:S(2)}) async-start(bf16[8,136,128]{2,1,0:T(8,128)(2,1)} %get-tuple-element.19), calls=%async_computation.3 | async-start | bytes 557056 | tf_op jit(solution)/shard_map/all_to_all | solution.py:323
  148.1 0.9 copy-start.3
  149.0 0.9 copy-start.5
  149.9 0.9 copy-start.7
  150.8 0.8 copy-start.10
  152.9 10.8 %all-to-all-start.4 = ((f32[8,3,256]{2,1,0:T(4,128)}), f32[8,3,256]{2,1,0:T(4,128)S(1)}, u32[]{:S(2)}, u32[]{:S(2)}) async-start(f32[8,3,256]{2,1,0:T(4,128)} %get-tuple-element.28), calls=%async_computation.4 | async-start | bytes 65536 | tf_op jit(solution)/shard_map/all_to_all | solution.py:329
Sparse Core Ops, SparseCore 0:
  10.3 91.9 all-gather.4

commit v6 on v5

--- a/solution.py
+++ b/solution.py
@@ -74,12 +74,18 @@
     return jnp.where(row == 0, hi, jnp.where(row == 1, mid, jnp.where(row == 2, lo, 0.0))).astype(bf16)
 
 
-def local_states(normed, first, taps, step, left, total, copies):
-    ext, _ = normed.shape
-    rows, ch = step.shape
-
-    def body(nref, wref, tref, sref, lref, logs, send, xs, w16, buf):
-        buf[...] = dot(nref[...], wref[...], 1, 0).astype(bf16).astype(f32)
+def local_states(halo, own, most, last, taps, step, left, total, copies):
+    rows, d = own.shape
+    ch = step.shape[1]
+    nz, main, _ = most.shape
+    size = main + last.shape[1]
+
+    def body(href, nref, mref, rref, tref, sref, lref, logs, send, xs, w16, buf, wall):
+        for z in range(nz):
+            wall[z * size : z * size + main, :] = mref[z]
+            wall[z * size + main : (z + 1) * size, :] = rref[z]
+        buf[:HALO, :] = dot(href[...], wall[...], 1, 0).astype(bf16).astype(f32)
+        buf[HALO:, :] = dot(nref[...], wall[...], 1, 0).astype(bf16).astype(f32)
         at = HALO - SHORT + 1
         mix = sum(buf[at + i : at + i + rows, :] * tref[i : i + 1, :] for i in range(SHORT))
         act = jax.nn.silu(mix)
@@ -96,11 +102,11 @@
     return pl.pallas_call(
         body,
         out_shape=(sds((copies, ch + LOGS, STATE), bf16), pltpu.VMEM((rows, ch), bf16), pltpu.VMEM((rows, STATE), bf16)),
-        in_specs=[VMEM] * 6,
+        in_specs=[VMEM] * 8,
         out_specs=(VMEM,) * 3,
-        scratch_shapes=[pltpu.VMEM((ext, 2 * ch), f32)],
+        scratch_shapes=[pltpu.VMEM((HALO + rows, 2 * ch), f32), pltpu.VMEM((d, 2 * ch), bf16)],
         compiler_params=SMALL, name="local_states",
-    )(*held(normed, first, taps, step, left, total))
+    )(*held(halo, own, most, last, taps, step, left, total))
 
 
 def spread_heads(c, heads, p):
@@ -140,82 +146,34 @@
     )(index, *held(got))
 
 
-def rows_local(normed, rest, ftaps, ltaps, xs, w16, cum, cum_t):
-    ext, d = normed.shape
-    rows, ch = xs.shape
+def rows_done(halo, own, rest, ltaps, got, enter, before, init, index, ftaps, xs, w16, cum, cum_t, gain, copies):
+    rows, d = own.shape
+    ch = xs.shape[1]
+    ext = HALO + rows
+    n, _, _ = got.shape
     heads = cum_t.shape[0]
     p = ch // heads
-    part, n = 64, 8
-    kc = d // n
-
-    def body(nref, wref, ftaps, ltaps, xs, w16, cum, cum_t, read16, zgate, mixed, inner, back, acc, glu, wall, sems):
+    part, parts = 64, 8
+    kc = d // parts
+
+    def body(
+        at, href, nref, wref, lref, got, enter, before, init, ftaps, xs, w16, cum, cum_t, gain,
+        sums, pre, back, acc, glu, wall, ltaps, sems,
+    ):
         def fetch(i):
-            at = slice(i * kc, (i + 1) * kc)
-            return pltpu.make_async_copy(wref.at[at, : 4 * ch], wall.at[at, :], sems.at[0, i])
+            here = slice(i * kc, (i + 1) * kc)
+            return pltpu.make_async_copy(wref.at[here, : 4 * ch], wall.at[here, :], sems.at[0, i])
 
         def fetch_back(i):
-            at = slice(i * kc, (i + 1) * kc)
-            return pltpu.make_async_copy(wref.at[at, 4 * ch :], back.at[at, :], sems.at[1, i])
-
-        for i in range(n):
+            here = slice(i * kc, (i + 1) * kc)
+            return pltpu.make_async_copy(wref.at[here, 4 * ch :], back.at[here, :], sems.at[1, i])
+
+        fetch_taps = pltpu.make_async_copy(lref, ltaps, sems.at[2, 0])
+        for i in range(parts):
             fetch(i).start()
-        for i in range(n):
+        fetch_taps.start()
+        for i in range(parts):
             fetch_back(i).start()
-        for i in range(n):
-            fetch(i).wait()
-            at = slice(i * kc, (i + 1) * kc)
-            term = dot(nref[:, at], wall[at, :], 1, 0)
-            acc[...] = term if i == 0 else acc[...] + term
-        glu[...] = acc[:, 2 * ch : 3 * ch].astype(bf16).astype(f32) * jax.nn.sigmoid(
-            acc[:, 3 * ch :].astype(bf16).astype(f32)
-        )
-        acc[:, : 2 * ch] = acc[:, : 2 * ch].astype(bf16).astype(f32)
-        s_at, l_at = HALO - SHORT + 1, HALO - WIDE + 1
-        read = sum(acc[s_at + i : s_at + i + rows, :ch] * ftaps[i : i + 1, :] for i in range(SHORT))
-        read = jax.nn.silu(read).astype(bf16)
-        read16[...] = read
-        zgate[...] = jax.nn.silu(acc[HALO:, ch : 2 * ch])
-        scores = dot(read, w16[...], 1, 1)
-        lower = lax.broadcasted_iota(jnp.int32, (rows, rows), 0) >= lax.broadcasted_iota(jnp.int32, (rows, rows), 1)
-        lane = lax.broadcasted_iota(jnp.int32, (rows, ch), 1)
-        y = jnp.zeros((rows, ch), f32)
-        for h in range(heads):
-            gap = jnp.where(lower, cum[:, h * p : h * p + 1] - cum_t[h : h + 1, :], 0.0)
-            m = jnp.where(lower, jnp.exp(gap) * scores, 0.0).astype(bf16)
-            x = jnp.where(lane // p == h, xs[...].astype(f32), 0.0).astype(bf16)
-            y = y + dot(m, x, 1, 0)
-        inner[...] = y
-        for r in range(0, rows, part):
-            mixed[r : r + part, :] = sum(
-                glu[l_at + r + i : l_at + r + i + part, :] * ltaps[i : i + 1, :] for i in range(WIDE)
-            )
-        for i in range(n):
-            fetch_back(i).wait()
-
-    small = (ftaps, ltaps, xs, w16, cum, cum_t)
-    return pl.pallas_call(
-        body,
-        out_shape=(
-            pltpu.VMEM((rows, STATE), bf16), pltpu.VMEM((rows, ch), f32), pltpu.VMEM((rows, ch), f32),
-            pltpu.VMEM((rows, ch), f32), pltpu.VMEM((d, 2 * ch), bf16),
-        ),
-        in_specs=[VMEM, pl.BlockSpec(memory_space=pltpu.HBM), *[VMEM] * len(small)],
-        out_specs=(VMEM,) * 5,
-        scratch_shapes=[
-            pltpu.VMEM((ext, 4 * ch), f32), pltpu.VMEM((ext, ch), f32), pltpu.VMEM((d, 4 * ch), bf16),
-            pltpu.SemaphoreType.DMA((2, n)),
-        ],
-        compiler_params=SMALL, name="rows_local",
-    )(*held(normed), *fetched(rest), *held(*small))
-
-
-def rows_done(got, enter, before, init, index, read16, zgate, mixed, inner, cum, gain, copies):
-    rows, ch = mixed.shape
-    n, _, _ = got.shape
-    heads = init.shape[0]
-    p = ch // heads
-
-    def body(at, got, enter, before, init, read16, zgate, mixed, inner, cum, gain, sums, pre):
         acc_in = jnp.zeros((1, STATE), f32)
         start = enter[...]
         b = before[0:1, :]
@@ -225,9 +183,39 @@
             start = start + got[j, :ch, :].astype(f32) * spread_heads(inside * jnp.exp(acc_in + b), heads, p)
             acc_in = acc_in + inside * logs
         start = start + init[...].reshape(ch, STATE) * spread_heads(jnp.exp(acc_in + b), heads, p)
-        y = inner[...] + dot(read16[...], start.astype(bf16), 1, 1) * jnp.exp(cum[...])
-        gated = y * zgate[...]
-        mix = mixed[...]
+        start = start.astype(bf16)
+        for i in range(parts):
+            fetch(i).wait()
+            here = slice(i * kc, (i + 1) * kc)
+            first = dot(href[:, here], wall[here, :], 1, 0)
+            term = dot(nref[:, here], wall[here, :], 1, 0)
+            acc[:HALO, :] = first if i == 0 else acc[:HALO, :] + first
+            acc[HALO:, :] = term if i == 0 else acc[HALO:, :] + term
+        glu[...] = acc[:, 2 * ch : 3 * ch].astype(bf16).astype(f32) * jax.nn.sigmoid(
+            acc[:, 3 * ch :].astype(bf16).astype(f32)
+        )
+        acc[:, : 2 * ch] = acc[:, : 2 * ch].astype(bf16).astype(f32)
+        s_at, l_at = HALO - SHORT + 1, HALO - WIDE + 1
+        read = sum(acc[s_at + i : s_at + i + rows, :ch] * ftaps[i : i + 1, :] for i in range(SHORT))
+        read = jax.nn.silu(read).astype(bf16)
+        y = dot(read, start, 1, 1) * jnp.exp(cum[...])
+        scores = dot(read, w16[...], 1, 1)
+        lower = lax.broadcasted_iota(jnp.int32, (rows, rows), 0) >= lax.broadcasted_iota(jnp.int32, (rows, rows), 1)
+        lane = lax.broadcasted_iota(jnp.int32, (rows, ch), 1)
+        for h in range(heads):
+            gap = jnp.where(lower, cum[:, h * p : h * p + 1] - cum_t[h : h + 1, :], 0.0)
+            m = jnp.where(lower, jnp.exp(gap) * scores, 0.0).astype(bf16)
+            x = jnp.where(lane // p == h, xs[...].astype(f32), 0.0).astype(bf16)
+            y = y + dot(m, x, 1, 0)
+        gated = y * jax.nn.silu(acc[HALO:, ch : 2 * ch])
+        fetch_taps.wait()
+        mix = jnp.concatenate(
+            [
+                sum(glu[l_at + r + i : l_at + r + i + part, :] * ltaps[i : i + 1, :] for i in range(WIDE))
+                for r in range(0, rows, part)
+            ],
+            0,
+        )
         squares = jnp.concatenate([mix, mix * mix, gated * gated], 1)
         pick = lax.broadcasted_iota(jnp.int32, (8, 3 * ch), 1) // ch == lax.broadcasted_iota(jnp.int32, (8, 3 * ch), 0)
         found = dot(jnp.where(pick, 1.0, 0.0), squares, 1, 1, HIGHEST)
@@ -235,14 +223,21 @@
             sums[j] = found[:3]
         pre[:, :ch] = mix.astype(bf16)
         pre[:, ch:] = (gated * gain[...]).astype(bf16)
-
+        for i in range(parts):
+            fetch_back(i).wait()
+
+    hbm = pl.BlockSpec(memory_space=pltpu.HBM)
     return pl.pallas_call(
         body,
-        out_shape=(sds((copies, 3, rows), f32), pltpu.VMEM((rows, 2 * ch), bf16)),
-        in_specs=[SMEM, *[VMEM] * 10],
-        out_specs=(VMEM, VMEM),
+        out_shape=(sds((copies, 3, rows), f32), pltpu.VMEM((rows, 2 * ch), bf16), pltpu.VMEM((d, 2 * ch), bf16)),
+        in_specs=[SMEM, VMEM, VMEM, hbm, hbm, *[VMEM] * 10],
+        out_specs=(VMEM,) * 3,
+        scratch_shapes=[
+            pltpu.VMEM((ext, 4 * ch), f32), pltpu.VMEM((ext, ch), f32), pltpu.VMEM((d, 4 * ch), bf16),
+            pltpu.VMEM(ltaps.shape, f32), pltpu.SemaphoreType.DMA((3, parts)),
+        ],
         compiler_params=SMALL, name="rows_done",
-    )(index, *held(got, enter, before, init, read16, zgate, mixed, inner, cum, gain))
+    )(index, *held(halo, own), *fetched(rest, ltaps), *held(got, enter, before, init, ftaps, xs, w16, cum, cum_t, gain))
 
 
 def output_rows(sums, both, gains, own, other, index, nf, nt):
@@ -299,13 +294,21 @@
     rest = lax.all_gather(rest[0], SP, axis=0, tiled=True)
     first = lay_out((state_input, write_projection), ny)
     first = lax.all_to_all(first, "sp_1", 0, 0, tiled=True)
-    first = copies_of(first, lax.axis_size("sp_0"))
-    first = lax.all_to_all(first, "sp_0", 0, 0, tiled=True).reshape(-1, 2 * ch)
+    first = first.reshape(-1, 2 * ch)
+    main = first.shape[0] - first.shape[0] // 16
+    last = copies_of(first[main:], lax.axis_size("sp_0"))
+    last = lax.all_to_all(last, "sp_0", 0, 0, tiled=True)
+    most = lax.all_gather(first[:main], "sp_0", axis=0)
     n = lax.axis_size(SP)
     halo = lax.ppermute(tokens[rows - HALO :], SP, [(i, i + 1) for i in range(n - 1)])
-    v = jnp.concatenate([halo, tokens], 0).astype(f32)
-    normed = (v * lax.rsqrt(jnp.mean(v * v, axis=1, keepdims=True) + EPS) * norm_gain).astype(bf16)
-    step_all = jnp.dot(normed[HALO:], step_proj, preferred_element_type=f32)
+
+    def unit(x):
+        v = x.astype(f32)
+        return (v * lax.rsqrt(jnp.mean(v * v, axis=1, keepdims=True) + EPS) * norm_gain).astype(bf16)
+
+    own = unit(tokens)
+    halo = unit(halo)
+    step_all = jnp.dot(own, step_proj, preferred_element_type=f32)
     me = lax.axis_index("fs") * nt + lax.axis_index("tp")
     step = jax.nn.softplus(lax.dynamic_slice_in_dim(step_all, me * heads, heads, 1) + step_bias)
     log_step = (-jnp.exp(decay_log) * step + decay_extra.T).T
@@ -317,15 +320,15 @@
     total = jnp.pad(total[None], ((0, 0), (0, STATE - heads)))
     gains = lax.all_gather(conv_gain, "tp")
     taps = jnp.concatenate([input_taps, write_taps], 1)
-    send, xs, w16 = local_states(normed, first, taps, step, left, total, ny)
+    send, xs, w16 = local_states(halo, own, most, last, taps, step, left, total, ny)
     got = lax.all_to_all(send, "sp_1", 0, 0, tiled=True)
     enter, before, send = line_states(got, iy, heads, p, lax.axis_size("sp_0"))
     got = lax.all_to_all(send, "sp_0", 0, 0, tiled=True)
-    read16, zgate, mixed, inner, back = rows_local(normed, rest, fetch_taps, long_taps, xs, w16, cum, cum_t)
+    sums, pre, back = rows_done(
+        halo, own, rest, long_taps, got, enter, before, initial_state, iz, fetch_taps, xs, w16, cum, cum_t,
+        state_gain[None], nf * nt,
+    )
     back_other = lax.ppermute(back, "tp", [(i, nt - 1 - i) for i in range(nt)])
-    sums, pre = rows_done(
-        got, enter, before, initial_state, iz, read16, zgate, mixed, inner, cum, state_gain[None], nf * nt
-    )
     sums = lax.all_to_all(sums, FT, 0, 0, tiled=True)
     both = lax.all_gather(pre, "tp", axis=0, tiled=True)
     out = output_rows(sums, both, gains, back, back_other, tp, nf, nt)

time: 184 us -> 144 us (0.78)
  waiting for transfers between devices: 87.1 us -> 33.3 us
  blocking collectives: 15.1 us -> 39.5 us
  local copies, waits for them, and re-layouts: 8.45 us -> 1.66 us
  starting transfers between devices: 41.5 us -> 38.1 us
    all_gather x1, waiting for transfers between devices: 32.5 us -> 4.74 us  [per_device(): rest = lax.all_gather(rest[0], SP, axis=0, tiled=True)]
    all_to_all x1, waiting for transfers between devices: 25 us -> 0.01 us  [per_device(): last = lax.all_to_all(last, 'sp_0', 0, 0, tiled=True)]
    all_gather x0 -> x1, blocking collectives: none -> 24.3 us  [per_device(): most = lax.all_gather(first[:main], 'sp_0', axis=0)]
    unnamed x37 -> x23, local copies, waits for them, and re-layouts: 6.87 us -> 0.07 us
    pallas_call x1, Pallas kernels: 1.27 us -> 4.63 us  [rows_done(): pl.pallas_call(body, out_shape=(sds((copies, 3, rows), f32), pltpu.VMEM((...]
    pallas_call x1 -> x0, Pallas kernels: 2.89 us -> none  [rows_local(): pl.pallas_call(body, out_shape=(pltpu.VMEM((rows, STATE), bf16), pltpu.VM...]
    all_to_all x1, waiting for transfers between devices: 5.05 us -> 2.26 us  [per_device(): first = lax.all_to_all(first, 'sp_1', 0, 0, tiled=True)]
    all_to_all x1, waiting for transfers between devices: 9.09 us -> 11.8 us  [per_device(): got = lax.all_to_all(send, 'sp_0', 0, 0, tiled=True)]
  transfers between devices with their start and end apart: 8 -> 8, of which waited for: 6 -> 5; matrix products, arithmetic and copies ran while one was open for 4% -> 5% of each run, Pallas kernels for 3% -> 3%
where the time goes in v6:
time: 144 us
  blocking collectives  39.5 us (27%)
  starting transfers between devices  38.1 us (26%)
  waiting for transfers between devices  33.3 us (23%)
  between operations  13.6 us (9%)
  Pallas kernels  11.8 us (8%)
  other arithmetic  5.3 us (4%)
  local copies, waits for them, and re-layouts  1.66 us (1%)
    all_gather x1, blocking collectives, per_device(): most = lax.all_gather(first[:main], 'sp_0', axis=0)  24.3 us
    all_to_all x1, waiting for transfers between devices, per_device(): got = lax.all_to_all(send, 'sp_0', 0, 0, tiled=True)  11.8 us
    all_to_all x1, waiting for transfers between devices, per_device(): got = lax.all_to_all(send, 'sp_1', 0, 0, tiled=True)  11.7 us
    all_to_all x1, blocking collectives, per_device(): pieces = lax.all_to_all(out, 'fs', 0, 0, tiled=True)  10.9 us
    all_to_all x1, starting transfers between devices, per_device(): last = lax.all_to_all(last, 'sp_0', 0, 0, tiled=True)  10 us
    all_to_all x1, starting transfers between devices, per_device(): first = lax.all_to_all(first, 'sp_1', 0, 0, tiled=True)  5.92 us
    ppermute x1, starting transfers between devices, per_device(): back_other = lax.ppermute(back, 'tp', [(i, nt - 1 - i) for i in range(nt)])  5.48 us
    all_to_all x1, starting transfers between devices, per_device(): sums = lax.all_to_all(sums, FT, 0, 0, tiled=True)  5.25 us
  transfers between devices with their start and end apart: 8, of which 5 were waited for; matrix products, arithmetic and copies ran while one was open for 5% of the time, Pallas kernels for 3%

profile of v6, /device:TPU:1, one launch (start us, length us, event | category | flops | bytes accessed | tf_op | source)
XLA Modules:
  0.0 143.6 jit_solution(6063701859525097754)
XLA Ops:
  6.5 1.5 %shard_map.199 = bf16[1,32,768]{2,1,0:T(8,128)(2,1)} custom-call(bf16[32,128]{1,0:T(8,128)(2,1)} %refs_0_.2, bf16[32,128]{1,0:T(8,128)(2,1)} %refs_1_.2, bf16[32,128]{1,0:T(8,128)(2,1)} %refs_2_.1, bf16[32,128]{1,0:T(8,128)(2,1)} %refs_3_.1, bf16[32,128]{1,0:T(8,128)(2,1)} %refs_4_.1, bf16[32,128]{1,0:T(8,128)(2,1)} %refs_5_.1), custom_call_target="tpu_custom_call" | custom-call | tf_op jit(solution)/shard_map/pallas_call | solution.py:54
  8.0 0.0 all-gather.6.cloned.1.call-update
  8.1 0.9 slice.18
  9.0 4.0 %collective-permute-start = (bf16[32,2048]{1,0:T(8,128)(2,1)S(1)}, bf16[32,2048]{1,0:T(8,128)(2,1)S(1)}, u32[]{:S(2)}, u32[]{:S(2)}) collective-permute-start(bf16[32,2048]{1,0:T(8,128)(2,1)S(1)} %slice.18), channel_id=1, source_target_pairs={{0,8},{8,16},{16,24},{24,32},{32,40},{40,48},{48,56},{56,64},{64,7... | collective-permute-start | bytes 393224 | tf_op jit(solution)/shard_map/ppermute | solution.py:303
  13.0 1.4 shard_map.200
  14.4 5.9 %all-to-all-start = ((bf16[8,32,256]{2,1,0:T(8,128)(2,1)}), bf16[8,32,256]{2,1,0:T(8,128)(2,1)S(1)}, u32[]{:S(2)}, u32[]{:S(2)}) async-start(bf16[8,32,256]{2,1,0:T(8,128)(2,1)} %shard_map.200), calls=%async_computation | async-start | bytes 262144 | tf_op jit(solution)/shard_map/all_to_all | solution.py:296
  20.3 0.0 copy-start.9
  20.3 1.5 %fusion = f32[256]{0:T(256)S(1)} fusion(bf16[256,2048]{1,0:T(8,128)(2,1)} %param.21), kind=kLoop, calls=%fused_computation.2 | loop fusion | flops 1572608 | bytes 1049600 | tf_op jit(solution)/shard_map/reduce_sum | solution.py:307
  21.9 0.0 copy-start.8
  21.9 0.7 exponential_negate_fusion
  22.6 0.0 copy-start.5
  22.6 1.1 fusion.2.nref
  23.7 0.4 fusion.8
  24.0 0.0 copy-done.9
  24.1 0.1 fusion.6
  24.2 0.6 reduce-window.6
  24.8 0.2 slice_reduce_fusion
  25.0 0.2 reduce-window.9
  25.1 0.1 add_bitcast_fusion
  25.2 0.2 slice_reduce_fusion.1
  25.4 0.1 exponential_bitcast_fusion
  25.5 0.1 copy.31.lref
  25.6 0.1 copy.30.sref
  25.8 0.1 fusion.3
  25.9 0.1 fusion.5.href
  26.0 2.3 %all-to-all-done = bf16[8,32,256]{2,1,0:T(8,128)(2,1)S(1)} async-done(((bf16[8,32,256]{2,1,0:T(8,128)(2,1)}), bf16[8,32,256]{2,1,0:T(8,128)(2,1)S(1)}, u32[]{:S(2)}, u32[]{:S(2)}) %all-to-all-start) | async-done | bytes 131104 | tf_op jit(solution)/shard_map/all_to_all | solution.py:296
  28.3 0.6 shard_map.201
  28.9 10.0 %all-to-all-start.1 = ((bf16[8,16,256]{2,1,0:T(8,128)(2,1)}), bf16[8,16,256]{2,1,0:T(8,128)(2,1)S(1)}, u32[]{:S(2)}, u32[]{:S(2)}) async-start(bf16[8,16,256]{2,1,0:T(8,128)(2,1)} %shard_map.201), calls=%async_computation.1 | async-start | bytes 131072 | tf_op jit(solution)/shard_map/all_to_all | solution.py:300
  39.0 24.3 %all-gather.1 = bf16[1920,256]{1,0:T(8,128)(2,1)S(1)} all-gather(bf16[240,256]{1,0:T(8,128)(2,1)S(1)} %slice.24), channel_id=3, replica_groups=mesh['sp_0'=8,'sp_1'=8,'fs'=4,'tp'=2] {'sp_0'}, dimensions={0}, use_global_device_ids=true | all-gather | bytes 1105920 | tf_op jit(solution)/shard_map/all_gather | solution.py:301
  63.3 0.0 all-to-all-done.1.rref
  63.3 0.0 copy-start.3
  63.3 1.7 %local_states.1 = (bf16[8,136,128]{2,1,0:T(8,128)(2,1)}, bf16[256,128]{1,0:T(8,128)(2,1)S(1)}, bf16[256,128]{1,0:T(8,128)(2,1)S(1)}) custom-call(bf16[32,2048]{1,0:T(8,128)(2,1)S(1)} %fusion.5.href, bf16[256,2048]{1,0:T(8,128)(2,1)S(1)} %fusion.2.nref, bf16[8,240,256]{2,1,0:T(8,128)(2,1)S(1)} %bitcast.36, bf16[8,16,256]{2,1,0:T(8,128)(2,1)S(1)} %all-to-all-done.1.rref, ...), custom_call_target="tpu_custom_call" | custom-call | tf_op jit(solution)/shard_map/local_states/pallas_call | solution.py:102
  65.0 3.7 %all-to-all-start.2 = ((bf16[8,136,128]{2,1,0:T(8,128)(2,1)}), bf16[8,136,128]{2,1,0:T(8,128)(2,1)S(1)}, u32[]{:S(2)}, u32[]{:S(2)}) async-start(bf16[8,136,128]{2,1,0:T(8,128)(2,1)} %get-tuple-element.14), calls=%async_computation.2 | async-start | bytes 557056 | tf_op jit(solution)/shard_map/all_to_all | solution.py:324
  68.7 11.7 %all-to-all-done.2.ref = bf16[8,136,128]{2,1,0:T(8,128)(2,1)S(1)} async-done(((bf16[8,136,128]{2,1,0:T(8,128)(2,1)}), bf16[8,136,128]{2,1,0:T(8,128)(2,1)S(1)}, u32[]{:S(2)}, u32[]{:S(2)}) %all-to-all-start.2) | async-done | bytes 278560 | tf_op jit(solution)/shard_map/all_to_all | solution.py:324
  80.4 0.9 line_states.1
  81.3 3.7 %all-to-all-start.3 = ((bf16[8,136,128]{2,1,0:T(8,128)(2,1)}), bf16[8,136,128]{2,1,0:T(8,128)(2,1)S(1)}, u32[]{:S(2)}, u32[]{:S(2)}) async-start(bf16[8,136,128]{2,1,0:T(8,128)(2,1)} %get-tuple-element.15), calls=%async_computation.3 | async-start | bytes 557056 | tf_op jit(solution)/shard_map/all_to_all | solution.py:326
  85.0 0.1 copy.32.cum
  85.1 11.8 %all-to-all-done.3.got = bf16[8,136,128]{2,1,0:T(8,128)(2,1)S(1)} async-done(((bf16[8,136,128]{2,1,0:T(8,128)(2,1)}), bf16[8,136,128]{2,1,0:T(8,128)(2,1)S(1)}, u32[]{:S(2)}, u32[]{:S(2)}) %all-to-all-start.3) | async-done | bytes 278560 | tf_op jit(solution)/shard_map/all_to_all | solution.py:326
  96.9 4.7 %all-gather.6.cloned.1.call-done = bf16[1,2048,768]{2,1,0:T(8,128)(2,1)} async-done(((bf16[1,32,768]{2,1,0:T(8,128)(2,1)}), bf16[1,2048,768]{2,1,0:T(8,128)(2,1)}) %all-gather.6.cloned.1.call-update) | async-done | bytes 3145744 | tf_op jit(solution)/shard_map/all_gather | solution.py:294
  101.7 4.6 %rows_done.1 = (f32[8,3,256]{2,1,0:T(4,128)}, bf16[256,256]{1,0:T(8,128)(2,1)S(1)}, bf16[2048,256]{1,0:T(8,128)(2,1)S(1)}) custom-call(s32[1]{0:T(128)} %bitcast.1.at, bf16[32,2048]{1,0:T(8,128)(2,1)S(1)} %fusion.5.href, bf16[256,2048]{1,0:T(8,128)(2,1)S(1)} %fusion.2.nref, bf16[2048,768]{1,0:T(8,128)(2,1)} %bitcast.42, f32[31,128]{1,0:T(8,128)} %lref.1, ...), custom_call_target="tpu_custom_call" | custom-call | tf_op jit(solution)/shard_map/rows_done/pallas_call | solution.py:230
  106.3 5.5 %collective-permute-start.1 = (bf16[2048,256]{1,0:T(8,128)(2,1)S(1)}, bf16[2048,256]{1,0:T(8,128)(2,1)S(1)}, u32[]{:S(2)}, u32[]{:S(2)}) collective-permute-start(bf16[2048,256]{1,0:T(8,128)(2,1)S(1)} %get-tuple-element.22.wa), channel_id=1, source_target_pairs={{0,1},{1,0},{2,3},{3,2},{4,5},{5,4},{6,7},{7,6},{8,9},{9,8},{10,11... | collective-permute-start | bytes 3145736 | tf_op jit(solution)/shard_map/ppermute | solution.py:331
  111.8 2.3 %all-gather.3 = f32[2,1,128]{2,1,0:T(1,128)S(1)} all-gather(f32[1,1,128]{2,1,0:T(1,128)S(1)} %bitcast.50), channel_id=4, replica_groups=mesh['sp_0'=8,'sp_1'=8,'fs'=4,'tp'=2] {'tp'}, dimensions={0}, use_global_device_ids=true | all-gather | bytes 1536 | tf_op jit(solution)/shard_map/all_gather | solution.py:321
  114.0 5.2 %all-to-all-start.4 = ((f32[8,3,256]{2,1,0:T(4,128)}), f32[8,3,256]{2,1,0:T(4,128)S(1)}, u32[]{:S(2)}, u32[]{:S(2)}) async-start(f32[8,3,256]{2,1,0:T(4,128)} %get-tuple-element.20), calls=%async_computation.4 | async-start | bytes 65536 | tf_op jit(solution)/shard_map/all_to_all | solution.py:332
  119.3 2.0 %all_gather.21.bref = bf16[512,256]{1,0:T(8,128)(2,1)S(1)} all-gather(bf16[256,256]{1,0:T(8,128)(2,1)S(1)} %get-tuple-element.21), channel_id=1, replica_groups=mesh['sp_0'=8,'sp_1'=8,'fs'=4,'tp'=2] {'tp'}, dimensions={0}, use_global_device_ids=true | all-gather | bytes 393216 | tf_op jit(solution)/shard_map/all_gather | solution.py:333
  121.3 2.7 %all-to-all-done.4.sref = f32[8,3,256]{2,1,0:T(4,128)S(1)} async-done(((f32[8,3,256]{2,1,0:T(4,128)}), f32[8,3,256]{2,1,0:T(4,128)S(1)}, u32[]{:S(2)}, u32[]{:S(2)}) %all-to-all-start.4) | async-done | bytes 24608 | tf_op jit(solution)/shard_map/all_to_all | solution.py:332
  124.0 1.1 output_rows.1
  125.1 10.9 %all_to_all.30 = bf16[4,32,2048]{2,1,0:T(8,128)(2,1)S(1)} all-to-all(bf16[4,32,2048]{2,1,0:T(8,128)(2,1)S(1)} %output_rows.1), channel_id=1, replica_groups=mesh['sp_0'=8,'sp_1'=8,'fs'=4,'tp'=2] {'fs'}, dimensions={0} | all-to-all | bytes 1048576 | tf_op jit(solution)/shard_map/all_to_all | solution.py:335
  136.0 0.7 reduce_sum.32
  (31 shorter events, 0.1 us)
Async XLA Ops:
  6.5 17.1 %copy-start = (bf16[2048,16]{0,1:T(8,128)(2,1)S(1)}, bf16[2048,16]{0,1:T(8,128)(2,1)}, u32[]{:S(2)}) copy-start(bf16[2048,16]{0,1:T(8,128)(2,1)} %param.29) | copy-start | bytes 196612
  6.5 16.0 %copy-start.4 = (bf16[256,2048]{1,0:T(8,128)(2,1)S(1)}, bf16[256,2048]{1,0:T(8,128)(2,1)}, u32[]{:S(2)}) copy-start(bf16[256,2048]{1,0:T(8,128)(2,1)} %param.21) | copy-start | bytes 3145732
  6.5 95.1 %all-gather.6.cloned.1.call-start = ((), (), s32[]{:S(2)}) async-start(), calls=%async_computation.6 | async-start | bytes 3194880 | tf_op jit(solution)/shard_map/all_gather | solution.py:294
  9.0 16.8 %collective-permute-start = (bf16[32,2048]{1,0:T(8,128)(2,1)S(1)}, bf16[32,2048]{1,0:T(8,128)(2,1)S(1)}, u32[]{:S(2)}, u32[]{:S(2)}) collective-permute-start(bf16[32,2048]{1,0:T(8,128)(2,1)S(1)} %slice.18), channel_id=1, source_target_pairs={{0,8},{8,16},{16,24},{24,32},{32,40},{40,48},{48,56},{56,64},{64,7... | collective-permute-start | bytes 393224 | tf_op jit(solution)/shard_map/ppermute | solution.py:303
  14.4 13.9 %all-to-all-start = ((bf16[8,32,256]{2,1,0:T(8,128)(2,1)}), bf16[8,32,256]{2,1,0:T(8,128)(2,1)S(1)}, u32[]{:S(2)}, u32[]{:S(2)}) async-start(bf16[8,32,256]{2,1,0:T(8,128)(2,1)} %shard_map.200), calls=%async_computation | async-start | bytes 262144 | tf_op jit(solution)/shard_map/all_to_all | solution.py:296
  20.3 3.7 %copy-start.6 = (f32[2,256]{1,0:T(2,128)S(1)}, f32[2,256]{1,0:T(2,128)}, u32[]{:S(2)}) copy-start(f32[2,256]{1,0:T(2,128)} %param.32) | copy-start | bytes 6148
  20.3 3.7 %copy-start.9 = (f32[2]{0:T(128)S(1)}, f32[2]{0:T(128)}, u32[]{:S(2)}) copy-start(f32[2]{0:T(128)} %param.30) | copy-start | bytes 28
  21.9 3.9 %copy-start.7 = (f32[4,128]{1,0:T(4,128)S(1)}, f32[4,128]{1,0:T(4,128)}, u32[]{:S(2)}) copy-start(f32[4,128]{1,0:T(4,128)} %param.34) | copy-start | bytes 6148
  21.9 3.9 %copy-start.8 = (f32[4,128]{1,0:T(4,128)S(1)}, f32[4,128]{1,0:T(4,128)}, u32[]{:S(2)}) copy-start(f32[4,128]{1,0:T(4,128)} %param.33) | copy-start | bytes 6148
  22.6 3.4 %copy-start.5 = (f32[2048]{0:T(1024)S(1)}, f32[2048]{0:T(1024)}, u32[]{:S(2)}) copy-start(f32[2048]{0:T(1024)} %param.22) | copy-start | bytes 24580
  28.9 34.3 %all-to-all-start.1 = ((bf16[8,16,256]{2,1,0:T(8,128)(2,1)}), bf16[8,16,256]{2,1,0:T(8,128)(2,1)S(1)}, u32[]{:S(2)}, u32[]{:S(2)}) async-start(bf16[8,16,256]{2,1,0:T(8,128)(2,1)} %shard_map.201), calls=%async_computation.1 | async-start | bytes 131072 | tf_op jit(solution)/shard_map/all_to_all | solution.py:300
  63.3 38.4 %copy-start.1 = (f32[2,64,128]{2,1,0:T(8,128)S(1)}, f32[2,64,128]{2,1,0:T(8,128)}, u32[]{:S(2)}) copy-start(f32[2,64,128]{2,1,0:T(8,128)} %init.1) | copy-start | bytes 196612
  63.3 38.4 %copy-start.2 = (f32[4,128]{1,0:T(4,128)S(1)}, f32[4,128]{1,0:T(4,128)}, u32[]{:S(2)}) copy-start(f32[4,128]{1,0:T(4,128)} %ftaps.1) | copy-start | bytes 6148
  63.3 38.4 %copy-start.3 = (f32[128]{0:T(128)S(1)}, f32[128]{0:T(128)}, u32[]{:S(2)}) copy-start(f32[128]{0:T(128)} %param.38) | copy-start | bytes 1540
  65.0 15.4 %all-to-all-start.2 = ((bf16[8,136,128]{2,1,0:T(8,128)(2,1)}), bf16[8,136,128]{2,1,0:T(8,128)(2,1)S(1)}, u32[]{:S(2)}, u32[]{:S(2)}) async-start(bf16[8,136,128]{2,1,0:T(8,128)(2,1)} %get-tuple-element.14), calls=%async_computation.2 | async-start | bytes 557056 | tf_op jit(solution)/shard_map/all_to_all | solution.py:324
  81.3 15.6 %all-to-all-start.3 = ((bf16[8,136,128]{2,1,0:T(8,128)(2,1)}), bf16[8,136,128]{2,1,0:T(8,128)(2,1)S(1)}, u32[]{:S(2)}, u32[]{:S(2)}) async-start(bf16[8,136,128]{2,1,0:T(8,128)(2,1)} %get-tuple-element.15), calls=%async_computation.3 | async-start | bytes 557056 | tf_op jit(solution)/shard_map/all_to_all | solution.py:326
  101.6 10.1 %copy-start.10 = (f32[128]{0:T(128)S(1)}, f32[128]{0:T(128)}, u32[]{:S(2)}) copy-start(f32[128]{0:T(128)} %param.37) | copy-start | bytes 1540
  106.3 17.7 %collective-permute-start.1 = (bf16[2048,256]{1,0:T(8,128)(2,1)S(1)}, bf16[2048,256]{1,0:T(8,128)(2,1)S(1)}, u32[]{:S(2)}, u32[]{:S(2)}) collective-permute-start(bf16[2048,256]{1,0:T(8,128)(2,1)S(1)} %get-tuple-element.22.wa), channel_id=1, source_target_pairs={{0,1},{1,0},{2,3},{3,2},{4,5},{5,4},{6,7},{7,6},{8,9},{9,8},{10,11... | collective-permute-start | bytes 3145736 | tf_op jit(solution)/shard_map/ppermute | solution.py:331
  114.0 10.0 %all-to-all-start.4 = ((f32[8,3,256]{2,1,0:T(4,128)}), f32[8,3,256]{2,1,0:T(4,128)S(1)}, u32[]{:S(2)}, u32[]{:S(2)}) async-start(f32[8,3,256]{2,1,0:T(4,128)} %get-tuple-element.20), calls=%async_computation.4 | async-start | bytes 65536 | tf_op jit(solution)/shard_map/all_to_all | solution.py:332
Sparse Core Ops, SparseCore 0:
  10.3 91.2 all-gather.5

commit v7 on v4

--- a/solution.py
+++ b/solution.py
@@ -56,6 +56,29 @@
     )(*fetched(*shards))
 
 
+def parted(near, first, copies):
+    ny, piece, width = near.shape
+    size = ny * piece
+    main = size - size // 16
+
+    def body(ref, rest, most, last):
+        for y in range(ny):
+            rest[y * piece : (y + 1) * piece, :] = ref[y, :, first:]
+            if (y + 1) * piece <= main:
+                most[y * piece : (y + 1) * piece, :] = ref[y, :, :first]
+        inside = main % piece
+        if inside:
+            most[main - inside :, :] = ref[main // piece, :inside, :first]
+        for k in range(copies):
+            last[k] = ref[ny - 1, piece - (size - main) :, :first]
+
+    return pl.pallas_call(
+        body,
+        out_shape=(sds((size, width - first), bf16), pltpu.VMEM((main, first), bf16), sds((copies, size - main, first), bf16)),
+        in_specs=[VMEM], out_specs=(VMEM,) * 3, compiler_params=SMALL, name="parted",
+    )(*held(near))
+
+
 def log_rows(logs):
     hi = logs.astype(bf16).astype(f32)
     mid = (logs - hi).astype(bf16).astype(f32)
@@ -64,12 +87,63 @@
     return jnp.where(row == 0, hi, jnp.where(row == 1, mid, jnp.where(row == 2, lo, 0.0))).astype(bf16)
 
 
-def local_states(normed, first, taps, step, left, total, copies):
-    ext, _ = normed.shape
-    rows, ch = step.shape
-
-    def body(nref, wref, tref, sref, lref, logs, send, xs, w16, buf):
-        buf[...] = dot(nref[...], wref[...], 1, 0).astype(bf16).astype(f32)
+def steps_of(own, step_proj, extra, bias, rate_log, index, p):
+    rows, _ = own.shape
+    heads = extra.shape[0]
+    ch = heads * p
+    every = step_proj.shape[1]
+
+    def body(at, bref, rref, nref, wref, eref, step, left, cum, cum_t, total):
+        raw = dot(wref[...], nref[...], 0, 1)
+        which = lax.broadcasted_iota(jnp.int32, (every, rows), 0)
+        size, logs = [], []
+        for h in range(heads):
+            x = jnp.sum(jnp.where(which == at[0] * heads + h, raw, 0.0), axis=0, keepdims=True) + bref[h]
+            size.append(jnp.maximum(x, 0.0) + jnp.log1p(jnp.exp(-jnp.abs(x))))
+            logs.append(-jnp.exp(jnp.full((1, rows), rref[h], f32)) * size[h] + eref[h : h + 1, :])
+        none = [jnp.zeros((8 - heads, rows), f32)]
+        upto = lax.broadcasted_iota(jnp.int32, (rows, rows), 0) <= lax.broadcasted_iota(jnp.int32, (rows, rows), 1)
+        run = dot(jnp.concatenate(logs + none, 0), jnp.where(upto, 1.0, 0.0), 1, 0, HIGHEST)
+        lane = lax.broadcasted_iota(jnp.int32, (rows, ch), 1) // p
+
+        def wide(cols):
+            out = jnp.broadcast_to(cols[:, 0:1], (rows, ch))
+            for h in range(1, heads):
+                out = jnp.where(lane == h, cols[:, h : h + 1], out)
+            return out
+
+        cum_t[...] = run[:heads]
+        cum[...] = wide(jnp.transpose(run))
+        left[...] = wide(jnp.transpose(jnp.exp(run[:, rows - 1 :] - run)))
+        step[...] = wide(jnp.transpose(jnp.concatenate(size + none, 0)))
+        place = lax.broadcasted_iota(jnp.int32, (1, STATE), 1)
+        ends = jnp.zeros((1, STATE), f32)
+        for h in range(heads):
+            ends = jnp.where(place == h, run[h : h + 1, rows - 1 :], ends)
+        total[...] = ends
+
+    wide = pltpu.VMEM((rows, ch), f32)
+    return pl.pallas_call(
+        body,
+        out_shape=(wide, wide, wide, pltpu.VMEM((heads, rows), f32), pltpu.VMEM((1, STATE), f32)),
+        in_specs=[SMEM, SMEM, SMEM, VMEM, VMEM, VMEM],
+        out_specs=(VMEM,) * 5,
+        compiler_params=SMALL, name="steps_of",
+    )(index, bias, rate_log, *held(own, step_proj, extra))
+
+
+def local_states(halo, own, most, last, taps, step, left, total, copies):
+    rows, d = own.shape
+    ch = step.shape[1]
+    nz, main, _ = most.shape
+    size = main + last.shape[1]
+
+    def body(href, nref, mref, rref, tref, sref, lref, logs, send, xs, w16, buf, wall):
+        for z in range(nz):
+            wall[z * size : z * size + main, :] = mref[z]
+            wall[z * size + main : (z + 1) * size, :] = rref[z]
+        buf[:HALO, :] = dot(href[...], wall[...], 1, 0).astype(bf16).astype(f32)
+        buf[HALO:, :] = dot(nref[...], wall[...], 1, 0).astype(bf16).astype(f32)
         at = HALO - SHORT + 1
         mix = sum(buf[at + i : at + i + rows, :] * tref[i : i + 1, :] for i in range(SHORT))
         act = jax.nn.silu(mix)
@@ -86,11 +160,11 @@
     return pl.pallas_call(
         body,
         out_shape=(sds((copies, ch + LOGS, STATE), bf16), pltpu.VMEM((rows, ch), bf16), pltpu.VMEM((rows, STATE), bf16)),
-        in_specs=[VMEM] * 6,
+        in_specs=[VMEM] * 8,
         out_specs=(VMEM,) * 3,
-        scratch_shapes=[pltpu.VMEM((ext, 2 * ch), f32)],
+        scratch_shapes=[pltpu.VMEM((HALO + rows, 2 * ch), f32), pltpu.VMEM((d, 2 * ch), bf16)],
         compiler_params=SMALL, name="local_states",
-    )(*held(normed, first, taps, step, left, total))
+    )(*held(halo, own, most, last, taps, step, left, total))
 
 
 def spread_heads(c, heads, p):
@@ -130,15 +204,18 @@
     )(index, *held(got))
 
 
-def rows_local(normed, rest, ftaps, ltaps, xs, w16, cum, cum_t):
-    ext, d = normed.shape
-    rows, ch = xs.shape
+def rows_local(halo, own, rest, ftaps, ltaps, xs, w16, cum, cum_t):
+    rows, d = own.shape
+    ch = xs.shape[1]
+    ext = HALO + rows
     heads = cum_t.shape[0]
     p = ch // heads
     part, n = 64, 8
     kc = d // n
 
-    def body(nref, wref, ftaps, ltaps, xs, w16, cum, cum_t, read16, zgate, mixed, inner, back, acc, glu, wall, sems):
+    def body(
+        hall, nall, wref, ftaps, ltaps, xs, w16, cum, cum_t, read16, zgate, mixed, inner, back, acc, glu, wall, href, nref, sems
+    ):
         def fetch(i):
             at = slice(i * kc, (i + 1) * kc)
             return pltpu.make_async_copy(wref.at[at, : 4 * ch], wall.at[at, :], sems.at[0, i])
@@ -147,15 +224,25 @@
             at = slice(i * kc, (i + 1) * kc)
             return pltpu.make_async_copy(wref.at[at, 4 * ch :], back.at[at, :], sems.at[1, i])
 
+        near = (
+            pltpu.make_async_copy(hall, href, sems.at[2, 0]),
+            pltpu.make_async_copy(nall, nref, sems.at[2, 1]),
+        )
+        for copy in near:
+            copy.start()
         for i in range(n):
             fetch(i).start()
         for i in range(n):
             fetch_back(i).start()
+        for copy in near:
+            copy.wait()
         for i in range(n):
             fetch(i).wait()
             at = slice(i * kc, (i + 1) * kc)
+            before = dot(href[:, at], wall[at, :], 1, 0)
             term = dot(nref[:, at], wall[at, :], 1, 0)
-            acc[...] = term if i == 0 else acc[...] + term
+            acc[:HALO, :] = before if i == 0 else acc[:HALO, :] + before
+            acc[HALO:, :] = term if i == 0 else acc[HALO:, :] + term
         glu[...] = acc[:, 2 * ch : 3 * ch].astype(bf16).astype(f32) * jax.nn.sigmoid(
             acc[:, 3 * ch :].astype(bf16).astype(f32)
         )
@@ -189,14 +276,14 @@
             pltpu.VMEM((rows, STATE), bf16), pltpu.VMEM((rows, ch), f32), pltpu.VMEM((rows, ch), f32),
             pltpu.VMEM((rows, ch), f32), pltpu.VMEM((d, 2 * ch), bf16),
         ),
-        in_specs=[VMEM, pl.BlockSpec(memory_space=pltpu.HBM), *[VMEM] * len(small)],
+        in_specs=[*[pl.BlockSpec(memory_space=pltpu.HBM)] * 3, *[VMEM] * len(small)],
         out_specs=(VMEM,) * 5,
         scratch_shapes=[
             pltpu.VMEM((ext, 4 * ch), f32), pltpu.VMEM((ext, ch), f32), pltpu.VMEM((d, 4 * ch), bf16),
-            pltpu.SemaphoreType.DMA((2, n)),
+            pltpu.VMEM(halo.shape, bf16), pltpu.VMEM(own.shape, bf16), pltpu.SemaphoreType.DMA((3, n)),
         ],
         compiler_params=SMALL, name="rows_local",
-    )(*held(normed), *fetched(rest), *held(*small))
+    )(*fetched(halo, own, rest), *held(*small))
 
 
 def rows_done(got, enter, before, init, index, read16, zgate, mixed, inner, cum, gain, copies):
@@ -223,12 +310,14 @@
         found = dot(jnp.where(pick, 1.0, 0.0), squares, 1, 1, HIGHEST)
         for j in range(copies):
             sums[j] = found[:3]
-        pre[:, :ch] = mix.astype(bf16)
-        pre[:, ch:] = (gated * gain[...]).astype(bf16)
-
-    return pl.pallas_call(
-        body,
-        out_shape=(sds((copies, 3, rows), f32), pltpu.VMEM((rows, 2 * ch), bf16)),
+        high = mix.astype(bf16)
+        pre[:, :ch] = high
+        pre[:, ch : 2 * ch] = (mix - high.astype(f32)).astype(bf16)
+        pre[:, 2 * ch :] = (gated * gain[...]).astype(bf16)
+
+    return pl.pallas_call(
+        body,
+        out_shape=(sds((copies, 3, rows), f32), pltpu.VMEM((rows, 3 * ch), bf16)),
         in_specs=[SMEM, *[VMEM] * 10],
         out_specs=(VMEM, VMEM),
         compiler_params=SMALL, name="rows_done",
@@ -257,9 +346,10 @@
             for j in range(nt):
                 src = tp if j == 0 else 1 - tp
                 a = bref[pl.ds(pl.multiple_of(src * rows + at_row, piece), piece), :].astype(f32)
-                conv = jax.nn.silu((a[:, :ch] - mean) * rstd * gref[pl.ds(src, 1), :])
+                mix = a[:, :ch] + a[:, ch : 2 * ch]
+                conv = jax.nn.silu((mix - mean) * rstd * gref[pl.ds(src, 1), :])
                 act[here, 2 * j * ch : (2 * j + 1) * ch] = conv.astype(bf16)
-                act[here, (2 * j + 1) * ch : (2 * j + 2) * ch] = (a[:, ch:] * scale).astype(bf16)
+                act[here, (2 * j + 1) * ch : (2 * j + 2) * ch] = (a[:, 2 * ch :] * scale).astype(bf16)
         term = dot(act[:, : 2 * ch], wa[...], 1, 1) + dot(act[:, 2 * ch :], wb[...], 1, 1)
         out[...] = term.astype(bf16).reshape(nf, piece, d)
 
@@ -285,32 +375,32 @@
     nf, nt = lax.axis_size("fs"), lax.axis_size("tp")
     iz, iy, tp = (lax.axis_index(a).astype(jnp.int32).reshape(1) for a in ("sp_0", "sp_1", "tp"))
     ny = lax.axis_size("sp_1")
-    rest = lay_out((state_read, mixer_gate, conv_value, conv_gate, conv_output, state_output), ny)
-    rest = lax.all_to_all(rest, "sp_1", 0, 0, tiled=True).reshape(-1, 6 * ch)
+    near = lay_out(
+        (state_input, write_projection, state_read, mixer_gate, conv_value, conv_gate, conv_output, state_output), ny
+    )
+    near = lax.all_to_all(near, "sp_1", 0, 0, tiled=True)
+    rest, most, last = parted(near, 2 * ch, lax.axis_size("sp_0"))
     rest = lax.all_gather(rest, "sp_0", axis=0, tiled=True)
-    first = lay_out((state_input, write_projection), lax.axis_size(SP))
-    first = lax.all_to_all(first, SP, 0, 0, tiled=True).reshape(-1, 2 * ch)
+    last = lax.all_to_all(last, "sp_0", 0, 0, tiled=True)
+    most = lax.all_gather(most, "sp_0", axis=0)
     n = lax.axis_size(SP)
     halo = lax.ppermute(tokens[rows - HALO :], SP, [(i, i + 1) for i in range(n - 1)])
-    v = jnp.concatenate([halo, tokens], 0).astype(f32)
-    normed = (v * lax.rsqrt(jnp.mean(v * v, axis=1, keepdims=True) + EPS) * norm_gain).astype(bf16)
-    step_all = jnp.dot(normed[HALO:], step_proj, preferred_element_type=f32)
-    me = lax.axis_index("fs") * nt + lax.axis_index("tp")
-    step = jax.nn.softplus(lax.dynamic_slice_in_dim(step_all, me * heads, heads, 1) + step_bias)
-    log_step = (-jnp.exp(decay_log) * step + decay_extra.T).T
-    cum_t = jnp.cumsum(log_step, axis=1)
-    total = cum_t[:, -1]
-    cum = jnp.repeat(cum_t.T, p, axis=1)
-    step = jnp.repeat(step, p, axis=1)
-    left = jnp.repeat(jnp.exp(total[:, None] - cum_t).T, p, axis=1)
-    total = jnp.pad(total[None], ((0, 0), (0, STATE - heads)))
+
+    def unit(x):
+        v = x.astype(f32)
+        return (v * lax.rsqrt(jnp.mean(v * v, axis=1, keepdims=True) + EPS) * norm_gain).astype(bf16)
+
+    own = unit(tokens)
+    halo = unit(halo)
+    me = lax.axis_index("fs").astype(jnp.int32).reshape(1) * nt + tp
+    step, left, cum, cum_t, total = steps_of(own, step_proj, decay_extra, step_bias, decay_log, me, p)
     gains = lax.all_gather(conv_gain, "tp")
     taps = jnp.concatenate([input_taps, write_taps], 1)
-    send, xs, w16 = local_states(normed, first, taps, step, left, total, ny)
+    send, xs, w16 = local_states(halo, own, most, last, taps, step, left, total, ny)
     got = lax.all_to_all(send, "sp_1", 0, 0, tiled=True)
     enter, before, send = line_states(got, iy, heads, p, lax.axis_size("sp_0"))
     got = lax.all_to_all(send, "sp_0", 0, 0, tiled=True)
-    read16, zgate, mixed, inner, back = rows_local(normed, rest, fetch_taps, long_taps, xs, w16, cum, cum_t)
+    read16, zgate, mixed, inner, back = rows_local(halo, own, rest, fetch_taps, long_taps, xs, w16, cum, cum_t)
     back_other = lax.ppermute(back, "tp", [(i, nt - 1 - i) for i in range(nt)])
     sums, pre = rows_done(
         got, enter, before, initial_state, iz, read16, zgate, mixed, inner, cum, state_gain[None], nf * nt

time: 180 us -> 151 us (0.84)
  waiting for transfers between devices: 72.4 us -> 12.2 us
  blocking collectives: 34.4 us -> 70.8 us
  local copies, waits for them, and re-layouts: 8.47 us -> 0.36 us
  Pallas kernels: 9.87 us -> 12 us
    all_gather x0 -> x1, blocking collectives: none -> 28.8 us  [per_device(): most = lax.all_gather(most, 'sp_0', axis=0)]
    all_to_all x1, waiting for transfers between devices: 22.8 us -> 0.01 us  [per_device(): last = lax.all_to_all(last, 'sp_0', 0, 0, tiled=True)]
    all_gather x1, waiting for transfers between devices: 25 us -> 6.71 us  [per_device(): rest = lax.all_gather(rest, 'sp_0', axis=0, tiled=True)]
    all_to_all x1, waiting for transfers between devices: 12.7 us -> 0.01 us  [per_device(): got = lax.all_to_all(send, 'sp_1', 0, 0, tiled=True)]
    unnamed x45 -> x31, local copies, waits for them, and re-layouts: 6.89 us -> 0.35 us
    all_to_all x1, waiting for transfers between devices: 9.09 us -> 2.77 us  [per_device(): got = lax.all_to_all(send, 'sp_0', 0, 0, tiled=True)]
    all_to_all x1, starting transfers between devices: 6.13 us -> 11 us  [per_device(): sums = lax.all_to_all(sums, FT, 0, 0, tiled=True)]
    all_gather x1, blocking collectives: 2.21 us -> 6.73 us  [per_device(): gains = lax.all_gather(conv_gain, 'tp')]
  transfers between devices with their start and end apart: 7 -> 7, of which waited for: 5 -> 3; matrix products, arithmetic and copies ran while one was open for 2% -> 2% of each run, Pallas kernels for 3% -> 6%
where the time goes in v7:
time: 151 us; the launch traced here: 150 us
  blocking collectives  70.8 us (47%)
  starting transfers between devices  38.2 us (25%)
  between operations  13.7 us (9%)
  waiting for transfers between devices  12.2 us (8%)
  Pallas kernels  12 us (8%)
  other arithmetic  2.83 us (2%)
    all_gather x1, blocking collectives, per_device(): most = lax.all_gather(most, 'sp_0', axis=0)  28.8 us
    all_to_all x1, blocking collectives, per_device(): near = lax.all_to_all(near, 'sp_1', 0, 0, tiled=True)  22.3 us
    all_to_all x1, starting transfers between devices, per_device(): last = lax.all_to_all(last, 'sp_0', 0, 0, tiled=True)  14.2 us
    all_to_all x1, starting transfers between devices, per_device(): sums = lax.all_to_all(sums, FT, 0, 0, tiled=True)  11 us
    all_to_all x1, blocking collectives, per_device(): pieces = lax.all_to_all(out, 'fs', 0, 0, tiled=True)  10.9 us
    all_gather x1, blocking collectives, per_device(): gains = lax.all_gather(conv_gain, 'tp')  6.73 us
    all_gather x1, waiting for transfers between devices, per_device(): rest = lax.all_gather(rest, 'sp_0', axis=0, tiled=True)  6.71 us
    all_to_all x1, starting transfers between devices, per_device(): got = lax.all_to_all(send, 'sp_0', 0, 0, tiled=True)  4.78 us
  transfers between devices with their start and end apart: 7, of which 3 were waited for; matrix products, arithmetic and copies ran while one was open for 2% of the time, Pallas kernels for 6%

profile of v7, /device:TPU:1, one launch (start us, length us, event | category | flops | bytes accessed | tf_op | source)
XLA Modules:
  0.0 150.1 jit_solution(1983027914015583702)
XLA Ops:
  6.5 0.0 all-gather.5.cloned.1.call-start
  6.5 1.0 shard_map.199
  7.5 22.3 %all_to_all.30.ref = bf16[8,32,1024]{2,1,0:T(8,128)(2,1)S(1)} all-to-all(bf16[8,32,1024]{2,1,0:T(8,128)(2,1)S(1)} %shard_map.199), channel_id=1, replica_groups=mesh['sp_0'=8,'sp_1'=8,'fs'=4,'tp'=2] {'sp_1'}, dimensions={0} | all-to-all | bytes 1048576 | tf_op jit(solution)/shard_map/all_to_all | solution.py:381
  29.9 0.8 parted.1
  30.7 0.0 all-gather.5.cloned.1.call-update
  30.7 0.0 copy-done.9
  30.7 0.0 copy-start.4
  30.7 0.0 copy-start.6
  30.8 0.0 copy-start.7
  30.8 2.1 %collective-permute-start = (bf16[32,2048]{1,0:T(8,128)(2,1)S(1)}, bf16[32,2048]{1,0:T(8,128)(2,1)S(1)}, u32[]{:S(2)}, u32[]{:S(2)}) collective-permute-start(bf16[32,2048]{1,0:T(8,128)(2,1)S(1)} %slice.3), channel_id=1, source_target_pairs={{0,8},{8,16},{16,24},{24,32},{32,40},{40,48},{48,56},{56,64},{64,7... | collective-permute-start | bytes 393224 | tf_op jit(solution)/shard_map/ppermute | solution.py:387
  32.9 0.3 fusion
  33.2 0.0 copy-done.11
  33.2 0.0 copy-start.12
  33.2 0.0 copy-start.13
  33.2 1.5 %fusion.2.nref.nall = bf16[256,2048]{1,0:T(8,128)(2,1)S(1)} fusion(bf16[256,2048]{1,0:T(8,128)(2,1)} %param.21, f32[2048]{0:T(1024)S(1)} %copy-done.11, f32[256]{0:T(256)S(1)} %add_rsqrt_fusion), kind=kLoop, calls=%fused_computation.4 | loop fusion | flops 2097152 | bytes 2106368 | tf_op jit(solution)/shard_map/convert_element_type | solution.py:391
  34.8 0.0 copy-start
  34.8 0.0 copy-done.10
  34.8 0.3 copy.24.wref
  35.1 1.7 %steps_of.1 = (f32[256,128]{1,0:T(8,128)S(1)}, f32[256,128]{1,0:T(8,128)S(1)}, f32[256,128]{1,0:T(8,128)S(1)}, f32[2,256]{1,0:T(2,128)S(1)}, f32[1,128]{1,0:T(1,128)S(1)}) custom-call(s32[1]{0:T(128)S(6)} %add.29.at, f32[2]{0:T(128)S(1)} %copy-done.6, f32[2]{0:T(128)S(1)} %copy-done.7, bf16[256,2048]{1,0:T(8,128)(2,1)S(1)} %fusion.2.nref.nall, ...), custom_call_target="tpu_custom_call" | custom-call | tf_op jit(solution)/shard_map/steps_of/pallas_call | solution.py:126
  36.8 0.0 collective-permute-done
  36.9 0.1 fusion.3
  37.0 0.1 fusion.5.href.hall
  37.1 0.0 copy-start.1
  37.1 14.2 %all-to-all-start.1 = ((bf16[8,16,256]{2,1,0:T(8,128)(2,1)}), bf16[8,16,256]{2,1,0:T(8,128)(2,1)S(1)}, u32[]{:S(2)}, u32[]{:S(2)}) async-start(bf16[8,16,256]{2,1,0:T(8,128)(2,1)} %get-tuple-element.27), calls=%async_computation.1 | async-start | bytes 131072 | tf_op jit(solution)/shard_map/all_to_all | solution.py:384
  51.3 0.0 copy-start.5
  51.3 28.8 %all-gather = bf16[1920,256]{1,0:T(8,128)(2,1)S(1)} all-gather(bf16[240,256]{1,0:T(8,128)(2,1)S(1)} %get-tuple-element.26), channel_id=2, replica_groups=mesh['sp_0'=8,'sp_1'=8,'fs'=4,'tp'=2] {'sp_0'}, dimensions={0}, use_global_device_ids=true | all-gather | bytes 1105920 | tf_op jit(solution)/shard_map/all_gather | solution.py:385
  80.1 0.0 all-to-all-done.1.rref
  80.1 1.7 %local_states.1 = (bf16[8,136,128]{2,1,0:T(8,128)(2,1)}, bf16[256,128]{1,0:T(8,128)(2,1)S(1)}, bf16[256,128]{1,0:T(8,128)(2,1)S(1)}) custom-call(bf16[32,2048]{1,0:T(8,128)(2,1)S(1)} %fusion.5.href.hall, bf16[256,2048]{1,0:T(8,128)(2,1)S(1)} %fusion.2.nref.nall, bf16[8,240,256]{2,1,0:T(8,128)(2,1)S(1)} %bitcast.8, ...), custom_call_target="tpu_custom_call" | custom-call | tf_op jit(solution)/shard_map/local_states/pallas_call | solution.py:160
  81.8 3.4 %all-to-all-start.2 = ((bf16[8,136,128]{2,1,0:T(8,128)(2,1)}), bf16[8,136,128]{2,1,0:T(8,128)(2,1)S(1)}, u32[]{:S(2)}, u32[]{:S(2)}) async-start(bf16[8,136,128]{2,1,0:T(8,128)(2,1)} %get-tuple-element.31), calls=%async_computation.2 | async-start | bytes 557056 | tf_op jit(solution)/shard_map/all_to_all | solution.py:400
  85.3 6.7 %all-gather.5.cloned.1.call-done.wref = bf16[2048,768]{1,0:T(8,128)(2,1)} async-done(((bf16[256,768]{1,0:T(8,128)(2,1)}), bf16[2048,768]{1,0:T(8,128)(2,1)}) %all-gather.5.cloned.1.call-update) | async-done | bytes 3145744 | tf_op jit(solution)/shard_map/all_gather | solution.py:383
  92.0 0.0 copy-done.3
  92.0 0.0 copy-start.8
  92.0 3.6 %rows_local.1 = (bf16[256,128]{1,0:T(8,128)(2,1)S(1)}, f32[256,128]{1,0:T(8,128)S(1)}, f32[256,128]{1,0:T(8,128)S(1)}, f32[256,128]{1,0:T(8,128)S(1)}, bf16[2048,256]{1,0:T(8,128)(2,1)S(1)}) custom-call(bf16[32,2048]{1,0:T(8,128)(2,1)} %copy-done.1, bf16[256,2048]{1,0:T(8,128)(2,1)} %copy-done, bf16[2048,768]{1,0:T(8,128)(2,1)} %all-gather.5.cloned.1.call-done.wref, ...), custom_call_target="tpu_custom_call" | custom-call | tf_op jit(solution)/shard_map/rows_local/pallas_call | solution.py:273
  95.6 2.8 %collective-permute-start.1 = (bf16[2048,256]{1,0:T(8,128)(2,1)S(1)}, bf16[2048,256]{1,0:T(8,128)(2,1)S(1)}, u32[]{:S(2)}, u32[]{:S(2)}) collective-permute-start(bf16[2048,256]{1,0:T(8,128)(2,1)S(1)} %get-tuple-element.46.wa), channel_id=1, source_target_pairs={{0,1},{1,0},{2,3},{3,2},{4,5},{5,4},{6,7},{7,6},{8,9},{9,8},{10,11... | collective-permute-start | bytes 3145736 | tf_op jit(solution)/shard_map/ppermute | solution.py:404
  98.3 0.0 all-to-all-done.2.ref
  98.4 0.9 line_states.1
  99.2 4.8 %all-to-all-start.3 = ((bf16[8,136,128]{2,1,0:T(8,128)(2,1)}), bf16[8,136,128]{2,1,0:T(8,128)(2,1)S(1)}, u32[]{:S(2)}, u32[]{:S(2)}) async-start(bf16[8,136,128]{2,1,0:T(8,128)(2,1)} %get-tuple-element.32), calls=%async_computation.3 | async-start | bytes 557056 | tf_op jit(solution)/shard_map/all_to_all | solution.py:402
  104.0 6.7 %all-gather.2 = f32[2,1,128]{2,1,0:T(1,128)S(1)} all-gather(f32[1,1,128]{2,1,0:T(1,128)S(1)} %bitcast.11), channel_id=3, replica_groups=mesh['sp_0'=8,'sp_1'=8,'fs'=4,'tp'=2] {'tp'}, dimensions={0}, use_global_device_ids=true | all-gather | bytes 1536 | tf_op jit(solution)/shard_map/all_gather | solution.py:397
  110.8 2.8 %all-to-all-done.3.got = bf16[8,136,128]{2,1,0:T(8,128)(2,1)S(1)} async-done(((bf16[8,136,128]{2,1,0:T(8,128)(2,1)}), bf16[8,136,128]{2,1,0:T(8,128)(2,1)S(1)}, u32[]{:S(2)}, u32[]{:S(2)}) %all-to-all-start.3) | async-done | bytes 278560 | tf_op jit(solution)/shard_map/all_to_all | solution.py:402
  113.5 0.0 copy-done.8
  113.5 1.3 rows_done.1
  114.8 11.0 %all-to-all-start.4 = ((f32[8,3,256]{2,1,0:T(4,128)}), f32[8,3,256]{2,1,0:T(4,128)S(1)}, u32[]{:S(2)}, u32[]{:S(2)}) async-start(f32[8,3,256]{2,1,0:T(4,128)} %get-tuple-element.44), calls=%async_computation.4 | async-start | bytes 65536 | tf_op jit(solution)/shard_map/all_to_all | solution.py:408
  125.8 2.1 %all_gather.21.bref = bf16[512,384]{1,0:T(8,128)(2,1)S(1)} all-gather(bf16[256,384]{1,0:T(8,128)(2,1)S(1)} %get-tuple-element.45), channel_id=1, replica_groups=mesh['sp_0'=8,'sp_1'=8,'fs'=4,'tp'=2] {'tp'}, dimensions={0}, use_global_device_ids=true | all-gather | bytes 589824 | tf_op jit(solution)/shard_map/all_gather | solution.py:409
  127.9 2.6 %all-to-all-done.4.sref = f32[8,3,256]{2,1,0:T(4,128)S(1)} async-done(((f32[8,3,256]{2,1,0:T(4,128)}), f32[8,3,256]{2,1,0:T(4,128)S(1)}, u32[]{:S(2)}, u32[]{:S(2)}) %all-to-all-start.4) | async-done | bytes 24608 | tf_op jit(solution)/shard_map/all_to_all | solution.py:408
  130.5 0.0 collective-permute-done.1.wb
  130.5 1.1 output_rows.1
  131.6 10.9 %all_to_all.31 = bf16[4,32,2048]{2,1,0:T(8,128)(2,1)S(1)} all-to-all(bf16[4,32,2048]{2,1,0:T(8,128)(2,1)S(1)} %output_rows.1), channel_id=1, replica_groups=mesh['sp_0'=8,'sp_1'=8,'fs'=4,'tp'=2] {'fs'}, dimensions={0} | all-to-all | bytes 1048576 | tf_op jit(solution)/shard_map/all_to_all | solution.py:411
  142.5 0.7 reduce_sum.32
  (20 shorter events, 0.1 us)
Async XLA Ops:
  6.5 24.2 %copy-start.9 = (bf16[256,2048]{1,0:T(8,128)(2,1)S(1)}, bf16[256,2048]{1,0:T(8,128)(2,1)}, u32[]{:S(2)}) copy-start(bf16[256,2048]{1,0:T(8,128)(2,1)} %param.21) | copy-start | bytes 3145732
  6.5 26.6 %copy-start.11 = (f32[2048]{0:T(1024)S(1)}, f32[2048]{0:T(1024)}, u32[]{:S(2)}) copy-start(f32[2048]{0:T(1024)} %param.22) | copy-start | bytes 24580
  6.5 85.4 %all-gather.5.cloned.1.call-start = ((), (), s32[]{:S(2)}) async-start(), calls=%async_computation.6 | async-start | bytes 3538944 | tf_op jit(solution)/shard_map/all_gather | solution.py:383
  29.9 4.9 %copy-start.10 = (bf16[2048,16]{0,1:T(8,128)(2,1)S(1)}, bf16[2048,16]{0,1:T(8,128)(2,1)}, u32[]{:S(2)}) copy-start(bf16[2048,16]{0,1:T(8,128)(2,1)} %param.29) | copy-start | bytes 196612
  30.7 4.3 %copy-start.4 = (f32[2,256]{1,0:T(2,128)S(1)}, f32[2,256]{1,0:T(2,128)}, u32[]{:S(2)}) copy-start(f32[2,256]{1,0:T(2,128)} %eref.1) | copy-start | bytes 6148
  30.7 4.3 %copy-start.6 = (f32[2]{0:T(128)S(1)}, f32[2]{0:T(128)}, u32[]{:S(2)}) copy-start(f32[2]{0:T(128)} %bref.1) | copy-start | bytes 28
  30.8 4.3 %copy-start.7 = (f32[2]{0:T(128)S(1)}, f32[2]{0:T(128)}, u32[]{:S(2)}) copy-start(f32[2]{0:T(128)} %rref.1) | copy-start | bytes 28
  30.8 6.1 %collective-permute-start = (bf16[32,2048]{1,0:T(8,128)(2,1)S(1)}, bf16[32,2048]{1,0:T(8,128)(2,1)S(1)}, u32[]{:S(2)}, u32[]{:S(2)}) collective-permute-start(bf16[32,2048]{1,0:T(8,128)(2,1)S(1)} %slice.3), channel_id=1, source_target_pairs={{0,8},{8,16},{16,24},{24,32},{32,40},{40,48},{48,56},{56,64},{64,7... | collective-permute-start | bytes 393224 | tf_op jit(solution)/shard_map/ppermute | solution.py:387
  33.2 3.6 %copy-start.12 = (f32[4,128]{1,0:T(4,128)S(1)}, f32[4,128]{1,0:T(4,128)}, u32[]{:S(2)}) copy-start(f32[4,128]{1,0:T(4,128)} %param.34) | copy-start | bytes 6148
  33.2 3.6 %copy-start.13 = (f32[4,128]{1,0:T(4,128)S(1)}, f32[4,128]{1,0:T(4,128)}, u32[]{:S(2)}) copy-start(f32[4,128]{1,0:T(4,128)} %param.33) | copy-start | bytes 6148
  34.8 47.1 %copy-start = (bf16[256,2048]{1,0:T(8,128)(2,1)}, bf16[256,2048]{1,0:T(8,128)(2,1)S(1)}, u32[]{:S(2)}) copy-start(bf16[256,2048]{1,0:T(8,128)(2,1)S(1)} %fusion.2.nref.nall) | copy-start | bytes 3145732
  37.1 44.7 %copy-start.1 = (bf16[32,2048]{1,0:T(8,128)(2,1)}, bf16[32,2048]{1,0:T(8,128)(2,1)S(1)}, u32[]{:S(2)}) copy-start(bf16[32,2048]{1,0:T(8,128)(2,1)S(1)} %fusion.5.href.hall) | copy-start | bytes 393220
  37.1 43.0 %all-to-all-start.1 = ((bf16[8,16,256]{2,1,0:T(8,128)(2,1)}), bf16[8,16,256]{2,1,0:T(8,128)(2,1)S(1)}, u32[]{:S(2)}, u32[]{:S(2)}) async-start(bf16[8,16,256]{2,1,0:T(8,128)(2,1)} %get-tuple-element.27), calls=%async_computation.1 | async-start | bytes 131072 | tf_op jit(solution)/shard_map/all_to_all | solution.py:384
  51.3 40.6 %copy-start.3 = (f32[31,128]{1,0:T(8,128)S(1)}, f32[31,128]{1,0:T(8,128)}, u32[]{:S(2)}) copy-start(f32[31,128]{1,0:T(8,128)} %ltaps.1) | copy-start | bytes 47620
  51.3 40.6 %copy-start.5 = (f32[4,128]{1,0:T(4,128)S(1)}, f32[4,128]{1,0:T(4,128)}, u32[]{:S(2)}) copy-start(f32[4,128]{1,0:T(4,128)} %ftaps.1) | copy-start | bytes 6148
  81.8 16.5 %all-to-all-start.2 = ((bf16[8,136,128]{2,1,0:T(8,128)(2,1)}), bf16[8,136,128]{2,1,0:T(8,128)(2,1)S(1)}, u32[]{:S(2)}, u32[]{:S(2)}) async-start(bf16[8,136,128]{2,1,0:T(8,128)(2,1)} %get-tuple-element.31), calls=%async_computation.2 | async-start | bytes 557056 | tf_op jit(solution)/shard_map/all_to_all | solution.py:400
  92.0 12.1 %copy-start.14 = (f32[128]{0:T(128)S(1)}, f32[128]{0:T(128)}, u32[]{:S(2)}) copy-start(f32[128]{0:T(128)} %param.37) | copy-start | bytes 1540
  92.0 21.6 %copy-start.2 = (f32[2,64,128]{2,1,0:T(8,128)S(1)}, f32[2,64,128]{2,1,0:T(8,128)}, u32[]{:S(2)}) copy-start(f32[2,64,128]{2,1,0:T(8,128)} %init.1) | copy-start | bytes 196612
  92.0 21.6 %copy-start.8 = (f32[128]{0:T(128)S(1)}, f32[128]{0:T(128)}, u32[]{:S(2)}) copy-start(f32[128]{0:T(128)} %param.38) | copy-start | bytes 1540
  95.6 34.9 %collective-permute-start.1 = (bf16[2048,256]{1,0:T(8,128)(2,1)S(1)}, bf16[2048,256]{1,0:T(8,128)(2,1)S(1)}, u32[]{:S(2)}, u32[]{:S(2)}) collective-permute-start(bf16[2048,256]{1,0:T(8,128)(2,1)S(1)} %get-tuple-element.46.wa), channel_id=1, source_target_pairs={{0,1},{1,0},{2,3},{3,2},{4,5},{5,4},{6,7},{7,6},{8,9},{9,8},{10,11... | collective-permute-start | bytes 3145736 | tf_op jit(solution)/shard_map/ppermute | solution.py:404
  99.2 14.3 %all-to-all-start.3 = ((bf16[8,136,128]{2,1,0:T(8,128)(2,1)}), bf16[8,136,128]{2,1,0:T(8,128)(2,1)S(1)}, u32[]{:S(2)}, u32[]{:S(2)}) async-start(bf16[8,136,128]{2,1,0:T(8,128)(2,1)} %get-tuple-element.32), calls=%async_computation.3 | async-start | bytes 557056 | tf_op jit(solution)/shard_map/all_to_all | solution.py:402
  114.8 15.7 %all-to-all-start.4 = ((f32[8,3,256]{2,1,0:T(4,128)}), f32[8,3,256]{2,1,0:T(4,128)S(1)}, u32[]{:S(2)}, u32[]{:S(2)}) async-start(f32[8,3,256]{2,1,0:T(4,128)} %get-tuple-element.44), calls=%async_computation.4 | async-start | bytes 65536 | tf_op jit(solution)/shard_map/all_to_all | solution.py:408
Sparse Core Ops, SparseCore 0:
  30.8 61.0 all-gather.4

commit v8 on v4

--- a/solution.py
+++ b/solution.py
@@ -223,12 +223,14 @@
         found = dot(jnp.where(pick, 1.0, 0.0), squares, 1, 1, HIGHEST)
         for j in range(copies):
             sums[j] = found[:3]
-        pre[:, :ch] = mix.astype(bf16)
-        pre[:, ch:] = (gated * gain[...]).astype(bf16)
-
-    return pl.pallas_call(
-        body,
-        out_shape=(sds((copies, 3, rows), f32), pltpu.VMEM((rows, 2 * ch), bf16)),
+        high = mix.astype(bf16)
+        pre[:, :ch] = high
+        pre[:, ch : 2 * ch] = (mix - high.astype(f32)).astype(bf16)
+        pre[:, 2 * ch :] = (gated * gain[...]).astype(bf16)
+
+    return pl.pallas_call(
+        body,
+        out_shape=(sds((copies, 3, rows), f32), pltpu.VMEM((rows, 3 * ch), bf16)),
         in_specs=[SMEM, *[VMEM] * 10],
         out_specs=(VMEM, VMEM),
         compiler_params=SMALL, name="rows_done",
@@ -257,9 +259,10 @@
             for j in range(nt):
                 src = tp if j == 0 else 1 - tp
                 a = bref[pl.ds(pl.multiple_of(src * rows + at_row, piece), piece), :].astype(f32)
-                conv = jax.nn.silu((a[:, :ch] - mean) * rstd * gref[pl.ds(src, 1), :])
+                mix = a[:, :ch] + a[:, ch : 2 * ch]
+                conv = jax.nn.silu((mix - mean) * rstd * gref[pl.ds(src, 1), :])
                 act[here, 2 * j * ch : (2 * j + 1) * ch] = conv.astype(bf16)
-                act[here, (2 * j + 1) * ch : (2 * j + 2) * ch] = (a[:, ch:] * scale).astype(bf16)
+                act[here, (2 * j + 1) * ch : (2 * j + 2) * ch] = (a[:, 2 * ch :] * scale).astype(bf16)
         term = dot(act[:, : 2 * ch], wa[...], 1, 1) + dot(act[:, 2 * ch :], wb[...], 1, 1)
         out[...] = term.astype(bf16).reshape(nf, piece, d)
 

time: 180 us -> 156 us (0.87)
  waiting for transfers between devices: 72.4 us -> 51.4 us
  local copies, waits for them, and re-layouts: 8.47 us -> 1.67 us
  starting transfers between devices: 37.4 us -> 39.5 us
  Pallas kernels: 9.87 us -> 11.8 us
    all_to_all x1, waiting for transfers between devices: 12.7 us -> 0.01 us  [per_device(): got = lax.all_to_all(send, 'sp_1', 0, 0, tiled=True)]
    all_gather x1, waiting for transfers between devices: 25 us -> 14.9 us  [per_device(): rest = lax.all_gather(rest, 'sp_0', axis=0, tiled=True)]
    unnamed x45 -> x27, local copies, waits for them, and re-layouts: 6.89 us -> 0.09 us
    all_to_all x1, starting transfers between devices: 6.46 us -> 9.98 us  [per_device(): got = lax.all_to_all(send, 'sp_1', 0, 0, tiled=True)]
    all_to_all x1, waiting for transfers between devices: 9.09 us -> 10.9 us  [per_device(): got = lax.all_to_all(send, 'sp_0', 0, 0, tiled=True)]
  transfers between devices with their start and end apart: 7 -> 7, of which waited for: 5 -> 4; matrix products, arithmetic and copies ran while one was open for 2% -> 2% of each run, Pallas kernels for 3% -> 6%
where the time goes in v8:
time: 156 us; the launch traced here: 155 us
  waiting for transfers between devices  51.4 us (33%)
  starting transfers between devices  39.5 us (25%)
  blocking collectives  34.1 us (22%)
  between operations  13.7 us (9%)
  Pallas kernels  11.8 us (8%)
  other arithmetic  2.46 us (2%)
  local copies, waits for them, and re-layouts  1.67 us (1%)
    all_to_all x1, waiting for transfers between devices, per_device(): first = lax.all_to_all(first, SP, 0, 0, tiled=True).reshape(-1, 2 * ch)  22.9 us
    all_to_all x1, blocking collectives, per_device(): rest = lax.all_to_all(rest, 'sp_1', 0, 0, tiled=True).reshape(-1, 6 * ch)  19.3 us
    all_to_all x1, starting transfers between devices, per_device(): first = lax.all_to_all(first, SP, 0, 0, tiled=True).reshape(-1, 2 * ch)  16.6 us
    all_gather x1, waiting for transfers between devices, per_device(): rest = lax.all_gather(rest, 'sp_0', axis=0, tiled=True)  14.9 us
    all_to_all x1, blocking collectives, per_device(): pieces = lax.all_to_all(out, 'fs', 0, 0, tiled=True)  10.9 us
    all_to_all x1, waiting for transfers between devices, per_device(): got = lax.all_to_all(send, 'sp_0', 0, 0, tiled=True)  10.9 us
    all_to_all x1, starting transfers between devices, per_device(): got = lax.all_to_all(send, 'sp_1', 0, 0, tiled=True)  9.98 us
    all_to_all x1, starting transfers between devices, per_device(): sums = lax.all_to_all(sums, FT, 0, 0, tiled=True)  4.71 us
  transfers between devices with their start and end apart: 7, of which 4 were waited for; matrix products, arithmetic and copies ran while one was open for 2% of the time, Pallas kernels for 6%

profile of v8, /device:TPU:1, one launch (start us, length us, event | category | flops | bytes accessed | tf_op | source)
XLA Modules:
  0.0 155.1 jit_solution(15566261916873977197)
XLA Ops:
  6.5 0.9 shard_map.200
  7.4 0.0 copy-start.11
  7.4 0.0 copy-start.8
  7.4 0.0 copy-start.9
  7.4 0.0 copy-start.5
  7.5 19.3 %all_to_all.30 = bf16[8,32,768]{2,1,0:T(8,128)(2,1)} all-to-all(bf16[8,32,768]{2,1,0:T(8,128)(2,1)S(1)} %shard_map.200), channel_id=1, replica_groups=mesh['sp_0'=8,'sp_1'=8,'fs'=4,'tp'=2] {'sp_1'}, dimensions={0} | all-to-all | bytes 786432 | tf_op jit(solution)/shard_map/all_to_all | solution.py:292
  26.7 0.0 all-gather.4.cloned.1.call-update
  26.8 0.0 copy-start.6
  26.8 0.9 slice.15
  27.7 1.6 %collective-permute-start = (bf16[32,2048]{1,0:T(8,128)(2,1)S(1)}, bf16[32,2048]{1,0:T(8,128)(2,1)S(1)}, u32[]{:S(2)}, u32[]{:S(2)}) collective-permute-start(bf16[32,2048]{1,0:T(8,128)(2,1)S(1)} %slice.15), channel_id=1, source_target_pairs={{0,8},{8,16},{16,24},{24,32},{32,40},{40,48},{48,56},{56,64},{64,7... | collective-permute-start | bytes 393224 | tf_op jit(solution)/shard_map/ppermute | solution.py:297
  29.3 2.0 %shard_map.199 = bf16[64,32,256]{2,1,0:T(8,128)(2,1)} custom-call(bf16[32,128]{1,0:T(8,128)(2,1)} %refs_0_.2, bf16[32,128]{1,0:T(8,128)(2,1)} %refs_1_.2), custom_call_target="tpu_custom_call" | custom-call | tf_op jit(solution)/shard_map/pallas_call | solution.py:54
  31.3 16.6 %all-to-all-start = ((bf16[64,32,256]{2,1,0:T(8,128)(2,1)}), bf16[64,32,256]{2,1,0:T(8,128)(2,1)S(1)}, u32[]{:S(2)}, u32[]{:S(2)}) async-start(bf16[64,32,256]{2,1,0:T(8,128)(2,1)} %shard_map.199), calls=%async_computation | async-start | bytes 2097152 | tf_op jit(solution)/shard_map/all_to_all | solution.py:295
  48.0 0.0 copy-start.7
  48.0 0.0 copy-start.10
  48.0 0.3 fusion
  48.3 0.3 fusion.2.nref
  48.7 0.4 fusion.3
  49.1 0.0 copy-done.10
  49.1 0.0 copy-start.2
  49.1 0.0 copy-start.3
  49.1 0.1 fusion.5
  49.2 0.6 reduce-window.6
  49.9 0.2 slice_reduce_fusion
  50.0 0.2 reduce-window.9
  50.2 0.1 add_bitcast_fusion
  50.3 0.2 slice_reduce_fusion.1
  50.5 0.1 exponential_bitcast_fusion
  50.6 0.1 copy.32.lref
  50.7 0.1 copy.31.sref
  50.8 22.9 %all-to-all-done = bf16[64,32,256]{2,1,0:T(8,128)(2,1)S(1)} async-done(((bf16[64,32,256]{2,1,0:T(8,128)(2,1)}), bf16[64,32,256]{2,1,0:T(8,128)(2,1)S(1)}, u32[]{:S(2)}, u32[]{:S(2)}) %all-to-all-start) | async-done | bytes 1048608 | tf_op jit(solution)/shard_map/all_to_all | solution.py:295
  73.7 1.6 %local_states.1 = (bf16[8,136,128]{2,1,0:T(8,128)(2,1)}, bf16[256,128]{1,0:T(8,128)(2,1)S(1)}, bf16[256,128]{1,0:T(8,128)(2,1)S(1)}) custom-call(bf16[288,2048]{1,0:T(8,128)(2,1)S(1)} %fusion.2.nref, bf16[2048,256]{1,0:T(8,128)(2,1)S(1)} %bitcast.34, f32[4,256]{1,0:T(4,128)S(1)} %pad_maximum_fusion.1.tref, f32[256,128]{1,0:T(8,128)S(1)} %copy.31.sref, ...), custom_call_target="tpu_custom_call" | custom-call | tf_op jit(solution)/shard_map/local_states/pallas_call | solution.py:86
  75.4 10.0 %all-to-all-start.1 = ((bf16[8,136,128]{2,1,0:T(8,128)(2,1)}), bf16[8,136,128]{2,1,0:T(8,128)(2,1)S(1)}, u32[]{:S(2)}, u32[]{:S(2)}) async-start(bf16[8,136,128]{2,1,0:T(8,128)(2,1)} %get-tuple-element.18), calls=%async_computation.1 | async-start | bytes 557056 | tf_op jit(solution)/shard_map/all_to_all | solution.py:313
  85.4 0.1 copy.33.cum
  85.5 14.9 %all-gather.4.cloned.1.call-done.wref = bf16[2048,768]{1,0:T(8,128)(2,1)} async-done(((bf16[256,768]{1,0:T(8,128)(2,1)}), bf16[2048,768]{1,0:T(8,128)(2,1)}) %all-gather.4.cloned.1.call-update) | async-done | bytes 3145744 | tf_op jit(solution)/shard_map/all_gather | solution.py:293
  100.3 0.0 copy-start.4
  100.4 2.9 %rows_local.1 = (bf16[256,128]{1,0:T(8,128)(2,1)S(1)}, f32[256,128]{1,0:T(8,128)S(1)}, f32[256,128]{1,0:T(8,128)S(1)}, f32[256,128]{1,0:T(8,128)S(1)}, bf16[2048,256]{1,0:T(8,128)(2,1)S(1)}) custom-call(bf16[288,2048]{1,0:T(8,128)(2,1)S(1)} %fusion.2.nref, bf16[2048,768]{1,0:T(8,128)(2,1)} %all-gather.4.cloned.1.call-done.wref, f32[4,128]{1,0:T(4,128)S(1)} %copy-done.3, ...), custom_call_target="tpu_custom_call" | custom-call | tf_op jit(solution)/shard_map/rows_local/pallas_call | solution.py:186
  103.3 2.7 %collective-permute-start.1 = (bf16[2048,256]{1,0:T(8,128)(2,1)S(1)}, bf16[2048,256]{1,0:T(8,128)(2,1)}, u32[]{:S(2)}, u32[]{:S(2)}) collective-permute-start(bf16[2048,256]{1,0:T(8,128)(2,1)S(1)} %get-tuple-element.30.wa), channel_id=1, source_target_pairs={{0,1},{1,0},{2,3},{3,2},{4,5},{5,4},{6,7},{7,6},{8,9},{9,8},{10,11... | collective-permute-start | bytes 3145736 | tf_op jit(solution)/shard_map/ppermute | solution.py:317
  106.0 0.9 line_states.1
  106.9 3.9 %all-to-all-start.2 = ((bf16[8,136,128]{2,1,0:T(8,128)(2,1)}), bf16[8,136,128]{2,1,0:T(8,128)(2,1)S(1)}, u32[]{:S(2)}, u32[]{:S(2)}) async-start(bf16[8,136,128]{2,1,0:T(8,128)(2,1)} %get-tuple-element.19), calls=%async_computation.2 | async-start | bytes 557056 | tf_op jit(solution)/shard_map/all_to_all | solution.py:315
  110.8 1.8 %all-gather.1 = f32[2,1,128]{2,1,0:T(1,128)S(1)} all-gather(f32[1,1,128]{2,1,0:T(1,128)S(1)} %bitcast.46), channel_id=2, replica_groups=mesh['sp_0'=8,'sp_1'=8,'fs'=4,'tp'=2] {'tp'}, dimensions={0}, use_global_device_ids=true | all-gather | bytes 1536 | tf_op jit(solution)/shard_map/all_gather | solution.py:310
  112.6 10.9 %all-to-all-done.2.got = bf16[8,136,128]{2,1,0:T(8,128)(2,1)S(1)} async-done(((bf16[8,136,128]{2,1,0:T(8,128)(2,1)}), bf16[8,136,128]{2,1,0:T(8,128)(2,1)S(1)}, u32[]{:S(2)}, u32[]{:S(2)}) %all-to-all-start.2) | async-done | bytes 278560 | tf_op jit(solution)/shard_map/all_to_all | solution.py:315
  123.5 1.3 rows_done.1
  124.8 4.7 %all-to-all-start.4 = ((f32[8,3,256]{2,1,0:T(4,128)}), f32[8,3,256]{2,1,0:T(4,128)S(1)}, u32[]{:S(2)}, u32[]{:S(2)}) async-start(f32[8,3,256]{2,1,0:T(4,128)} %get-tuple-element.28), calls=%async_computation.4 | async-start | bytes 65536 | tf_op jit(solution)/shard_map/all_to_all | solution.py:321
  129.5 2.1 %all_gather.13.bref = bf16[512,384]{1,0:T(8,128)(2,1)S(1)} all-gather(bf16[256,384]{1,0:T(8,128)(2,1)S(1)} %get-tuple-element.29), channel_id=1, replica_groups=mesh['sp_0'=8,'sp_1'=8,'fs'=4,'tp'=2] {'tp'}, dimensions={0}, use_global_device_ids=true | all-gather | bytes 589824 | tf_op jit(solution)/shard_map/all_gather | solution.py:322
  131.6 2.6 %all-to-all-done.4.sref = f32[8,3,256]{2,1,0:T(4,128)S(1)} async-done(((f32[8,3,256]{2,1,0:T(4,128)}), f32[8,3,256]{2,1,0:T(4,128)S(1)}, u32[]{:S(2)}, u32[]{:S(2)}) %all-to-all-start.4) | async-done | bytes 24608 | tf_op jit(solution)/shard_map/all_to_all | solution.py:321
  134.2 2.3 %output_rows.1 = bf16[4,32,2048]{2,1,0:T(8,128)(2,1)S(1)} custom-call(s32[1]{0:T(128)} %bitcast.at, f32[8,3,256]{2,1,0:T(4,128)S(1)} %all-to-all-done.4.sref, bf16[512,384]{1,0:T(8,128)(2,1)S(1)} %all_gather.13.bref, f32[2,128]{1,0:T(2,128)S(1)} %bitcast.38, bf16[2048,256]{1,0:T(8,128)(2,1)S(1)} %get-tuple-element.30.wa, ...), custom_call_target="tpu_custom_call" | custom-call | tf_op jit(solution)/shard_map/output_rows/pallas_call | solution.py:269
  136.5 10.9 %all_to_all.31 = bf16[4,32,2048]{2,1,0:T(8,128)(2,1)S(1)} all-to-all(bf16[4,32,2048]{2,1,0:T(8,128)(2,1)S(1)} %output_rows.1), channel_id=1, replica_groups=mesh['sp_0'=8,'sp_1'=8,'fs'=4,'tp'=2] {'fs'}, dimensions={0} | all-to-all | bytes 1048576 | tf_op jit(solution)/shard_map/all_to_all | solution.py:324
  147.5 0.7 reduce_sum.22
  (28 shorter events, 0.1 us)
Async XLA Ops:
  6.5 42.2 %copy-start = (bf16[2048,16]{0,1:T(8,128)(2,1)S(1)}, bf16[2048,16]{0,1:T(8,128)(2,1)}, u32[]{:S(2)}) copy-start(bf16[2048,16]{0,1:T(8,128)(2,1)} %param.29) | copy-start | bytes 196612
  6.5 93.8 %all-gather.4.cloned.1.call-start = ((), (), s32[]{:S(2)}) async-start(), calls=%async_computation.6 | async-start | bytes 3538944 | tf_op jit(solution)/shard_map/all_gather | solution.py:293
  7.4 40.5 %copy-start.11 = (f32[2]{0:T(128)S(1)}, f32[2]{0:T(128)}, u32[]{:S(2)}) copy-start(f32[2]{0:T(128)} %param.31) | copy-start | bytes 28
  7.4 40.5 %copy-start.8 = (f32[4,128]{1,0:T(4,128)S(1)}, f32[4,128]{1,0:T(4,128)}, u32[]{:S(2)}) copy-start(f32[4,128]{1,0:T(4,128)} %param.34) | copy-start | bytes 6148
  7.4 40.5 %copy-start.9 = (f32[4,128]{1,0:T(4,128)S(1)}, f32[4,128]{1,0:T(4,128)}, u32[]{:S(2)}) copy-start(f32[4,128]{1,0:T(4,128)} %param.33) | copy-start | bytes 6148
  7.4 40.6 %copy-start.5 = (bf16[256,2048]{1,0:T(8,128)(2,1)S(1)}, bf16[256,2048]{1,0:T(8,128)(2,1)}, u32[]{:S(2)}) copy-start(bf16[256,2048]{1,0:T(8,128)(2,1)} %param.21) | copy-start | bytes 3145732
  26.8 21.6 %copy-start.6 = (f32[2048]{0:T(1024)S(1)}, f32[2048]{0:T(1024)}, u32[]{:S(2)}) copy-start(f32[2048]{0:T(1024)} %param.22) | copy-start | bytes 24580
  27.7 20.3 %collective-permute-start = (bf16[32,2048]{1,0:T(8,128)(2,1)S(1)}, bf16[32,2048]{1,0:T(8,128)(2,1)S(1)}, u32[]{:S(2)}, u32[]{:S(2)}) collective-permute-start(bf16[32,2048]{1,0:T(8,128)(2,1)S(1)} %slice.15), channel_id=1, source_target_pairs={{0,8},{8,16},{16,24},{24,32},{32,40},{40,48},{48,56},{56,64},{64,7... | collective-permute-start | bytes 393224 | tf_op jit(solution)/shard_map/ppermute | solution.py:297
  31.3 42.4 %all-to-all-start = ((bf16[64,32,256]{2,1,0:T(8,128)(2,1)}), bf16[64,32,256]{2,1,0:T(8,128)(2,1)S(1)}, u32[]{:S(2)}, u32[]{:S(2)}) async-start(bf16[64,32,256]{2,1,0:T(8,128)(2,1)} %shard_map.199), calls=%async_computation | async-start | bytes 2097152 | tf_op jit(solution)/shard_map/all_to_all | solution.py:295
  48.0 1.1 copy-start.7
  48.0 1.1 copy-start.10
  49.1 51.2 %copy-start.2 = (f32[31,128]{1,0:T(8,128)S(1)}, f32[31,128]{1,0:T(8,128)}, u32[]{:S(2)}) copy-start(f32[31,128]{1,0:T(8,128)} %ltaps.1) | copy-start | bytes 47620
  49.1 51.2 %copy-start.3 = (f32[4,128]{1,0:T(4,128)S(1)}, f32[4,128]{1,0:T(4,128)}, u32[]{:S(2)}) copy-start(f32[4,128]{1,0:T(4,128)} %ftaps.1) | copy-start | bytes 6148
  75.4 30.7 %all-to-all-start.1 = ((bf16[8,136,128]{2,1,0:T(8,128)(2,1)}), bf16[8,136,128]{2,1,0:T(8,128)(2,1)S(1)}, u32[]{:S(2)}, u32[]{:S(2)}) async-start(bf16[8,136,128]{2,1,0:T(8,128)(2,1)} %get-tuple-element.18), calls=%async_computation.1 | async-start | bytes 557056 | tf_op jit(solution)/shard_map/all_to_all | solution.py:313
  100.3 10.5 %copy-start.12 = (f32[128]{0:T(128)S(1)}, f32[128]{0:T(128)}, u32[]{:S(2)}) copy-start(f32[128]{0:T(128)} %param.37) | copy-start | bytes 1540
  100.3 23.2 %copy-start.1 = (f32[2,64,128]{2,1,0:T(8,128)S(1)}, f32[2,64,128]{2,1,0:T(8,128)}, u32[]{:S(2)}) copy-start(f32[2,64,128]{2,1,0:T(8,128)} %init.1) | copy-start | bytes 196612
  100.3 23.2 %copy-start.4 = (f32[128]{0:T(128)S(1)}, f32[128]{0:T(128)}, u32[]{:S(2)}) copy-start(f32[128]{0:T(128)} %param.38) | copy-start | bytes 1540
  103.3 31.0 %collective-permute-start.1 = (bf16[2048,256]{1,0:T(8,128)(2,1)S(1)}, bf16[2048,256]{1,0:T(8,128)(2,1)}, u32[]{:S(2)}, u32[]{:S(2)}) collective-permute-start(bf16[2048,256]{1,0:T(8,128)(2,1)S(1)} %get-tuple-element.30.wa), channel_id=1, source_target_pairs={{0,1},{1,0},{2,3},{3,2},{4,5},{5,4},{6,7},{7,6},{8,9},{9,8},{10,11... | collective-permute-start | bytes 3145736 | tf_op jit(solution)/shard_map/ppermute | solution.py:317
  106.9 16.6 %all-to-all-start.2 = ((bf16[8,136,128]{2,1,0:T(8,128)(2,1)}), bf16[8,136,128]{2,1,0:T(8,128)(2,1)S(1)}, u32[]{:S(2)}, u32[]{:S(2)}) async-start(bf16[8,136,128]{2,1,0:T(8,128)(2,1)} %get-tuple-element.19), calls=%async_computation.2 | async-start | bytes 557056 | tf_op jit(solution)/shard_map/all_to_all | solution.py:315
  124.8 9.4 %all-to-all-start.4 = ((f32[8,3,256]{2,1,0:T(4,128)}), f32[8,3,256]{2,1,0:T(4,128)S(1)}, u32[]{:S(2)}, u32[]{:S(2)}) async-start(f32[8,3,256]{2,1,0:T(4,128)} %get-tuple-element.28), calls=%async_computation.4 | async-start | bytes 65536 | tf_op jit(solution)/shard_map/all_to_all | solution.py:321
Sparse Core Ops, SparseCore 0:
  26.9 73.3 all-gather.3

commit v9 on v7

--- a/solution.py
+++ b/solution.py
@@ -56,27 +56,32 @@
     )(*fetched(*shards))
 
 
-def parted(near, first, copies):
+def first_columns(near, first, copies):
+    ny, piece, _ = near.shape
+
+    def body(ref, out):
+        for y in range(ny):
+            w = ref[y, :, :first]
+            for k in range(copies):
+                out[k, y * piece : (y + 1) * piece, :] = w
+
+    return pl.pallas_call(
+        body, out_shape=pltpu.HBM((copies, ny * piece, first), bf16), in_specs=[VMEM], out_specs=VMEM,
+        compiler_params=SMALL, name="first_columns",
+    )(*held(near))
+
+
+def other_columns(near, first, after):
     ny, piece, width = near.shape
-    size = ny * piece
-    main = size - size // 16
-
-    def body(ref, rest, most, last):
+
+    def body(ref, late, out):
         for y in range(ny):
-            rest[y * piece : (y + 1) * piece, :] = ref[y, :, first:]
-            if (y + 1) * piece <= main:
-                most[y * piece : (y + 1) * piece, :] = ref[y, :, :first]
-        inside = main % piece
-        if inside:
-            most[main - inside :, :] = ref[main // piece, :inside, :first]
-        for k in range(copies):
-            last[k] = ref[ny - 1, piece - (size - main) :, :first]
-
-    return pl.pallas_call(
-        body,
-        out_shape=(sds((size, width - first), bf16), pltpu.VMEM((main, first), bf16), sds((copies, size - main, first), bf16)),
-        in_specs=[VMEM], out_specs=(VMEM,) * 3, compiler_params=SMALL, name="parted",
-    )(*held(near))
+            out[y * piece : (y + 1) * piece, :] = ref[y, :, first:]
+
+    return pl.pallas_call(
+        body, out_shape=sds((ny * piece, width - first), bf16), in_specs=[VMEM, VMEM], out_specs=VMEM,
+        compiler_params=SMALL, name="other_columns",
+    )(*held(near, after))
 
 
 def log_rows(logs):
@@ -132,18 +137,13 @@
     )(index, bias, rate_log, *held(own, step_proj, extra))
 
 
-def local_states(halo, own, most, last, taps, step, left, total, copies):
-    rows, d = own.shape
+def local_states(halo, own, first, taps, step, left, total, copies):
+    rows, _ = own.shape
     ch = step.shape[1]
-    nz, main, _ = most.shape
-    size = main + last.shape[1]
-
-    def body(href, nref, mref, rref, tref, sref, lref, logs, send, xs, w16, buf, wall):
-        for z in range(nz):
-            wall[z * size : z * size + main, :] = mref[z]
-            wall[z * size + main : (z + 1) * size, :] = rref[z]
-        buf[:HALO, :] = dot(href[...], wall[...], 1, 0).astype(bf16).astype(f32)
-        buf[HALO:, :] = dot(nref[...], wall[...], 1, 0).astype(bf16).astype(f32)
+
+    def body(href, nref, wref, tref, sref, lref, logs, send, xs, w16, buf):
+        buf[:HALO, :] = dot(href[...], wref[...], 1, 0).astype(bf16).astype(f32)
+        buf[HALO:, :] = dot(nref[...], wref[...], 1, 0).astype(bf16).astype(f32)
         at = HALO - SHORT + 1
         mix = sum(buf[at + i : at + i + rows, :] * tref[i : i + 1, :] for i in range(SHORT))
         act = jax.nn.silu(mix)
@@ -160,11 +160,11 @@
     return pl.pallas_call(
         body,
         out_shape=(sds((copies, ch + LOGS, STATE), bf16), pltpu.VMEM((rows, ch), bf16), pltpu.VMEM((rows, STATE), bf16)),
-        in_specs=[VMEM] * 8,
+        in_specs=[VMEM] * 7,
         out_specs=(VMEM,) * 3,
-        scratch_shapes=[pltpu.VMEM((HALO + rows, 2 * ch), f32), pltpu.VMEM((d, 2 * ch), bf16)],
+        scratch_shapes=[pltpu.VMEM((HALO + rows, 2 * ch), f32)],
         compiler_params=SMALL, name="local_states",
-    )(*held(halo, own, most, last, taps, step, left, total))
+    )(*held(halo, own, first, taps, step, left, total))
 
 
 def spread_heads(c, heads, p):
@@ -379,10 +379,8 @@
         (state_input, write_projection, state_read, mixer_gate, conv_value, conv_gate, conv_output, state_output), ny
     )
     near = lax.all_to_all(near, "sp_1", 0, 0, tiled=True)
-    rest, most, last = parted(near, 2 * ch, lax.axis_size("sp_0"))
-    rest = lax.all_gather(rest, "sp_0", axis=0, tiled=True)
-    last = lax.all_to_all(last, "sp_0", 0, 0, tiled=True)
-    most = lax.all_gather(most, "sp_0", axis=0)
+    first = first_columns(near, 2 * ch, lax.axis_size("sp_0"))
+    first = lax.all_to_all(first, "sp_0", 0, 0, tiled=True).reshape(-1, 2 * ch)
     n = lax.axis_size(SP)
     halo = lax.ppermute(tokens[rows - HALO :], SP, [(i, i + 1) for i in range(n - 1)])
 
@@ -394,9 +392,11 @@
     halo = unit(halo)
     me = lax.axis_index("fs").astype(jnp.int32).reshape(1) * nt + tp
     step, left, cum, cum_t, total = steps_of(own, step_proj, decay_extra, step_bias, decay_log, me, p)
+    rest = other_columns(near, 2 * ch, total)
+    rest = lax.all_gather(rest, "sp_0", axis=0, tiled=True)
     gains = lax.all_gather(conv_gain, "tp")
     taps = jnp.concatenate([input_taps, write_taps], 1)
-    send, xs, w16 = local_states(halo, own, most, last, taps, step, left, total, ny)
+    send, xs, w16 = local_states(halo, own, first, taps, step, left, total, ny)
     got = lax.all_to_all(send, "sp_1", 0, 0, tiled=True)
     enter, before, send = line_states(got, iy, heads, p, lax.axis_size("sp_0"))
     got = lax.all_to_all(send, "sp_0", 0, 0, tiled=True)

time: 151 us -> 160 us (1.060)
  waiting for transfers between devices: 12.2 us -> 74.5 us
  blocking collectives: 70.8 us -> 14.8 us
  Pallas kernels: 12 us -> 13.9 us
  local copies, waits for them, and re-layouts: 0.36 us -> 2.15 us
    all_to_all x1 -> x2, waiting for transfers between devices: 0.01 us -> 48.3 us  [the longest x1 38.3 us: per_device(): first = lax.all_to_all(first, 'sp_0', 0, 0, tiled=True).reshape(-1, 2 * ch)]
    all_gather x1 -> x0, blocking collectives: 28.8 us -> none  [per_device(): most = lax.all_gather(most, 'sp_0', axis=0)]
    all_to_all x1 -> x0, blocking collectives: 22.3 us -> none  [per_device(): near = lax.all_to_all(near, 'sp_1', 0, 0, tiled=True)]
    all_to_all x1, waiting for transfers between devices: 2.77 us -> 10.9 us  [per_device(): got = lax.all_to_all(send, 'sp_0', 0, 0, tiled=True)]
    all_to_all x1 -> x2, starting transfers between devices: 14.2 us -> 20.7 us  [the longest x1 13 us: per_device(): first = lax.all_to_all(first, 'sp_0', 0, 0, tiled=True).reshape(-1, 2 * ch)]
    all_to_all x1, starting transfers between devices: 11 us -> 4.74 us  [per_device(): sums = lax.all_to_all(sums, FT, 0, 0, tiled=True)]
    all_gather x1, blocking collectives: 6.73 us -> 1.81 us  [per_device(): gains = lax.all_gather(conv_gain, 'tp')]
    all_gather x1, waiting for transfers between devices: 6.71 us -> 10.7 us  [per_device(): rest = lax.all_gather(rest, 'sp_0', axis=0, tiled=True)]
  transfers between devices with their start and end apart: 7 -> 8, of which waited for: 3 -> 6; matrix products, arithmetic and copies ran while one was open for 2% -> 3% of each run, Pallas kernels for 6% -> 6%
where the time goes in v9:
time: 160 us
  waiting for transfers between devices  74.5 us (47%)
  starting transfers between devices  37.7 us (24%)
  blocking collectives  14.8 us (9%)
  Pallas kernels  13.9 us (9%)
  between operations  13.6 us (8%)
  other arithmetic  2.82 us (2%)
  local copies, waits for them, and re-layouts  2.15 us (1%)
    all_to_all x1, waiting for transfers between devices, per_device(): first = lax.all_to_all(first, 'sp_0', 0, 0, tiled=True).reshape(-1, 2 * ch)  38.3 us
    all_to_all x1, starting transfers between devices, per_device(): first = lax.all_to_all(first, 'sp_0', 0, 0, tiled=True).reshape(-1, 2 * ch)  13 us
    all_to_all x1, blocking collectives, per_device(): pieces = lax.all_to_all(out, 'fs', 0, 0, tiled=True)  10.9 us
    all_to_all x1, waiting for transfers between devices, per_device(): got = lax.all_to_all(send, 'sp_0', 0, 0, tiled=True)  10.9 us
    all_gather x1, waiting for transfers between devices, per_device(): rest = lax.all_gather(rest, 'sp_0', axis=0, tiled=True)  10.7 us
    all_to_all x1, waiting for transfers between devices, per_device(): near = lax.all_to_all(near, 'sp_1', 0, 0, tiled=True)  10.1 us
    all_to_all x1, starting transfers between devices, per_device(): near = lax.all_to_all(near, 'sp_1', 0, 0, tiled=True)  7.64 us
    all_to_all x1, starting transfers between devices, per_device(): sums = lax.all_to_all(sums, FT, 0, 0, tiled=True)  4.74 us
  transfers between devices with their start and end apart: 8, of which 6 were waited for; matrix products, arithmetic and copies ran while one was open for 3% of the time, Pallas kernels for 6%

profile of v9, /device:TPU:1, one launch (start us, length us, event | category | flops | bytes accessed | tf_op | source)
XLA Modules:
  0.0 159.6 jit_solution(9496825901031873678)
XLA Ops:
  6.5 1.8 %shard_map.199 = bf16[8,32,1024]{2,1,0:T(8,128)(2,1)} custom-call(bf16[32,128]{1,0:T(8,128)(2,1)} %refs_0_.1, bf16[32,128]{1,0:T(8,128)(2,1)} %refs_1_.1, bf16[32,128]{1,0:T(8,128)(2,1)} %refs_2_.1, bf16[32,128]{1,0:T(8,128)(2,1)} %refs_3_.1, bf16[32,128]{1,0:T(8,128)(2,1)} %refs_4_.1, bf16[32,128]{1,0:T(8,128)(2,1)} %refs_5_.1, bf16[32,128]{1,0:T(8,128)(2,1)} %refs_6_.1, ...), custom_call_target="tpu_custom_call" | custom-call | tf_op jit(solution)/shard_map/pallas_call | solution.py:54
  8.3 7.6 %all-to-all-start = ((bf16[8,32,1024]{2,1,0:T(8,128)(2,1)}), bf16[8,32,1024]{2,1,0:T(8,128)(2,1)S(1)}, u32[]{:S(2)}, u32[]{:S(2)}) async-start(bf16[8,32,1024]{2,1,0:T(8,128)(2,1)} %shard_map.199), calls=%async_computation | async-start | bytes 1048576 | tf_op jit(solution)/shard_map/all_to_all | solution.py:381
  16.0 0.0 copy-start.6
  16.0 0.0 copy-start.7
  16.0 0.0 all-gather.4.cloned.1.call-start
  16.1 1.2 copy.24.wref
  17.3 0.3 fusion
  17.6 1.5 fusion.2.nref.nall
  19.1 0.0 copy-done.4
  19.1 0.0 copy-done.6
  19.1 0.0 copy-done.7
  19.1 0.0 copy-start
  19.1 1.7 %steps_of.1 = (f32[256,128]{1,0:T(8,128)S(1)}, f32[256,128]{1,0:T(8,128)S(1)}, f32[256,128]{1,0:T(8,128)S(1)}, f32[2,256]{1,0:T(2,128)S(1)}, f32[1,128]{1,0:T(1,128)S(1)}) custom-call(s32[1]{0:T(128)S(6)} %add.29.at, f32[2]{0:T(128)S(1)} %copy-done.6, f32[2]{0:T(128)S(1)} %copy-done.7, bf16[256,2048]{1,0:T(8,128)(2,1)S(1)} %fusion.2.nref.nall, ...), custom_call_target="tpu_custom_call" | custom-call | tf_op jit(solution)/shard_map/steps_of/pallas_call | solution.py:131
  20.8 10.1 %all-to-all-done.ref = bf16[8,32,1024]{2,1,0:T(8,128)(2,1)S(1)} async-done(((bf16[8,32,1024]{2,1,0:T(8,128)(2,1)}), bf16[8,32,1024]{2,1,0:T(8,128)(2,1)S(1)}, u32[]{:S(2)}, u32[]{:S(2)}) %all-to-all-start) | async-done | bytes 524320 | tf_op jit(solution)/shard_map/all_to_all | solution.py:381
  30.9 0.8 other_columns.1
  31.7 0.0 all-gather.4.cloned.1.call-update
  31.8 1.1 first_columns.1
  32.8 13.0 %all-to-all-start.1 = ((bf16[8,256,256]{2,1,0:T(8,128)(2,1)}), bf16[8,256,256]{2,1,0:T(8,128)(2,1)S(1)}, u32[]{:S(2)}, u32[]{:S(2)}) async-start(bf16[8,256,256]{2,1,0:T(8,128)(2,1)} %first_columns.1), calls=%async_computation.1 | async-start | bytes 2097152 | tf_op jit(solution)/shard_map/all_to_all | solution.py:383
  45.9 0.0 copy-start.5
  45.9 0.9 slice.3
  46.8 1.3 collective-permute-start
  48.1 0.0 copy-done.11
  48.1 0.0 copy-done.12
  48.2 1.9 %collective-permute-done = bf16[32,2048]{1,0:T(8,128)(2,1)S(1)} collective-permute-done((bf16[32,2048]{1,0:T(8,128)(2,1)S(1)}, bf16[32,2048]{1,0:T(8,128)(2,1)S(1)}, u32[]{:S(2)}, u32[]{:S(2)}) %collective-permute-start) | collective-permute-done | bytes 131104 | tf_op jit(solution)/shard_map/ppermute | solution.py:385
  50.0 0.1 fusion.3
  50.2 0.1 fusion.5.href.hall
  50.3 0.0 copy-start.1
  50.3 38.3 %all-to-all-done.1 = bf16[8,256,256]{2,1,0:T(8,128)(2,1)S(1)} async-done(((bf16[8,256,256]{2,1,0:T(8,128)(2,1)}), bf16[8,256,256]{2,1,0:T(8,128)(2,1)S(1)}, u32[]{:S(2)}, u32[]{:S(2)}) %all-to-all-start.1) | async-done | bytes 1048608 | tf_op jit(solution)/shard_map/all_to_all | solution.py:383
  88.6 1.7 %local_states.1 = (bf16[8,136,128]{2,1,0:T(8,128)(2,1)}, bf16[256,128]{1,0:T(8,128)(2,1)S(1)}, bf16[256,128]{1,0:T(8,128)(2,1)S(1)}) custom-call(bf16[32,2048]{1,0:T(8,128)(2,1)S(1)} %fusion.5.href.hall, bf16[256,2048]{1,0:T(8,128)(2,1)S(1)} %fusion.2.nref.nall, bf16[2048,256]{1,0:T(8,128)(2,1)S(1)} %bitcast.8, f32[4,256]{1,0:T(4,128)S(1)} %pad_maximum_fusion.tref, ...), custom_call_target="tpu_custom_call" | custom-call | tf_op jit(solution)/shard_map/local_states/pallas_call | solution.py:160
  90.3 3.4 %all-to-all-start.2 = ((bf16[8,136,128]{2,1,0:T(8,128)(2,1)}), bf16[8,136,128]{2,1,0:T(8,128)(2,1)S(1)}, u32[]{:S(2)}, u32[]{:S(2)}) async-start(bf16[8,136,128]{2,1,0:T(8,128)(2,1)} %get-tuple-element.26), calls=%async_computation.2 | async-start | bytes 557056 | tf_op jit(solution)/shard_map/all_to_all | solution.py:400
  93.7 10.7 %all-gather.4.cloned.1.call-done.wref = bf16[2048,768]{1,0:T(8,128)(2,1)} async-done(((bf16[256,768]{1,0:T(8,128)(2,1)}), bf16[2048,768]{1,0:T(8,128)(2,1)}) %all-gather.4.cloned.1.call-update) | async-done | bytes 3145744 | tf_op jit(solution)/shard_map/all_gather | solution.py:396
  104.5 0.0 copy-start.2
  104.5 0.0 copy-start.8
  104.5 3.5 %rows_local.1 = (bf16[256,128]{1,0:T(8,128)(2,1)S(1)}, f32[256,128]{1,0:T(8,128)S(1)}, f32[256,128]{1,0:T(8,128)S(1)}, f32[256,128]{1,0:T(8,128)S(1)}, bf16[2048,256]{1,0:T(8,128)(2,1)S(1)}) custom-call(bf16[32,2048]{1,0:T(8,128)(2,1)} %copy-done.1, bf16[256,2048]{1,0:T(8,128)(2,1)} %copy-done, bf16[2048,768]{1,0:T(8,128)(2,1)} %all-gather.4.cloned.1.call-done.wref, ...), custom_call_target="tpu_custom_call" | custom-call | tf_op jit(solution)/shard_map/rows_local/pallas_call | solution.py:273
  108.0 3.2 %collective-permute-start.1 = (bf16[2048,256]{1,0:T(8,128)(2,1)S(1)}, bf16[2048,256]{1,0:T(8,128)(2,1)S(1)}, u32[]{:S(2)}, u32[]{:S(2)}) collective-permute-start(bf16[2048,256]{1,0:T(8,128)(2,1)S(1)} %get-tuple-element.40.wa), channel_id=1, source_target_pairs={{0,1},{1,0},{2,3},{3,2},{4,5},{5,4},{6,7},{7,6},{8,9},{9,8},{10,11... | collective-permute-start | bytes 3145736 | tf_op jit(solution)/shard_map/ppermute | solution.py:404
  111.3 0.0 all-to-all-done.2.ref
  111.3 0.9 line_states.1
  112.2 4.3 %all-to-all-start.3 = ((bf16[8,136,128]{2,1,0:T(8,128)(2,1)}), bf16[8,136,128]{2,1,0:T(8,128)(2,1)S(1)}, u32[]{:S(2)}, u32[]{:S(2)}) async-start(bf16[8,136,128]{2,1,0:T(8,128)(2,1)} %get-tuple-element.27), calls=%async_computation.3 | async-start | bytes 557056 | tf_op jit(solution)/shard_map/all_to_all | solution.py:402
  116.5 1.8 %all-gather.1 = f32[2,1,128]{2,1,0:T(1,128)S(1)} all-gather(f32[1,1,128]{2,1,0:T(1,128)S(1)} %bitcast.11), channel_id=2, replica_groups=mesh['sp_0'=8,'sp_1'=8,'fs'=4,'tp'=2] {'tp'}, dimensions={0}, use_global_device_ids=true | all-gather | bytes 1536 | tf_op jit(solution)/shard_map/all_gather | solution.py:397
  118.3 10.9 %all-to-all-done.3.got = bf16[8,136,128]{2,1,0:T(8,128)(2,1)S(1)} async-done(((bf16[8,136,128]{2,1,0:T(8,128)(2,1)}), bf16[8,136,128]{2,1,0:T(8,128)(2,1)S(1)}, u32[]{:S(2)}, u32[]{:S(2)}) %all-to-all-start.3) | async-done | bytes 278560 | tf_op jit(solution)/shard_map/all_to_all | solution.py:402
  129.2 1.3 rows_done.1
  130.5 4.7 %all-to-all-start.4 = ((f32[8,3,256]{2,1,0:T(4,128)}), f32[8,3,256]{2,1,0:T(4,128)S(1)}, u32[]{:S(2)}, u32[]{:S(2)}) async-start(f32[8,3,256]{2,1,0:T(4,128)} %get-tuple-element.38), calls=%async_computation.4 | async-start | bytes 65536 | tf_op jit(solution)/shard_map/all_to_all | solution.py:408
  135.2 2.1 %all_gather.13.bref = bf16[512,384]{1,0:T(8,128)(2,1)S(1)} all-gather(bf16[256,384]{1,0:T(8,128)(2,1)S(1)} %get-tuple-element.39), channel_id=1, replica_groups=mesh['sp_0'=8,'sp_1'=8,'fs'=4,'tp'=2] {'tp'}, dimensions={0}, use_global_device_ids=true | all-gather | bytes 589824 | tf_op jit(solution)/shard_map/all_gather | solution.py:409
  137.3 2.6 %all-to-all-done.4.sref = f32[8,3,256]{2,1,0:T(4,128)S(1)} async-done(((f32[8,3,256]{2,1,0:T(4,128)}), f32[8,3,256]{2,1,0:T(4,128)S(1)}, u32[]{:S(2)}, u32[]{:S(2)}) %all-to-all-start.4) | async-done | bytes 24608 | tf_op jit(solution)/shard_map/all_to_all | solution.py:408
  139.9 0.0 collective-permute-done.1.wb
  139.9 1.1 output_rows.1
  141.0 10.9 %all_to_all.30 = bf16[4,32,2048]{2,1,0:T(8,128)(2,1)S(1)} all-to-all(bf16[4,32,2048]{2,1,0:T(8,128)(2,1)S(1)} %output_rows.1), channel_id=1, replica_groups=mesh['sp_0'=8,'sp_1'=8,'fs'=4,'tp'=2] {'fs'}, dimensions={0} | all-to-all | bytes 1048576 | tf_op jit(solution)/shard_map/all_to_all | solution.py:411
  152.0 0.7 reduce_sum.32
  (19 shorter events, 0.1 us)
Async XLA Ops:
  6.5 10.7 %copy-start.9 = (bf16[256,2048]{1,0:T(8,128)(2,1)S(1)}, bf16[256,2048]{1,0:T(8,128)(2,1)}, u32[]{:S(2)}) copy-start(bf16[256,2048]{1,0:T(8,128)(2,1)} %param.21) | copy-start | bytes 3145732
  6.5 11.0 %copy-start.10 = (f32[2048]{0:T(1024)S(1)}, f32[2048]{0:T(1024)}, u32[]{:S(2)}) copy-start(f32[2048]{0:T(1024)} %param.22) | copy-start | bytes 24580
  8.3 22.6 %all-to-all-start = ((bf16[8,32,1024]{2,1,0:T(8,128)(2,1)}), bf16[8,32,1024]{2,1,0:T(8,128)(2,1)S(1)}, u32[]{:S(2)}, u32[]{:S(2)}) async-start(bf16[8,32,1024]{2,1,0:T(8,128)(2,1)} %shard_map.199), calls=%async_computation | async-start | bytes 1048576 | tf_op jit(solution)/shard_map/all_to_all | solution.py:381
  16.0 3.1 %copy-start.4 = (f32[2,256]{1,0:T(2,128)S(1)}, f32[2,256]{1,0:T(2,128)}, u32[]{:S(2)}) copy-start(f32[2,256]{1,0:T(2,128)} %eref.1) | copy-start | bytes 6148
  16.0 3.1 %copy-start.6 = (f32[2]{0:T(128)S(1)}, f32[2]{0:T(128)}, u32[]{:S(2)}) copy-start(f32[2]{0:T(128)} %bref.1) | copy-start | bytes 28
  16.0 3.1 %copy-start.7 = (f32[2]{0:T(128)S(1)}, f32[2]{0:T(128)}, u32[]{:S(2)}) copy-start(f32[2]{0:T(128)} %rref.1) | copy-start | bytes 28
  16.0 88.4 %all-gather.4.cloned.1.call-start = ((), (), s32[]{:S(2)}) async-start(), calls=%async_computation.6 | async-start | bytes 3538944 | tf_op jit(solution)/shard_map/all_gather | solution.py:396
  19.1 69.4 %copy-start = (bf16[256,2048]{1,0:T(8,128)(2,1)}, bf16[256,2048]{1,0:T(8,128)(2,1)S(1)}, u32[]{:S(2)}) copy-start(bf16[256,2048]{1,0:T(8,128)(2,1)S(1)} %fusion.2.nref.nall) | copy-start | bytes 3145732
  31.7 16.4 %copy-start.11 = (f32[4,128]{1,0:T(4,128)S(1)}, f32[4,128]{1,0:T(4,128)}, u32[]{:S(2)}) copy-start(f32[4,128]{1,0:T(4,128)} %param.34) | copy-start | bytes 6148
  31.7 16.4 %copy-start.12 = (f32[4,128]{1,0:T(4,128)S(1)}, f32[4,128]{1,0:T(4,128)}, u32[]{:S(2)}) copy-start(f32[4,128]{1,0:T(4,128)} %param.33) | copy-start | bytes 6148
  32.8 55.7 %all-to-all-start.1 = ((bf16[8,256,256]{2,1,0:T(8,128)(2,1)}), bf16[8,256,256]{2,1,0:T(8,128)(2,1)S(1)}, u32[]{:S(2)}, u32[]{:S(2)}) async-start(bf16[8,256,256]{2,1,0:T(8,128)(2,1)} %first_columns.1), calls=%async_computation.1 | async-start | bytes 2097152 | tf_op jit(solution)/shard_map/all_to_all | solution.py:383
  45.9 58.6 %copy-start.3 = (f32[31,128]{1,0:T(8,128)S(1)}, f32[31,128]{1,0:T(8,128)}, u32[]{:S(2)}) copy-start(f32[31,128]{1,0:T(8,128)} %ltaps.1) | copy-start | bytes 47620
  45.9 58.6 %copy-start.5 = (f32[4,128]{1,0:T(4,128)S(1)}, f32[4,128]{1,0:T(4,128)}, u32[]{:S(2)}) copy-start(f32[4,128]{1,0:T(4,128)} %ftaps.1) | copy-start | bytes 6148
  46.8 3.2 %collective-permute-start = (bf16[32,2048]{1,0:T(8,128)(2,1)S(1)}, bf16[32,2048]{1,0:T(8,128)(2,1)S(1)}, u32[]{:S(2)}, u32[]{:S(2)}) collective-permute-start(bf16[32,2048]{1,0:T(8,128)(2,1)S(1)} %slice.3), channel_id=1, source_target_pairs={{0,8},{8,16},{16,24},{24,32},{32,40},{40,48},{48,56},{56,64},{64,7... | collective-permute-start | bytes 393224 | tf_op jit(solution)/shard_map/ppermute | solution.py:385
  50.3 54.1 %copy-start.1 = (bf16[32,2048]{1,0:T(8,128)(2,1)}, bf16[32,2048]{1,0:T(8,128)(2,1)S(1)}, u32[]{:S(2)}) copy-start(bf16[32,2048]{1,0:T(8,128)(2,1)S(1)} %fusion.5.href.hall) | copy-start | bytes 393220
  90.3 21.0 %all-to-all-start.2 = ((bf16[8,136,128]{2,1,0:T(8,128)(2,1)}), bf16[8,136,128]{2,1,0:T(8,128)(2,1)S(1)}, u32[]{:S(2)}, u32[]{:S(2)}) async-start(bf16[8,136,128]{2,1,0:T(8,128)(2,1)} %get-tuple-element.26), calls=%async_computation.2 | async-start | bytes 557056 | tf_op jit(solution)/shard_map/all_to_all | solution.py:400
  104.5 12.0 %copy-start.13 = (f32[128]{0:T(128)S(1)}, f32[128]{0:T(128)}, u32[]{:S(2)}) copy-start(f32[128]{0:T(128)} %param.37) | copy-start | bytes 1540
  104.5 24.7 %copy-start.2 = (f32[2,64,128]{2,1,0:T(8,128)S(1)}, f32[2,64,128]{2,1,0:T(8,128)}, u32[]{:S(2)}) copy-start(f32[2,64,128]{2,1,0:T(8,128)} %init.1) | copy-start | bytes 196612
  104.5 24.7 %copy-start.8 = (f32[128]{0:T(128)S(1)}, f32[128]{0:T(128)}, u32[]{:S(2)}) copy-start(f32[128]{0:T(128)} %param.38) | copy-start | bytes 1540
  108.0 31.9 %collective-permute-start.1 = (bf16[2048,256]{1,0:T(8,128)(2,1)S(1)}, bf16[2048,256]{1,0:T(8,128)(2,1)S(1)}, u32[]{:S(2)}, u32[]{:S(2)}) collective-permute-start(bf16[2048,256]{1,0:T(8,128)(2,1)S(1)} %get-tuple-element.40.wa), channel_id=1, source_target_pairs={{0,1},{1,0},{2,3},{3,2},{4,5},{5,4},{6,7},{7,6},{8,9},{9,8},{10,11... | collective-permute-start | bytes 3145736 | tf_op jit(solution)/shard_map/ppermute | solution.py:404
  112.2 17.0 %all-to-all-start.3 = ((bf16[8,136,128]{2,1,0:T(8,128)(2,1)}), bf16[8,136,128]{2,1,0:T(8,128)(2,1)S(1)}, u32[]{:S(2)}, u32[]{:S(2)}) async-start(bf16[8,136,128]{2,1,0:T(8,128)(2,1)} %get-tuple-element.27), calls=%async_computation.3 | async-start | bytes 557056 | tf_op jit(solution)/shard_map/all_to_all | solution.py:402
  130.5 9.5 %all-to-all-start.4 = ((f32[8,3,256]{2,1,0:T(4,128)}), f32[8,3,256]{2,1,0:T(4,128)S(1)}, u32[]{:S(2)}, u32[]{:S(2)}) async-start(f32[8,3,256]{2,1,0:T(4,128)} %get-tuple-element.38), calls=%async_computation.4 | async-start | bytes 65536 | tf_op jit(solution)/shard_map/all_to_all | solution.py:408
Sparse Core Ops, SparseCore 0:
  31.9 72.5 all-gather.3

commit v10 on v8

--- a/solution.py
+++ b/solution.py
@@ -130,6 +130,13 @@
     )(index, *held(got))
 
 
+def row_sums(arrays, at):
+    _, ch = arrays[0].shape
+    wide = (8, len(arrays) * ch)
+    pick = lax.broadcasted_iota(jnp.int32, wide, 1) // ch + at == lax.broadcasted_iota(jnp.int32, wide, 0)
+    return dot(jnp.where(pick, 1.0, 0.0), jnp.concatenate(arrays, 1), 1, 1, HIGHEST)
+
+
 def rows_local(normed, rest, ftaps, ltaps, xs, w16, cum, cum_t):
     ext, d = normed.shape
     rows, ch = xs.shape
@@ -138,19 +145,13 @@
     part, n = 64, 8
     kc = d // n
 
-    def body(nref, wref, ftaps, ltaps, xs, w16, cum, cum_t, read16, zgate, mixed, inner, back, acc, glu, wall, sems):
+    def body(nref, wref, ftaps, ltaps, xs, w16, cum, cum_t, read16, zgate, mixed, inner, moments, acc, glu, wall, sems):
         def fetch(i):
             at = slice(i * kc, (i + 1) * kc)
-            return pltpu.make_async_copy(wref.at[at, : 4 * ch], wall.at[at, :], sems.at[0, i])
-
-        def fetch_back(i):
-            at = slice(i * kc, (i + 1) * kc)
-            return pltpu.make_async_copy(wref.at[at, 4 * ch :], back.at[at, :], sems.at[1, i])
+            return pltpu.make_async_copy(wref.at[at, : 4 * ch], wall.at[at, :], sems.at[i])
 
         for i in range(n):
             fetch(i).start()
-        for i in range(n):
-            fetch_back(i).start()
         for i in range(n):
             fetch(i).wait()
             at = slice(i * kc, (i + 1) * kc)
@@ -175,37 +176,51 @@
             x = jnp.where(lane // p == h, xs[...].astype(f32), 0.0).astype(bf16)
             y = y + dot(m, x, 1, 0)
         inner[...] = y
-        for r in range(0, rows, part):
-            mixed[r : r + part, :] = sum(
-                glu[l_at + r + i : l_at + r + i + part, :] * ltaps[i : i + 1, :] for i in range(WIDE)
-            )
-        for i in range(n):
-            fetch_back(i).wait()
+        mix = jnp.concatenate(
+            [
+                sum(glu[l_at + r + i : l_at + r + i + part, :] * ltaps[i : i + 1, :] for i in range(WIDE))
+                for r in range(0, rows, part)
+            ],
+            0,
+        )
+        high = mix.astype(bf16)
+        mixed[:, :ch] = high
+        mixed[:, ch:] = (mix - high.astype(f32)).astype(bf16)
+        moments[...] = row_sums([mix, mix * mix], 0)
 
     small = (ftaps, ltaps, xs, w16, cum, cum_t)
     return pl.pallas_call(
         body,
         out_shape=(
-            pltpu.VMEM((rows, STATE), bf16), pltpu.VMEM((rows, ch), f32), pltpu.VMEM((rows, ch), f32),
-            pltpu.VMEM((rows, ch), f32), pltpu.VMEM((d, 2 * ch), bf16),
+            pltpu.VMEM((rows, STATE), bf16), pltpu.VMEM((rows, ch), f32), pltpu.VMEM((rows, 2 * ch), bf16),
+            pltpu.VMEM((rows, ch), f32), pltpu.VMEM((8, rows), f32),
         ),
         in_specs=[VMEM, pl.BlockSpec(memory_space=pltpu.HBM), *[VMEM] * len(small)],
         out_specs=(VMEM,) * 5,
         scratch_shapes=[
             pltpu.VMEM((ext, 4 * ch), f32), pltpu.VMEM((ext, ch), f32), pltpu.VMEM((d, 4 * ch), bf16),
-            pltpu.SemaphoreType.DMA((2, n)),
+            pltpu.SemaphoreType.DMA((n,)),
         ],
         compiler_params=SMALL, name="rows_local",
     )(*held(normed), *fetched(rest), *held(*small))
 
 
-def rows_done(got, enter, before, init, index, read16, zgate, mixed, inner, cum, gain, copies):
-    rows, ch = mixed.shape
+def rows_done(rest, got, enter, before, init, index, read16, zgate, mixed, inner, moments, cum, gain, copies):
+    rows, ch = inner.shape
+    d = rest.shape[0]
+    parts = 4
+    kc = d // parts
     n, _, _ = got.shape
     heads = init.shape[0]
     p = ch // heads
 
-    def body(at, got, enter, before, init, read16, zgate, mixed, inner, cum, gain, sums, pre):
+    def body(at, wref, got, enter, before, init, read16, zgate, mixed, inner, moments, cum, gain, sums, pre, back, sems):
+        def fetch(i):
+            here = slice(i * kc, (i + 1) * kc)
+            return pltpu.make_async_copy(wref.at[here, 4 * ch :], back.at[here, :], sems.at[i])
+
+        for i in range(parts):
+            fetch(i).start()
         acc_in = jnp.zeros((1, STATE), f32)
         start = enter[...]
         b = before[0:1, :]
@@ -217,24 +232,22 @@
         start = start + init[...].reshape(ch, STATE) * spread_heads(jnp.exp(acc_in + b), heads, p)
         y = inner[...] + dot(read16[...], start.astype(bf16), 1, 1) * jnp.exp(cum[...])
         gated = y * zgate[...]
-        mix = mixed[...]
-        squares = jnp.concatenate([mix, mix * mix, gated * gated], 1)
-        pick = lax.broadcasted_iota(jnp.int32, (8, 3 * ch), 1) // ch == lax.broadcasted_iota(jnp.int32, (8, 3 * ch), 0)
-        found = dot(jnp.where(pick, 1.0, 0.0), squares, 1, 1, HIGHEST)
+        found = moments[...] + row_sums([gated * gated], 2)
         for j in range(copies):
             sums[j] = found[:3]
-        high = mix.astype(bf16)
-        pre[:, :ch] = high
-        pre[:, ch : 2 * ch] = (mix - high.astype(f32)).astype(bf16)
+        pre[:, : 2 * ch] = mixed[...]
         pre[:, 2 * ch :] = (gated * gain[...]).astype(bf16)
-
-    return pl.pallas_call(
-        body,
-        out_shape=(sds((copies, 3, rows), f32), pltpu.VMEM((rows, 3 * ch), bf16)),
-        in_specs=[SMEM, *[VMEM] * 10],
-        out_specs=(VMEM, VMEM),
+        for i in range(parts):
+            fetch(i).wait()
+
+    return pl.pallas_call(
+        body,
+        out_shape=(sds((copies, 3, rows), f32), pltpu.VMEM((rows, 3 * ch), bf16), pltpu.VMEM((d, 2 * ch), bf16)),
+        in_specs=[SMEM, pl.BlockSpec(memory_space=pltpu.HBM), *[VMEM] * 11],
+        out_specs=(VMEM,) * 3,
+        scratch_shapes=[pltpu.SemaphoreType.DMA((parts,))],
         compiler_params=SMALL, name="rows_done",
-    )(index, *held(got, enter, before, init, read16, zgate, mixed, inner, cum, gain))
+    )(index, *fetched(rest), *held(got, enter, before, init, read16, zgate, mixed, inner, moments, cum, gain))
 
 
 def output_rows(sums, both, gains, own, other, index, nf, nt):
@@ -313,11 +326,12 @@
     got = lax.all_to_all(send, "sp_1", 0, 0, tiled=True)
     enter, before, send = line_states(got, iy, heads, p, lax.axis_size("sp_0"))
     got = lax.all_to_all(send, "sp_0", 0, 0, tiled=True)
-    read16, zgate, mixed, inner, back = rows_local(normed, rest, fetch_taps, long_taps, xs, w16, cum, cum_t)
+    read16, zgate, mixed, inner, moments = rows_local(normed, rest, fetch_taps, long_taps, xs, w16, cum, cum_t)
+    sums, pre, back = rows_done(
+        rest, got, enter, before, initial_state, iz, read16, zgate, mixed, inner, moments, cum, state_gain[None],
+        nf * nt,
+    )
     back_other = lax.ppermute(back, "tp", [(i, nt - 1 - i) for i in range(nt)])
-    sums, pre = rows_done(
-        got, enter, before, initial_state, iz, read16, zgate, mixed, inner, cum, state_gain[None], nf * nt
-    )
     sums = lax.all_to_all(sums, FT, 0, 0, tiled=True)
     both = lax.all_gather(pre, "tp", axis=0, tiled=True)
     out = output_rows(sums, both, gains, back, back_other, tp, nf, nt)

time: 156 us -> 149 us (0.955)
  waiting for transfers between devices: 51.4 us -> 41.6 us
  starting transfers between devices: 39.5 us -> 42.4 us
    all_gather x1, waiting for transfers between devices: 14.9 us -> 0.41 us  [per_device(): rest = lax.all_gather(rest, 'sp_0', axis=0, tiled=True)]
    all_to_all x1, waiting for transfers between devices: 0.01 us -> 10.1 us  [per_device(): got = lax.all_to_all(send, 'sp_1', 0, 0, tiled=True)]
    all_to_all x1, waiting for transfers between devices: 10.9 us -> 5.44 us  [per_device(): got = lax.all_to_all(send, 'sp_0', 0, 0, tiled=True)]
    ppermute x1, starting transfers between devices: 2.75 us -> 6.08 us  [per_device(): back_other = lax.ppermute(back, 'tp', [(i, nt - 1 - i) for i in range(nt)])]
  transfers between devices with their start and end apart: 7 -> 7, of which waited for: 4 -> 5; matrix products, arithmetic and copies ran while one was open for 2% -> 2% of each run, Pallas kernels for 6% -> 5%
where the time goes in v10:
time: 149 us
  starting transfers between devices  42.4 us (28%)
  waiting for transfers between devices  41.6 us (28%)
  blocking collectives  34.6 us (23%)
  between operations  13.7 us (9%)
  Pallas kernels  11.9 us (8%)
  other arithmetic  2.46 us (2%)
  local copies, waits for them, and re-layouts  1.69 us (1%)
    all_to_all x1, waiting for transfers between devices, per_device(): first = lax.all_to_all(first, SP, 0, 0, tiled=True).reshape(-1, 2 * ch)  22.9 us
    all_to_all x1, blocking collectives, per_device(): rest = lax.all_to_all(rest, 'sp_1', 0, 0, tiled=True).reshape(-1, 6 * ch)  19.3 us
    all_to_all x1, starting transfers between devices, per_device(): first = lax.all_to_all(first, SP, 0, 0, tiled=True).reshape(-1, 2 * ch)  16.6 us
    all_to_all x1, blocking collectives, per_device(): pieces = lax.all_to_all(out, 'fs', 0, 0, tiled=True)  10.9 us
    all_to_all x1, waiting for transfers between devices, per_device(): got = lax.all_to_all(send, 'sp_1', 0, 0, tiled=True)  10.1 us
    all_to_all x1, starting transfers between devices, per_device(): got = lax.all_to_all(send, 'sp_1', 0, 0, tiled=True)  9.98 us
    ppermute x1, starting transfers between devices, per_device(): back_other = lax.ppermute(back, 'tp', [(i, nt - 1 - i) for i in range(nt)])  6.08 us
    all_to_all x1, waiting for transfers between devices, per_device(): got = lax.all_to_all(send, 'sp_0', 0, 0, tiled=True)  5.44 us
  transfers between devices with their start and end apart: 7, of which 5 were waited for; matrix products, arithmetic and copies ran while one was open for 2% of the time, Pallas kernels for 5%

profile of v10, /device:TPU:1, one launch (start us, length us, event | category | flops | bytes accessed | tf_op | source)
XLA Modules:
  0.0 148.7 jit_solution(1791739484439790262)
XLA Ops:
  6.5 0.9 shard_map.199
  7.4 0.0 copy-start.11
  7.4 0.0 copy-start.9
  7.4 0.0 copy-start.5
  7.5 19.3 %all_to_all.30 = bf16[8,32,768]{2,1,0:T(8,128)(2,1)} all-to-all(bf16[8,32,768]{2,1,0:T(8,128)(2,1)S(1)} %shard_map.199), channel_id=1, replica_groups=mesh['sp_0'=8,'sp_1'=8,'fs'=4,'tp'=2] {'sp_1'}, dimensions={0} | all-to-all | bytes 786432 | tf_op jit(solution)/shard_map/all_to_all | solution.py:305
  26.7 0.0 all-gather.4.cloned.1.call-update
  26.8 0.0 copy-start.6
  26.8 0.9 slice.15
  27.7 1.6 %collective-permute-start = (bf16[32,2048]{1,0:T(8,128)(2,1)S(1)}, bf16[32,2048]{1,0:T(8,128)(2,1)S(1)}, u32[]{:S(2)}, u32[]{:S(2)}) collective-permute-start(bf16[32,2048]{1,0:T(8,128)(2,1)S(1)} %slice.15), channel_id=1, source_target_pairs={{0,8},{8,16},{16,24},{24,32},{32,40},{40,48},{48,56},{56,64},{64,7... | collective-permute-start | bytes 393224 | tf_op jit(solution)/shard_map/ppermute | solution.py:310
  29.3 2.0 %shard_map.200 = bf16[64,32,256]{2,1,0:T(8,128)(2,1)} custom-call(bf16[32,128]{1,0:T(8,128)(2,1)} %refs_0_.3, bf16[32,128]{1,0:T(8,128)(2,1)} %refs_1_.3), custom_call_target="tpu_custom_call" | custom-call | tf_op jit(solution)/shard_map/pallas_call | solution.py:54
  31.3 16.6 %all-to-all-start.1 = ((bf16[64,32,256]{2,1,0:T(8,128)(2,1)}), bf16[64,32,256]{2,1,0:T(8,128)(2,1)S(1)}, u32[]{:S(2)}, u32[]{:S(2)}) async-start(bf16[64,32,256]{2,1,0:T(8,128)(2,1)} %shard_map.200), calls=%async_computation.1 | async-start | bytes 2097152 | tf_op jit(solution)/shard_map/all_to_all | solution.py:308
  48.0 0.0 copy-start.7
  48.0 0.0 copy-start.10
  48.0 0.3 fusion
  48.3 0.3 fusion.2.nref
  48.7 0.4 fusion.3
  49.1 0.0 copy-done.10
  49.1 0.1 fusion.5
  49.2 0.6 reduce-window.6
  49.8 0.2 slice_reduce_fusion
  50.0 0.2 reduce-window.9
  50.2 0.1 add_bitcast_fusion
  50.2 0.2 slice_reduce_fusion.1
  50.4 0.1 exponential_bitcast_fusion
  50.5 0.1 copy.32.lref
  50.6 0.0 copy-start.2
  50.7 0.1 copy.31.sref
  50.8 22.9 %all-to-all-done.1 = bf16[64,32,256]{2,1,0:T(8,128)(2,1)S(1)} async-done(((bf16[64,32,256]{2,1,0:T(8,128)(2,1)}), bf16[64,32,256]{2,1,0:T(8,128)(2,1)S(1)}, u32[]{:S(2)}, u32[]{:S(2)}) %all-to-all-start.1) | async-done | bytes 1048608 | tf_op jit(solution)/shard_map/all_to_all | solution.py:308
  73.7 1.6 %local_states.1 = (bf16[8,136,128]{2,1,0:T(8,128)(2,1)}, bf16[256,128]{1,0:T(8,128)(2,1)S(1)}, bf16[256,128]{1,0:T(8,128)(2,1)S(1)}) custom-call(bf16[288,2048]{1,0:T(8,128)(2,1)S(1)} %fusion.2.nref, bf16[2048,256]{1,0:T(8,128)(2,1)S(1)} %bitcast.34, f32[4,256]{1,0:T(4,128)S(1)} %pad_maximum_fusion.1.tref, f32[256,128]{1,0:T(8,128)S(1)} %copy.31.sref, ...), custom_call_target="tpu_custom_call" | custom-call | tf_op jit(solution)/shard_map/local_states/pallas_call | solution.py:86
  75.4 10.0 %all-to-all-start.2 = ((bf16[8,136,128]{2,1,0:T(8,128)(2,1)}), bf16[8,136,128]{2,1,0:T(8,128)(2,1)S(1)}, u32[]{:S(2)}, u32[]{:S(2)}) async-start(bf16[8,136,128]{2,1,0:T(8,128)(2,1)} %get-tuple-element.19), calls=%async_computation.2 | async-start | bytes 557056 | tf_op jit(solution)/shard_map/all_to_all | solution.py:326
  85.3 10.1 %all-to-all-done.2.ref = bf16[8,136,128]{2,1,0:T(8,128)(2,1)S(1)} async-done(((bf16[8,136,128]{2,1,0:T(8,128)(2,1)}), bf16[8,136,128]{2,1,0:T(8,128)(2,1)S(1)}, u32[]{:S(2)}, u32[]{:S(2)}) %all-to-all-start.2) | async-done | bytes 278560 | tf_op jit(solution)/shard_map/all_to_all | solution.py:326
  95.5 0.9 line_states.1
  96.4 3.4 %all-to-all-start.3 = ((bf16[8,136,128]{2,1,0:T(8,128)(2,1)}), bf16[8,136,128]{2,1,0:T(8,128)(2,1)S(1)}, u32[]{:S(2)}, u32[]{:S(2)}) async-start(bf16[8,136,128]{2,1,0:T(8,128)(2,1)} %get-tuple-element.20), calls=%async_computation.3 | async-start | bytes 557056 | tf_op jit(solution)/shard_map/all_to_all | solution.py:328
  99.8 0.1 copy.33.cum
  99.9 0.0 copy-start.4
  99.9 0.4 all-gather.4.cloned.1.call-done.wref
  100.3 3.4 %rows_local.1 = (bf16[256,128]{1,0:T(8,128)(2,1)S(1)}, f32[256,128]{1,0:T(8,128)S(1)}, bf16[256,256]{1,0:T(8,128)(2,1)S(1)}, f32[256,128]{1,0:T(8,128)S(1)}, f32[8,256]{1,0:T(8,128)S(1)}) custom-call(bf16[288,2048]{1,0:T(8,128)(2,1)S(1)} %fusion.2.nref, bf16[2048,768]{1,0:T(8,128)(2,1)} %all-gather.4.cloned.1.call-done.wref, f32[4,128]{1,0:T(4,128)S(1)} %copy-done.3, ...), custom_call_target="tpu_custom_call" | custom-call | tf_op jit(solution)/shard_map/rows_local/pallas_call | solution.py:192
  103.8 0.0 copy-start.12
  103.8 5.4 %all-to-all-done.3.got = bf16[8,136,128]{2,1,0:T(8,128)(2,1)S(1)} async-done(((bf16[8,136,128]{2,1,0:T(8,128)(2,1)}), bf16[8,136,128]{2,1,0:T(8,128)(2,1)S(1)}, u32[]{:S(2)}, u32[]{:S(2)}) %all-to-all-start.3) | async-done | bytes 278560 | tf_op jit(solution)/shard_map/all_to_all | solution.py:328
  109.2 2.1 %rows_done.1 = (f32[8,3,256]{2,1,0:T(4,128)}, bf16[256,384]{1,0:T(8,128)(2,1)S(1)}, bf16[2048,256]{1,0:T(8,128)(2,1)S(1)}) custom-call(s32[1]{0:T(128)} %bitcast.1.at, bf16[2048,768]{1,0:T(8,128)(2,1)} %all-gather.4.cloned.1.call-done.wref, bf16[8,136,128]{2,1,0:T(8,128)(2,1)S(1)} %all-to-all-done.3.got, f32[128,128]{1,0:T(8,128)S(1)} %get-tuple-element.21.enter, ...), custom_call_target="tpu_custom_call" | custom-call | tf_op jit(solution)/shard_map/rows_done/pallas_call | solution.py:243
  111.3 6.1 %collective-permute-start.1 = (bf16[2048,256]{1,0:T(8,128)(2,1)S(1)}, bf16[2048,256]{1,0:T(8,128)(2,1)S(1)}, u32[]{:S(2)}, u32[]{:S(2)}) collective-permute-start(bf16[2048,256]{1,0:T(8,128)(2,1)S(1)} %get-tuple-element.32.wa), channel_id=1, source_target_pairs={{0,1},{1,0},{2,3},{3,2},{4,5},{5,4},{6,7},{7,6},{8,9},{9,8},{10,11... | collective-permute-start | bytes 3145736 | tf_op jit(solution)/shard_map/ppermute | solution.py:334
  117.4 2.3 %all-gather.1 = f32[2,1,128]{2,1,0:T(1,128)S(1)} all-gather(f32[1,1,128]{2,1,0:T(1,128)S(1)} %bitcast.46), channel_id=2, replica_groups=mesh['sp_0'=8,'sp_1'=8,'fs'=4,'tp'=2] {'tp'}, dimensions={0}, use_global_device_ids=true | all-gather | bytes 1536 | tf_op jit(solution)/shard_map/all_gather | solution.py:323
  119.7 4.7 %all-to-all-start.4 = ((f32[8,3,256]{2,1,0:T(4,128)}), f32[8,3,256]{2,1,0:T(4,128)S(1)}, u32[]{:S(2)}, u32[]{:S(2)}) async-start(f32[8,3,256]{2,1,0:T(4,128)} %get-tuple-element.30), calls=%async_computation.4 | async-start | bytes 65536 | tf_op jit(solution)/shard_map/all_to_all | solution.py:335
  124.3 2.1 %all_gather.13.bref = bf16[512,384]{1,0:T(8,128)(2,1)S(1)} all-gather(bf16[256,384]{1,0:T(8,128)(2,1)S(1)} %get-tuple-element.31), channel_id=1, replica_groups=mesh['sp_0'=8,'sp_1'=8,'fs'=4,'tp'=2] {'tp'}, dimensions={0}, use_global_device_ids=true | all-gather | bytes 589824 | tf_op jit(solution)/shard_map/all_gather | solution.py:336
  126.4 2.6 %all-to-all-done.4.sref = f32[8,3,256]{2,1,0:T(4,128)S(1)} async-done(((f32[8,3,256]{2,1,0:T(4,128)}), f32[8,3,256]{2,1,0:T(4,128)S(1)}, u32[]{:S(2)}, u32[]{:S(2)}) %all-to-all-start.4) | async-done | bytes 24608 | tf_op jit(solution)/shard_map/all_to_all | solution.py:335
  129.1 1.1 output_rows.1
  130.1 10.9 %all_to_all.31 = bf16[4,32,2048]{2,1,0:T(8,128)(2,1)S(1)} all-to-all(bf16[4,32,2048]{2,1,0:T(8,128)(2,1)S(1)} %output_rows.1), channel_id=1, replica_groups=mesh['sp_0'=8,'sp_1'=8,'fs'=4,'tp'=2] {'fs'}, dimensions={0} | all-to-all | bytes 1048576 | tf_op jit(solution)/shard_map/all_to_all | solution.py:338
  141.1 0.7 reduce_sum.22
  (28 shorter events, 0.1 us)
Async XLA Ops:
  6.5 42.2 %copy-start = (bf16[2048,16]{0,1:T(8,128)(2,1)S(1)}, bf16[2048,16]{0,1:T(8,128)(2,1)}, u32[]{:S(2)}) copy-start(bf16[2048,16]{0,1:T(8,128)(2,1)} %param.29) | copy-start | bytes 196612
  6.5 93.8 %all-gather.4.cloned.1.call-start = ((), (), s32[]{:S(2)}) async-start(), calls=%async_computation.6 | async-start | bytes 3538944 | tf_op jit(solution)/shard_map/all_gather | solution.py:306
  7.4 40.5 %copy-start.11 = (f32[2]{0:T(128)S(1)}, f32[2]{0:T(128)}, u32[]{:S(2)}) copy-start(f32[2]{0:T(128)} %param.31) | copy-start | bytes 28
  7.4 40.5 %copy-start.8 = (f32[4,128]{1,0:T(4,128)S(1)}, f32[4,128]{1,0:T(4,128)}, u32[]{:S(2)}) copy-start(f32[4,128]{1,0:T(4,128)} %param.34) | copy-start | bytes 6148
  7.4 40.5 %copy-start.9 = (f32[4,128]{1,0:T(4,128)S(1)}, f32[4,128]{1,0:T(4,128)}, u32[]{:S(2)}) copy-start(f32[4,128]{1,0:T(4,128)} %param.33) | copy-start | bytes 6148
  7.4 40.6 %copy-start.5 = (bf16[256,2048]{1,0:T(8,128)(2,1)S(1)}, bf16[256,2048]{1,0:T(8,128)(2,1)}, u32[]{:S(2)}) copy-start(bf16[256,2048]{1,0:T(8,128)(2,1)} %param.21) | copy-start | bytes 3145732
  26.8 21.6 %copy-start.6 = (f32[2048]{0:T(1024)S(1)}, f32[2048]{0:T(1024)}, u32[]{:S(2)}) copy-start(f32[2048]{0:T(1024)} %param.22) | copy-start | bytes 24580
  27.7 20.3 %collective-permute-start = (bf16[32,2048]{1,0:T(8,128)(2,1)S(1)}, bf16[32,2048]{1,0:T(8,128)(2,1)S(1)}, u32[]{:S(2)}, u32[]{:S(2)}) collective-permute-start(bf16[32,2048]{1,0:T(8,128)(2,1)S(1)} %slice.15), channel_id=1, source_target_pairs={{0,8},{8,16},{16,24},{24,32},{32,40},{40,48},{48,56},{56,64},{64,7... | collective-permute-start | bytes 393224 | tf_op jit(solution)/shard_map/ppermute | solution.py:310
  31.3 42.4 %all-to-all-start.1 = ((bf16[64,32,256]{2,1,0:T(8,128)(2,1)}), bf16[64,32,256]{2,1,0:T(8,128)(2,1)S(1)}, u32[]{:S(2)}, u32[]{:S(2)}) async-start(bf16[64,32,256]{2,1,0:T(8,128)(2,1)} %shard_map.200), calls=%async_computation.1 | async-start | bytes 2097152 | tf_op jit(solution)/shard_map/all_to_all | solution.py:308
  48.0 1.1 copy-start.7
  48.0 1.1 copy-start.10
  50.6 49.7 %copy-start.2 = (f32[31,128]{1,0:T(8,128)S(1)}, f32[31,128]{1,0:T(8,128)}, u32[]{:S(2)}) copy-start(f32[31,128]{1,0:T(8,128)} %ltaps.1) | copy-start | bytes 47620
  50.6 49.7 %copy-start.3 = (f32[4,128]{1,0:T(4,128)S(1)}, f32[4,128]{1,0:T(4,128)}, u32[]{:S(2)}) copy-start(f32[4,128]{1,0:T(4,128)} %ftaps.1) | copy-start | bytes 6148
  75.4 20.1 %all-to-all-start.2 = ((bf16[8,136,128]{2,1,0:T(8,128)(2,1)}), bf16[8,136,128]{2,1,0:T(8,128)(2,1)S(1)}, u32[]{:S(2)}, u32[]{:S(2)}) async-start(bf16[8,136,128]{2,1,0:T(8,128)(2,1)} %get-tuple-element.19), calls=%async_computation.2 | async-start | bytes 557056 | tf_op jit(solution)/shard_map/all_to_all | solution.py:326
  96.4 12.9 %all-to-all-start.3 = ((bf16[8,136,128]{2,1,0:T(8,128)(2,1)}), bf16[8,136,128]{2,1,0:T(8,128)(2,1)S(1)}, u32[]{:S(2)}, u32[]{:S(2)}) async-start(bf16[8,136,128]{2,1,0:T(8,128)(2,1)} %get-tuple-element.20), calls=%async_computation.3 | async-start | bytes 557056 | tf_op jit(solution)/shard_map/all_to_all | solution.py:328
  99.9 9.3 %copy-start.1 = (f32[2,64,128]{2,1,0:T(8,128)S(1)}, f32[2,64,128]{2,1,0:T(8,128)}, u32[]{:S(2)}) copy-start(f32[2,64,128]{2,1,0:T(8,128)} %init.1) | copy-start | bytes 196612
  99.9 9.3 %copy-start.4 = (f32[128]{0:T(128)S(1)}, f32[128]{0:T(128)}, u32[]{:S(2)}) copy-start(f32[128]{0:T(128)} %param.38) | copy-start | bytes 1540
  103.8 13.6 %copy-start.12 = (f32[128]{0:T(128)S(1)}, f32[128]{0:T(128)}, u32[]{:S(2)}) copy-start(f32[128]{0:T(128)} %param.37) | copy-start | bytes 1540
  111.3 17.7 %collective-permute-start.1 = (bf16[2048,256]{1,0:T(8,128)(2,1)S(1)}, bf16[2048,256]{1,0:T(8,128)(2,1)S(1)}, u32[]{:S(2)}, u32[]{:S(2)}) collective-permute-start(bf16[2048,256]{1,0:T(8,128)(2,1)S(1)} %get-tuple-element.32.wa), channel_id=1, source_target_pairs={{0,1},{1,0},{2,3},{3,2},{4,5},{5,4},{6,7},{7,6},{8,9},{9,8},{10,11... | collective-permute-start | bytes 3145736 | tf_op jit(solution)/shard_map/ppermute | solution.py:334
  119.7 9.4 %all-to-all-start.4 = ((f32[8,3,256]{2,1,0:T(4,128)}), f32[8,3,256]{2,1,0:T(4,128)S(1)}, u32[]{:S(2)}, u32[]{:S(2)}) async-start(f32[8,3,256]{2,1,0:T(4,128)} %get-tuple-element.30), calls=%async_computation.4 | async-start | bytes 65536 | tf_op jit(solution)/shard_map/all_to_all | solution.py:335
Sparse Core Ops, SparseCore 0:
  26.9 73.3 all-gather.3

commit v11 on v8

--- a/solution.py
+++ b/solution.py
@@ -64,11 +64,56 @@
     return jnp.where(row == 0, hi, jnp.where(row == 1, mid, jnp.where(row == 2, lo, 0.0))).astype(bf16)
 
 
-def local_states(normed, first, taps, step, left, total, copies):
+def steps_of(own, step_proj, extra, bias, rate_log, index, p):
+    rows = own.shape[0] - HALO
+    heads = extra.shape[0]
+    ch = heads * p
+    every = step_proj.shape[1]
+
+    def body(at, bref, rref, nref, wref, eref, step, left, cum, cum_t, total):
+        raw = dot(wref[...], nref[HALO:, :], 0, 1)
+        which = lax.broadcasted_iota(jnp.int32, (every, rows), 0)
+        size, logs = [], []
+        for h in range(heads):
+            x = jnp.sum(jnp.where(which == at[3] * heads + h, raw, 0.0), axis=0, keepdims=True) + bref[h]
+            size.append(jnp.maximum(x, 0.0) + jnp.log1p(jnp.exp(-jnp.abs(x))))
+            logs.append(-jnp.exp(jnp.full((1, rows), rref[h], f32)) * size[h] + eref[h : h + 1, :])
+        none = [jnp.zeros((8 - heads, rows), f32)]
+        upto = lax.broadcasted_iota(jnp.int32, (rows, rows), 0) <= lax.broadcasted_iota(jnp.int32, (rows, rows), 1)
+        run = dot(jnp.concatenate(logs + none, 0), jnp.where(upto, 1.0, 0.0), 1, 0, HIGHEST)
+        lane = lax.broadcasted_iota(jnp.int32, (rows, ch), 1) // p
+
+        def wide(cols):
+            out = jnp.broadcast_to(cols[:, 0:1], (rows, ch))
+            for h in range(1, heads):
+                out = jnp.where(lane == h, cols[:, h : h + 1], out)
+            return out
+
+        cum_t[...] = run[:heads]
+        cum[...] = wide(jnp.transpose(run))
+        left[...] = wide(jnp.transpose(jnp.exp(run[:, rows - 1 :] - run)))
+        step[...] = wide(jnp.transpose(jnp.concatenate(size + none, 0)))
+        place = lax.broadcasted_iota(jnp.int32, (1, STATE), 1)
+        ends = jnp.zeros((1, STATE), f32)
+        for h in range(heads):
+            ends = jnp.where(place == h, run[h : h + 1, rows - 1 :], ends)
+        total[...] = ends
+
+    wide = pltpu.VMEM((rows, ch), f32)
+    return pl.pallas_call(
+        body,
+        out_shape=(wide, wide, wide, pltpu.VMEM((heads, rows), f32), pltpu.VMEM((1, STATE), f32)),
+        in_specs=[SMEM, SMEM, SMEM, VMEM, VMEM, VMEM],
+        out_specs=(VMEM,) * 5,
+        compiler_params=SMALL, name="steps_of",
+    )(index, bias, rate_log, *held(own, step_proj, extra))
+
+
+def local_states(normed, first, taps, step, left, total, index, copies):
     ext, _ = normed.shape
     rows, ch = step.shape
 
-    def body(nref, wref, tref, sref, lref, logs, send, xs, w16, buf):
+    def body(at, nref, wref, tref, sref, lref, logs, send, xs, w16, buf):
         buf[...] = dot(nref[...], wref[...], 1, 0).astype(bf16).astype(f32)
         at = HALO - SHORT + 1
         mix = sum(buf[at + i : at + i + rows, :] * tref[i : i + 1, :] for i in range(SHORT))
@@ -86,11 +131,11 @@
     return pl.pallas_call(
         body,
         out_shape=(sds((copies, ch + LOGS, STATE), bf16), pltpu.VMEM((rows, ch), bf16), pltpu.VMEM((rows, STATE), bf16)),
-        in_specs=[VMEM] * 6,
+        in_specs=[SMEM, *[VMEM] * 6],
         out_specs=(VMEM,) * 3,
         scratch_shapes=[pltpu.VMEM((ext, 2 * ch), f32)],
         compiler_params=SMALL, name="local_states",
-    )(*held(normed, first, taps, step, left, total))
+    )(index, *held(normed, first, taps, step, left, total))
 
 
 def spread_heads(c, heads, p):
@@ -108,7 +153,7 @@
         tot = jnp.zeros((ch, STATE), f32)
         for k in reversed(range(n)):
             logs = jnp.sum(ref[k, ch:, :].astype(f32), axis=0, keepdims=True)
-            inside = (k < at[0]).astype(f32)
+            inside = (k < at[1]).astype(f32)
             piece = ref[k, :ch, :].astype(f32)
             ent = ent + piece * spread_heads(inside * jnp.exp(acc_in), heads, p)
             tot = tot + piece * spread_heads(jnp.exp(acc_all), heads, p)
@@ -244,7 +289,7 @@
     piece = rows // (nf * nt)
 
     def body(at, sref, bref, gref, wa, wb, out, cols, act):
-        tp = at[0]
+        tp = at[2]
         s = sref[0]
         for j in range(1, copies):
             s = s + sref[j]
@@ -286,7 +331,8 @@
     heads = step_bias.shape[0]
     p = ch // heads
     nf, nt = lax.axis_size("fs"), lax.axis_size("tp")
-    iz, iy, tp = (lax.axis_index(a).astype(jnp.int32).reshape(1) for a in ("sp_0", "sp_1", "tp"))
+    iz, iy, tp = (lax.axis_index(a).astype(jnp.int32) for a in ("sp_0", "sp_1", "tp"))
+    at = jnp.stack([iz, iy, tp, lax.axis_index("fs").astype(jnp.int32) * nt + tp])
     ny = lax.axis_size("sp_1")
     rest = lay_out((state_read, mixer_gate, conv_value, conv_gate, conv_output, state_output), ny)
     rest = lax.all_to_all(rest, "sp_1", 0, 0, tiled=True).reshape(-1, 6 * ch)
@@ -297,30 +343,21 @@
     halo = lax.ppermute(tokens[rows - HALO :], SP, [(i, i + 1) for i in range(n - 1)])
     v = jnp.concatenate([halo, tokens], 0).astype(f32)
     normed = (v * lax.rsqrt(jnp.mean(v * v, axis=1, keepdims=True) + EPS) * norm_gain).astype(bf16)
-    step_all = jnp.dot(normed[HALO:], step_proj, preferred_element_type=f32)
-    me = lax.axis_index("fs") * nt + lax.axis_index("tp")
-    step = jax.nn.softplus(lax.dynamic_slice_in_dim(step_all, me * heads, heads, 1) + step_bias)
-    log_step = (-jnp.exp(decay_log) * step + decay_extra.T).T
-    cum_t = jnp.cumsum(log_step, axis=1)
-    total = cum_t[:, -1]
-    cum = jnp.repeat(cum_t.T, p, axis=1)
-    step = jnp.repeat(step, p, axis=1)
-    left = jnp.repeat(jnp.exp(total[:, None] - cum_t).T, p, axis=1)
-    total = jnp.pad(total[None], ((0, 0), (0, STATE - heads)))
+    step, left, cum, cum_t, total = steps_of(normed, step_proj, decay_extra, step_bias, decay_log, at, p)
     gains = lax.all_gather(conv_gain, "tp")
     taps = jnp.concatenate([input_taps, write_taps], 1)
-    send, xs, w16 = local_states(normed, first, taps, step, left, total, ny)
+    send, xs, w16 = local_states(normed, first, taps, step, left, total, at, ny)
     got = lax.all_to_all(send, "sp_1", 0, 0, tiled=True)
-    enter, before, send = line_states(got, iy, heads, p, lax.axis_size("sp_0"))
+    enter, before, send = line_states(got, at, heads, p, lax.axis_size("sp_0"))
     got = lax.all_to_all(send, "sp_0", 0, 0, tiled=True)
     read16, zgate, mixed, inner, back = rows_local(normed, rest, fetch_taps, long_taps, xs, w16, cum, cum_t)
     back_other = lax.ppermute(back, "tp", [(i, nt - 1 - i) for i in range(nt)])
     sums, pre = rows_done(
-        got, enter, before, initial_state, iz, read16, zgate, mixed, inner, cum, state_gain[None], nf * nt
+        got, enter, before, initial_state, at, read16, zgate, mixed, inner, cum, state_gain[None], nf * nt
     )
     sums = lax.all_to_all(sums, FT, 0, 0, tiled=True)
     both = lax.all_gather(pre, "tp", axis=0, tiled=True)
-    out = output_rows(sums, both, gains, back, back_other, tp, nf, nt)
+    out = output_rows(sums, both, gains, back, back_other, at, nf, nt)
     pieces = lax.all_to_all(out, "fs", 0, 0, tiled=True)
     return jnp.sum(pieces.astype(f32), 0).astype(bf16)
 

time: 156 us -> 167 us (1.071)
  local copies, waits for them, and re-layouts: 1.67 us -> 10.1 us
  waiting for transfers between devices: 51.4 us -> 54.1 us
  Pallas kernels: 11.8 us -> 14.5 us
  starting transfers between devices: 39.5 us -> 37.4 us
    all_to_all x1, waiting for transfers between devices: 22.9 us -> 0.73 us  [per_device(): first = lax.all_to_all(first, SP, 0, 0, tiled=True).reshape(-1, 2 * ch)]
    ppermute x1, waiting for transfers between devices: 0.01 us -> 19.4 us  [per_device(): lax.ppermute(tokens[rows - HALO:], SP, [(i, i + 1) for i in range(n - 1)])]
    unnamed x27 -> x55, local copies, waits for them, and re-layouts: 0.09 us -> 10.1 us
    all_gather x1, waiting for transfers between devices: 14.9 us -> 20.4 us  [per_device(): rest = lax.all_gather(rest, 'sp_0', axis=0, tiled=True)]
    all_to_all x1, starting transfers between devices: 16.6 us -> 14 us  [per_device(): first = lax.all_to_all(first, SP, 0, 0, tiled=True).reshape(-1, 2 * ch)]
    pallas_call x0 -> x1, Pallas kernels: none -> 1.71 us  [steps_of(): pl.pallas_call(body, out_shape=(wide, wide, wide, pltpu.VMEM((heads, rows...]
  transfers between devices with their start and end apart: 7 -> 7, of which waited for: 4 -> 5; matrix products, arithmetic and copies ran while one was open for 2% -> 1% of each run, Pallas kernels for 6% -> 7%
where the time goes in v11:
time: 167 us; the launch traced here: 166 us
  waiting for transfers between devices  54.1 us (32%)
  starting transfers between devices  37.4 us (22%)
  blocking collectives  34 us (20%)
  Pallas kernels  14.5 us (9%)
  between operations  13.7 us (8%)
  local copies, waits for them, and re-layouts  10.1 us (6%)
  other arithmetic  2.71 us (2%)
    all_gather x1, waiting for transfers between devices, per_device(): rest = lax.all_gather(rest, 'sp_0', axis=0, tiled=True)  20.4 us
    ppermute x1, waiting for transfers between devices, per_device(): lax.ppermute(tokens[rows - HALO:], SP, [(i, i + 1) for i in range(n - 1)])  19.4 us
    all_to_all x1, blocking collectives, per_device(): rest = lax.all_to_all(rest, 'sp_1', 0, 0, tiled=True).reshape(-1, 6 * ch)  19.2 us
    all_to_all x1, starting transfers between devices, per_device(): first = lax.all_to_all(first, SP, 0, 0, tiled=True).reshape(-1, 2 * ch)  14 us
    all_to_all x1, blocking collectives, per_device(): pieces = lax.all_to_all(out, 'fs', 0, 0, tiled=True)  10.9 us
    all_to_all x1, waiting for transfers between devices, per_device(): got = lax.all_to_all(send, 'sp_0', 0, 0, tiled=True)  10.9 us
    unnamed x55, local copies, waits for them, and re-layouts  10.1 us
    all_to_all x1, starting transfers between devices, per_device(): got = lax.all_to_all(send, 'sp_1', 0, 0, tiled=True)  8.71 us
  transfers between devices with their start and end apart: 7, of which 5 were waited for; matrix products, arithmetic and copies ran while one was open for 1% of the time, Pallas kernels for 7%

profile of v11, /device:TPU:1, one launch (start us, length us, event | category | flops | bytes accessed | tf_op | source)
XLA Modules:
  0.0 166.4 jit_solution(9234468608721667009)
XLA Ops:
  6.5 0.9 shard_map.200
  7.5 0.0 copy-start.22
  7.5 19.2 %all_to_all.30 = bf16[8,32,768]{2,1,0:T(8,128)(2,1)} all-to-all(bf16[8,32,768]{2,1,0:T(8,128)(2,1)S(1)} %shard_map.200), channel_id=1, replica_groups=mesh['sp_0'=8,'sp_1'=8,'fs'=4,'tp'=2] {'sp_1'}, dimensions={0} | all-to-all | bytes 786432 | tf_op jit(solution)/shard_map/all_to_all | solution.py:338
  26.6 0.0 all-gather.4.cloned.1.call-update
  26.7 0.0 copy-start.23
  26.7 2.0 %shard_map.199 = bf16[64,32,256]{2,1,0:T(8,128)(2,1)} custom-call(bf16[32,128]{1,0:T(8,128)(2,1)} %refs_0_.2, bf16[32,128]{1,0:T(8,128)(2,1)} %refs_1_.2), custom_call_target="tpu_custom_call" | custom-call | tf_op jit(solution)/shard_map/pallas_call | solution.py:54
  28.6 14.0 %all-to-all-start = ((bf16[64,32,256]{2,1,0:T(8,128)(2,1)}), bf16[64,32,256]{2,1,0:T(8,128)(2,1)S(1)}, u32[]{:S(2)}, u32[]{:S(2)}) async-start(bf16[64,32,256]{2,1,0:T(8,128)(2,1)} %shard_map.199), calls=%async_computation | async-start | bytes 2097152 | tf_op jit(solution)/shard_map/all_to_all | solution.py:341
  42.7 0.0 copy-start.16
  42.7 0.0 copy-start.18
  42.7 0.0 copy-start.19
  42.7 2.9 %collective-permute-start = (bf16[32,2048]{1,0:T(8,128)(2,1)S(1)}, bf16[32,2048]{1,0:T(8,128)(2,1)S(1)}, u32[]{:S(2)}, u32[]{:S(2)}) collective-permute-start(bf16[32,2048]{1,0:T(8,128)(2,1)S(1)} %slice.3), channel_id=1, source_target_pairs={{0,8},{8,16},{16,24},{24,32},{32,40},{40,48},{48,56},{56,64},{64,7... | collective-permute-start | bytes 393224 | tf_op jit(solution)/shard_map/ppermute | solution.py:343
  45.7 0.1 pad_add_fusion.at
  45.8 0.3 copy.24.wref
  46.1 19.4 %collective-permute-done = bf16[32,2048]{1,0:T(8,128)(2,1)S(1)} collective-permute-done((bf16[32,2048]{1,0:T(8,128)(2,1)S(1)}, bf16[32,2048]{1,0:T(8,128)(2,1)S(1)}, u32[]{:S(2)}, u32[]{:S(2)}) %collective-permute-start) | collective-permute-done | bytes 131104 | tf_op jit(solution)/shard_map/ppermute | solution.py:343
  65.5 0.3 fusion
  65.8 1.6 fusion.2.nref
  67.5 0.0 copy-start.15
  67.5 1.7 %steps_of.1 = (f32[256,128]{1,0:T(8,128)S(1)}, f32[256,128]{1,0:T(8,128)S(1)}, f32[256,128]{1,0:T(8,128)S(1)}, f32[2,256]{1,0:T(2,128)S(1)}, f32[1,128]{1,0:T(1,128)S(1)}) custom-call(s32[4]{0:T(128)S(1)} %pad_add_fusion.at, f32[2]{0:T(128)S(1)} %copy-done.18, f32[2]{0:T(128)S(1)} %copy-done.19, bf16[288,2048]{1,0:T(8,128)(2,1)S(1)} %fusion.2.nref, ...), custom_call_target="tpu_custom_call" | custom-call | tf_op jit(solution)/shard_map/steps_of/pallas_call | solution.py:103
  69.2 0.7 all-to-all-done
  69.9 2.2 %local_states.1 = (bf16[8,136,128]{2,1,0:T(8,128)(2,1)}, bf16[256,128]{1,0:T(8,128)(2,1)S(1)}, bf16[256,128]{1,0:T(8,128)(2,1)S(1)}) custom-call(s32[4]{0:T(128)S(1)} %pad_add_fusion.at, bf16[288,2048]{1,0:T(8,128)(2,1)S(1)} %fusion.2.nref, bf16[2048,256]{1,0:T(8,128)(2,1)S(1)} %bitcast.9, f32[4,256]{1,0:T(4,128)S(1)} %pad_maximum_fusion.1.tref, ...), custom_call_target="tpu_custom_call" | custom-call | tf_op jit(solution)/shard_map/local_states/pallas_call | solution.py:131
  72.1 8.7 %all-to-all-start.1 = ((bf16[8,136,128]{2,1,0:T(8,128)(2,1)}), bf16[8,136,128]{2,1,0:T(8,128)(2,1)S(1)}, u32[]{:S(2)}, u32[]{:S(2)}) async-start(bf16[8,136,128]{2,1,0:T(8,128)(2,1)} %get-tuple-element.26), calls=%async_computation.1 | async-start | bytes 557056 | tf_op jit(solution)/shard_map/all_to_all | solution.py:350
  80.8 20.4 %all-gather.4.cloned.1.call-done.wref = bf16[2048,768]{1,0:T(8,128)(2,1)} async-done(((bf16[256,768]{1,0:T(8,128)(2,1)}), bf16[2048,768]{1,0:T(8,128)(2,1)}) %all-gather.4.cloned.1.call-update) | async-done | bytes 3145744 | tf_op jit(solution)/shard_map/all_gather | solution.py:339
  101.2 2.9 %rows_local.1 = (bf16[256,128]{1,0:T(8,128)(2,1)S(1)}, f32[256,128]{1,0:T(8,128)S(1)}, f32[256,128]{1,0:T(8,128)S(1)}, f32[256,128]{1,0:T(8,128)S(1)}, bf16[2048,256]{1,0:T(8,128)(2,1)S(1)}) custom-call(bf16[288,2048]{1,0:T(8,128)(2,1)S(1)} %fusion.2.nref, bf16[2048,768]{1,0:T(8,128)(2,1)} %all-gather.4.cloned.1.call-done.wref, f32[4,128]{1,0:T(4,128)S(1)} %copy-done.17, ...), custom_call_target="tpu_custom_call" | custom-call | tf_op jit(solution)/shard_map/rows_local/pallas_call | solution.py:231
  104.1 0.6 copy-done.2
  104.8 0.7 copy-done.4
  105.4 0.7 copy-done.6
  106.1 0.6 copy-done.9
  106.7 3.1 %collective-permute-start.1 = (bf16[2048,256]{1,0:T(8,128)(2,1)S(1)}, bf16[2048,256]{1,0:T(8,128)(2,1)S(1)}, u32[]{:S(2)}, u32[]{:S(2)}) collective-permute-start(bf16[2048,256]{1,0:T(8,128)(2,1)S(1)} %get-tuple-element.40.wa), channel_id=1, source_target_pairs={{0,1},{1,0},{2,3},{3,2},{4,5},{5,4},{6,7},{7,6},{8,9},{9,8},{10,11... | collective-permute-start | bytes 3145736 | tf_op jit(solution)/shard_map/ppermute | solution.py:354
  109.8 0.6 copy-done.12
  110.4 1.4 line_states.1
  111.8 3.9 %all-to-all-start.2 = ((bf16[8,136,128]{2,1,0:T(8,128)(2,1)}), bf16[8,136,128]{2,1,0:T(8,128)(2,1)S(1)}, u32[]{:S(2)}, u32[]{:S(2)}) async-start(bf16[8,136,128]{2,1,0:T(8,128)(2,1)} %get-tuple-element.27), calls=%async_computation.2 | async-start | bytes 557056 | tf_op jit(solution)/shard_map/all_to_all | solution.py:352
  115.7 1.8 %all-gather.1 = f32[2,1,128]{2,1,0:T(1,128)S(1)} all-gather(f32[1,1,128]{2,1,0:T(1,128)S(1)} %bitcast.13), channel_id=2, replica_groups=mesh['sp_0'=8,'sp_1'=8,'fs'=4,'tp'=2] {'tp'}, dimensions={0}, use_global_device_ids=true | all-gather | bytes 1536 | tf_op jit(solution)/shard_map/all_gather | solution.py:347
  117.5 10.9 %all-to-all-done.2.got = bf16[8,136,128]{2,1,0:T(8,128)(2,1)S(1)} async-done(((bf16[8,136,128]{2,1,0:T(8,128)(2,1)}), bf16[8,136,128]{2,1,0:T(8,128)(2,1)S(1)}, u32[]{:S(2)}, u32[]{:S(2)}) %all-to-all-start.2) | async-done | bytes 278560 | tf_op jit(solution)/shard_map/all_to_all | solution.py:352
  128.5 0.9 copy-done.1
  129.4 0.9 copy-done.3
  130.3 0.9 copy-done.5
  131.2 0.9 copy-done.7
  132.1 0.8 copy-done.8
  132.9 0.8 copy-done.10
  133.8 0.6 copy-done.13
  134.4 0.7 copy-done.20
  135.0 1.8 %rows_done.1 = (f32[8,3,256]{2,1,0:T(4,128)}, bf16[256,384]{1,0:T(8,128)(2,1)S(1)}) custom-call(s32[4]{0:T(128)S(1)} %copy-done.13, bf16[8,136,128]{2,1,0:T(8,128)(2,1)S(1)} %all-to-all-done.2.got, f32[128,128]{1,0:T(8,128)S(1)} %get-tuple-element.28.enter, f32[8,128]{1,0:T(8,128)S(1)} %get-tuple-element.29.before, f32[2,64,128]{2,1,0:T(8,128)S(1)} %copy-done.8, ...), custom_call_target="tpu_custom_call" | custom-call | tf_op jit(solution)/shard_map/rows_done/pallas_call | solution.py:276
  136.8 4.7 %all-to-all-start.4 = ((f32[8,3,256]{2,1,0:T(4,128)}), f32[8,3,256]{2,1,0:T(4,128)S(1)}, u32[]{:S(2)}, u32[]{:S(2)}) async-start(f32[8,3,256]{2,1,0:T(4,128)} %get-tuple-element.38), calls=%async_computation.4 | async-start | bytes 65536 | tf_op jit(solution)/shard_map/all_to_all | solution.py:358
  141.6 2.1 %all_gather.13.bref = bf16[512,384]{1,0:T(8,128)(2,1)S(1)} all-gather(bf16[256,384]{1,0:T(8,128)(2,1)S(1)} %get-tuple-element.39), channel_id=1, replica_groups=mesh['sp_0'=8,'sp_1'=8,'fs'=4,'tp'=2] {'tp'}, dimensions={0}, use_global_device_ids=true | all-gather | bytes 589824 | tf_op jit(solution)/shard_map/all_gather | solution.py:359
  143.6 2.6 %all-to-all-done.4.sref = f32[8,3,256]{2,1,0:T(4,128)S(1)} async-done(((f32[8,3,256]{2,1,0:T(4,128)}), f32[8,3,256]{2,1,0:T(4,128)S(1)}, u32[]{:S(2)}, u32[]{:S(2)}) %all-to-all-start.4) | async-done | bytes 24608 | tf_op jit(solution)/shard_map/all_to_all | solution.py:358
  146.3 1.6 output_rows.1
  147.9 10.9 %all_to_all.31 = bf16[4,32,2048]{2,1,0:T(8,128)(2,1)S(1)} all-to-all(bf16[4,32,2048]{2,1,0:T(8,128)(2,1)S(1)} %output_rows.1), channel_id=1, replica_groups=mesh['sp_0'=8,'sp_1'=8,'fs'=4,'tp'=2] {'fs'}, dimensions={0} | all-to-all | bytes 1048576 | tf_op jit(solution)/shard_map/all_to_all | solution.py:361
  158.8 0.7 reduce_sum.22
  (41 shorter events, 0.1 us)
Async XLA Ops:
  6.5 36.2 %copy-start.21 = (bf16[256,2048]{1,0:T(8,128)(2,1)S(1)}, bf16[256,2048]{1,0:T(8,128)(2,1)}, u32[]{:S(2)}) copy-start(bf16[256,2048]{1,0:T(8,128)(2,1)} %param.21) | copy-start | bytes 3145732
  6.5 94.7 %all-gather.4.cloned.1.call-start = ((), (), s32[]{:S(2)}) async-start(), calls=%async_computation.6 | async-start | bytes 3538944 | tf_op jit(solution)/shard_map/all_gather | solution.py:339
  7.5 38.3 %copy-start.22 = (bf16[2048,16]{0,1:T(8,128)(2,1)S(1)}, bf16[2048,16]{0,1:T(8,128)(2,1)}, u32[]{:S(2)}) copy-start(bf16[2048,16]{0,1:T(8,128)(2,1)} %param.29) | copy-start | bytes 196612
  26.6 19.4 %copy-start.24 = (f32[4,128]{1,0:T(4,128)S(1)}, f32[4,128]{1,0:T(4,128)}, u32[]{:S(2)}) copy-start(f32[4,128]{1,0:T(4,128)} %param.34) | copy-start | bytes 6148
  26.6 19.4 %copy-start.25 = (f32[4,128]{1,0:T(4,128)S(1)}, f32[4,128]{1,0:T(4,128)}, u32[]{:S(2)}) copy-start(f32[4,128]{1,0:T(4,128)} %param.33) | copy-start | bytes 6148
  26.7 39.2 %copy-start.23 = (f32[2048]{0:T(1024)S(1)}, f32[2048]{0:T(1024)}, u32[]{:S(2)}) copy-start(f32[2048]{0:T(1024)} %param.22) | copy-start | bytes 24580
  28.6 41.3 %all-to-all-start = ((bf16[64,32,256]{2,1,0:T(8,128)(2,1)}), bf16[64,32,256]{2,1,0:T(8,128)(2,1)S(1)}, u32[]{:S(2)}, u32[]{:S(2)}) async-start(bf16[64,32,256]{2,1,0:T(8,128)(2,1)} %shard_map.199), calls=%async_computation | async-start | bytes 2097152 | tf_op jit(solution)/shard_map/all_to_all | solution.py:341
  42.7 24.7 %copy-start.16 = (f32[2,256]{1,0:T(2,128)S(1)}, f32[2,256]{1,0:T(2,128)}, u32[]{:S(2)}) copy-start(f32[2,256]{1,0:T(2,128)} %eref.1) | copy-start | bytes 6148
  42.7 24.7 %copy-start.18 = (f32[2]{0:T(128)S(1)}, f32[2]{0:T(128)}, u32[]{:S(2)}) copy-start(f32[2]{0:T(128)} %bref.1) | copy-start | bytes 28
  42.7 24.7 %copy-start.19 = (f32[2]{0:T(128)S(1)}, f32[2]{0:T(128)}, u32[]{:S(2)}) copy-start(f32[2]{0:T(128)} %rref.1) | copy-start | bytes 28
  42.7 22.8 %collective-permute-start = (bf16[32,2048]{1,0:T(8,128)(2,1)S(1)}, bf16[32,2048]{1,0:T(8,128)(2,1)S(1)}, u32[]{:S(2)}, u32[]{:S(2)}) collective-permute-start(bf16[32,2048]{1,0:T(8,128)(2,1)S(1)} %slice.3), channel_id=1, source_target_pairs={{0,8},{8,16},{16,24},{24,32},{32,40},{40,48},{48,56},{56,64},{64,7... | collective-permute-start | bytes 393224 | tf_op jit(solution)/shard_map/ppermute | solution.py:343
  45.8 24.2 %copy-start.11 = (s32[4]{0:T(128)}, s32[4]{0:T(128)S(1)}, u32[]{:S(2)}) copy-start(s32[4]{0:T(128)S(1)} %pad_add_fusion.at) | copy-start | bytes 52
  67.5 33.8 %copy-start.15 = (f32[31,128]{1,0:T(8,128)S(1)}, f32[31,128]{1,0:T(8,128)}, u32[]{:S(2)}) copy-start(f32[31,128]{1,0:T(8,128)} %ltaps.1) | copy-start | bytes 47620
  67.5 33.8 %copy-start.17 = (f32[4,128]{1,0:T(4,128)S(1)}, f32[4,128]{1,0:T(4,128)}, u32[]{:S(2)}) copy-start(f32[4,128]{1,0:T(4,128)} %ftaps.1) | copy-start | bytes 6148
  69.2 34.9 %copy-start = (f32[256,128]{1,0:T(8,128)}, f32[256,128]{1,0:T(8,128)S(1)}, u32[]{:S(2)}) copy-start(f32[256,128]{1,0:T(8,128)S(1)} %get-tuple-element.32.cum) | copy-start | bytes 393220
  72.1 37.7 %all-to-all-start.1 = ((bf16[8,136,128]{2,1,0:T(8,128)(2,1)}), bf16[8,136,128]{2,1,0:T(8,128)(2,1)S(1)}, u32[]{:S(2)}, u32[]{:S(2)}) async-start(bf16[8,136,128]{2,1,0:T(8,128)(2,1)} %get-tuple-element.26), calls=%async_computation.1 | async-start | bytes 557056 | tf_op jit(solution)/shard_map/all_to_all | solution.py:350
  101.2 14.5 %copy-start.26 = (f32[128]{0:T(128)S(1)}, f32[128]{0:T(128)}, u32[]{:S(2)}) copy-start(f32[128]{0:T(128)} %param.37) | copy-start | bytes 1540
  104.1 0.7 copy-start.2
  104.8 0.7 copy-start.4
  105.4 0.7 copy-start.6
  106.1 0.6 copy-start.9
  106.7 39.6 %copy-start.14 = (s32[4]{0:T(128)S(1)}, s32[4]{0:T(128)}, u32[]{:S(2)}) copy-start(s32[4]{0:T(128)} %copy-done.11) | copy-start | bytes 52
  106.7 39.6 %collective-permute-start.1 = (bf16[2048,256]{1,0:T(8,128)(2,1)S(1)}, bf16[2048,256]{1,0:T(8,128)(2,1)S(1)}, u32[]{:S(2)}, u32[]{:S(2)}) collective-permute-start(bf16[2048,256]{1,0:T(8,128)(2,1)S(1)} %get-tuple-element.40.wa), channel_id=1, source_target_pairs={{0,1},{1,0},{2,3},{3,2},{4,5},{5,4},{6,7},{7,6},{8,9},{9,8},{10,11... | collective-permute-start | bytes 3145736 | tf_op jit(solution)/shard_map/ppermute | solution.py:354
  109.8 0.6 copy-start.12
  111.8 16.6 %all-to-all-start.2 = ((bf16[8,136,128]{2,1,0:T(8,128)(2,1)}), bf16[8,136,128]{2,1,0:T(8,128)(2,1)S(1)}, u32[]{:S(2)}, u32[]{:S(2)}) async-start(bf16[8,136,128]{2,1,0:T(8,128)(2,1)} %get-tuple-element.27), calls=%async_computation.2 | async-start | bytes 557056 | tf_op jit(solution)/shard_map/all_to_all | solution.py:352
  128.4 0.9 copy-start.1
  129.4 0.9 copy-start.3
  130.3 0.9 copy-start.5
  131.2 0.9 copy-start.7
  132.1 0.8 copy-start.8
  132.9 0.8 copy-start.10
  133.7 0.6 copy-start.13
  134.4 0.7 copy-start.20
  136.8 9.5 %all-to-all-start.4 = ((f32[8,3,256]{2,1,0:T(4,128)}), f32[8,3,256]{2,1,0:T(4,128)S(1)}, u32[]{:S(2)}, u32[]{:S(2)}) async-start(f32[8,3,256]{2,1,0:T(4,128)} %get-tuple-element.38), calls=%async_computation.4 | async-start | bytes 65536 | tf_op jit(solution)/shard_map/all_to_all | solution.py:358
Sparse Core Ops, SparseCore 0:
  26.8 74.4 all-gather.3

commit v12 on v11

--- a/solution.py
+++ b/solution.py
@@ -70,12 +70,12 @@
     ch = heads * p
     every = step_proj.shape[1]
 
-    def body(at, bref, rref, nref, wref, eref, step, left, cum, cum_t, total):
+    def body(iz, iy, shard, tp, bref, rref, nref, wref, eref, step, left, cum, cum_t, total, at):
         raw = dot(wref[...], nref[HALO:, :], 0, 1)
         which = lax.broadcasted_iota(jnp.int32, (every, rows), 0)
         size, logs = [], []
         for h in range(heads):
-            x = jnp.sum(jnp.where(which == at[3] * heads + h, raw, 0.0), axis=0, keepdims=True) + bref[h]
+            x = jnp.sum(jnp.where(which == shard[0] * heads + h, raw, 0.0), axis=0, keepdims=True) + bref[h]
             size.append(jnp.maximum(x, 0.0) + jnp.log1p(jnp.exp(-jnp.abs(x))))
             logs.append(-jnp.exp(jnp.full((1, rows), rref[h], f32)) * size[h] + eref[h : h + 1, :])
         none = [jnp.zeros((8 - heads, rows), f32)]
@@ -98,22 +98,27 @@
         for h in range(heads):
             ends = jnp.where(place == h, run[h : h + 1, rows - 1 :], ends)
         total[...] = ends
+        row = lax.broadcasted_iota(jnp.int32, (8, STATE), 0)
+        at[...] = jnp.where(row == 0, iz[0], jnp.where(row == 1, iy[0], tp[0]))
 
     wide = pltpu.VMEM((rows, ch), f32)
     return pl.pallas_call(
         body,
-        out_shape=(wide, wide, wide, pltpu.VMEM((heads, rows), f32), pltpu.VMEM((1, STATE), f32)),
-        in_specs=[SMEM, SMEM, SMEM, VMEM, VMEM, VMEM],
-        out_specs=(VMEM,) * 5,
+        out_shape=(
+            wide, wide, wide, pltpu.VMEM((heads, rows), f32), pltpu.VMEM((1, STATE), f32),
+            pltpu.VMEM((8, STATE), jnp.int32),
+        ),
+        in_specs=[*[SMEM] * 6, VMEM, VMEM, VMEM],
+        out_specs=(VMEM,) * 6,
         compiler_params=SMALL, name="steps_of",
-    )(index, bias, rate_log, *held(own, step_proj, extra))
-
-
-def local_states(normed, first, taps, step, left, total, index, copies):
+    )(*index, bias, rate_log, *held(own, step_proj, extra))
+
+
+def local_states(normed, first, taps, step, left, total, copies):
     ext, _ = normed.shape
     rows, ch = step.shape
 
-    def body(at, nref, wref, tref, sref, lref, logs, send, xs, w16, buf):
+    def body(nref, wref, tref, sref, lref, logs, send, xs, w16, buf):
         buf[...] = dot(nref[...], wref[...], 1, 0).astype(bf16).astype(f32)
         at = HALO - SHORT + 1
         mix = sum(buf[at + i : at + i + rows, :] * tref[i : i + 1, :] for i in range(SHORT))
@@ -131,11 +136,11 @@
     return pl.pallas_call(
         body,
         out_shape=(sds((copies, ch + LOGS, STATE), bf16), pltpu.VMEM((rows, ch), bf16), pltpu.VMEM((rows, STATE), bf16)),
-        in_specs=[SMEM, *[VMEM] * 6],
+        in_specs=[VMEM] * 6,
         out_specs=(VMEM,) * 3,
         scratch_shapes=[pltpu.VMEM((ext, 2 * ch), f32)],
         compiler_params=SMALL, name="local_states",
-    )(index, *held(normed, first, taps, step, left, total))
+    )(*held(normed, first, taps, step, left, total))
 
 
 def spread_heads(c, heads, p):
@@ -153,7 +158,7 @@
         tot = jnp.zeros((ch, STATE), f32)
         for k in reversed(range(n)):
             logs = jnp.sum(ref[k, ch:, :].astype(f32), axis=0, keepdims=True)
-            inside = (k < at[1]).astype(f32)
+            inside = jnp.where(k < at[1:2, :], 1.0, 0.0)
             piece = ref[k, :ch, :].astype(f32)
             ent = ent + piece * spread_heads(inside * jnp.exp(acc_in), heads, p)
             tot = tot + piece * spread_heads(jnp.exp(acc_all), heads, p)
@@ -169,10 +174,10 @@
     return pl.pallas_call(
         body,
         out_shape=(pltpu.VMEM((ch, STATE), f32), pltpu.VMEM((8, STATE), f32), sds((copies, size, STATE), bf16)),
-        in_specs=[SMEM, VMEM],
+        in_specs=[VMEM, VMEM],
         out_specs=(VMEM,) * 3,
         compiler_params=SMALL, name="line_states",
-    )(index, *held(got))
+    )(*held(index, got))
 
 
 def rows_local(normed, rest, ftaps, ltaps, xs, w16, cum, cum_t):
@@ -256,16 +261,15 @@
         b = before[0:1, :]
         for j in reversed(range(n)):
             logs = jnp.sum(got[j, ch:, :].astype(f32), axis=0, keepdims=True)
-            inside = (j < at[0]).astype(f32)
+            inside = jnp.where(j < at[0:1, :], 1.0, 0.0)
             start = start + got[j, :ch, :].astype(f32) * spread_heads(inside * jnp.exp(acc_in + b), heads, p)
             acc_in = acc_in + inside * logs
         start = start + init[...].reshape(ch, STATE) * spread_heads(jnp.exp(acc_in + b), heads, p)
         y = inner[...] + dot(read16[...], start.astype(bf16), 1, 1) * jnp.exp(cum[...])
         gated = y * zgate[...]
         mix = mixed[...]
-        squares = jnp.concatenate([mix, mix * mix, gated * gated], 1)
-        pick = lax.broadcasted_iota(jnp.int32, (8, 3 * ch), 1) // ch == lax.broadcasted_iota(jnp.int32, (8, 3 * ch), 0)
-        found = dot(jnp.where(pick, 1.0, 0.0), squares, 1, 1, HIGHEST)
+        cols = [jnp.sum(v, axis=1, keepdims=True) for v in (mix, mix * mix, gated * gated)]
+        found = jnp.transpose(jnp.concatenate([*cols, jnp.zeros((rows, 5), f32)], 1))
         for j in range(copies):
             sums[j] = found[:3]
         high = mix.astype(bf16)
@@ -276,10 +280,10 @@
     return pl.pallas_call(
         body,
         out_shape=(sds((copies, 3, rows), f32), pltpu.VMEM((rows, 3 * ch), bf16)),
-        in_specs=[SMEM, *[VMEM] * 10],
+        in_specs=[VMEM] * 11,
         out_specs=(VMEM, VMEM),
         compiler_params=SMALL, name="rows_done",
-    )(index, *held(got, enter, before, init, read16, zgate, mixed, inner, cum, gain))
+    )(*held(index, got, enter, before, init, read16, zgate, mixed, inner, cum, gain))
 
 
 def output_rows(sums, both, gains, own, other, index, nf, nt):
@@ -289,7 +293,7 @@
     piece = rows // (nf * nt)
 
     def body(at, sref, bref, gref, wa, wb, out, cols, act):
-        tp = at[2]
+        tp = at[2, 0]
         s = sref[0]
         for j in range(1, copies):
             s = s + sref[j]
@@ -314,11 +318,11 @@
     return pl.pallas_call(
         body,
         out_shape=sds((nf, piece, d), bf16),
-        in_specs=[SMEM, *[VMEM] * 5],
+        in_specs=[VMEM] * 6,
         out_specs=VMEM,
         scratch_shapes=[pltpu.VMEM((rows, 8), f32), pltpu.VMEM((nf * piece, 4 * ch), bf16)],
         compiler_params=SMALL, name="output_rows",
-    )(index, *held(sums, both, gains, own, other))
+    )(*held(index, sums, both, gains, own, other))
 
 
 def per_device(
@@ -331,8 +335,7 @@
     heads = step_bias.shape[0]
     p = ch // heads
     nf, nt = lax.axis_size("fs"), lax.axis_size("tp")
-    iz, iy, tp = (lax.axis_index(a).astype(jnp.int32) for a in ("sp_0", "sp_1", "tp"))
-    at = jnp.stack([iz, iy, tp, lax.axis_index("fs").astype(jnp.int32) * nt + tp])
+    iz, iy, ix, tp = (lax.axis_index(a).astype(jnp.int32).reshape(1) for a in ("sp_0", "sp_1", "fs", "tp"))
     ny = lax.axis_size("sp_1")
     rest = lay_out((state_read, mixer_gate, conv_value, conv_gate, conv_output, state_output), ny)
     rest = lax.all_to_all(rest, "sp_1", 0, 0, tiled=True).reshape(-1, 6 * ch)
@@ -343,10 +346,12 @@
     halo = lax.ppermute(tokens[rows - HALO :], SP, [(i, i + 1) for i in range(n - 1)])
     v = jnp.concatenate([halo, tokens], 0).astype(f32)
     normed = (v * lax.rsqrt(jnp.mean(v * v, axis=1, keepdims=True) + EPS) * norm_gain).astype(bf16)
-    step, left, cum, cum_t, total = steps_of(normed, step_proj, decay_extra, step_bias, decay_log, at, p)
+    step, left, cum, cum_t, total, at = steps_of(
+        normed, step_proj, decay_extra, step_bias, decay_log, (iz, iy, ix * nt + tp, tp), p
+    )
     gains = lax.all_gather(conv_gain, "tp")
     taps = jnp.concatenate([input_taps, write_taps], 1)
-    send, xs, w16 = local_states(normed, first, taps, step, left, total, at, ny)
+    send, xs, w16 = local_states(normed, first, taps, step, left, total, ny)
     got = lax.all_to_all(send, "sp_1", 0, 0, tiled=True)
     enter, before, send = line_states(got, at, heads, p, lax.axis_size("sp_0"))
     got = lax.all_to_all(send, "sp_0", 0, 0, tiled=True)

time: 167 us -> 166 us (level)
  Pallas kernels: 14.5 us -> 12.2 us
  transfers between devices with their start and end apart: 7 -> 7, of which waited for: 5 -> 5; matrix products, arithmetic and copies ran while one was open for 1% -> 1% of each run, Pallas kernels for 7% -> 6%
where the time goes in v12:
time: 166 us; the launch traced here: 165 us
  waiting for transfers between devices  53.6 us (32%)
  starting transfers between devices  37.8 us (23%)
  blocking collectives  34 us (20%)
  between operations  13.7 us (8%)
  Pallas kernels  12.2 us (7%)
  local copies, waits for them, and re-layouts  11.5 us (7%)
  other arithmetic  2.64 us (2%)
    all_gather x1, waiting for transfers between devices, per_device(): rest = lax.all_gather(rest, 'sp_0', axis=0, tiled=True)  20.4 us
    ppermute x1, waiting for transfers between devices, per_device(): lax.ppermute(tokens[rows - HALO:], SP, [(i, i + 1) for i in range(n - 1)])  19.5 us
    all_to_all x1, blocking collectives, per_device(): rest = lax.all_to_all(rest, 'sp_1', 0, 0, tiled=True).reshape(-1, 6 * ch)  19.2 us
    all_to_all x1, starting transfers between devices, per_device(): first = lax.all_to_all(first, SP, 0, 0, tiled=True).reshape(-1, 2 * ch)  14 us
    unnamed x55, local copies, waits for them, and re-layouts  11.4 us
    all_to_all x1, blocking collectives, per_device(): pieces = lax.all_to_all(out, 'fs', 0, 0, tiled=True)  10.9 us
    all_to_all x1, waiting for transfers between devices, per_device(): got = lax.all_to_all(send, 'sp_0', 0, 0, tiled=True)  10.9 us
    all_to_all x1, starting transfers between devices, per_device(): got = lax.all_to_all(send, 'sp_1', 0, 0, tiled=True)  9.28 us
  transfers between devices with their start and end apart: 7, of which 5 were waited for; matrix products, arithmetic and copies ran while one was open for 1% of the time, Pallas kernels for 6%

profile of v12, /device:TPU:1, one launch (start us, length us, event | category | flops | bytes accessed | tf_op | source)
XLA Modules:
  0.0 165.3 jit_solution(9951329835238074534)
XLA Ops:
  6.5 0.9 shard_map.200
  7.5 0.0 copy-start.22
  7.5 19.2 %all_to_all.30 = bf16[8,32,768]{2,1,0:T(8,128)(2,1)} all-to-all(bf16[8,32,768]{2,1,0:T(8,128)(2,1)S(1)} %shard_map.200), channel_id=1, replica_groups=mesh['sp_0'=8,'sp_1'=8,'fs'=4,'tp'=2] {'sp_1'}, dimensions={0} | all-to-all | bytes 786432 | tf_op jit(solution)/shard_map/all_to_all | solution.py:341
  26.6 0.0 all-gather.4.cloned.1.call-update
  26.7 0.0 copy-start.23
  26.7 2.0 %shard_map.199 = bf16[64,32,256]{2,1,0:T(8,128)(2,1)} custom-call(bf16[32,128]{1,0:T(8,128)(2,1)} %refs_0_.2, bf16[32,128]{1,0:T(8,128)(2,1)} %refs_1_.2), custom_call_target="tpu_custom_call" | custom-call | tf_op jit(solution)/shard_map/pallas_call | solution.py:54
  28.6 14.0 %all-to-all-start = ((bf16[64,32,256]{2,1,0:T(8,128)(2,1)}), bf16[64,32,256]{2,1,0:T(8,128)(2,1)S(1)}, u32[]{:S(2)}, u32[]{:S(2)}) async-start(bf16[64,32,256]{2,1,0:T(8,128)(2,1)} %shard_map.199), calls=%async_computation | async-start | bytes 2097152 | tf_op jit(solution)/shard_map/all_to_all | solution.py:344
  42.7 0.0 copy-start.16
  42.7 0.0 copy-start.19
  42.7 0.0 copy-start.20
  42.7 2.9 %collective-permute-start = (bf16[32,2048]{1,0:T(8,128)(2,1)S(1)}, bf16[32,2048]{1,0:T(8,128)(2,1)S(1)}, u32[]{:S(2)}, u32[]{:S(2)}) collective-permute-start(bf16[32,2048]{1,0:T(8,128)(2,1)S(1)} %slice.3), channel_id=1, source_target_pairs={{0,8},{8,16},{16,24},{24,32},{32,40},{40,48},{48,56},{56,64},{64,7... | collective-permute-start | bytes 393224 | tf_op jit(solution)/shard_map/ppermute | solution.py:346
  45.7 0.3 copy.24.wref
  46.0 19.5 %collective-permute-done = bf16[32,2048]{1,0:T(8,128)(2,1)S(1)} collective-permute-done((bf16[32,2048]{1,0:T(8,128)(2,1)S(1)}, bf16[32,2048]{1,0:T(8,128)(2,1)S(1)}, u32[]{:S(2)}, u32[]{:S(2)}) %collective-permute-start) | collective-permute-done | bytes 131104 | tf_op jit(solution)/shard_map/ppermute | solution.py:346
  65.5 0.3 fusion
  65.8 1.6 fusion.2.nref
  67.5 1.7 %steps_of.1 = (f32[256,128]{1,0:T(8,128)S(1)}, f32[256,128]{1,0:T(8,128)S(1)}, f32[256,128]{1,0:T(8,128)S(1)}, f32[2,256]{1,0:T(2,128)S(1)}, f32[1,128]{1,0:T(1,128)S(1)}, /*index=5*/s32[8,128]{1,0:T(8,128)S(1)}) custom-call(s32[1]{0:T(128)} %bitcast.iz, s32[1]{0:T(128)} %bitcast.1.iy, s32[1]{0:T(128)S(6)} %add.14.shard, s32[1]{0:T(128)} %bitcast.3.tp, ...), custom_call_target="tpu_custom_call" | custom-call | tf_op jit(solution)/shard_map/steps_of/pallas_call | solution.py:105
  69.2 0.6 copy-done.11
  69.8 0.1 all-to-all-done
  69.9 1.6 local_states.1
  71.6 9.3 %all-to-all-start.1 = ((bf16[8,136,128]{2,1,0:T(8,128)(2,1)}), bf16[8,136,128]{2,1,0:T(8,128)(2,1)S(1)}, u32[]{:S(2)}, u32[]{:S(2)}) async-start(bf16[8,136,128]{2,1,0:T(8,128)(2,1)} %get-tuple-element.28), calls=%async_computation.1 | async-start | bytes 557056 | tf_op jit(solution)/shard_map/all_to_all | solution.py:355
  80.9 20.4 %all-gather.4.cloned.1.call-done.wref = bf16[2048,768]{1,0:T(8,128)(2,1)} async-done(((bf16[256,768]{1,0:T(8,128)(2,1)}), bf16[2048,768]{1,0:T(8,128)(2,1)}) %all-gather.4.cloned.1.call-update) | async-done | bytes 3145744 | tf_op jit(solution)/shard_map/all_gather | solution.py:342
  101.2 2.9 %rows_local.1 = (bf16[256,128]{1,0:T(8,128)(2,1)S(1)}, f32[256,128]{1,0:T(8,128)S(1)}, f32[256,128]{1,0:T(8,128)S(1)}, f32[256,128]{1,0:T(8,128)S(1)}, bf16[2048,256]{1,0:T(8,128)(2,1)S(1)}) custom-call(bf16[288,2048]{1,0:T(8,128)(2,1)S(1)} %fusion.2.nref, bf16[2048,768]{1,0:T(8,128)(2,1)} %all-gather.4.cloned.1.call-done.wref, f32[4,128]{1,0:T(4,128)S(1)} %copy-done.17, ...), custom_call_target="tpu_custom_call" | custom-call | tf_op jit(solution)/shard_map/rows_local/pallas_call | solution.py:236
  104.1 0.6 copy-done.2
  104.8 0.7 copy-done.4
  105.4 0.7 copy-done.6
  106.1 0.6 copy-done.9
  106.7 2.9 %collective-permute-start.1 = (bf16[2048,256]{1,0:T(8,128)(2,1)S(1)}, bf16[2048,256]{1,0:T(8,128)(2,1)S(1)}, u32[]{:S(2)}, u32[]{:S(2)}) collective-permute-start(bf16[2048,256]{1,0:T(8,128)(2,1)S(1)} %get-tuple-element.42.wa), channel_id=1, source_target_pairs={{0,1},{1,0},{2,3},{3,2},{4,5},{5,4},{6,7},{7,6},{8,9},{9,8},{10,11... | collective-permute-start | bytes 3145736 | tf_op jit(solution)/shard_map/ppermute | solution.py:359
  109.7 0.7 copy-done.12
  110.3 0.9 line_states.1
  111.2 3.9 %all-to-all-start.2 = ((bf16[8,136,128]{2,1,0:T(8,128)(2,1)}), bf16[8,136,128]{2,1,0:T(8,128)(2,1)S(1)}, u32[]{:S(2)}, u32[]{:S(2)}) async-start(bf16[8,136,128]{2,1,0:T(8,128)(2,1)} %get-tuple-element.29), calls=%async_computation.2 | async-start | bytes 557056 | tf_op jit(solution)/shard_map/all_to_all | solution.py:357
  115.1 1.8 %all-gather.1 = f32[2,1,128]{2,1,0:T(1,128)S(1)} all-gather(f32[1,1,128]{2,1,0:T(1,128)S(1)} %bitcast.13), channel_id=2, replica_groups=mesh['sp_0'=8,'sp_1'=8,'fs'=4,'tp'=2] {'tp'}, dimensions={0}, use_global_device_ids=true | all-gather | bytes 1536 | tf_op jit(solution)/shard_map/all_gather | solution.py:352
  116.9 10.9 %all-to-all-done.2.got = bf16[8,136,128]{2,1,0:T(8,128)(2,1)S(1)} async-done(((bf16[8,136,128]{2,1,0:T(8,128)(2,1)}), bf16[8,136,128]{2,1,0:T(8,128)(2,1)S(1)}, u32[]{:S(2)}, u32[]{:S(2)}) %all-to-all-start.2) | async-done | bytes 278560 | tf_op jit(solution)/shard_map/all_to_all | solution.py:357
  127.8 0.9 copy-done.1
  128.7 0.9 copy-done.3
  129.6 0.9 copy-done.5
  130.5 0.9 copy-done.7
  131.5 0.8 copy-done.8
  132.3 0.8 copy-done.10
  133.1 0.7 copy-done.13
  133.8 0.7 copy-done.18
  134.5 1.1 rows_done.1
  135.5 4.7 %all-to-all-start.4 = ((f32[8,3,256]{2,1,0:T(4,128)}), f32[8,3,256]{2,1,0:T(4,128)S(1)}, u32[]{:S(2)}, u32[]{:S(2)}) async-start(f32[8,3,256]{2,1,0:T(4,128)} %get-tuple-element.40), calls=%async_computation.4 | async-start | bytes 65536 | tf_op jit(solution)/shard_map/all_to_all | solution.py:363
  140.3 2.1 %all_gather.13.bref = bf16[512,384]{1,0:T(8,128)(2,1)S(1)} all-gather(bf16[256,384]{1,0:T(8,128)(2,1)S(1)} %get-tuple-element.41), channel_id=1, replica_groups=mesh['sp_0'=8,'sp_1'=8,'fs'=4,'tp'=2] {'tp'}, dimensions={0}, use_global_device_ids=true | all-gather | bytes 589824 | tf_op jit(solution)/shard_map/all_gather | solution.py:364
  142.4 2.6 %all-to-all-done.4.sref = f32[8,3,256]{2,1,0:T(4,128)S(1)} async-done(((f32[8,3,256]{2,1,0:T(4,128)}), f32[8,3,256]{2,1,0:T(4,128)S(1)}, u32[]{:S(2)}, u32[]{:S(2)}) %all-to-all-start.4) | async-done | bytes 24608 | tf_op jit(solution)/shard_map/all_to_all | solution.py:363
  145.0 0.7 copy-done.14
  145.7 1.1 output_rows.1
  146.8 10.9 %all_to_all.31 = bf16[4,32,2048]{2,1,0:T(8,128)(2,1)S(1)} all-to-all(bf16[4,32,2048]{2,1,0:T(8,128)(2,1)S(1)} %output_rows.1), channel_id=1, replica_groups=mesh['sp_0'=8,'sp_1'=8,'fs'=4,'tp'=2] {'fs'}, dimensions={0} | all-to-all | bytes 1048576 | tf_op jit(solution)/shard_map/all_to_all | solution.py:366
  157.7 0.7 reduce_sum.22
  (40 shorter events, 0.1 us)
Async XLA Ops:
  6.5 36.2 %copy-start.21 = (bf16[256,2048]{1,0:T(8,128)(2,1)S(1)}, bf16[256,2048]{1,0:T(8,128)(2,1)}, u32[]{:S(2)}) copy-start(bf16[256,2048]{1,0:T(8,128)(2,1)} %param.21) | copy-start | bytes 3145732
  6.5 94.7 %all-gather.4.cloned.1.call-start = ((), (), s32[]{:S(2)}) async-start(), calls=%async_computation.6 | async-start | bytes 3538944 | tf_op jit(solution)/shard_map/all_gather | solution.py:342
  7.5 38.2 %copy-start.22 = (bf16[2048,16]{0,1:T(8,128)(2,1)S(1)}, bf16[2048,16]{0,1:T(8,128)(2,1)}, u32[]{:S(2)}) copy-start(bf16[2048,16]{0,1:T(8,128)(2,1)} %param.29) | copy-start | bytes 196612
  26.6 19.4 %copy-start.24 = (f32[4,128]{1,0:T(4,128)S(1)}, f32[4,128]{1,0:T(4,128)}, u32[]{:S(2)}) copy-start(f32[4,128]{1,0:T(4,128)} %param.34) | copy-start | bytes 6148
  26.6 19.4 %copy-start.25 = (f32[4,128]{1,0:T(4,128)S(1)}, f32[4,128]{1,0:T(4,128)}, u32[]{:S(2)}) copy-start(f32[4,128]{1,0:T(4,128)} %param.33) | copy-start | bytes 6148
  26.7 39.2 %copy-start.23 = (f32[2048]{0:T(1024)S(1)}, f32[2048]{0:T(1024)}, u32[]{:S(2)}) copy-start(f32[2048]{0:T(1024)} %param.22) | copy-start | bytes 24580
  28.6 41.3 %all-to-all-start = ((bf16[64,32,256]{2,1,0:T(8,128)(2,1)}), bf16[64,32,256]{2,1,0:T(8,128)(2,1)S(1)}, u32[]{:S(2)}, u32[]{:S(2)}) async-start(bf16[64,32,256]{2,1,0:T(8,128)(2,1)} %shard_map.199), calls=%async_computation | async-start | bytes 2097152 | tf_op jit(solution)/shard_map/all_to_all | solution.py:344
  42.7 24.7 %copy-start.16 = (f32[2,256]{1,0:T(2,128)S(1)}, f32[2,256]{1,0:T(2,128)}, u32[]{:S(2)}) copy-start(f32[2,256]{1,0:T(2,128)} %eref.1) | copy-start | bytes 6148
  42.7 24.7 %copy-start.19 = (f32[2]{0:T(128)S(1)}, f32[2]{0:T(128)}, u32[]{:S(2)}) copy-start(f32[2]{0:T(128)} %bref.1) | copy-start | bytes 28
  42.7 24.7 %copy-start.20 = (f32[2]{0:T(128)S(1)}, f32[2]{0:T(128)}, u32[]{:S(2)}) copy-start(f32[2]{0:T(128)} %rref.1) | copy-start | bytes 28
  42.7 22.8 %collective-permute-start = (bf16[32,2048]{1,0:T(8,128)(2,1)S(1)}, bf16[32,2048]{1,0:T(8,128)(2,1)S(1)}, u32[]{:S(2)}, u32[]{:S(2)}) collective-permute-start(bf16[32,2048]{1,0:T(8,128)(2,1)S(1)} %slice.3), channel_id=1, source_target_pairs={{0,8},{8,16},{16,24},{24,32},{32,40},{40,48},{48,56},{56,64},{64,7... | collective-permute-start | bytes 393224 | tf_op jit(solution)/shard_map/ppermute | solution.py:346
  67.5 33.8 %copy-start.15 = (f32[31,128]{1,0:T(8,128)S(1)}, f32[31,128]{1,0:T(8,128)}, u32[]{:S(2)}) copy-start(f32[31,128]{1,0:T(8,128)} %ltaps.1) | copy-start | bytes 47620
  67.5 33.8 %copy-start.17 = (f32[4,128]{1,0:T(4,128)S(1)}, f32[4,128]{1,0:T(4,128)}, u32[]{:S(2)}) copy-start(f32[4,128]{1,0:T(4,128)} %ftaps.1) | copy-start | bytes 6148
  69.2 0.6 copy-start.11
  69.8 34.3 %copy-start = (f32[256,128]{1,0:T(8,128)}, f32[256,128]{1,0:T(8,128)S(1)}, u32[]{:S(2)}) copy-start(f32[256,128]{1,0:T(8,128)S(1)} %get-tuple-element.34.cum) | copy-start | bytes 393220
  71.6 38.1 %all-to-all-start.1 = ((bf16[8,136,128]{2,1,0:T(8,128)(2,1)}), bf16[8,136,128]{2,1,0:T(8,128)(2,1)S(1)}, u32[]{:S(2)}, u32[]{:S(2)}) async-start(bf16[8,136,128]{2,1,0:T(8,128)(2,1)} %get-tuple-element.28), calls=%async_computation.1 | async-start | bytes 557056 | tf_op jit(solution)/shard_map/all_to_all | solution.py:355
  101.2 13.9 %copy-start.26 = (f32[128]{0:T(128)S(1)}, f32[128]{0:T(128)}, u32[]{:S(2)}) copy-start(f32[128]{0:T(128)} %param.37) | copy-start | bytes 1540
  104.1 0.7 copy-start.2
  104.8 0.7 copy-start.4
  105.4 0.7 copy-start.6
  106.1 0.6 copy-start.9
  106.7 38.3 %collective-permute-start.1 = (bf16[2048,256]{1,0:T(8,128)(2,1)S(1)}, bf16[2048,256]{1,0:T(8,128)(2,1)S(1)}, u32[]{:S(2)}, u32[]{:S(2)}) collective-permute-start(bf16[2048,256]{1,0:T(8,128)(2,1)S(1)} %get-tuple-element.42.wa), channel_id=1, source_target_pairs={{0,1},{1,0},{2,3},{3,2},{4,5},{5,4},{6,7},{7,6},{8,9},{9,8},{10,11... | collective-permute-start | bytes 3145736 | tf_op jit(solution)/shard_map/ppermute | solution.py:359
  109.7 0.7 copy-start.12
  111.2 16.6 %all-to-all-start.2 = ((bf16[8,136,128]{2,1,0:T(8,128)(2,1)}), bf16[8,136,128]{2,1,0:T(8,128)(2,1)S(1)}, u32[]{:S(2)}, u32[]{:S(2)}) async-start(bf16[8,136,128]{2,1,0:T(8,128)(2,1)} %get-tuple-element.29), calls=%async_computation.2 | async-start | bytes 557056 | tf_op jit(solution)/shard_map/all_to_all | solution.py:357
  127.8 0.9 copy-start.1
  128.7 0.9 copy-start.3
  129.6 0.9 copy-start.5
  130.5 0.9 copy-start.7
  131.4 0.8 copy-start.8
  132.3 0.8 copy-start.10
  133.1 0.7 copy-start.13
  133.8 0.7 copy-start.18
  135.5 9.5 %all-to-all-start.4 = ((f32[8,3,256]{2,1,0:T(4,128)}), f32[8,3,256]{2,1,0:T(4,128)S(1)}, u32[]{:S(2)}, u32[]{:S(2)}) async-start(f32[8,3,256]{2,1,0:T(4,128)} %get-tuple-element.40), calls=%async_computation.4 | async-start | bytes 65536 | tf_op jit(solution)/shard_map/all_to_all | solution.py:363
  145.0 0.7 copy-start.14
Sparse Core Ops, SparseCore 0:
  26.8 74.4 all-gather.3

commit v13 on v12

--- a/solution.py
+++ b/solution.py
@@ -23,6 +23,7 @@
 SMEM = pl.BlockSpec(memory_space=pltpu.SMEM)
 HIGHEST = lax.Precision.HIGHEST
 SMALL = pltpu.CompilerParams(vmem_limit_bytes=12 * 2**20)
+LARGE = pltpu.CompilerParams(vmem_limit_bytes=64 * 2**20 - 2**17)
 
 
 def dot(a, b, ca, cb, precision=None):
@@ -41,7 +42,7 @@
     return tuple(pltpu.with_memory_space_constraint(a, pltpu.HBM) for a in arrays)
 
 
-def lay_out(shards, copies):
+def lay_out(shards, copies, params):
     rows, ch = shards[0].shape
     n = len(shards)
 
@@ -52,7 +53,7 @@
                 refs[n][k, :, i * ch : (i + 1) * ch] = w
 
     return pl.pallas_call(
-        body, out_shape=sds((copies, rows, n * ch), bf16), in_specs=[VMEM] * n, out_specs=VMEM, compiler_params=SMALL
+        body, out_shape=sds((copies, rows, n * ch), bf16), in_specs=[VMEM] * n, out_specs=VMEM, compiler_params=params
     )(*fetched(*shards))
 
 
@@ -337,10 +338,10 @@
     nf, nt = lax.axis_size("fs"), lax.axis_size("tp")
     iz, iy, ix, tp = (lax.axis_index(a).astype(jnp.int32).reshape(1) for a in ("sp_0", "sp_1", "fs", "tp"))
     ny = lax.axis_size("sp_1")
-    rest = lay_out((state_read, mixer_gate, conv_value, conv_gate, conv_output, state_output), ny)
+    rest = lay_out((state_read, mixer_gate, conv_value, conv_gate, conv_output, state_output), ny, SMALL)
     rest = lax.all_to_all(rest, "sp_1", 0, 0, tiled=True).reshape(-1, 6 * ch)
     rest = lax.all_gather(rest, "sp_0", axis=0, tiled=True)
-    first = lay_out((state_input, write_projection), lax.axis_size(SP))
+    first = lay_out((state_input, write_projection), lax.axis_size(SP), LARGE)
     first = lax.all_to_all(first, SP, 0, 0, tiled=True).reshape(-1, 2 * ch)
     n = lax.axis_size(SP)
     halo = lax.ppermute(tokens[rows - HALO :], SP, [(i, i + 1) for i in range(n - 1)])

time: 166 us -> 166 us (level)
  transfers between devices with their start and end apart: 7 -> 7, of which waited for: 5 -> 5; matrix products, arithmetic and copies ran while one was open for 1% -> 2% of each run, Pallas kernels for 6% -> 6%
where the time goes in v13:
time: 166 us; the launch traced here: 165 us
  waiting for transfers between devices  52.5 us (32%)
  starting transfers between devices  38.1 us (23%)
  blocking collectives  34.1 us (21%)
  between operations  13.7 us (8%)
  local copies, waits for them, and re-layouts  12.4 us (7%)
  Pallas kernels  12.1 us (7%)
  other arithmetic  2.64 us (2%)
    all_gather x1, waiting for transfers between devices, per_device(): rest = lax.all_gather(rest, 'sp_0', axis=0, tiled=True)  20.2 us
    all_to_all x1, blocking collectives, per_device(): rest = lax.all_to_all(rest, 'sp_1', 0, 0, tiled=True).reshape(-1, 6 * ch)  19.3 us
    ppermute x1, waiting for transfers between devices, per_device(): lax.ppermute(tokens[rows - HALO:], SP, [(i, i + 1) for i in range(n - 1)])  18.6 us
    all_to_all x1, starting transfers between devices, per_device(): first = lax.all_to_all(first, SP, 0, 0, tiled=True).reshape(-1, 2 * ch)  14.2 us
    unnamed x55, local copies, waits for them, and re-layouts  11.4 us
    all_to_all x1, blocking collectives, per_device(): pieces = lax.all_to_all(out, 'fs', 0, 0, tiled=True)  10.9 us
    all_to_all x1, waiting for transfers between devices, per_device(): got = lax.all_to_all(send, 'sp_0', 0, 0, tiled=True)  10.9 us
    all_to_all x1, starting transfers between devices, per_device(): got = lax.all_to_all(send, 'sp_1', 0, 0, tiled=True)  9.28 us
  transfers between devices with their start and end apart: 7, of which 5 were waited for; matrix products, arithmetic and copies ran while one was open for 2% of the time, Pallas kernels for 6%

profile of v13, /device:TPU:1, one launch (start us, length us, event | category | flops | bytes accessed | tf_op | source)
XLA Modules:
  0.0 165.4 jit_solution(4917940096380015776)
XLA Ops:
  6.5 0.8 shard_map.200
  7.4 0.0 copy-start.22
  7.4 19.3 %all_to_all.30 = bf16[8,32,768]{2,1,0:T(8,128)(2,1)} all-to-all(bf16[8,32,768]{2,1,0:T(8,128)(2,1)S(1)} %shard_map.200), channel_id=1, replica_groups=mesh['sp_0'=8,'sp_1'=8,'fs'=4,'tp'=2] {'sp_1'}, dimensions={0} | all-to-all | bytes 786432 | tf_op jit(solution)/shard_map/all_to_all | solution.py:342
  26.7 0.0 all-gather.4.cloned.1.call-update
  26.7 2.0 %shard_map.199 = bf16[64,32,256]{2,1,0:T(8,128)(2,1)} custom-call(bf16[32,128]{1,0:T(8,128)(2,1)} %refs_0_.2, bf16[32,128]{1,0:T(8,128)(2,1)} %refs_1_.2), custom_call_target="tpu_custom_call" | custom-call | tf_op jit(solution)/shard_map/pallas_call | solution.py:55
  28.7 14.2 %all-to-all-start = ((bf16[64,32,256]{2,1,0:T(8,128)(2,1)}), bf16[64,32,256]{2,1,0:T(8,128)(2,1)S(1)}, u32[]{:S(2)}, u32[]{:S(2)}) async-start(bf16[64,32,256]{2,1,0:T(8,128)(2,1)} %shard_map.199), calls=%async_computation | async-start | bytes 2097152 | tf_op jit(solution)/shard_map/all_to_all | solution.py:345
  42.9 0.0 copy-start.16
  42.9 0.9 slice.3
  43.8 2.9 %collective-permute-start = (bf16[32,2048]{1,0:T(8,128)(2,1)S(1)}, bf16[32,2048]{1,0:T(8,128)(2,1)S(1)}, u32[]{:S(2)}, u32[]{:S(2)}) collective-permute-start(bf16[32,2048]{1,0:T(8,128)(2,1)S(1)} %slice.3), channel_id=1, source_target_pairs={{0,8},{8,16},{16,24},{24,32},{32,40},{40,48},{48,56},{56,64},{64,7... | collective-permute-start | bytes 393224 | tf_op jit(solution)/shard_map/ppermute | solution.py:347
  46.8 0.3 copy.24.wref
  47.1 18.6 %collective-permute-done = bf16[32,2048]{1,0:T(8,128)(2,1)S(1)} collective-permute-done((bf16[32,2048]{1,0:T(8,128)(2,1)S(1)}, bf16[32,2048]{1,0:T(8,128)(2,1)S(1)}, u32[]{:S(2)}, u32[]{:S(2)}) %collective-permute-start) | collective-permute-done | bytes 131104 | tf_op jit(solution)/shard_map/ppermute | solution.py:347
  65.7 0.3 fusion
  66.0 1.6 fusion.2.nref
  67.6 0.0 copy-start.15
  67.7 1.7 %steps_of.1 = (f32[256,128]{1,0:T(8,128)S(1)}, f32[256,128]{1,0:T(8,128)S(1)}, f32[256,128]{1,0:T(8,128)S(1)}, f32[2,256]{1,0:T(2,128)S(1)}, f32[1,128]{1,0:T(1,128)S(1)}, /*index=5*/s32[8,128]{1,0:T(8,128)S(1)}) custom-call(s32[1]{0:T(128)} %bitcast.iz, s32[1]{0:T(128)} %bitcast.1.iy, s32[1]{0:T(128)S(6)} %add.14.shard, s32[1]{0:T(128)} %bitcast.3.tp, ...), custom_call_target="tpu_custom_call" | custom-call | tf_op jit(solution)/shard_map/steps_of/pallas_call | solution.py:106
  69.4 0.6 copy-done.11
  70.0 0.1 all-to-all-done
  70.1 1.6 local_states.1
  71.8 9.3 %all-to-all-start.1 = ((bf16[8,136,128]{2,1,0:T(8,128)(2,1)}), bf16[8,136,128]{2,1,0:T(8,128)(2,1)S(1)}, u32[]{:S(2)}, u32[]{:S(2)}) async-start(bf16[8,136,128]{2,1,0:T(8,128)(2,1)} %get-tuple-element.28), calls=%async_computation.1 | async-start | bytes 557056 | tf_op jit(solution)/shard_map/all_to_all | solution.py:356
  81.0 20.2 %all-gather.4.cloned.1.call-done.wref = bf16[2048,768]{1,0:T(8,128)(2,1)} async-done(((bf16[256,768]{1,0:T(8,128)(2,1)}), bf16[2048,768]{1,0:T(8,128)(2,1)}) %all-gather.4.cloned.1.call-update) | async-done | bytes 3145744 | tf_op jit(solution)/shard_map/all_gather | solution.py:343
  101.2 2.9 %rows_local.1 = (bf16[256,128]{1,0:T(8,128)(2,1)S(1)}, f32[256,128]{1,0:T(8,128)S(1)}, f32[256,128]{1,0:T(8,128)S(1)}, f32[256,128]{1,0:T(8,128)S(1)}, bf16[2048,256]{1,0:T(8,128)(2,1)S(1)}) custom-call(bf16[288,2048]{1,0:T(8,128)(2,1)S(1)} %fusion.2.nref, bf16[2048,768]{1,0:T(8,128)(2,1)} %all-gather.4.cloned.1.call-done.wref, f32[4,128]{1,0:T(4,128)S(1)} %copy-done.17, ...), custom_call_target="tpu_custom_call" | custom-call | tf_op jit(solution)/shard_map/rows_local/pallas_call | solution.py:237
  104.1 0.0 copy-start.2
  104.1 0.6 copy-done.2
  104.8 0.7 copy-done.4
  105.4 0.7 copy-done.6
  106.1 0.6 copy-done.9
  106.7 3.1 %collective-permute-start.1 = (bf16[2048,256]{1,0:T(8,128)(2,1)S(1)}, bf16[2048,256]{1,0:T(8,128)(2,1)S(1)}, u32[]{:S(2)}, u32[]{:S(2)}) collective-permute-start(bf16[2048,256]{1,0:T(8,128)(2,1)S(1)} %get-tuple-element.42.wa), channel_id=1, source_target_pairs={{0,1},{1,0},{2,3},{3,2},{4,5},{5,4},{6,7},{7,6},{8,9},{9,8},{10,11... | collective-permute-start | bytes 3145736 | tf_op jit(solution)/shard_map/ppermute | solution.py:360
  109.8 0.7 copy-done.12
  110.5 0.9 line_states.1
  111.4 3.9 %all-to-all-start.2 = ((bf16[8,136,128]{2,1,0:T(8,128)(2,1)}), bf16[8,136,128]{2,1,0:T(8,128)(2,1)S(1)}, u32[]{:S(2)}, u32[]{:S(2)}) async-start(bf16[8,136,128]{2,1,0:T(8,128)(2,1)} %get-tuple-element.29), calls=%async_computation.2 | async-start | bytes 557056 | tf_op jit(solution)/shard_map/all_to_all | solution.py:358
  115.3 1.8 %all-gather.1 = f32[2,1,128]{2,1,0:T(1,128)S(1)} all-gather(f32[1,1,128]{2,1,0:T(1,128)S(1)} %bitcast.13), channel_id=2, replica_groups=mesh['sp_0'=8,'sp_1'=8,'fs'=4,'tp'=2] {'tp'}, dimensions={0}, use_global_device_ids=true | all-gather | bytes 1536 | tf_op jit(solution)/shard_map/all_gather | solution.py:353
  117.1 10.9 %all-to-all-done.2.got = bf16[8,136,128]{2,1,0:T(8,128)(2,1)S(1)} async-done(((bf16[8,136,128]{2,1,0:T(8,128)(2,1)}), bf16[8,136,128]{2,1,0:T(8,128)(2,1)S(1)}, u32[]{:S(2)}, u32[]{:S(2)}) %all-to-all-start.2) | async-done | bytes 278560 | tf_op jit(solution)/shard_map/all_to_all | solution.py:358
  128.0 0.9 copy-done.1
  128.9 0.9 copy-done.3
  129.8 0.9 copy-done.5
  130.7 0.9 copy-done.7
  131.6 0.8 copy-done.8
  132.4 0.8 copy-done.10
  133.3 0.7 copy-done.13
  133.9 0.7 copy-done.18
  134.6 1.1 rows_done.1
  135.7 4.7 %all-to-all-start.4 = ((f32[8,3,256]{2,1,0:T(4,128)}), f32[8,3,256]{2,1,0:T(4,128)S(1)}, u32[]{:S(2)}, u32[]{:S(2)}) async-start(f32[8,3,256]{2,1,0:T(4,128)} %get-tuple-element.40), calls=%async_computation.4 | async-start | bytes 65536 | tf_op jit(solution)/shard_map/all_to_all | solution.py:364
  140.4 2.1 %all_gather.13.bref = bf16[512,384]{1,0:T(8,128)(2,1)S(1)} all-gather(bf16[256,384]{1,0:T(8,128)(2,1)S(1)} %get-tuple-element.41), channel_id=1, replica_groups=mesh['sp_0'=8,'sp_1'=8,'fs'=4,'tp'=2] {'tp'}, dimensions={0}, use_global_device_ids=true | all-gather | bytes 589824 | tf_op jit(solution)/shard_map/all_gather | solution.py:365
  142.5 2.6 %all-to-all-done.4.sref = f32[8,3,256]{2,1,0:T(4,128)S(1)} async-done(((f32[8,3,256]{2,1,0:T(4,128)}), f32[8,3,256]{2,1,0:T(4,128)S(1)}, u32[]{:S(2)}, u32[]{:S(2)}) %all-to-all-start.4) | async-done | bytes 24608 | tf_op jit(solution)/shard_map/all_to_all | solution.py:364
  145.2 0.7 copy-done.14
  145.8 1.1 output_rows.1
  146.9 10.9 %all_to_all.31 = bf16[4,32,2048]{2,1,0:T(8,128)(2,1)S(1)} all-to-all(bf16[4,32,2048]{2,1,0:T(8,128)(2,1)S(1)} %output_rows.1), channel_id=1, replica_groups=mesh['sp_0'=8,'sp_1'=8,'fs'=4,'tp'=2] {'fs'}, dimensions={0} | all-to-all | bytes 1048576 | tf_op jit(solution)/shard_map/all_to_all | solution.py:367
  157.9 0.7 reduce_sum.22
  (40 shorter events, 0.1 us)
Async XLA Ops:
  6.5 94.7 %all-gather.4.cloned.1.call-start = ((), (), s32[]{:S(2)}) async-start(), calls=%async_computation.6 | async-start | bytes 3538944 | tf_op jit(solution)/shard_map/all_gather | solution.py:343
  7.4 39.4 %copy-start.22 = (bf16[2048,16]{0,1:T(8,128)(2,1)S(1)}, bf16[2048,16]{0,1:T(8,128)(2,1)}, u32[]{:S(2)}) copy-start(bf16[2048,16]{0,1:T(8,128)(2,1)} %param.29) | copy-start | bytes 196612
  28.7 18.4 %copy-start.24 = (f32[4,128]{1,0:T(4,128)S(1)}, f32[4,128]{1,0:T(4,128)}, u32[]{:S(2)}) copy-start(f32[4,128]{1,0:T(4,128)} %param.34) | copy-start | bytes 6148
  28.7 18.4 %copy-start.25 = (f32[4,128]{1,0:T(4,128)S(1)}, f32[4,128]{1,0:T(4,128)}, u32[]{:S(2)}) copy-start(f32[4,128]{1,0:T(4,128)} %param.33) | copy-start | bytes 6148
  28.7 37.0 %copy-start.21 = (bf16[256,2048]{1,0:T(8,128)(2,1)S(1)}, bf16[256,2048]{1,0:T(8,128)(2,1)}, u32[]{:S(2)}) copy-start(bf16[256,2048]{1,0:T(8,128)(2,1)} %param.21) | copy-start | bytes 3145732
  28.7 37.4 %copy-start.23 = (f32[2048]{0:T(1024)S(1)}, f32[2048]{0:T(1024)}, u32[]{:S(2)}) copy-start(f32[2048]{0:T(1024)} %param.22) | copy-start | bytes 24580
  28.7 41.4 %all-to-all-start = ((bf16[64,32,256]{2,1,0:T(8,128)(2,1)}), bf16[64,32,256]{2,1,0:T(8,128)(2,1)S(1)}, u32[]{:S(2)}, u32[]{:S(2)}) async-start(bf16[64,32,256]{2,1,0:T(8,128)(2,1)} %shard_map.199), calls=%async_computation | async-start | bytes 2097152 | tf_op jit(solution)/shard_map/all_to_all | solution.py:345
  42.9 24.7 %copy-start.16 = (f32[2,256]{1,0:T(2,128)S(1)}, f32[2,256]{1,0:T(2,128)}, u32[]{:S(2)}) copy-start(f32[2,256]{1,0:T(2,128)} %eref.1) | copy-start | bytes 6148
  42.9 24.7 %copy-start.19 = (f32[2]{0:T(128)S(1)}, f32[2]{0:T(128)}, u32[]{:S(2)}) copy-start(f32[2]{0:T(128)} %bref.1) | copy-start | bytes 28
  42.9 24.7 %copy-start.20 = (f32[2]{0:T(128)S(1)}, f32[2]{0:T(128)}, u32[]{:S(2)}) copy-start(f32[2]{0:T(128)} %rref.1) | copy-start | bytes 28
  43.8 21.9 %collective-permute-start = (bf16[32,2048]{1,0:T(8,128)(2,1)S(1)}, bf16[32,2048]{1,0:T(8,128)(2,1)S(1)}, u32[]{:S(2)}, u32[]{:S(2)}) collective-permute-start(bf16[32,2048]{1,0:T(8,128)(2,1)S(1)} %slice.3), channel_id=1, source_target_pairs={{0,8},{8,16},{16,24},{24,32},{32,40},{40,48},{48,56},{56,64},{64,7... | collective-permute-start | bytes 393224 | tf_op jit(solution)/shard_map/ppermute | solution.py:347
  67.6 33.6 %copy-start.15 = (f32[31,128]{1,0:T(8,128)S(1)}, f32[31,128]{1,0:T(8,128)}, u32[]{:S(2)}) copy-start(f32[31,128]{1,0:T(8,128)} %ltaps.1) | copy-start | bytes 47620
  67.6 33.6 %copy-start.17 = (f32[4,128]{1,0:T(4,128)S(1)}, f32[4,128]{1,0:T(4,128)}, u32[]{:S(2)}) copy-start(f32[4,128]{1,0:T(4,128)} %ftaps.1) | copy-start | bytes 6148
  69.4 0.6 copy-start.11
  70.0 34.1 %copy-start = (f32[256,128]{1,0:T(8,128)}, f32[256,128]{1,0:T(8,128)S(1)}, u32[]{:S(2)}) copy-start(f32[256,128]{1,0:T(8,128)S(1)} %get-tuple-element.34.cum) | copy-start | bytes 393220
  71.8 38.1 %all-to-all-start.1 = ((bf16[8,136,128]{2,1,0:T(8,128)(2,1)}), bf16[8,136,128]{2,1,0:T(8,128)(2,1)S(1)}, u32[]{:S(2)}, u32[]{:S(2)}) async-start(bf16[8,136,128]{2,1,0:T(8,128)(2,1)} %get-tuple-element.28), calls=%async_computation.1 | async-start | bytes 557056 | tf_op jit(solution)/shard_map/all_to_all | solution.py:356
  101.2 14.0 %copy-start.26 = (f32[128]{0:T(128)S(1)}, f32[128]{0:T(128)}, u32[]{:S(2)}) copy-start(f32[128]{0:T(128)} %param.37) | copy-start | bytes 1540
  104.1 0.7 copy-start.2
  104.8 0.7 copy-start.4
  105.4 0.7 copy-start.6
  106.1 0.6 copy-start.9
  106.7 38.5 %collective-permute-start.1 = (bf16[2048,256]{1,0:T(8,128)(2,1)S(1)}, bf16[2048,256]{1,0:T(8,128)(2,1)S(1)}, u32[]{:S(2)}, u32[]{:S(2)}) collective-permute-start(bf16[2048,256]{1,0:T(8,128)(2,1)S(1)} %get-tuple-element.42.wa), channel_id=1, source_target_pairs={{0,1},{1,0},{2,3},{3,2},{4,5},{5,4},{6,7},{7,6},{8,9},{9,8},{10,11... | collective-permute-start | bytes 3145736 | tf_op jit(solution)/shard_map/ppermute | solution.py:360
  109.8 0.7 copy-start.12
  111.4 16.6 %all-to-all-start.2 = ((bf16[8,136,128]{2,1,0:T(8,128)(2,1)}), bf16[8,136,128]{2,1,0:T(8,128)(2,1)S(1)}, u32[]{:S(2)}, u32[]{:S(2)}) async-start(bf16[8,136,128]{2,1,0:T(8,128)(2,1)} %get-tuple-element.29), calls=%async_computation.2 | async-start | bytes 557056 | tf_op jit(solution)/shard_map/all_to_all | solution.py:358
  128.0 0.9 copy-start.1
  128.9 0.9 copy-start.3
  129.8 0.9 copy-start.5
  130.7 0.9 copy-start.7
  131.6 0.8 copy-start.8
  132.4 0.8 copy-start.10
  133.3 0.7 copy-start.13
  133.9 0.7 copy-start.18
  135.7 9.5 %all-to-all-start.4 = ((f32[8,3,256]{2,1,0:T(4,128)}), f32[8,3,256]{2,1,0:T(4,128)S(1)}, u32[]{:S(2)}, u32[]{:S(2)}) async-start(f32[8,3,256]{2,1,0:T(4,128)} %get-tuple-element.40), calls=%async_computation.4 | async-start | bytes 65536 | tf_op jit(solution)/shard_map/all_to_all | solution.py:364
  145.2 0.7 copy-start.14
Sparse Core Ops, SparseCore 0:
  26.8 74.3 all-gather.3

commit v14 on v13

--- a/solution.py
+++ b/solution.py
@@ -238,7 +238,7 @@
         body,
         out_shape=(
             pltpu.VMEM((rows, STATE), bf16), pltpu.VMEM((rows, ch), f32), pltpu.VMEM((rows, ch), f32),
-            pltpu.VMEM((rows, ch), f32), pltpu.VMEM((d, 2 * ch), bf16),
+            pltpu.VMEM((rows, ch), f32), pltpu.VMEM((d + 3 * rows // 4, 2 * ch), bf16),
         ),
         in_specs=[VMEM, pl.BlockSpec(memory_space=pltpu.HBM), *[VMEM] * len(small)],
         out_specs=(VMEM,) * 5,
@@ -250,13 +250,15 @@
     )(*held(normed), *fetched(rest), *held(*small))
 
 
-def rows_done(got, enter, before, init, index, read16, zgate, mixed, inner, cum, gain, copies):
+def rows_done(got, enter, before, init, index, read16, zgate, mixed, inner, cum, gain, back, nf, nt):
     rows, ch = mixed.shape
     n, _, _ = got.shape
     heads = init.shape[0]
     p = ch // heads
-
-    def body(at, got, enter, before, init, read16, zgate, mixed, inner, cum, gain, sums, pre):
+    half, piece = rows // 2, rows // (nf * nt)
+    d = back.shape[0] - 3 * rows // 4
+
+    def body(at, got, enter, before, init, read16, zgate, mixed, inner, cum, gain, _, sums, pack, keep, last):
         acc_in = jnp.zeros((1, STATE), f32)
         start = enter[...]
         b = before[0:1, :]
@@ -271,29 +273,45 @@
         mix = mixed[...]
         cols = [jnp.sum(v, axis=1, keepdims=True) for v in (mix, mix * mix, gated * gated)]
         found = jnp.transpose(jnp.concatenate([*cols, jnp.zeros((rows, 5), f32)], 1))
-        for j in range(copies):
+        for j in range(nf * nt):
             sums[j] = found[:3]
-        high = mix.astype(bf16)
-        pre[:, :ch] = high
-        pre[:, ch : 2 * ch] = (mix - high.astype(f32)).astype(bf16)
-        pre[:, 2 * ch :] = (gated * gain[...]).astype(bf16)
-
-    return pl.pallas_call(
-        body,
-        out_shape=(sds((copies, 3, rows), f32), pltpu.VMEM((rows, 3 * ch), bf16)),
-        in_specs=[VMEM] * 11,
-        out_specs=(VMEM, VMEM),
+        last[...] = gated * gain[...]
+        tp = at[2, 0]
+
+        def values(start):
+            rows_at = pl.ds(pl.multiple_of(start, piece), piece)
+            high = mixed[rows_at, :].astype(bf16)
+            return high, (mixed[rows_at, :] - high.astype(f32)).astype(bf16), last[rows_at, :].astype(bf16)
+
+        for i in range(nf):
+            here = slice(i * piece, (i + 1) * piece)
+            for k, v in enumerate(values(i * (nt * piece) + tp * piece)):
+                keep[here, k * ch : (k + 1) * ch] = v
+            high, low, scaled = values(i * (nt * piece) + (1 - tp) * piece)
+            pack[d + i * piece : d + (i + 1) * piece, :ch] = high
+            pack[d + i * piece : d + (i + 1) * piece, ch:] = low
+            right, up = divmod(i * piece, half // 2)
+            pack[d + half + up : d + half + up + piece, right * ch : (right + 1) * ch] = scaled
+
+    return pl.pallas_call(
+        body,
+        out_shape=(sds((nf * nt, 3, rows), f32), pltpu.VMEM(back.shape, bf16), pltpu.VMEM((half, 3 * ch), bf16)),
+        in_specs=[VMEM] * 12,
+        out_specs=(VMEM,) * 3,
+        input_output_aliases={11: 1},
+        scratch_shapes=[pltpu.VMEM((rows, ch), f32)],
         compiler_params=SMALL, name="rows_done",
-    )(*held(index, got, enter, before, init, read16, zgate, mixed, inner, cum, gain))
-
-
-def output_rows(sums, both, gains, own, other, index, nf, nt):
+    )(*held(index, got, enter, before, init, read16, zgate, mixed, inner, cum, gain, back))
+
+
+def output_rows(sums, gains, keep, own, other, index, nf, nt):
     copies, _, rows = sums.shape
     ch = gains.shape[1]
-    d = own.shape[0]
+    half = rows // 2
+    d = own.shape[0] - 3 * rows // 4
     piece = rows // (nf * nt)
 
-    def body(at, sref, bref, gref, wa, wb, out, cols, act):
+    def body(at, sref, gref, keep, own, other, out, cols, act):
         tp = at[2, 0]
         s = sref[0]
         for j in range(1, copies):
@@ -306,14 +324,17 @@
             mean = t[:, 0:1] / C_CH
             rstd = lax.rsqrt(t[:, 1:2] / C_CH - mean * mean + EPS)
             scale = lax.rsqrt(t[:, 2:3] / D_INNER + EPS)
-            for j in range(nt):
+            right, up = divmod(i * piece, half // 2)
+            mine = [keep[here, k * ch : (k + 1) * ch] for k in range(3)]
+            got = other[d + i * piece : d + (i + 1) * piece, :]
+            last = other[d + half + up : d + half + up + piece, right * ch : (right + 1) * ch]
+            for j, (high, low, gated) in enumerate((mine, (got[:, :ch], got[:, ch:], last))):
                 src = tp if j == 0 else 1 - tp
-                a = bref[pl.ds(pl.multiple_of(src * rows + at_row, piece), piece), :].astype(f32)
-                mix = a[:, :ch] + a[:, ch : 2 * ch]
+                mix = high.astype(f32) + low.astype(f32)
                 conv = jax.nn.silu((mix - mean) * rstd * gref[pl.ds(src, 1), :])
                 act[here, 2 * j * ch : (2 * j + 1) * ch] = conv.astype(bf16)
-                act[here, (2 * j + 1) * ch : (2 * j + 2) * ch] = (a[:, 2 * ch :] * scale).astype(bf16)
-        term = dot(act[:, : 2 * ch], wa[...], 1, 1) + dot(act[:, 2 * ch :], wb[...], 1, 1)
+                act[here, (2 * j + 1) * ch : (2 * j + 2) * ch] = (gated.astype(f32) * scale).astype(bf16)
+        term = dot(act[:, : 2 * ch], own[:d, :], 1, 1) + dot(act[:, 2 * ch :], other[:d, :], 1, 1)
         out[...] = term.astype(bf16).reshape(nf, piece, d)
 
     return pl.pallas_call(
@@ -323,7 +344,7 @@
         out_specs=VMEM,
         scratch_shapes=[pltpu.VMEM((rows, 8), f32), pltpu.VMEM((nf * piece, 4 * ch), bf16)],
         compiler_params=SMALL, name="output_rows",
-    )(*held(index, sums, both, gains, own, other))
+    )(*held(index, sums, gains, keep, own, other))
 
 
 def per_device(
@@ -357,13 +378,12 @@
     enter, before, send = line_states(got, at, heads, p, lax.axis_size("sp_0"))
     got = lax.all_to_all(send, "sp_0", 0, 0, tiled=True)
     read16, zgate, mixed, inner, back = rows_local(normed, rest, fetch_taps, long_taps, xs, w16, cum, cum_t)
-    back_other = lax.ppermute(back, "tp", [(i, nt - 1 - i) for i in range(nt)])
-    sums, pre = rows_done(
-        got, enter, before, initial_state, at, read16, zgate, mixed, inner, cum, state_gain[None], nf * nt
+    sums, pack, keep = rows_done(
+        got, enter, before, initial_state, at, read16, zgate, mixed, inner, cum, state_gain[None], back, nf, nt
     )
     sums = lax.all_to_all(sums, FT, 0, 0, tiled=True)
-    both = lax.all_gather(pre, "tp", axis=0, tiled=True)
-    out = output_rows(sums, both, gains, back, back_other, at, nf, nt)
+    other = lax.ppermute(pack, "tp", [(i, nt - 1 - i) for i in range(nt)])
+    out = output_rows(sums, gains, keep, pack, other, at, nf, nt)
     pieces = lax.all_to_all(out, "fs", 0, 0, tiled=True)
     return jnp.sum(pieces.astype(f32), 0).astype(bf16)
 

time: 166 us -> 143 us (0.86)
  waiting for transfers between devices: 52.5 us -> 28.9 us
  blocking collectives: 34.1 us -> 51 us
  local copies, waits for them, and re-layouts: 12.4 us -> 1.27 us
  starting transfers between devices: 38.1 us -> 34 us
    all_to_all x0 -> x1, blocking collectives: none -> 18.9 us  [per_device(): got = lax.all_to_all(send, 'sp_1', 0, 0, tiled=True)]
    all_gather x1, waiting for transfers between devices: 20.2 us -> 3.98 us  [per_device(): rest = lax.all_gather(rest, 'sp_0', axis=0, tiled=True)]
    unnamed x55 -> x27, local copies, waits for them, and re-layouts: 11.4 us -> 0.34 us
    all_to_all x1 -> x0, starting transfers between devices: 9.28 us -> none  [per_device(): got = lax.all_to_all(send, 'sp_1', 0, 0, tiled=True)]
    all_to_all x1, waiting for transfers between devices: 10.9 us -> 2.67 us  [per_device(): got = lax.all_to_all(send, 'sp_0', 0, 0, tiled=True)]
    ppermute x1, starting transfers between devices: 3.13 us -> 6.06 us  [per_device(): other = lax.ppermute(pack, 'tp', [(i, nt - 1 - i) for i in range(nt)])]
    all_to_all x1, starting transfers between devices: 3.87 us -> 6.41 us  [per_device(): got = lax.all_to_all(send, 'sp_0', 0, 0, tiled=True)]
    all_gather x1 -> x0, blocking collectives: 2.07 us -> none  [per_device(): both = lax.all_gather(pre, 'tp', axis=0, tiled=True)]
  transfers between devices with their start and end apart: 7 -> 6, of which waited for: 5 -> 5; matrix products, arithmetic and copies ran while one was open for 2% -> 2% of each run, Pallas kernels for 6% -> 6%
where the time goes in v14:
time: 143 us
  blocking collectives  51 us (36%)
  starting transfers between devices  34 us (24%)
  waiting for transfers between devices  28.9 us (20%)
  between operations  13.6 us (10%)
  Pallas kernels  11.3 us (8%)
  other arithmetic  2.64 us (2%)
    all_to_all x1, blocking collectives, per_device(): rest = lax.all_to_all(rest, 'sp_1', 0, 0, tiled=True).reshape(-1, 6 * ch)  19.3 us
    all_to_all x1, blocking collectives, per_device(): got = lax.all_to_all(send, 'sp_1', 0, 0, tiled=True)  18.9 us
    ppermute x1, waiting for transfers between devices, per_device(): lax.ppermute(tokens[rows - HALO:], SP, [(i, i + 1) for i in range(n - 1)])  18.6 us
    all_to_all x1, starting transfers between devices, per_device(): first = lax.all_to_all(first, SP, 0, 0, tiled=True).reshape(-1, 2 * ch)  14.2 us
    all_to_all x1, blocking collectives, per_device(): pieces = lax.all_to_all(out, 'fs', 0, 0, tiled=True)  10.9 us
    all_to_all x1, starting transfers between devices, per_device(): got = lax.all_to_all(send, 'sp_0', 0, 0, tiled=True)  6.41 us
    ppermute x1, starting transfers between devices, per_device(): other = lax.ppermute(pack, 'tp', [(i, nt - 1 - i) for i in range(nt)])  6.06 us
    all_to_all x1, starting transfers between devices, per_device(): sums = lax.all_to_all(sums, FT, 0, 0, tiled=True)  4.42 us
  transfers between devices with their start and end apart: 6, of which 5 were waited for; matrix products, arithmetic and copies ran while one was open for 2% of the time, Pallas kernels for 6%

profile of v14, /device:TPU:1, one launch (start us, length us, event | category | flops | bytes accessed | tf_op | source)
XLA Modules:
  0.0 142.7 jit_solution(4398637944798427178)
XLA Ops:
  6.5 0.0 all-gather.4.cloned.1.call-start
  6.5 0.8 shard_map.200
  7.4 0.0 copy-start.8
  7.4 19.3 %all_to_all.30 = bf16[8,32,768]{2,1,0:T(8,128)(2,1)} all-to-all(bf16[8,32,768]{2,1,0:T(8,128)(2,1)S(1)} %shard_map.200), channel_id=1, replica_groups=mesh['sp_0'=8,'sp_1'=8,'fs'=4,'tp'=2] {'sp_1'}, dimensions={0} | all-to-all | bytes 786432 | tf_op jit(solution)/shard_map/all_to_all | solution.py:363
  26.7 0.0 all-gather.4.cloned.1.call-update
  26.7 1.9 %shard_map.199 = bf16[64,32,256]{2,1,0:T(8,128)(2,1)} custom-call(bf16[32,128]{1,0:T(8,128)(2,1)} %refs_0_.2, bf16[32,128]{1,0:T(8,128)(2,1)} %refs_1_.2), custom_call_target="tpu_custom_call" | custom-call | tf_op jit(solution)/shard_map/pallas_call | solution.py:55
  28.6 14.2 %all-to-all-start = ((bf16[64,32,256]{2,1,0:T(8,128)(2,1)}), bf16[64,32,256]{2,1,0:T(8,128)(2,1)S(1)}, u32[]{:S(2)}, u32[]{:S(2)}) async-start(bf16[64,32,256]{2,1,0:T(8,128)(2,1)} %shard_map.199), calls=%async_computation | async-start | bytes 2097152 | tf_op jit(solution)/shard_map/all_to_all | solution.py:366
  42.8 0.0 copy-start.2
  42.8 0.0 copy-start.4
  42.9 0.0 copy-start.5
  42.9 0.9 slice.3
  43.8 2.9 %collective-permute-start = (bf16[32,2048]{1,0:T(8,128)(2,1)S(1)}, bf16[32,2048]{1,0:T(8,128)(2,1)S(1)}, u32[]{:S(2)}, u32[]{:S(2)}) collective-permute-start(bf16[32,2048]{1,0:T(8,128)(2,1)S(1)} %slice.3), channel_id=1, source_target_pairs={{0,8},{8,16},{16,24},{24,32},{32,40},{40,48},{48,56},{56,64},{64,7... | collective-permute-start | bytes 393224 | tf_op jit(solution)/shard_map/ppermute | solution.py:368
  46.7 0.0 copy-done.8
  46.7 0.3 copy.25.wref
  47.0 0.0 copy-done.10
  47.0 0.0 copy-done.11
  47.1 18.6 %collective-permute-done = bf16[32,2048]{1,0:T(8,128)(2,1)S(1)} collective-permute-done((bf16[32,2048]{1,0:T(8,128)(2,1)S(1)}, bf16[32,2048]{1,0:T(8,128)(2,1)S(1)}, u32[]{:S(2)}, u32[]{:S(2)}) %collective-permute-start) | collective-permute-done | bytes 131104 | tf_op jit(solution)/shard_map/ppermute | solution.py:368
  65.7 0.0 copy-done.7
  65.7 0.3 fusion
  66.0 0.0 copy-done.9
  66.0 1.6 %fusion.2.nref = bf16[288,2048]{1,0:T(8,128)(2,1)S(1)} fusion(f32[2048]{0:T(1024)S(1)} %copy-done.9, f32[288]{0:T(512)S(1)} %add_rsqrt_fusion, bf16[256,2048]{1,0:T(8,128)(2,1)} %param.21, bf16[32,2048]{1,0:T(8,128)(2,1)S(1)} %collective-permute-done), kind=kLoop, calls=%fused_computation.4 | loop fusion | flops 4128768 | bytes 2368640 | tf_op jit(solution)/shard_map/convert_element_type | solution.py:370
  67.6 0.0 copy-done.2
  67.6 0.0 copy-done.4
  67.6 0.0 copy-done.5
  67.6 1.7 %steps_of.1 = (f32[256,128]{1,0:T(8,128)S(1)}, f32[256,128]{1,0:T(8,128)S(1)}, f32[256,128]{1,0:T(8,128)S(1)}, f32[2,256]{1,0:T(2,128)S(1)}, f32[1,128]{1,0:T(1,128)S(1)}, /*index=5*/s32[8,128]{1,0:T(8,128)S(1)}) custom-call(s32[1]{0:T(128)} %bitcast.iz, s32[1]{0:T(128)} %bitcast.1.iy, s32[1]{0:T(128)S(6)} %add.14.shard, s32[1]{0:T(128)} %bitcast.3.tp, ...), custom_call_target="tpu_custom_call" | custom-call | tf_op jit(solution)/shard_map/steps_of/pallas_call | solution.py:106
  69.3 0.0 copy-start.1
  69.3 0.0 copy-start.3
  69.3 0.7 all-to-all-done
  70.1 0.9 local_states.1
  71.0 18.9 %all_to_all.31.ref = bf16[8,136,128]{2,1,0:T(8,128)(2,1)S(1)} all-to-all(bf16[8,136,128]{2,1,0:T(8,128)(2,1)S(1)} %get-tuple-element.29), channel_id=1, replica_groups=mesh['sp_0'=8,'sp_1'=8,'fs'=4,'tp'=2] {'sp_1'}, dimensions={0} | all-to-all | bytes 557056 | tf_op jit(solution)/shard_map/all_to_all | solution.py:377
  90.0 0.9 line_states.1
  90.9 6.4 %all-to-all-start.2 = ((bf16[8,136,128]{2,1,0:T(8,128)(2,1)}), bf16[8,136,128]{2,1,0:T(8,128)(2,1)S(1)}, u32[]{:S(2)}, u32[]{:S(2)}) async-start(bf16[8,136,128]{2,1,0:T(8,128)(2,1)} %get-tuple-element.30), calls=%async_computation.2 | async-start | bytes 557056 | tf_op jit(solution)/shard_map/all_to_all | solution.py:379
  97.3 0.0 copy-start.6
  97.3 4.0 %all-gather.4.cloned.1.call-done.wref = bf16[2048,768]{1,0:T(8,128)(2,1)} async-done(((bf16[256,768]{1,0:T(8,128)(2,1)}), bf16[2048,768]{1,0:T(8,128)(2,1)}) %all-gather.4.cloned.1.call-update) | async-done | bytes 3145744 | tf_op jit(solution)/shard_map/all_gather | solution.py:364
  101.3 0.0 copy-done.1
  101.3 0.0 copy-done.3
  101.3 2.9 %rows_local.1 = (bf16[256,128]{1,0:T(8,128)(2,1)S(1)}, f32[256,128]{1,0:T(8,128)S(1)}, f32[256,128]{1,0:T(8,128)S(1)}, f32[256,128]{1,0:T(8,128)S(1)}, bf16[2240,256]{1,0:T(8,128)(2,1)S(1)}) custom-call(bf16[288,2048]{1,0:T(8,128)(2,1)S(1)} %fusion.2.nref, bf16[2048,768]{1,0:T(8,128)(2,1)} %all-gather.4.cloned.1.call-done.wref, f32[4,128]{1,0:T(4,128)S(1)} %copy-done.3, ...), custom_call_target="tpu_custom_call" | custom-call | tf_op jit(solution)/shard_map/rows_local/pallas_call | solution.py:237
  104.1 2.7 %all-to-all-done.2.got = bf16[8,136,128]{2,1,0:T(8,128)(2,1)S(1)} async-done(((bf16[8,136,128]{2,1,0:T(8,128)(2,1)}), bf16[8,136,128]{2,1,0:T(8,128)(2,1)S(1)}, u32[]{:S(2)}, u32[]{:S(2)}) %all-to-all-start.2) | async-done | bytes 278560 | tf_op jit(solution)/shard_map/all_to_all | solution.py:379
  106.8 0.0 copy-done
  106.8 1.1 rows_done.1
  107.9 6.1 %collective-permute-start.1 = (bf16[2240,256]{1,0:T(8,128)(2,1)S(1)}, bf16[2240,256]{1,0:T(8,128)(2,1)S(1)}, u32[]{:S(2)}, u32[]{:S(2)}) collective-permute-start(bf16[2240,256]{1,0:T(8,128)(2,1)S(1)} %get-tuple-element.44.own), channel_id=1, source_target_pairs={{0,1},{1,0},{2,3},{3,2},{4,5},{5,4},{6,7},{7,6},{8,9},{9,8},{10,11... | collective-permute-start | bytes 3440648 | tf_op jit(solution)/shard_map/ppermute | solution.py:385
  114.0 4.4 %all-to-all-start.4 = ((f32[8,3,256]{2,1,0:T(4,128)}), f32[8,3,256]{2,1,0:T(4,128)S(1)}, u32[]{:S(2)}, u32[]{:S(2)}) async-start(f32[8,3,256]{2,1,0:T(4,128)} %get-tuple-element.42), calls=%async_computation.4 | async-start | bytes 65536 | tf_op jit(solution)/shard_map/all_to_all | solution.py:384
  118.4 1.8 %all-gather.1 = f32[2,1,128]{2,1,0:T(1,128)S(1)} all-gather(f32[1,1,128]{2,1,0:T(1,128)S(1)} %bitcast.13), channel_id=2, replica_groups=mesh['sp_0'=8,'sp_1'=8,'fs'=4,'tp'=2] {'tp'}, dimensions={0}, use_global_device_ids=true | all-gather | bytes 1536 | tf_op jit(solution)/shard_map/all_gather | solution.py:374
  120.2 2.9 %all-to-all-done.4.sref = f32[8,3,256]{2,1,0:T(4,128)S(1)} async-done(((f32[8,3,256]{2,1,0:T(4,128)}), f32[8,3,256]{2,1,0:T(4,128)S(1)}, u32[]{:S(2)}, u32[]{:S(2)}) %all-to-all-start.4) | async-done | bytes 24608 | tf_op jit(solution)/shard_map/all_to_all | solution.py:384
  123.1 0.0 collective-permute-done.1.other
  123.1 1.1 output_rows.1
  124.2 10.9 %all_to_all.32 = bf16[4,32,2048]{2,1,0:T(8,128)(2,1)S(1)} all-to-all(bf16[4,32,2048]{2,1,0:T(8,128)(2,1)S(1)} %output_rows.1), channel_id=1, replica_groups=mesh['sp_0'=8,'sp_1'=8,'fs'=4,'tp'=2] {'fs'}, dimensions={0} | all-to-all | bytes 1048576 | tf_op jit(solution)/shard_map/all_to_all | solution.py:387
  135.1 0.7 reduce_sum.22
  (10 shorter events, 0.0 us)
Async XLA Ops:
  6.5 94.7 %all-gather.4.cloned.1.call-start = ((), (), s32[]{:S(2)}) async-start(), calls=%async_computation.6 | async-start | bytes 3538944 | tf_op jit(solution)/shard_map/all_gather | solution.py:364
  7.4 39.4 %copy-start.8 = (bf16[2048,16]{0,1:T(8,128)(2,1)S(1)}, bf16[2048,16]{0,1:T(8,128)(2,1)}, u32[]{:S(2)}) copy-start(bf16[2048,16]{0,1:T(8,128)(2,1)} %param.29) | copy-start | bytes 196612
  28.6 18.4 %copy-start.10 = (f32[4,128]{1,0:T(4,128)S(1)}, f32[4,128]{1,0:T(4,128)}, u32[]{:S(2)}) copy-start(f32[4,128]{1,0:T(4,128)} %param.34) | copy-start | bytes 6148
  28.6 18.4 %copy-start.11 = (f32[4,128]{1,0:T(4,128)S(1)}, f32[4,128]{1,0:T(4,128)}, u32[]{:S(2)}) copy-start(f32[4,128]{1,0:T(4,128)} %param.33) | copy-start | bytes 6148
  28.6 37.0 %copy-start.7 = (bf16[256,2048]{1,0:T(8,128)(2,1)S(1)}, bf16[256,2048]{1,0:T(8,128)(2,1)}, u32[]{:S(2)}) copy-start(bf16[256,2048]{1,0:T(8,128)(2,1)} %param.21) | copy-start | bytes 3145732
  28.6 37.4 %copy-start.9 = (f32[2048]{0:T(1024)S(1)}, f32[2048]{0:T(1024)}, u32[]{:S(2)}) copy-start(f32[2048]{0:T(1024)} %param.22) | copy-start | bytes 24580
  28.6 41.5 %all-to-all-start = ((bf16[64,32,256]{2,1,0:T(8,128)(2,1)}), bf16[64,32,256]{2,1,0:T(8,128)(2,1)S(1)}, u32[]{:S(2)}, u32[]{:S(2)}) async-start(bf16[64,32,256]{2,1,0:T(8,128)(2,1)} %shard_map.199), calls=%async_computation | async-start | bytes 2097152 | tf_op jit(solution)/shard_map/all_to_all | solution.py:366
  42.8 24.7 %copy-start.2 = (f32[2,256]{1,0:T(2,128)S(1)}, f32[2,256]{1,0:T(2,128)}, u32[]{:S(2)}) copy-start(f32[2,256]{1,0:T(2,128)} %eref.1) | copy-start | bytes 6148
  42.8 24.7 %copy-start.4 = (f32[2]{0:T(128)S(1)}, f32[2]{0:T(128)}, u32[]{:S(2)}) copy-start(f32[2]{0:T(128)} %bref.1) | copy-start | bytes 28
  42.9 24.7 %copy-start.5 = (f32[2]{0:T(128)S(1)}, f32[2]{0:T(128)}, u32[]{:S(2)}) copy-start(f32[2]{0:T(128)} %rref.1) | copy-start | bytes 28
  43.8 21.9 %collective-permute-start = (bf16[32,2048]{1,0:T(8,128)(2,1)S(1)}, bf16[32,2048]{1,0:T(8,128)(2,1)S(1)}, u32[]{:S(2)}, u32[]{:S(2)}) collective-permute-start(bf16[32,2048]{1,0:T(8,128)(2,1)S(1)} %slice.3), channel_id=1, source_target_pairs={{0,8},{8,16},{16,24},{24,32},{32,40},{40,48},{48,56},{56,64},{64,7... | collective-permute-start | bytes 393224 | tf_op jit(solution)/shard_map/ppermute | solution.py:368
  69.3 31.9 %copy-start.1 = (f32[31,128]{1,0:T(8,128)S(1)}, f32[31,128]{1,0:T(8,128)}, u32[]{:S(2)}) copy-start(f32[31,128]{1,0:T(8,128)} %ltaps.1) | copy-start | bytes 47620
  69.3 31.9 %copy-start.3 = (f32[4,128]{1,0:T(4,128)S(1)}, f32[4,128]{1,0:T(4,128)}, u32[]{:S(2)}) copy-start(f32[4,128]{1,0:T(4,128)} %ftaps.1) | copy-start | bytes 6148
  90.9 16.0 %all-to-all-start.2 = ((bf16[8,136,128]{2,1,0:T(8,128)(2,1)}), bf16[8,136,128]{2,1,0:T(8,128)(2,1)S(1)}, u32[]{:S(2)}, u32[]{:S(2)}) async-start(bf16[8,136,128]{2,1,0:T(8,128)(2,1)} %get-tuple-element.30), calls=%async_computation.2 | async-start | bytes 557056 | tf_op jit(solution)/shard_map/all_to_all | solution.py:379
  97.3 9.6 %copy-start = (f32[2,64,128]{2,1,0:T(8,128)S(1)}, f32[2,64,128]{2,1,0:T(8,128)}, u32[]{:S(2)}) copy-start(f32[2,64,128]{2,1,0:T(8,128)} %init.1) | copy-start | bytes 196612
  97.3 9.6 %copy-start.6 = (f32[128]{0:T(128)S(1)}, f32[128]{0:T(128)}, u32[]{:S(2)}) copy-start(f32[128]{0:T(128)} %param.38) | copy-start | bytes 1540
  101.3 17.1 %copy-start.12 = (f32[128]{0:T(128)S(1)}, f32[128]{0:T(128)}, u32[]{:S(2)}) copy-start(f32[128]{0:T(128)} %param.37) | copy-start | bytes 1540
  107.9 15.2 %collective-permute-start.1 = (bf16[2240,256]{1,0:T(8,128)(2,1)S(1)}, bf16[2240,256]{1,0:T(8,128)(2,1)S(1)}, u32[]{:S(2)}, u32[]{:S(2)}) collective-permute-start(bf16[2240,256]{1,0:T(8,128)(2,1)S(1)} %get-tuple-element.44.own), channel_id=1, source_target_pairs={{0,1},{1,0},{2,3},{3,2},{4,5},{5,4},{6,7},{7,6},{8,9},{9,8},{10,11... | collective-permute-start | bytes 3440648 | tf_op jit(solution)/shard_map/ppermute | solution.py:385
  114.0 9.1 %all-to-all-start.4 = ((f32[8,3,256]{2,1,0:T(4,128)}), f32[8,3,256]{2,1,0:T(4,128)S(1)}, u32[]{:S(2)}, u32[]{:S(2)}) async-start(f32[8,3,256]{2,1,0:T(4,128)} %get-tuple-element.42), calls=%async_computation.4 | async-start | bytes 65536 | tf_op jit(solution)/shard_map/all_to_all | solution.py:384
Sparse Core Ops, SparseCore 0:
  26.8 74.4 all-gather.3

commit v15 on v14

--- a/solution.py
+++ b/solution.py
@@ -120,7 +120,8 @@
     rows, ch = step.shape
 
     def body(nref, wref, tref, sref, lref, logs, send, xs, w16, buf):
-        buf[...] = dot(nref[...], wref[...], 1, 0).astype(bf16).astype(f32)
+        w = jnp.concatenate([wref[:, z].reshape(-1, 2 * ch) for z in range(wref.shape[1])], 0)
+        buf[...] = dot(nref[...], w, 1, 0).astype(bf16).astype(f32)
         at = HALO - SHORT + 1
         mix = sum(buf[at + i : at + i + rows, :] * tref[i : i + 1, :] for i in range(SHORT))
         act = jax.nn.silu(mix)
@@ -363,7 +364,7 @@
     rest = lax.all_to_all(rest, "sp_1", 0, 0, tiled=True).reshape(-1, 6 * ch)
     rest = lax.all_gather(rest, "sp_0", axis=0, tiled=True)
     first = lay_out((state_input, write_projection), lax.axis_size(SP), LARGE)
-    first = lax.all_to_all(first, SP, 0, 0, tiled=True).reshape(-1, 2 * ch)
+    first = lax.all_to_all(first, SP[::-1], 0, 0, tiled=True).reshape(ny, -1, *first.shape[1:])
     n = lax.axis_size(SP)
     halo = lax.ppermute(tokens[rows - HALO :], SP, [(i, i + 1) for i in range(n - 1)])
     v = jnp.concatenate([halo, tokens], 0).astype(f32)

time: 143 us -> 143 us (level)
  no operation moved by 1% of the time
where the time goes in v15:
time: 143 us
  blocking collectives  51.5 us (36%)
  starting transfers between devices  33.7 us (24%)
  waiting for transfers between devices  28.7 us (20%)
  between operations  13.6 us (10%)
  Pallas kernels  11.3 us (8%)
  other arithmetic  2.64 us (2%)
    all_to_all x1, blocking collectives, per_device(): got = lax.all_to_all(send, 'sp_1', 0, 0, tiled=True)  19.5 us
    all_to_all x1, blocking collectives, per_device(): rest = lax.all_to_all(rest, 'sp_1', 0, 0, tiled=True).reshape(-1, 6 * ch)  19.3 us
    ppermute x1, waiting for transfers between devices, per_device(): lax.ppermute(tokens[rows - HALO:], SP, [(i, i + 1) for i in range(n - 1)])  18 us
    all_to_all x1, starting transfers between devices, per_device(): lax.all_to_all(first, SP[::-1], 0, 0, tiled=True)  14.2 us
    all_to_all x1, blocking collectives, per_device(): pieces = lax.all_to_all(out, 'fs', 0, 0, tiled=True)  10.9 us
    ppermute x1, starting transfers between devices, per_device(): other = lax.ppermute(pack, 'tp', [(i, nt - 1 - i) for i in range(nt)])  6.09 us
    all_to_all x1, starting transfers between devices, per_device(): got = lax.all_to_all(send, 'sp_0', 0, 0, tiled=True)  6.08 us
    all_to_all x1, starting transfers between devices, per_device(): sums = lax.all_to_all(sums, FT, 0, 0, tiled=True)  4.42 us
  transfers between devices with their start and end apart: 6, of which 5 were waited for; matrix products, arithmetic and copies ran while one was open for 2% of the time, Pallas kernels for 6%

profile of v15, /device:TPU:1, one launch (start us, length us, event | category | flops | bytes accessed | tf_op | source)
XLA Modules:
  0.0 142.7 jit_solution(3300277801731641694)
XLA Ops:
  6.5 0.0 all-gather.4.cloned.1.call-start
  6.5 0.8 shard_map.200
  7.4 0.0 copy-start.8
  7.4 19.3 %all_to_all.30 = bf16[8,32,768]{2,1,0:T(8,128)(2,1)} all-to-all(bf16[8,32,768]{2,1,0:T(8,128)(2,1)S(1)} %shard_map.200), channel_id=1, replica_groups=mesh['sp_0'=8,'sp_1'=8,'fs'=4,'tp'=2] {'sp_1'}, dimensions={0} | all-to-all | bytes 786432 | tf_op jit(solution)/shard_map/all_to_all | solution.py:364
  26.7 0.0 all-gather.4.cloned.1.call-update
  26.7 1.9 %shard_map.199 = bf16[64,32,256]{2,1,0:T(8,128)(2,1)} custom-call(bf16[32,128]{1,0:T(8,128)(2,1)} %refs_0_.2, bf16[32,128]{1,0:T(8,128)(2,1)} %refs_1_.2), custom_call_target="tpu_custom_call" | custom-call | tf_op jit(solution)/shard_map/pallas_call | solution.py:55
  28.6 14.2 %all-to-all-start = ((bf16[64,32,256]{2,1,0:T(8,128)(2,1)}), bf16[64,32,256]{2,1,0:T(8,128)(2,1)S(1)}, u32[]{:S(2)}, u32[]{:S(2)}) async-start(bf16[64,32,256]{2,1,0:T(8,128)(2,1)} %shard_map.199), calls=%async_computation | async-start | bytes 2097152 | tf_op jit(solution)/shard_map/all_to_all | solution.py:367
  42.8 0.0 copy-start.2
  42.8 0.0 copy-start.4
  42.9 0.0 copy-start.5
  42.9 0.9 slice.3
  43.8 2.9 %collective-permute-start = (bf16[32,2048]{1,0:T(8,128)(2,1)S(1)}, bf16[32,2048]{1,0:T(8,128)(2,1)S(1)}, u32[]{:S(2)}, u32[]{:S(2)}) collective-permute-start(bf16[32,2048]{1,0:T(8,128)(2,1)S(1)} %slice.3), channel_id=1, source_target_pairs={{0,8},{8,16},{16,24},{24,32},{32,40},{40,48},{48,56},{56,64},{64,7... | collective-permute-start | bytes 393224 | tf_op jit(solution)/shard_map/ppermute | solution.py:369
  46.7 0.0 copy-done.8
  46.8 0.3 copy.25.wref
  47.0 0.0 copy-done.10
  47.0 0.0 copy-done.11
  47.1 18.0 %collective-permute-done = bf16[32,2048]{1,0:T(8,128)(2,1)S(1)} collective-permute-done((bf16[32,2048]{1,0:T(8,128)(2,1)S(1)}, bf16[32,2048]{1,0:T(8,128)(2,1)S(1)}, u32[]{:S(2)}, u32[]{:S(2)}) %collective-permute-start) | collective-permute-done | bytes 131104 | tf_op jit(solution)/shard_map/ppermute | solution.py:369
  65.0 0.0 copy-done.7
  65.0 0.3 fusion
  65.4 0.0 copy-done.9
  65.4 1.6 %fusion.2.nref = bf16[288,2048]{1,0:T(8,128)(2,1)S(1)} fusion(f32[2048]{0:T(1024)S(1)} %copy-done.9, f32[288]{0:T(512)S(1)} %add_rsqrt_fusion, bf16[256,2048]{1,0:T(8,128)(2,1)} %param.21, bf16[32,2048]{1,0:T(8,128)(2,1)S(1)} %collective-permute-done), kind=kLoop, calls=%fused_computation.4 | loop fusion | flops 4128768 | bytes 2368640 | tf_op jit(solution)/shard_map/convert_element_type | solution.py:371
  66.9 0.0 copy-done.2
  67.0 0.0 copy-done.4
  67.0 0.0 copy-done.5
  67.0 1.7 %steps_of.1 = (f32[256,128]{1,0:T(8,128)S(1)}, f32[256,128]{1,0:T(8,128)S(1)}, f32[256,128]{1,0:T(8,128)S(1)}, f32[2,256]{1,0:T(2,128)S(1)}, f32[1,128]{1,0:T(1,128)S(1)}, /*index=5*/s32[8,128]{1,0:T(8,128)S(1)}) custom-call(s32[1]{0:T(128)} %bitcast.iz, s32[1]{0:T(128)} %bitcast.1.iy, s32[1]{0:T(128)S(6)} %add.14.shard, s32[1]{0:T(128)} %bitcast.3.tp, ...), custom_call_target="tpu_custom_call" | custom-call | tf_op jit(solution)/shard_map/steps_of/pallas_call | solution.py:106
  68.7 0.0 copy-start.1
  68.7 0.0 copy-start.3
  68.7 1.1 all-to-all-done
  69.9 0.9 local_states.1
  70.8 19.5 %all_to_all.31.ref = bf16[8,136,128]{2,1,0:T(8,128)(2,1)S(1)} all-to-all(bf16[8,136,128]{2,1,0:T(8,128)(2,1)S(1)} %get-tuple-element.29), channel_id=1, replica_groups=mesh['sp_0'=8,'sp_1'=8,'fs'=4,'tp'=2] {'sp_1'}, dimensions={0} | all-to-all | bytes 557056 | tf_op jit(solution)/shard_map/all_to_all | solution.py:378
  90.3 0.9 line_states.1
  91.1 6.1 %all-to-all-start.2 = ((bf16[8,136,128]{2,1,0:T(8,128)(2,1)}), bf16[8,136,128]{2,1,0:T(8,128)(2,1)S(1)}, u32[]{:S(2)}, u32[]{:S(2)}) async-start(bf16[8,136,128]{2,1,0:T(8,128)(2,1)} %get-tuple-element.30), calls=%async_computation.2 | async-start | bytes 557056 | tf_op jit(solution)/shard_map/all_to_all | solution.py:380
  97.2 0.0 copy-start.6
  97.2 4.0 %all-gather.4.cloned.1.call-done.wref = bf16[2048,768]{1,0:T(8,128)(2,1)} async-done(((bf16[256,768]{1,0:T(8,128)(2,1)}), bf16[2048,768]{1,0:T(8,128)(2,1)}) %all-gather.4.cloned.1.call-update) | async-done | bytes 3145744 | tf_op jit(solution)/shard_map/all_gather | solution.py:365
  101.3 0.0 copy-done.1
  101.3 0.0 copy-done.3
  101.3 2.9 %rows_local.1 = (bf16[256,128]{1,0:T(8,128)(2,1)S(1)}, f32[256,128]{1,0:T(8,128)S(1)}, f32[256,128]{1,0:T(8,128)S(1)}, f32[256,128]{1,0:T(8,128)S(1)}, bf16[2240,256]{1,0:T(8,128)(2,1)S(1)}) custom-call(bf16[288,2048]{1,0:T(8,128)(2,1)S(1)} %fusion.2.nref, bf16[2048,768]{1,0:T(8,128)(2,1)} %all-gather.4.cloned.1.call-done.wref, f32[4,128]{1,0:T(4,128)S(1)} %copy-done.3, ...), custom_call_target="tpu_custom_call" | custom-call | tf_op jit(solution)/shard_map/rows_local/pallas_call | solution.py:238
  104.1 2.6 %all-to-all-done.2.got = bf16[8,136,128]{2,1,0:T(8,128)(2,1)S(1)} async-done(((bf16[8,136,128]{2,1,0:T(8,128)(2,1)}), bf16[8,136,128]{2,1,0:T(8,128)(2,1)S(1)}, u32[]{:S(2)}, u32[]{:S(2)}) %all-to-all-start.2) | async-done | bytes 278560 | tf_op jit(solution)/shard_map/all_to_all | solution.py:380
  106.8 0.0 copy-done
  106.8 1.1 rows_done.1
  107.9 6.1 %collective-permute-start.1 = (bf16[2240,256]{1,0:T(8,128)(2,1)S(1)}, bf16[2240,256]{1,0:T(8,128)(2,1)S(1)}, u32[]{:S(2)}, u32[]{:S(2)}) collective-permute-start(bf16[2240,256]{1,0:T(8,128)(2,1)S(1)} %get-tuple-element.44.own), channel_id=1, source_target_pairs={{0,1},{1,0},{2,3},{3,2},{4,5},{5,4},{6,7},{7,6},{8,9},{9,8},{10,11... | collective-permute-start | bytes 3440648 | tf_op jit(solution)/shard_map/ppermute | solution.py:386
  114.0 4.4 %all-to-all-start.4 = ((f32[8,3,256]{2,1,0:T(4,128)}), f32[8,3,256]{2,1,0:T(4,128)S(1)}, u32[]{:S(2)}, u32[]{:S(2)}) async-start(f32[8,3,256]{2,1,0:T(4,128)} %get-tuple-element.42), calls=%async_computation.4 | async-start | bytes 65536 | tf_op jit(solution)/shard_map/all_to_all | solution.py:385
  118.4 1.8 %all-gather.1 = f32[2,1,128]{2,1,0:T(1,128)S(1)} all-gather(f32[1,1,128]{2,1,0:T(1,128)S(1)} %bitcast.13), channel_id=2, replica_groups=mesh['sp_0'=8,'sp_1'=8,'fs'=4,'tp'=2] {'tp'}, dimensions={0}, use_global_device_ids=true | all-gather | bytes 1536 | tf_op jit(solution)/shard_map/all_gather | solution.py:375
  120.2 2.9 %all-to-all-done.4.sref = f32[8,3,256]{2,1,0:T(4,128)S(1)} async-done(((f32[8,3,256]{2,1,0:T(4,128)}), f32[8,3,256]{2,1,0:T(4,128)S(1)}, u32[]{:S(2)}, u32[]{:S(2)}) %all-to-all-start.4) | async-done | bytes 24608 | tf_op jit(solution)/shard_map/all_to_all | solution.py:385
  123.1 0.0 collective-permute-done.1.other
  123.1 1.1 output_rows.1
  124.2 10.9 %all_to_all.32 = bf16[4,32,2048]{2,1,0:T(8,128)(2,1)S(1)} all-to-all(bf16[4,32,2048]{2,1,0:T(8,128)(2,1)S(1)} %output_rows.1), channel_id=1, replica_groups=mesh['sp_0'=8,'sp_1'=8,'fs'=4,'tp'=2] {'fs'}, dimensions={0} | all-to-all | bytes 1048576 | tf_op jit(solution)/shard_map/all_to_all | solution.py:388
  135.1 0.7 reduce_sum.22
  (10 shorter events, 0.0 us)
Async XLA Ops:
  6.5 94.7 %all-gather.4.cloned.1.call-start = ((), (), s32[]{:S(2)}) async-start(), calls=%async_computation.6 | async-start | bytes 3538944 | tf_op jit(solution)/shard_map/all_gather | solution.py:365
  7.4 39.4 %copy-start.8 = (bf16[2048,16]{0,1:T(8,128)(2,1)S(1)}, bf16[2048,16]{0,1:T(8,128)(2,1)}, u32[]{:S(2)}) copy-start(bf16[2048,16]{0,1:T(8,128)(2,1)} %param.29) | copy-start | bytes 196612
  28.6 18.4 %copy-start.10 = (f32[4,128]{1,0:T(4,128)S(1)}, f32[4,128]{1,0:T(4,128)}, u32[]{:S(2)}) copy-start(f32[4,128]{1,0:T(4,128)} %param.34) | copy-start | bytes 6148
  28.6 18.4 %copy-start.11 = (f32[4,128]{1,0:T(4,128)S(1)}, f32[4,128]{1,0:T(4,128)}, u32[]{:S(2)}) copy-start(f32[4,128]{1,0:T(4,128)} %param.33) | copy-start | bytes 6148
  28.6 36.4 %copy-start.7 = (bf16[256,2048]{1,0:T(8,128)(2,1)S(1)}, bf16[256,2048]{1,0:T(8,128)(2,1)}, u32[]{:S(2)}) copy-start(bf16[256,2048]{1,0:T(8,128)(2,1)} %param.21) | copy-start | bytes 3145732
  28.6 36.7 %copy-start.9 = (f32[2048]{0:T(1024)S(1)}, f32[2048]{0:T(1024)}, u32[]{:S(2)}) copy-start(f32[2048]{0:T(1024)} %param.22) | copy-start | bytes 24580
  28.6 41.2 %all-to-all-start = ((bf16[64,32,256]{2,1,0:T(8,128)(2,1)}), bf16[64,32,256]{2,1,0:T(8,128)(2,1)S(1)}, u32[]{:S(2)}, u32[]{:S(2)}) async-start(bf16[64,32,256]{2,1,0:T(8,128)(2,1)} %shard_map.199), calls=%async_computation | async-start | bytes 2097152 | tf_op jit(solution)/shard_map/all_to_all | solution.py:367
  42.8 24.1 %copy-start.2 = (f32[2,256]{1,0:T(2,128)S(1)}, f32[2,256]{1,0:T(2,128)}, u32[]{:S(2)}) copy-start(f32[2,256]{1,0:T(2,128)} %eref.1) | copy-start | bytes 6148
  42.8 24.1 %copy-start.4 = (f32[2]{0:T(128)S(1)}, f32[2]{0:T(128)}, u32[]{:S(2)}) copy-start(f32[2]{0:T(128)} %bref.1) | copy-start | bytes 28
  42.9 24.1 %copy-start.5 = (f32[2]{0:T(128)S(1)}, f32[2]{0:T(128)}, u32[]{:S(2)}) copy-start(f32[2]{0:T(128)} %rref.1) | copy-start | bytes 28
  43.8 21.2 %collective-permute-start = (bf16[32,2048]{1,0:T(8,128)(2,1)S(1)}, bf16[32,2048]{1,0:T(8,128)(2,1)S(1)}, u32[]{:S(2)}, u32[]{:S(2)}) collective-permute-start(bf16[32,2048]{1,0:T(8,128)(2,1)S(1)} %slice.3), channel_id=1, source_target_pairs={{0,8},{8,16},{16,24},{24,32},{32,40},{40,48},{48,56},{56,64},{64,7... | collective-permute-start | bytes 393224 | tf_op jit(solution)/shard_map/ppermute | solution.py:369
  68.7 32.6 %copy-start.1 = (f32[31,128]{1,0:T(8,128)S(1)}, f32[31,128]{1,0:T(8,128)}, u32[]{:S(2)}) copy-start(f32[31,128]{1,0:T(8,128)} %ltaps.1) | copy-start | bytes 47620
  68.7 32.6 %copy-start.3 = (f32[4,128]{1,0:T(4,128)S(1)}, f32[4,128]{1,0:T(4,128)}, u32[]{:S(2)}) copy-start(f32[4,128]{1,0:T(4,128)} %ftaps.1) | copy-start | bytes 6148
  91.1 15.6 %all-to-all-start.2 = ((bf16[8,136,128]{2,1,0:T(8,128)(2,1)}), bf16[8,136,128]{2,1,0:T(8,128)(2,1)S(1)}, u32[]{:S(2)}, u32[]{:S(2)}) async-start(bf16[8,136,128]{2,1,0:T(8,128)(2,1)} %get-tuple-element.30), calls=%async_computation.2 | async-start | bytes 557056 | tf_op jit(solution)/shard_map/all_to_all | solution.py:380
  97.2 9.5 %copy-start = (f32[2,64,128]{2,1,0:T(8,128)S(1)}, f32[2,64,128]{2,1,0:T(8,128)}, u32[]{:S(2)}) copy-start(f32[2,64,128]{2,1,0:T(8,128)} %init.1) | copy-start | bytes 196612
  97.2 9.5 %copy-start.6 = (f32[128]{0:T(128)S(1)}, f32[128]{0:T(128)}, u32[]{:S(2)}) copy-start(f32[128]{0:T(128)} %param.38) | copy-start | bytes 1540
  101.3 17.1 %copy-start.12 = (f32[128]{0:T(128)S(1)}, f32[128]{0:T(128)}, u32[]{:S(2)}) copy-start(f32[128]{0:T(128)} %param.37) | copy-start | bytes 1540
  107.9 15.2 %collective-permute-start.1 = (bf16[2240,256]{1,0:T(8,128)(2,1)S(1)}, bf16[2240,256]{1,0:T(8,128)(2,1)S(1)}, u32[]{:S(2)}, u32[]{:S(2)}) collective-permute-start(bf16[2240,256]{1,0:T(8,128)(2,1)S(1)} %get-tuple-element.44.own), channel_id=1, source_target_pairs={{0,1},{1,0},{2,3},{3,2},{4,5},{5,4},{6,7},{7,6},{8,9},{9,8},{10,11... | collective-permute-start | bytes 3440648 | tf_op jit(solution)/shard_map/ppermute | solution.py:386
  114.0 9.1 %all-to-all-start.4 = ((f32[8,3,256]{2,1,0:T(4,128)}), f32[8,3,256]{2,1,0:T(4,128)S(1)}, u32[]{:S(2)}, u32[]{:S(2)}) async-start(f32[8,3,256]{2,1,0:T(4,128)} %get-tuple-element.42), calls=%async_computation.4 | async-start | bytes 65536 | tf_op jit(solution)/shard_map/all_to_all | solution.py:385
Sparse Core Ops, SparseCore 0:
  26.8 74.3 all-gather.3

commit v16 on v14

--- a/solution.py
+++ b/solution.py
@@ -189,7 +189,7 @@
     part, n = 64, 8
     kc = d // n
 
-    def body(nref, wref, ftaps, ltaps, xs, w16, cum, cum_t, read16, zgate, mixed, inner, back, acc, glu, wall, sems):
+    def body(nref, wref, ftaps, ltaps, xs, w16, cum, cum_t, read16, zgate, mixed, inner, back, acc, glu, wall, decay, owned, sems):
         def fetch(i):
             at = slice(i * kc, (i + 1) * kc)
             return pltpu.make_async_copy(wref.at[at, : 4 * ch], wall.at[at, :], sems.at[0, i])
@@ -202,6 +202,12 @@
             fetch(i).start()
         for i in range(n):
             fetch_back(i).start()
+        lower = lax.broadcasted_iota(jnp.int32, (rows, rows), 0) >= lax.broadcasted_iota(jnp.int32, (rows, rows), 1)
+        lane = lax.broadcasted_iota(jnp.int32, (rows, ch), 1)
+        for h in range(heads):
+            gap = jnp.where(lower, cum[:, h * p : h * p + 1] - cum_t[h : h + 1, :], 0.0)
+            decay[h] = jnp.exp(gap)
+            owned[h] = jnp.where(lane // p == h, xs[...].astype(f32), 0.0).astype(bf16)
         for i in range(n):
             fetch(i).wait()
             at = slice(i * kc, (i + 1) * kc)
@@ -217,14 +223,10 @@
         read16[...] = read
         zgate[...] = jax.nn.silu(acc[HALO:, ch : 2 * ch])
         scores = dot(read, w16[...], 1, 1)
-        lower = lax.broadcasted_iota(jnp.int32, (rows, rows), 0) >= lax.broadcasted_iota(jnp.int32, (rows, rows), 1)
-        lane = lax.broadcasted_iota(jnp.int32, (rows, ch), 1)
         y = jnp.zeros((rows, ch), f32)
         for h in range(heads):
-            gap = jnp.where(lower, cum[:, h * p : h * p + 1] - cum_t[h : h + 1, :], 0.0)
-            m = jnp.where(lower, jnp.exp(gap) * scores, 0.0).astype(bf16)
-            x = jnp.where(lane // p == h, xs[...].astype(f32), 0.0).astype(bf16)
-            y = y + dot(m, x, 1, 0)
+            m = jnp.where(lower, decay[h] * scores, 0.0).astype(bf16)
+            y = y + dot(m, owned[h], 1, 0)
         inner[...] = y
         for r in range(0, rows, part):
             mixed[r : r + part, :] = sum(
@@ -244,7 +246,7 @@
         out_specs=(VMEM,) * 5,
         scratch_shapes=[
             pltpu.VMEM((ext, 4 * ch), f32), pltpu.VMEM((ext, ch), f32), pltpu.VMEM((d, 4 * ch), bf16),
-            pltpu.SemaphoreType.DMA((2, n)),
+            pltpu.VMEM((heads, rows, rows), f32), pltpu.VMEM((heads, rows, ch), bf16), pltpu.SemaphoreType.DMA((2, n)),
         ],
         compiler_params=SMALL, name="rows_local",
     )(*held(normed), *fetched(rest), *held(*small))

time: 143 us -> 143 us (level)
  no operation moved by 1% of the time
where the time goes in v16:
time: 143 us
  blocking collectives  51 us (36%)
  starting transfers between devices  34 us (24%)
  waiting for transfers between devices  29 us (20%)
  between operations  13.6 us (10%)
  Pallas kernels  11.2 us (8%)
  other arithmetic  2.64 us (2%)
    all_to_all x1, blocking collectives, per_device(): rest = lax.all_to_all(rest, 'sp_1', 0, 0, tiled=True).reshape(-1, 6 * ch)  19.3 us
    all_to_all x1, blocking collectives, per_device(): got = lax.all_to_all(send, 'sp_1', 0, 0, tiled=True)  18.9 us
    ppermute x1, waiting for transfers between devices, per_device(): lax.ppermute(tokens[rows - HALO:], SP, [(i, i + 1) for i in range(n - 1)])  18.6 us
    all_to_all x1, starting transfers between devices, per_device(): first = lax.all_to_all(first, SP, 0, 0, tiled=True).reshape(-1, 2 * ch)  14.2 us
    all_to_all x1, blocking collectives, per_device(): pieces = lax.all_to_all(out, 'fs', 0, 0, tiled=True)  10.9 us
    all_to_all x1, starting transfers between devices, per_device(): got = lax.all_to_all(send, 'sp_0', 0, 0, tiled=True)  6.41 us
    ppermute x1, starting transfers between devices, per_device(): other = lax.ppermute(pack, 'tp', [(i, nt - 1 - i) for i in range(nt)])  6.06 us
    all_to_all x1, starting transfers between devices, per_device(): sums = lax.all_to_all(sums, FT, 0, 0, tiled=True)  4.42 us
  transfers between devices with their start and end apart: 6, of which 5 were waited for; matrix products, arithmetic and copies ran while one was open for 2% of the time, Pallas kernels for 6%

profile of v16, /device:TPU:1, one launch (start us, length us, event | category | flops | bytes accessed | tf_op | source)
XLA Modules:
  0.0 142.7 jit_solution(11913262305721946432)
XLA Ops:
  6.5 0.0 all-gather.4.cloned.1.call-start
  6.5 0.8 shard_map.200
  7.4 0.0 copy-start.8
  7.4 19.3 %all_to_all.30 = bf16[8,32,768]{2,1,0:T(8,128)(2,1)} all-to-all(bf16[8,32,768]{2,1,0:T(8,128)(2,1)S(1)} %shard_map.200), channel_id=1, replica_groups=mesh['sp_0'=8,'sp_1'=8,'fs'=4,'tp'=2] {'sp_1'}, dimensions={0} | all-to-all | bytes 786432 | tf_op jit(solution)/shard_map/all_to_all | solution.py:365
  26.7 0.0 all-gather.4.cloned.1.call-update
  26.7 1.9 %shard_map.199 = bf16[64,32,256]{2,1,0:T(8,128)(2,1)} custom-call(bf16[32,128]{1,0:T(8,128)(2,1)} %refs_0_.2, bf16[32,128]{1,0:T(8,128)(2,1)} %refs_1_.2), custom_call_target="tpu_custom_call" | custom-call | tf_op jit(solution)/shard_map/pallas_call | solution.py:55
  28.6 14.2 %all-to-all-start = ((bf16[64,32,256]{2,1,0:T(8,128)(2,1)}), bf16[64,32,256]{2,1,0:T(8,128)(2,1)S(1)}, u32[]{:S(2)}, u32[]{:S(2)}) async-start(bf16[64,32,256]{2,1,0:T(8,128)(2,1)} %shard_map.199), calls=%async_computation | async-start | bytes 2097152 | tf_op jit(solution)/shard_map/all_to_all | solution.py:368
  42.8 0.0 copy-start.2
  42.8 0.0 copy-start.4
  42.9 0.0 copy-start.5
  42.9 0.9 slice.3
  43.8 2.9 %collective-permute-start = (bf16[32,2048]{1,0:T(8,128)(2,1)S(1)}, bf16[32,2048]{1,0:T(8,128)(2,1)S(1)}, u32[]{:S(2)}, u32[]{:S(2)}) collective-permute-start(bf16[32,2048]{1,0:T(8,128)(2,1)S(1)} %slice.3), channel_id=1, source_target_pairs={{0,8},{8,16},{16,24},{24,32},{32,40},{40,48},{48,56},{56,64},{64,7... | collective-permute-start | bytes 393224 | tf_op jit(solution)/shard_map/ppermute | solution.py:370
  46.7 0.0 copy-done.8
  46.7 0.3 copy.25.wref
  47.0 0.0 copy-done.10
  47.0 0.0 copy-done.11
  47.1 18.6 %collective-permute-done = bf16[32,2048]{1,0:T(8,128)(2,1)S(1)} collective-permute-done((bf16[32,2048]{1,0:T(8,128)(2,1)S(1)}, bf16[32,2048]{1,0:T(8,128)(2,1)S(1)}, u32[]{:S(2)}, u32[]{:S(2)}) %collective-permute-start) | collective-permute-done | bytes 131104 | tf_op jit(solution)/shard_map/ppermute | solution.py:370
  65.7 0.0 copy-done.7
  65.7 0.3 fusion
  66.0 0.0 copy-done.9
  66.0 1.6 %fusion.2.nref = bf16[288,2048]{1,0:T(8,128)(2,1)S(1)} fusion(f32[2048]{0:T(1024)S(1)} %copy-done.9, f32[288]{0:T(512)S(1)} %add_rsqrt_fusion, bf16[256,2048]{1,0:T(8,128)(2,1)} %param.21, bf16[32,2048]{1,0:T(8,128)(2,1)S(1)} %collective-permute-done), kind=kLoop, calls=%fused_computation.4 | loop fusion | flops 4128768 | bytes 2368640 | tf_op jit(solution)/shard_map/convert_element_type | solution.py:372
  67.6 0.0 copy-done.2
  67.6 0.0 copy-done.4
  67.6 0.0 copy-done.5
  67.6 1.7 %steps_of.1 = (f32[256,128]{1,0:T(8,128)S(1)}, f32[256,128]{1,0:T(8,128)S(1)}, f32[256,128]{1,0:T(8,128)S(1)}, f32[2,256]{1,0:T(2,128)S(1)}, f32[1,128]{1,0:T(1,128)S(1)}, /*index=5*/s32[8,128]{1,0:T(8,128)S(1)}) custom-call(s32[1]{0:T(128)} %bitcast.iz, s32[1]{0:T(128)} %bitcast.1.iy, s32[1]{0:T(128)S(6)} %add.14.shard, s32[1]{0:T(128)} %bitcast.3.tp, ...), custom_call_target="tpu_custom_call" | custom-call | tf_op jit(solution)/shard_map/steps_of/pallas_call | solution.py:106
  69.3 0.0 copy-start.1
  69.3 0.0 copy-start.3
  69.3 0.7 all-to-all-done
  70.1 0.9 local_states.1
  71.0 18.9 %all_to_all.31.ref = bf16[8,136,128]{2,1,0:T(8,128)(2,1)S(1)} all-to-all(bf16[8,136,128]{2,1,0:T(8,128)(2,1)S(1)} %get-tuple-element.29), channel_id=1, replica_groups=mesh['sp_0'=8,'sp_1'=8,'fs'=4,'tp'=2] {'sp_1'}, dimensions={0} | all-to-all | bytes 557056 | tf_op jit(solution)/shard_map/all_to_all | solution.py:379
  90.0 0.9 line_states.1
  90.9 6.4 %all-to-all-start.2 = ((bf16[8,136,128]{2,1,0:T(8,128)(2,1)}), bf16[8,136,128]{2,1,0:T(8,128)(2,1)S(1)}, u32[]{:S(2)}, u32[]{:S(2)}) async-start(bf16[8,136,128]{2,1,0:T(8,128)(2,1)} %get-tuple-element.30), calls=%async_computation.2 | async-start | bytes 557056 | tf_op jit(solution)/shard_map/all_to_all | solution.py:381
  97.3 0.0 copy-start.6
  97.3 4.0 %all-gather.4.cloned.1.call-done.wref = bf16[2048,768]{1,0:T(8,128)(2,1)} async-done(((bf16[256,768]{1,0:T(8,128)(2,1)}), bf16[2048,768]{1,0:T(8,128)(2,1)}) %all-gather.4.cloned.1.call-update) | async-done | bytes 3145744 | tf_op jit(solution)/shard_map/all_gather | solution.py:366
  101.3 0.0 copy-done.1
  101.3 0.0 copy-done.3
  101.3 2.8 %rows_local.1 = (bf16[256,128]{1,0:T(8,128)(2,1)S(1)}, f32[256,128]{1,0:T(8,128)S(1)}, f32[256,128]{1,0:T(8,128)S(1)}, f32[256,128]{1,0:T(8,128)S(1)}, bf16[2240,256]{1,0:T(8,128)(2,1)S(1)}) custom-call(bf16[288,2048]{1,0:T(8,128)(2,1)S(1)} %fusion.2.nref, bf16[2048,768]{1,0:T(8,128)(2,1)} %all-gather.4.cloned.1.call-done.wref, f32[4,128]{1,0:T(4,128)S(1)} %copy-done.3, ...), custom_call_target="tpu_custom_call" | custom-call | tf_op jit(solution)/shard_map/rows_local/pallas_call | solution.py:239
  104.1 2.8 %all-to-all-done.2.got = bf16[8,136,128]{2,1,0:T(8,128)(2,1)S(1)} async-done(((bf16[8,136,128]{2,1,0:T(8,128)(2,1)}), bf16[8,136,128]{2,1,0:T(8,128)(2,1)S(1)}, u32[]{:S(2)}, u32[]{:S(2)}) %all-to-all-start.2) | async-done | bytes 278560 | tf_op jit(solution)/shard_map/all_to_all | solution.py:381
  106.8 0.0 copy-done
  106.8 1.1 rows_done.1
  107.9 6.1 %collective-permute-start.1 = (bf16[2240,256]{1,0:T(8,128)(2,1)S(1)}, bf16[2240,256]{1,0:T(8,128)(2,1)S(1)}, u32[]{:S(2)}, u32[]{:S(2)}) collective-permute-start(bf16[2240,256]{1,0:T(8,128)(2,1)S(1)} %get-tuple-element.44.own), channel_id=1, source_target_pairs={{0,1},{1,0},{2,3},{3,2},{4,5},{5,4},{6,7},{7,6},{8,9},{9,8},{10,11... | collective-permute-start | bytes 3440648 | tf_op jit(solution)/shard_map/ppermute | solution.py:387
  114.0 4.4 %all-to-all-start.4 = ((f32[8,3,256]{2,1,0:T(4,128)}), f32[8,3,256]{2,1,0:T(4,128)S(1)}, u32[]{:S(2)}, u32[]{:S(2)}) async-start(f32[8,3,256]{2,1,0:T(4,128)} %get-tuple-element.42), calls=%async_computation.4 | async-start | bytes 65536 | tf_op jit(solution)/shard_map/all_to_all | solution.py:386
  118.4 1.8 %all-gather.1 = f32[2,1,128]{2,1,0:T(1,128)S(1)} all-gather(f32[1,1,128]{2,1,0:T(1,128)S(1)} %bitcast.13), channel_id=2, replica_groups=mesh['sp_0'=8,'sp_1'=8,'fs'=4,'tp'=2] {'tp'}, dimensions={0}, use_global_device_ids=true | all-gather | bytes 1536 | tf_op jit(solution)/shard_map/all_gather | solution.py:376
  120.2 2.9 %all-to-all-done.4.sref = f32[8,3,256]{2,1,0:T(4,128)S(1)} async-done(((f32[8,3,256]{2,1,0:T(4,128)}), f32[8,3,256]{2,1,0:T(4,128)S(1)}, u32[]{:S(2)}, u32[]{:S(2)}) %all-to-all-start.4) | async-done | bytes 24608 | tf_op jit(solution)/shard_map/all_to_all | solution.py:386
  123.1 0.0 collective-permute-done.1.other
  123.1 1.1 output_rows.1
  124.2 10.9 %all_to_all.32 = bf16[4,32,2048]{2,1,0:T(8,128)(2,1)S(1)} all-to-all(bf16[4,32,2048]{2,1,0:T(8,128)(2,1)S(1)} %output_rows.1), channel_id=1, replica_groups=mesh['sp_0'=8,'sp_1'=8,'fs'=4,'tp'=2] {'fs'}, dimensions={0} | all-to-all | bytes 1048576 | tf_op jit(solution)/shard_map/all_to_all | solution.py:389
  135.1 0.7 reduce_sum.22
  (10 shorter events, 0.0 us)
Async XLA Ops:
  6.5 94.7 %all-gather.4.cloned.1.call-start = ((), (), s32[]{:S(2)}) async-start(), calls=%async_computation.6 | async-start | bytes 3538944 | tf_op jit(solution)/shard_map/all_gather | solution.py:366
  7.4 39.4 %copy-start.8 = (bf16[2048,16]{0,1:T(8,128)(2,1)S(1)}, bf16[2048,16]{0,1:T(8,128)(2,1)}, u32[]{:S(2)}) copy-start(bf16[2048,16]{0,1:T(8,128)(2,1)} %param.29) | copy-start | bytes 196612
  28.6 18.4 %copy-start.10 = (f32[4,128]{1,0:T(4,128)S(1)}, f32[4,128]{1,0:T(4,128)}, u32[]{:S(2)}) copy-start(f32[4,128]{1,0:T(4,128)} %param.34) | copy-start | bytes 6148
  28.6 18.4 %copy-start.11 = (f32[4,128]{1,0:T(4,128)S(1)}, f32[4,128]{1,0:T(4,128)}, u32[]{:S(2)}) copy-start(f32[4,128]{1,0:T(4,128)} %param.33) | copy-start | bytes 6148
  28.6 37.0 %copy-start.7 = (bf16[256,2048]{1,0:T(8,128)(2,1)S(1)}, bf16[256,2048]{1,0:T(8,128)(2,1)}, u32[]{:S(2)}) copy-start(bf16[256,2048]{1,0:T(8,128)(2,1)} %param.21) | copy-start | bytes 3145732
  28.6 37.4 %copy-start.9 = (f32[2048]{0:T(1024)S(1)}, f32[2048]{0:T(1024)}, u32[]{:S(2)}) copy-start(f32[2048]{0:T(1024)} %param.22) | copy-start | bytes 24580
  28.6 41.5 %all-to-all-start = ((bf16[64,32,256]{2,1,0:T(8,128)(2,1)}), bf16[64,32,256]{2,1,0:T(8,128)(2,1)S(1)}, u32[]{:S(2)}, u32[]{:S(2)}) async-start(bf16[64,32,256]{2,1,0:T(8,128)(2,1)} %shard_map.199), calls=%async_computation | async-start | bytes 2097152 | tf_op jit(solution)/shard_map/all_to_all | solution.py:368
  42.8 24.7 %copy-start.2 = (f32[2,256]{1,0:T(2,128)S(1)}, f32[2,256]{1,0:T(2,128)}, u32[]{:S(2)}) copy-start(f32[2,256]{1,0:T(2,128)} %eref.1) | copy-start | bytes 6148
  42.8 24.7 %copy-start.4 = (f32[2]{0:T(128)S(1)}, f32[2]{0:T(128)}, u32[]{:S(2)}) copy-start(f32[2]{0:T(128)} %bref.1) | copy-start | bytes 28
  42.9 24.7 %copy-start.5 = (f32[2]{0:T(128)S(1)}, f32[2]{0:T(128)}, u32[]{:S(2)}) copy-start(f32[2]{0:T(128)} %rref.1) | copy-start | bytes 28
  43.8 21.9 %collective-permute-start = (bf16[32,2048]{1,0:T(8,128)(2,1)S(1)}, bf16[32,2048]{1,0:T(8,128)(2,1)S(1)}, u32[]{:S(2)}, u32[]{:S(2)}) collective-permute-start(bf16[32,2048]{1,0:T(8,128)(2,1)S(1)} %slice.3), channel_id=1, source_target_pairs={{0,8},{8,16},{16,24},{24,32},{32,40},{40,48},{48,56},{56,64},{64,7... | collective-permute-start | bytes 393224 | tf_op jit(solution)/shard_map/ppermute | solution.py:370
  69.3 31.9 %copy-start.1 = (f32[31,128]{1,0:T(8,128)S(1)}, f32[31,128]{1,0:T(8,128)}, u32[]{:S(2)}) copy-start(f32[31,128]{1,0:T(8,128)} %ltaps.1) | copy-start | bytes 47620
  69.3 31.9 %copy-start.3 = (f32[4,128]{1,0:T(4,128)S(1)}, f32[4,128]{1,0:T(4,128)}, u32[]{:S(2)}) copy-start(f32[4,128]{1,0:T(4,128)} %ftaps.1) | copy-start | bytes 6148
  90.9 16.0 %all-to-all-start.2 = ((bf16[8,136,128]{2,1,0:T(8,128)(2,1)}), bf16[8,136,128]{2,1,0:T(8,128)(2,1)S(1)}, u32[]{:S(2)}, u32[]{:S(2)}) async-start(bf16[8,136,128]{2,1,0:T(8,128)(2,1)} %get-tuple-element.30), calls=%async_computation.2 | async-start | bytes 557056 | tf_op jit(solution)/shard_map/all_to_all | solution.py:381
  97.3 9.6 %copy-start = (f32[2,64,128]{2,1,0:T(8,128)S(1)}, f32[2,64,128]{2,1,0:T(8,128)}, u32[]{:S(2)}) copy-start(f32[2,64,128]{2,1,0:T(8,128)} %init.1) | copy-start | bytes 196612
  97.3 9.6 %copy-start.6 = (f32[128]{0:T(128)S(1)}, f32[128]{0:T(128)}, u32[]{:S(2)}) copy-start(f32[128]{0:T(128)} %param.38) | copy-start | bytes 1540
  101.3 17.1 %copy-start.12 = (f32[128]{0:T(128)S(1)}, f32[128]{0:T(128)}, u32[]{:S(2)}) copy-start(f32[128]{0:T(128)} %param.37) | copy-start | bytes 1540
  107.9 15.2 %collective-permute-start.1 = (bf16[2240,256]{1,0:T(8,128)(2,1)S(1)}, bf16[2240,256]{1,0:T(8,128)(2,1)S(1)}, u32[]{:S(2)}, u32[]{:S(2)}) collective-permute-start(bf16[2240,256]{1,0:T(8,128)(2,1)S(1)} %get-tuple-element.44.own), channel_id=1, source_target_pairs={{0,1},{1,0},{2,3},{3,2},{4,5},{5,4},{6,7},{7,6},{8,9},{9,8},{10,11... | collective-permute-start | bytes 3440648 | tf_op jit(solution)/shard_map/ppermute | solution.py:387
  114.0 9.1 %all-to-all-start.4 = ((f32[8,3,256]{2,1,0:T(4,128)}), f32[8,3,256]{2,1,0:T(4,128)S(1)}, u32[]{:S(2)}, u32[]{:S(2)}) async-start(f32[8,3,256]{2,1,0:T(4,128)} %get-tuple-element.42), calls=%async_computation.4 | async-start | bytes 65536 | tf_op jit(solution)/shard_map/all_to_all | solution.py:386
Sparse Core Ops, SparseCore 0:
  26.8 74.4 all-gather.3
